TPU v7x, 32 devices: a whole 2x2x4 slice. The times are simulated.
32 devices in a mesh: ep: 8 (over z, x), tp: 4 (over y, core).
Axes of the slice: x: 2, y: 2, z: 4, core: 2. Of those that a mesh axis runs over, the one named last changes fastest.
Arguments:
- tokens: bfloat16 [1024, 2048], P('ep'), may hold values from -6 to 6
- routing: int32 [1024, 2], P('ep'), may hold values from 0 to 7, all different within a row; in each aligned block of 128 rows (0 to 127, 128 to 255, ...) at most 56 rows name the same one
- router_weight: bfloat16 [2048, 8], replicated, may hold values from -0.125 to 0.125
- gate_weight: bfloat16 [8, 2048, 2048], P('ep', None, 'tp'), may hold values from -0.125 to 0.125
- up_weight: bfloat16 [8, 2048, 2048], P('ep', None, 'tp'), may hold values from -0.125 to 0.125
- down_weight: bfloat16 [8, 2048, 2048], P('ep', 'tp'), may hold values from -0.125 to 0.125
- cotangent: bfloat16 [1024, 2048], P('ep'), may hold values from -0.796875 to 0.796875
Outputs:
- token_grad: bfloat16 [1024, 2048], P('ep')
- router_grad: float32 [2048, 8], P('tp')
- router_rows: float32 [2048], P('tp')
- gate_grad: bfloat16 [8, 2048, 2048], P('ep', None, 'tp')
- up_grad: bfloat16 [8, 2048, 2048], P('ep', None, 'tp')
- down_grad: bfloat16 [8, 2048, 2048], P('ep', 'tp')
- gate_rows: float32 [8, 2048], P('ep')
- up_rows: float32 [8, 2048], P('ep')
- down_rows: float32 [8, 2048], P('ep', 'tp')
Inputs may be any that keep to these rules, and one draw needn't show every extreme that they name: `routing`: A row's 2 experts differ. Within the rows of one index of ep (128 rows), no expert is named more than 56 times, a bound that some block reaches.
All inputs are finite; a program needn't handle non-finite values.
Results may differ from a plain program's by a relative error of at most 0.01.
Values may be sent and summed in bfloat16 or wider, within the bound.
No kernel may reach another device: no remote copies, remote signals or barrier semaphores. Data moves between devices by JAX's collectives and lax.ppermute only.
A program may use at most 64 MiB of HBM per device.

v0:
```python
import jax
import jax.numpy as jnp
from jax import lax
from jax.sharding import PartitionSpec as P


def expert_backward(rows_in, cots_in, slot_scale, w_gate, w_up, w_down):
    pre_gate = jnp.dot(rows_in, w_gate, preferred_element_type=jnp.float32)
    pre_up = jnp.dot(rows_in, w_up, preferred_element_type=jnp.float32)
    sigmoid_gate = jax.nn.sigmoid(pre_gate)
    hidden = (pre_gate * sigmoid_gate * pre_up).astype(jnp.bfloat16)
    back_proj = lax.dot_general(
        cots_in, w_down, (((1,), (1,)), ((), ())), preferred_element_type=jnp.float32
    )
    gate_term = jnp.sum(hidden.astype(jnp.float32) * back_proj, axis=1)
    scaled = slot_scale * back_proj
    grad_up_pre = (scaled * pre_gate * sigmoid_gate).astype(jnp.bfloat16)
    grad_gate_pre = (
        scaled * pre_up * sigmoid_gate * (1.0 + pre_gate * (1.0 - sigmoid_gate))
    ).astype(jnp.bfloat16)
    weighted = (slot_scale * cots_in.astype(jnp.float32)).astype(jnp.bfloat16)
    contract_rows = (((0,), (0,)), ((), ()))
    grad_down = lax.dot_general(hidden, weighted, contract_rows, preferred_element_type=jnp.float32)
    grad_gate = lax.dot_general(
        rows_in, grad_gate_pre, contract_rows, preferred_element_type=jnp.float32
    )
    grad_up = lax.dot_general(
        rows_in, grad_up_pre, contract_rows, preferred_element_type=jnp.float32
    )
    contract_hidden = (((1,), (1,)), ((), ()))
    partial_value = lax.dot_general(
        grad_gate_pre, w_gate, contract_hidden, preferred_element_type=jnp.float32
    )
    partial_value = partial_value + lax.dot_general(
        grad_up_pre, w_up, contract_hidden, preferred_element_type=jnp.float32
    )
    return (partial_value, gate_term, grad_gate, grad_up, grad_down)


def per_device(tokens, routing, router_weight, gate_weight, up_weight, down_weight, cotangent):
    groups = lax.axis_size("ep")
    shares = lax.axis_size("tp")
    tok_count, model_width = tokens.shape
    top_count = routing.shape[1]
    local_experts = gate_weight.shape[0]
    experts = local_experts * groups
    capacity = 7 * tok_count * top_count // (4 * experts)
    slot_span = groups * capacity
    assigns = tok_count * top_count
    col_width = model_width // shares
    col_start = lax.axis_index("tp") * col_width
    logits = jnp.dot(tokens, router_weight, preferred_element_type=jnp.float32)
    affinity = jax.nn.sigmoid(logits)
    chosen = jnp.take_along_axis(affinity, routing, axis=1)
    total_aff = jnp.sum(chosen, axis=1, keepdims=True)
    weights = chosen / total_aff
    flat_ids = routing.reshape(-1)
    onehot_ids = (flat_ids[:, None] == jnp.arange(experts, dtype=jnp.int32)[None, :]).astype(
        jnp.int32
    )
    position = jnp.sum((jnp.cumsum(onehot_ids, axis=0) - 1) * onehot_ids, axis=1)
    slot_of = flat_ids % local_experts * slot_span + flat_ids // local_experts * capacity + position
    slot_table = jnp.full((local_experts * slot_span,), assigns, jnp.int32)
    slot_table = slot_table.at[slot_of].set(jnp.arange(assigns, dtype=jnp.int32))
    zero_row = jnp.zeros((1, model_width), jnp.bfloat16)
    tok_pad = jnp.concatenate([tokens, zero_row], axis=0)
    cot_pad = jnp.concatenate([cotangent, zero_row], axis=0)
    weight_pad = jnp.concatenate(
        [weights.astype(jnp.bfloat16).reshape(-1), jnp.zeros((1,), jnp.bfloat16)]
    )
    source_tok = slot_table // top_count
    rows_send = tok_pad[source_tok].reshape(local_experts, groups, capacity, model_width)
    cots_send = cot_pad[source_tok].reshape(local_experts, groups, capacity, model_width)
    scale_send = weight_pad[slot_table].reshape(local_experts, groups, capacity)
    rows_recv, cots_recv, scale_recv = (
        lax.all_to_all(rows_send, "ep", split_axis=1, concat_axis=1, tiled=True),
        lax.all_to_all(cots_send, "ep", split_axis=1, concat_axis=1, tiled=True),
        lax.all_to_all(scale_send, "ep", split_axis=1, concat_axis=1, tiled=True),
    )
    partials, gate_terms, gate_grads, up_grads, down_grads = ([], [], [], [], [])
    slot_scale = scale_recv[0].reshape(slot_span).astype(jnp.float32)[:, None]
    result = expert_backward(
        rows_recv[0].reshape(slot_span, model_width),
        cots_recv[0].reshape(slot_span, model_width),
        slot_scale,
        gate_weight[0],
        up_weight[0],
        down_weight[0],
    )
    partials.append(result[0])
    gate_terms.append(result[1])
    gate_grads.append(result[2])
    up_grads.append(result[3])
    down_grads.append(result[4])
    partial_value = jnp.stack(partials)
    gate_term = jnp.stack(gate_terms)
    grad_gate = jnp.stack(gate_grads)
    grad_up = jnp.stack(up_grads)
    grad_down = jnp.stack(down_grads)
    gate_rows, up_rows = lax.psum(
        (jnp.sum(grad_gate * grad_gate, axis=2), jnp.sum(grad_up * grad_up, axis=2)), "tp"
    )
    down_rows = jnp.sum(grad_down * grad_down, axis=2)
    summed = lax.psum_scatter(partial_value, "tp", scatter_dimension=2, tiled=True)
    gate_sum = lax.psum(gate_term, "tp")
    back_send = summed.astype(jnp.bfloat16).reshape(local_experts, groups, capacity, col_width)
    gate_send = gate_sum.astype(jnp.bfloat16).reshape(local_experts, groups, capacity)
    back_recv, gate_recv = (
        lax.all_to_all(back_send, "ep", split_axis=1, concat_axis=1, tiled=True),
        lax.all_to_all(gate_send, "ep", split_axis=1, concat_axis=1, tiled=True),
    )
    router_cols = lax.dynamic_slice_in_dim(router_weight, col_start, col_width, 0)
    back_flat = back_recv.reshape(local_experts * slot_span, -1)
    back_rows = jnp.sum(
        back_flat[slot_of].astype(jnp.float32).reshape(tok_count, top_count, -1), axis=1
    )
    d_weights = gate_recv.reshape(-1)[slot_of].astype(jnp.float32).reshape(tok_count, top_count)
    d_chosen = (d_weights - jnp.sum(d_weights * weights, axis=1, keepdims=True)) / total_aff
    d_logit = d_chosen * chosen * (1.0 - chosen)
    onehot = (routing[:, :, None] == jnp.arange(experts, dtype=jnp.int32)[None, None, :]).astype(
        jnp.float32
    )
    d_logits = jnp.sum(d_logit[:, :, None] * onehot, axis=1).astype(jnp.bfloat16)
    token_cols = lax.dynamic_slice_in_dim(tokens, col_start, col_width, 1)
    router_part = lax.dot_general(
        token_cols, d_logits, (((0,), (0,)), ((), ())), preferred_element_type=jnp.float32
    )
    router_grad = lax.psum(router_part, "ep")
    router_rows = jnp.sum(router_grad * router_grad, axis=1)
    router_back = lax.dot_general(
        d_logits, router_cols, (((1,), (1,)), ((), ())), preferred_element_type=jnp.float32
    )
    token_grad = (back_rows + router_back).astype(jnp.bfloat16)
    token_grad = lax.all_gather(token_grad, "tp", axis=1, tiled=True)
    return (
        token_grad,
        router_grad,
        router_rows,
        grad_gate.astype(jnp.bfloat16),
        grad_up.astype(jnp.bfloat16),
        grad_down.astype(jnp.bfloat16),
        gate_rows,
        up_rows,
        down_rows,
    )


def solution(mesh):
    return jax.shard_map(
        per_device,
        mesh=mesh,
        in_specs=(
            P("ep", None),
            P("ep", None),
            P(),
            P("ep", None, "tp"),
            P("ep", None, "tp"),
            P("ep", "tp", None),
            P("ep", None),
        ),
        out_specs=(
            P("ep", None),
            P("tp", None),
            P("tp"),
            P("ep", None, "tp"),
            P("ep", None, "tp"),
            P("ep", "tp", None),
            P("ep", None),
            P("ep", None),
            P("ep", "tp"),
        ),
        check_vma=False,
    )
```

profile of v0, /device:TPU:0, one launch (start us, length us, event | category | flops | bytes accessed | tf_op | source)
XLA Modules:
  0.0 255.0 jit_solution(7731860463774829727)
XLA Ops:
  7.2 0.8 broadcast_multiply_fusion
  8.0 0.8 copy.81
  8.8 0.1 eq.44
  8.9 0.1 eq.40
  9.1 0.7 bitcast_or_fusion
  9.8 0.1 copy.80
  9.9 0.1 mul.106
  10.0 0.6 reduce-window.6
  10.6 0.2 slice_reduce_fusion
  10.9 0.1 fusion.17
  11.0 1.4 scatter_custom_fusion
  12.4 0.1 copy.77
  12.6 0.1 reshape.207
  12.7 1.3 fusion.14
  14.0 1.4 gather_fusion.5
  15.4 0.1 reshape.210
  15.5 0.1 copy.78
  15.6 0.6 fusion.29
  16.2 0.1 copy.79
  16.4 0.1 convert_element_type.88
  16.6 3.2 %gather_fusion = bf16[448]{0:T(512)(128)(2,1)S(1)} fusion(bf16[257]{0:T(512)(128)(2,1)S(1)} %pad_maximum_fusion, s32[1024]{0:T(1024)S(1)} %get-tuple-element.83), kind=kCustom, calls=%fused_computation | custom fusion | bytes 3584 | tf_op jit(solution)/shard_map/gather | solution.py:74
  19.7 0.7 reshape.229
  20.4 7.3 %all-to-all-start = ((bf16[1,8,56]{2,0,1:T(2,128)(2,1)}), bf16[1,8,56]{2,0,1:T(2,128)(2,1)S(1)}, u32[]{:S(2)}, u32[]{:S(2)}) async-start(bf16[1,8,56]{2,0,1:T(2,128)(2,1)} %reshape.229), calls=%async_computation | async-start | bytes 8192 | tf_op jit(solution)/shard_map/all_to_all | solution.py:78
  27.7 3.2 %gather_fusion.2 = bf16[448,2048]{1,0:T(8,128)(2,1)} fusion(bf16[129,2048]{1,0:T(8,128)(2,1)S(1)} %concatenate.11, s32[1024]{0:T(1024)S(1)} %get-tuple-element.82), kind=kCustom, calls=%fused_computation.2 | custom fusion | bytes 3671808 | tf_op jit(solution)/shard_map/gather | solution.py:72
  30.9 3.2 %all-to-all-done = bf16[1,8,56]{2,0,1:T(2,128)(2,1)S(1)} async-done(((bf16[1,8,56]{2,0,1:T(2,128)(2,1)}), bf16[1,8,56]{2,0,1:T(2,128)(2,1)S(1)}, u32[]{:S(2)}, u32[]{:S(2)}) %all-to-all-start) | async-done | bytes 928 | tf_op jit(solution)/shard_map/all_to_all | solution.py:78
  34.1 4.3 %all-to-all-start.2 = ((bf16[1,8,56,2048]{3,2,0,1:T(8,128)(2,1)}), bf16[1,8,56,2048]{3,2,0,1:T(8,128)(2,1)}, u32[]{:S(2)}, u32[]{:S(2)}) async-start(bf16[1,8,56,2048]{3,2,0,1:T(8,128)(2,1)} %bitcast.67), calls=%async_computation.2 | async-start | bytes 3670016 | tf_op jit(solution)/shard_map/all_to_all | solution.py:76
  38.4 1.1 concatenate.10
  39.5 3.2 %gather_fusion.1 = bf16[448,2048]{1,0:T(8,128)(2,1)} fusion(bf16[129,2048]{1,0:T(8,128)(2,1)S(1)} %concatenate.10, s32[1024]{0:T(1024)S(1)} %get-tuple-element.82), kind=kCustom, calls=%fused_computation.1 | custom fusion | bytes 3671808 | tf_op jit(solution)/shard_map/gather | solution.py:73
  42.7 37.2 %all-to-all-done.2 = bf16[1,8,56,2048]{3,2,0,1:T(8,128)(2,1)} async-done(((bf16[1,8,56,2048]{3,2,0,1:T(8,128)(2,1)}), bf16[1,8,56,2048]{3,2,0,1:T(8,128)(2,1)}, u32[]{:S(2)}, u32[]{:S(2)}) %all-to-all-start.2) | async-done | bytes 1835040 | tf_op jit(solution)/shard_map/all_to_all | solution.py:76
  79.9 4.3 %all-to-all-start.1 = ((bf16[1,8,56,2048]{3,2,0,1:T(8,128)(2,1)}), bf16[1,8,56,2048]{3,2,0,1:T(8,128)(2,1)}, u32[]{:S(2)}, u32[]{:S(2)}) async-start(bf16[1,8,56,2048]{3,2,0,1:T(8,128)(2,1)} %bitcast.66), calls=%async_computation.1 | async-start | bytes 3670016 | tf_op jit(solution)/shard_map/all_to_all | solution.py:77
  84.2 0.2 reduce-scatter.2.cloned.1.call-start
  84.5 0.1 reshape.164
  84.6 4.2 %fusion.5 = f32[448,512]{1,0:T(8,128)} fusion(bf16[448,2048]{1,0:T(8,128)(2,1)} %bitcast.11, bf16[1,2048,512]{2,1,0:T(8,128)(2,1)} %param.11), kind=kOutput, calls=%fused_computation.17 | convolution fusion | flops 939524096 | bytes 4849664 | tf_op jit(solution)/shard_map/dot_general | solution.py:9
  88.8 3.5 %fusion.2 = f32[448,512]{1,0:T(8,128)} fusion(bf16[448,2048]{1,0:T(8,128)(2,1)} %bitcast.11, bf16[1,2048,512]{2,1,0:T(8,128)(2,1)S(1)} %copy-done), kind=kOutput, calls=%fused_computation.14 | convolution fusion | flops 939524096 | bytes 4849664 | tf_op jit(solution)/shard_map/dot_general | solution.py:8
  92.3 34.1 %all-to-all-done.1 = bf16[1,8,56,2048]{3,2,0,1:T(8,128)(2,1)} async-done(((bf16[1,8,56,2048]{3,2,0,1:T(8,128)(2,1)}), bf16[1,8,56,2048]{3,2,0,1:T(8,128)(2,1)}, u32[]{:S(2)}, u32[]{:S(2)}) %all-to-all-start.1) | async-done | bytes 1835040 | tf_op jit(solution)/shard_map/all_to_all | solution.py:77
  126.4 5.5 %multiply_reduce_fusion.3 = (f32[448]{0:T(512)}, bf16[448,512]{1,0:T(8,128)(2,1)}, bf16[448,512]{1,0:T(8,128)(2,1)S(1)}, bf16[448,512]{1,0:T(8,128)(2,1)S(1)}) fusion(f32[448,512]{1,0:T(8,128)} %fusion.5, f32[448,512]{1,0:T(8,128)} %fusion.2, f32[448]{0:T(512)S(1)} %reshape.164, bf16[448,2048]{1,0:T(8,128)(2,1)} %bitcast.7, bf16[1,512,2048]{2,1,0:T(8,128)(2,1)} %param.12), kind=kOutput, calls=%fused_computation.32 | convolution fusion | flops 944111168 | bytes 7147008 | tf_op jit(solution)/shard_map/dot_general | solution.py:12
  131.9 1.1 fusion
  133.1 0.4 copy-done.2
  133.5 3.0 %add_bitcast_fusion = f32[1,448,2048]{2,1,0:T(8,128)} fusion(f32[448,2048]{1,0:T(8,128)S(1)} %fusion, bf16[448,512]{1,0:T(8,128)(2,1)S(1)} %get-tuple-element.79, bf16[1,2048,512]{2,1,0:T(8,128)(2,1)S(1)} %copy-done.2), kind=kOutput, calls=%fused_computation.11 | convolution fusion | flops 940441600 | bytes 9895936 | tf_op jit(solution)/shard_map/dot_general | solution.py:34
  136.5 0.0 reduce-scatter.2.cloned.1.call-update
  136.6 4.1 %convert_bitcast_fusion.2 = (bf16[1,2048,512]{1,2,0:T(8,128)(2,1)}, f32[2048]{0:T(1024)S(1)}) fusion(bf16[448,2048]{1,0:T(8,128)(2,1)} %bitcast.11, bf16[448,512]{1,0:T(8,128)(2,1)S(1)} %get-tuple-element.78), kind=kOutput, calls=%fused_computation.23 | convolution fusion | flops 942667776 | bytes 4399104 | tf_op jit(solution)/shard_map/dot_general | solution.py:24
  140.7 4.3 %convert_bitcast_fusion.1 = (bf16[1,2048,512]{1,2,0:T(8,128)(2,1)}, f32[2048]{0:T(1024)S(1)}) fusion(bf16[448,2048]{1,0:T(8,128)(2,1)} %bitcast.11, bf16[448,512]{1,0:T(8,128)(2,1)S(1)} %get-tuple-element.79), kind=kOutput, calls=%fused_computation.22 | convolution fusion | flops 942667776 | bytes 4399104 | tf_op jit(solution)/shard_map/dot_general | solution.py:27
  145.0 11.0 %all-reduce.2 = (bf16[1,448]{1,0:T(2,128)(2,1)S(1)}, f32[1,2048]{1,0:T(1,128)}, f32[1,2048]{1,0:T(1,128)}) all-reduce(f32[1,448]{1,0:T(1,128)S(1)} %bitcast.73, f32[1,2048]{1,0:T(1,128)S(1)} %bitcast.68, f32[1,2048]{1,0:T(1,128)S(1)} %bitcast.69), channel_id=1, replica_groups=mesh['ep'=8,'tp'=4] {'tp'}, use_global_device_ids=true, to_apply=%region_8.9 | all-reduce | flops 4544 | bytes 35456 | tf_op jit(solution)/shard_map/psum | solution.py:105
  156.0 0.7 reshape.230
  156.7 4.5 %all-to-all-start.4 = ((bf16[1,8,56]{2,0,1:T(2,128)(2,1)}), bf16[1,8,56]{2,0,1:T(2,128)(2,1)S(1)}, u32[]{:S(2)}, u32[]{:S(2)}) async-start(bf16[1,8,56]{2,0,1:T(2,128)(2,1)} %reshape.230), calls=%async_computation.5 | async-start | bytes 8192 | tf_op jit(solution)/shard_map/all_to_all | solution.py:110
  161.3 15.6 %reduce-scatter.2.cloned.1.call-done = f32[1,448,512]{2,1,0:T(8,128)} async-done(((f32[1,448,2048]{2,1,0:T(8,128)}), f32[1,448,512]{2,1,0:T(8,128)}) %reduce-scatter.2.cloned.1.call-update) | async-done | bytes 917520 | tf_op jit(solution)/shard_map/reduce_scatter | solution.py:104
  176.9 2.0 convert_element_type.94
  178.9 5.5 %all-to-all-start.3 = ((bf16[1,8,56,512]{3,2,0,1:T(8,128)(2,1)}), bf16[1,8,56,512]{3,2,0,1:T(8,128)(2,1)S(1)}, u32[]{:S(2)}, u32[]{:S(2)}) async-start(bf16[1,8,56,512]{3,2,0,1:T(8,128)(2,1)} %bitcast.16), calls=%async_computation.4 | async-start | bytes 917504 | tf_op jit(solution)/shard_map/all_to_all | solution.py:109
  184.4 4.9 %multiply_reduce_fusion = (f32[512]{0:T(512)}, bf16[1,512,2048]{2,1,0:T(8,128)(2,1)}) fusion(bf16[448,512]{1,0:T(8,128)(2,1)} %get-tuple-element.67, bf16[448,2048]{1,0:T(8,128)(2,1)} %bitcast.7, f32[448]{0:T(512)S(1)} %copy-done.11), kind=kOutput, calls=%fused_computation.7 | convolution fusion | flops 945421824 | bytes 4394752 | tf_op jit(solution)/shard_map/dot_general | solution.py:23
  189.3 3.9 %copy.90 = bf16[1,2048,512]{2,1,0:T(8,128)(2,1)} copy(bf16[1,2048,512]{1,2,0:T(8,128)(2,1)} %get-tuple-element.76) | data formatting | bytes 4194304
  193.3 3.9 %copy.91 = bf16[1,2048,512]{2,1,0:T(8,128)(2,1)} copy(bf16[1,2048,512]{1,2,0:T(8,128)(2,1)} %get-tuple-element.74) | data formatting | bytes 4194304
  197.2 0.1 reshape.163
  197.3 1.9 gather_fusion.4
  199.2 0.1 reshape.166
  199.4 0.1 copy.89
  199.5 0.1 fusion.15
  199.7 37.5 %psum.29 = f32[512,8]{0,1:T(8,128)S(1)} all-reduce(f32[512,8]{0,1:T(8,128)S(1)} %fusion.15), channel_id=1, replica_groups=mesh['ep'=8,'tp'=4] {'ep'}, use_global_device_ids=true, to_apply=%region_11.12 | all-reduce | flops 4096 | bytes 32768 | tf_op jit(solution)/shard_map/psum | solution.py:128
  237.2 0.6 multiply_reduce_fusion.4
  237.8 1.2 gather_fusion.3
  239.0 0.3 reshape.165
  239.3 0.6 reduce_sum.101
  239.9 0.9 fusion.11
  240.9 6.5 %all_gather.3 = bf16[128,2048]{1,0:T(8,128)(2,1)S(1)} all-gather(bf16[128,512]{1,0:T(8,128)(2,1)S(1)} %fusion.11), channel_id=1, replica_groups=mesh['ep'=8,'tp'=4] {'tp'}, dimensions={1}, use_global_device_ids=true | all-gather | bytes 655360 | tf_op jit(solution)/shard_map/all_gather | solution.py:134
  247.4 0.8 copy.93
  (44 shorter events, 0.4 us)
Async XLA Ops:
  7.2 81.6 %copy-start = (bf16[1,2048,512]{2,1,0:T(8,128)(2,1)S(1)}, bf16[1,2048,512]{2,1,0:T(8,128)(2,1)}, u32[]{:S(2)}) copy-start(bf16[1,2048,512]{2,1,0:T(8,128)(2,1)} %param.10) | copy-start | bytes 6291460
  11.0 1.7 copy-start.7
  14.0 1.6 copy-start.4
  14.0 13.7 %copy-start.1 = (bf16[128,2048]{1,0:T(8,128)(2,1)S(1)}, bf16[128,2048]{1,0:T(8,128)(2,1)}, u32[]{:S(2)}) copy-start(bf16[128,2048]{1,0:T(8,128)(2,1)} %param.7) | copy-start | bytes 1572868
  15.6 15.3 %copy-start.5 = (f32[128]{0:T(128)}, f32[128]{0:T(128)S(1)}, u32[]{:S(2)}) copy-start(f32[128]{0:T(128)S(1)} %get-tuple-element.70) | copy-start | bytes 1540
  20.4 13.7 %all-to-all-start = ((bf16[1,8,56]{2,0,1:T(2,128)(2,1)}), bf16[1,8,56]{2,0,1:T(2,128)(2,1)S(1)}, u32[]{:S(2)}, u32[]{:S(2)}) async-start(bf16[1,8,56]{2,0,1:T(2,128)(2,1)} %reshape.229), calls=%async_computation | async-start | bytes 8192 | tf_op jit(solution)/shard_map/all_to_all | solution.py:78
  34.1 45.8 %all-to-all-start.2 = ((bf16[1,8,56,2048]{3,2,0,1:T(8,128)(2,1)}), bf16[1,8,56,2048]{3,2,0,1:T(8,128)(2,1)}, u32[]{:S(2)}, u32[]{:S(2)}) async-start(bf16[1,8,56,2048]{3,2,0,1:T(8,128)(2,1)} %bitcast.67), calls=%async_computation.2 | async-start | bytes 3670016 | tf_op jit(solution)/shard_map/all_to_all | solution.py:76
  79.9 46.5 %all-to-all-start.1 = ((bf16[1,8,56,2048]{3,2,0,1:T(8,128)(2,1)}), bf16[1,8,56,2048]{3,2,0,1:T(8,128)(2,1)}, u32[]{:S(2)}, u32[]{:S(2)}) async-start(bf16[1,8,56,2048]{3,2,0,1:T(8,128)(2,1)} %bitcast.66), calls=%async_computation.1 | async-start | bytes 3670016 | tf_op jit(solution)/shard_map/all_to_all | solution.py:77
  84.2 92.7 %reduce-scatter.2.cloned.1.call-start = ((), (), s32[]{:S(2)}) async-start(), calls=%async_computation.6 | async-start | bytes 4587520 | tf_op jit(solution)/shard_map/reduce_scatter | solution.py:104
  84.6 41.8 %copy-start.10 = (f32[448]{0:T(512)}, f32[448]{0:T(512)S(1)}, u32[]{:S(2)}) copy-start(f32[448]{0:T(512)S(1)} %reshape.164) | copy-start | bytes 5380
  131.9 1.6 copy-start.2
  140.7 4.3 %copy-start.12 = (f32[448]{0:T(512)S(1)}, f32[448]{0:T(512)}, u32[]{:S(2)}) copy-start(f32[448]{0:T(512)} %get-tuple-element.66) | copy-start | bytes 5380
  140.7 20.6 %copy-start.8 = (s32[256,1]{0,1:T(1,128)S(1)}, s32[256,1]{0,1:T(1,128)}, u32[]{:S(2)}) copy-start(s32[256,1]{0,1:T(1,128)} %copy-done.7) | copy-start | bytes 3076
  145.0 39.4 %copy-start.11 = (f32[448]{0:T(512)S(1)}, f32[448]{0:T(512)}, u32[]{:S(2)}) copy-start(f32[448]{0:T(512)} %copy-done.10) | copy-start | bytes 5380
  156.7 22.2 %all-to-all-start.4 = ((bf16[1,8,56]{2,0,1:T(2,128)(2,1)}), bf16[1,8,56]{2,0,1:T(2,128)(2,1)S(1)}, u32[]{:S(2)}, u32[]{:S(2)}) async-start(bf16[1,8,56]{2,0,1:T(2,128)(2,1)} %reshape.230), calls=%async_computation.5 | async-start | bytes 8192 | tf_op jit(solution)/shard_map/all_to_all | solution.py:110
  178.9 58.9 %all-to-all-start.3 = ((bf16[1,8,56,512]{3,2,0,1:T(8,128)(2,1)}), bf16[1,8,56,512]{3,2,0,1:T(8,128)(2,1)S(1)}, u32[]{:S(2)}, u32[]{:S(2)}) async-start(bf16[1,8,56,512]{3,2,0,1:T(8,128)(2,1)} %bitcast.16), calls=%async_computation.4 | async-start | bytes 917504 | tf_op jit(solution)/shard_map/all_to_all | solution.py:109
  193.3 6.2 %copy-start.9 = (f32[128,2]{0,1:T(2,128)S(1)}, f32[128,2]{0,1:T(2,128)}, u32[]{:S(2)}) copy-start(f32[128,2]{0,1:T(2,128)} %get-tuple-element.69) | copy-start | bytes 3076
  193.3 6.2 %copy-start.6 = (f32[128]{0:T(128)S(1)}, f32[128]{0:T(128)}, u32[]{:S(2)}) copy-start(f32[128]{0:T(128)} %copy-done.5) | copy-start | bytes 1540
  237.2 3.7 %copy-start.3 = (f32[512,8]{0,1:T(8,128)}, f32[512,8]{0,1:T(8,128)S(1)}, u32[]{:S(2)}) copy-start(f32[512,8]{0,1:T(8,128)S(1)} %psum.29) | copy-start | bytes 49156
Sparse Core Ops, SparseCore 0:
  136.7 40.1 reduce-scatter.1
where the time goes:
time: 256 us; the launch traced here: 255 us
  waiting for transfers between devices  90.1 us (35%)
  blocking collectives  55 us (21%)
  matrix products  33.1 us (13%)
  local copies, waits for them, and re-layouts  30 us (12%)
  starting transfers between devices  26.2 us (10%)
  between operations  14.3 us (6%)
  other arithmetic  6.23 us (2%)
    psum x1, blocking collectives, per_device(): router_grad = lax.psum(router_part, 'ep')  37.5 us
    all_to_all x1, waiting for transfers between devices, per_device(): lax.all_to_all(rows_send, 'ep', split_axis=1, concat_axis=1, tiled=True)  37.2 us
    all_to_all x1, waiting for transfers between devices, per_device(): lax.all_to_all(cots_send, 'ep', split_axis=1, concat_axis=1, tiled=True)  34.1 us
    reduce_scatter x1, waiting for transfers between devices, per_device(): lax.psum_scatter(partial_value, 'tp', scatter_dimension=2, tiled=True)  15.6 us
    psum x1, blocking collectives, per_device(): gate_sum = lax.psum(gate_term, 'tp')  11 us
    unnamed x30, local copies, waits for them, and re-layouts  9.92 us
    all_to_all x1, starting transfers between devices, per_device(): lax.all_to_all(scale_send, 'ep', split_axis=1, concat_axis=1, tiled=True)  7.28 us
    all_gather x1, blocking collectives, per_device(): token_grad = lax.all_gather(token_grad, 'tp', axis=1, tiled=True)  6.5 us
  transfers between devices with their start and end apart: 6, of which 4 were waited for; matrix products, arithmetic and copies ran while one was open for 17% of the time, Pallas kernels for 0%

commit v1 on v0

v1 whole, which is shorter than its diff:
```python
import functools

import jax
import jax.numpy as jnp
from jax import lax
from jax.experimental import pallas as pl
from jax.experimental.pallas import tpu as pltpu
from jax.sharding import PartitionSpec as P


BF16 = jnp.bfloat16
F32 = jnp.float32
VMEM = pl.BlockSpec(memory_space=pltpu.VMEM)
SMEM = pl.BlockSpec(memory_space=pltpu.SMEM)


def dot(a, b, ca=1, cb=0):
    return lax.dot_general(a, b, (((ca,), (cb,)), ((), ())), preferred_element_type=F32)


def params(mib=40):
    return pltpu.CompilerParams(vmem_limit_bytes=mib * 1024 * 1024)


def cost(flops, bytes_accessed):
    return pl.CostEstimate(flops=flops, bytes_accessed=bytes_accessed, transcendentals=0)


def one_hot(place, slots):
    experts, toks = place.shape
    rows = lax.broadcasted_iota(jnp.int32, (slots, toks), 0).astype(F32)
    return [(rows == place[e : e + 1, :]).astype(F32) for e in range(experts)]


def route_kernel(slots, q_ref, tok_ref, routing_ref, router_ref, rows_ref, aff_ref, place_ref):
    toks = tok_ref.shape[0]
    experts = router_ref.shape[0]
    cols = rows_ref.shape[2]
    start = pl.multiple_of(q_ref[0] * cols, 128)
    aff = jax.nn.sigmoid(dot(router_ref[...], tok_ref[...], 1, 1))
    ids = lax.broadcasted_iota(jnp.int32, (experts, toks), 0)
    routed = routing_ref[...]
    named = jnp.zeros((experts, toks), F32)
    for k in range(routed.shape[0]):
        named = named + (ids == routed[k : k + 1, :]).astype(F32)
    before = lax.broadcasted_iota(jnp.int32, (toks, toks), 0)
    after = lax.broadcasted_iota(jnp.int32, (toks, toks), 1)
    earlier = (before < after).astype(F32).astype(BF16)
    position = dot(named.astype(BF16), earlier)
    place = jnp.where(named > 0, position, -1.0)
    chosen = named * aff
    weights = chosen / jnp.sum(chosen, axis=0, keepdims=True)
    aff_ref[...] = aff
    place_ref[...] = place
    hot = one_hot(place, slots)
    full = jnp.concatenate(hot, axis=0).astype(BF16)
    sent = dot(full, tok_ref[:, pl.ds(start, cols)])
    lane = lax.broadcasted_iota(jnp.int32, (8, cols), 1)
    for e in range(experts):
        column = jnp.sum(hot[e] * weights[e : e + 1, :], axis=1, keepdims=True)
        tile = jnp.zeros((8, cols), F32)
        for g in range(slots // 8):
            tile = jnp.where(lane == g, column[8 * g : 8 * g + 8, :], tile)
        block = jnp.concatenate([sent[e * slots : (e + 1) * slots, :], tile], axis=0)
        rows_ref[e] = block.astype(BF16)


def cots_kernel(slots, q_ref, cot_ref, place_ref, cots_ref):
    cols = cots_ref.shape[2]
    start = pl.multiple_of((q_ref[0] % 2) * cols, 128)
    hot = one_hot(place_ref[...], slots)
    full = jnp.concatenate(hot, axis=0).astype(BF16)
    sent = dot(full, cot_ref[:, pl.ds(start, cols)])
    for e in range(len(hot)):
        cots_ref[e] = sent[e * slots : (e + 1) * slots, :].astype(BF16)


def gate_up_kernel(slots, shares, q_ref, *refs):
    x_refs = refs[:shares]
    wg_ref, wu_ref, hid_ref, up_ref, gate_ref, acc_g, acc_u = refs[shares:]
    groups, span, cols = x_refs[0].shape
    for r in range(shares):
        x = x_refs[r][...].reshape(groups * span, cols)
        rows = pl.ds(pl.multiple_of((q_ref[0] ^ r) * cols, 128), cols)
        part_g = dot(x, wg_ref[rows, :])
        part_u = dot(x, wu_ref[rows, :])
        if r == 0:
            acc_g[...] = part_g
            acc_u[...] = part_u
        else:
            acc_g[...] += part_g
            acc_u[...] += part_u
    for e in range(groups):
        scale = scale_column(x_refs[0], e, slots)
        at = slice(e * span, e * span + slots)
        pre_gate = acc_g[at, :]
        pre_up = acc_u[at, :]
        sig = jax.nn.sigmoid(pre_gate)
        act = pre_gate * sig
        hid_ref[e] = (act * pre_up).astype(BF16)
        up_ref[e] = scale * act
        gate_ref[e] = scale * (pre_up * sig * (1.0 + pre_gate * (1.0 - sig)))


def scale_column(x_ref, e, slots):
    tile = x_ref[e, slots:, :128].astype(F32)
    return jnp.concatenate([tile[:, g : g + 1] for g in range(slots // 8)], axis=0)


def back_kernel(half, q_ref, z_ref, wd_ref, back_ref):
    cols = z_ref.shape[1]
    start = pl.multiple_of(((q_ref[0] % 2) ^ half) * cols, 128)
    back_ref[...] = dot(z_ref[...], wd_ref[:, pl.ds(start, cols)], 1, 1)


def slot_parts(q_ref, first, gg, gu, wg_ref, wu_ref, shares):
    cols = wg_ref.shape[0] // shares
    start = pl.multiple_of((q_ref[0] ^ first) * cols, 128)
    return dot(gg, wg_ref[pl.ds(start, cols), :], 1, 1) + dot(
        gu, wu_ref[pl.ds(start, cols), :], 1, 1
    )


def middle_kernel(
    slots, shares, q_ref, back_ref, z_ref, wd_ref, hid_ref, up_ref, gate_ref,
    wg_ref, wu_ref, gg_ref, gu_ref, odd_ref, term_ref,
):
    cols = z_ref.shape[1]
    groups = gg_ref.shape[0]
    start = pl.multiple_of(((q_ref[0] % 2) ^ 1) * cols, 128)
    back = back_ref[...] + dot(z_ref[...], wd_ref[:, pl.ds(start, cols)], 1, 1)
    term = jnp.sum(hid_ref[...].astype(F32) * back, axis=1, keepdims=True)
    gu = back * up_ref[...]
    gg = back * gate_ref[...]
    pad = jnp.zeros((8, gu.shape[1]), F32)
    for e in range(groups):
        at = slice(e * slots, (e + 1) * slots)
        gu_ref[e] = jnp.concatenate([gu[at], pad], axis=0).astype(BF16)
        gg_ref[e] = jnp.concatenate([gg[at], pad], axis=0).astype(BF16)
    lane = lax.broadcasted_iota(jnp.int32, term_ref.shape, 1)
    tile = jnp.zeros(term_ref.shape, F32)
    for c in range(term.shape[0] // 8):
        tile = jnp.where(lane == c, term[8 * c : 8 * c + 8, :], tile)
    term_ref[...] = tile
    gg = gg.astype(BF16)
    gu = gu.astype(BF16)
    for j in range(shares // 2):
        part = slot_parts(q_ref, 2 * j + 1, gg, gu, wg_ref, wu_ref, shares)
        odd_ref[j] = part.astype(BF16)


def even_kernel(slots, shares, q_ref, gg_ref, gu_ref, wg_ref, wu_ref, even_ref):
    groups, span, hidden = gg_ref.shape
    gg = gg_ref[...].reshape(groups * span, hidden)
    gu = gu_ref[...].reshape(groups * span, hidden)
    for j in range(shares // 2):
        part = slot_parts(q_ref, 2 * j, gg, gu, wg_ref, wu_ref, shares)
        for e in range(groups):
            even_ref[j, e] = part[e * span : e * span + slots, :]


def add_core_kernel(own_ref, got_ref, out_ref):
    for j in range(out_ref.shape[0]):
        out_ref[j] = (own_ref[j + 1] + got_ref[j + 1].astype(F32)).astype(BF16)


def add_chip_kernel(own_ref, core_ref, *refs):
    total = own_ref[0] + core_ref[0].astype(F32)
    for chip_ref in refs[:-1]:
        total = total + chip_ref[...].astype(F32)
    refs[-1][...] = total.astype(BF16)


def term_kernel(slots, own_ref, got_ref, out_ref):
    total = (own_ref[...] + got_ref[...]).astype(BF16).astype(F32)
    count = slots // 8
    out_ref[...] = jnp.zeros(out_ref.shape, F32)
    for b in range(out_ref.shape[0]):
        out_ref[b, :, :count] = total[:, b * count : (b + 1) * count]


def grads_kernel(shares, q_ref, *refs):
    x_refs = refs[:shares]
    gg_ref, gu_ref, gate_out, up_out, rows_out = refs[shares:]
    groups, span, cols = x_refs[0].shape
    hidden = gg_ref.shape[2]
    for r in range(shares):

        @pl.when(pl.program_id(0) == r)
        def _(x_ref=x_refs[r]):
            x = x_ref[...].reshape(groups * span, cols)
            gate = dot(x, gg_ref[...].reshape(groups * span, hidden), 0, 0)
            up = dot(x, gu_ref[...].reshape(groups * span, hidden), 0, 0)
            gate_out[...] = gate.astype(BF16)
            up_out[...] = up.astype(BF16)
            rows_out[0, 0:1, :] = square_rows(gate)
            rows_out[0, 1:2, :] = square_rows(up)


def square_rows(value):
    square = value * value
    folded = square[:, :128]
    for at in range(128, value.shape[1], 128):
        folded = folded + square[:, at : at + 128]
    return jnp.sum(folded.T, axis=0, keepdims=True)


def down_kernel(slots, q_ref, own_ref, far_ref, x_ref, hid_ref, down_out, rows_out):
    groups = x_ref.shape[0]
    for h, z_ref in enumerate((own_ref, far_ref)):

        @pl.when(pl.program_id(0) == h)
        def _(z_ref=z_ref):
            scale = jnp.concatenate([scale_column(x_ref, e, slots) for e in range(groups)], axis=0)
            weighted = (scale * z_ref[...].astype(F32)).astype(BF16)
            down = dot(hid_ref[...], weighted, 0, 0)
            down_out[...] = down.astype(BF16)
            rows_out[0] = square_rows(down)


def router_kernel(slots, q_ref, term_ref, place_ref, aff_ref, tok_ref, logit_out, part_out):
    experts, toks = place_ref.shape
    cols = part_out.shape[1]
    start = pl.multiple_of(q_ref[0] * cols, 128)
    place = place_ref[...]
    aff = aff_ref[...]
    hot = one_hot(place, slots)
    rows = []
    for e in range(experts):
        tile = term_ref[e]
        total = jnp.zeros((8, toks), F32)
        for g in range(slots // 8):
            total = total + hot[e][8 * g : 8 * g + 8, :] * tile[:, g : g + 1]
        rows.append(jnp.sum(total, axis=0, keepdims=True))
    term = jnp.concatenate(rows, axis=0)
    named = (place >= 0).astype(F32)
    chosen = named * aff
    total_aff = jnp.sum(chosen, axis=0, keepdims=True)
    weights = chosen / total_aff
    d_chosen = (term - jnp.sum(term * weights, axis=0, keepdims=True)) / total_aff
    d_logit = named * d_chosen * aff * (1.0 - aff)
    logit_out[...] = d_logit
    part_out[...] = dot(d_logit.astype(BF16), tok_ref[:, pl.ds(start, cols)])


def home_kernel(q_ref, got_ref, place_ref, logit_ref, router_ref, token_out):
    cols = got_ref.shape[1]
    start = pl.multiple_of(q_ref[0] * cols, 128)
    experts = place_ref.shape[0]
    full = jnp.concatenate(one_hot(place_ref[...], got_ref.shape[0] // experts), axis=0).astype(BF16)
    back = dot(full, got_ref[...], 0, 0)
    router_back = dot(logit_ref[...].T.astype(BF16), router_ref[:, pl.ds(start, cols)])
    token_out[...] = (back + router_back).astype(BF16)


def assemble_kernel(q_ref, *refs):
    out_ref = refs[-1]
    for r, ref in enumerate(refs[:-1]):
        cols = ref.shape[1]
        out_ref[:, pl.ds(pl.multiple_of((q_ref[0] ^ r) * cols, 128), cols)] = ref[...]


def call(kernel, outs, scalar, *args, flops=0, nbytes=0, scratch=()):
    single = not isinstance(outs, tuple)
    return pl.pallas_call(
        kernel,
        out_shape=outs,
        in_specs=([SMEM] if scalar else []) + [VMEM] * (len(args) - int(scalar)),
        out_specs=VMEM if single else tuple(VMEM for _ in outs),
        scratch_shapes=list(scratch),
        compiler_params=params(),
        cost_estimate=cost(flops, nbytes),
    )(*args)


def shape(*dims, dtype=BF16):
    return jax.ShapeDtypeStruct(dims, dtype)


def per_device(tokens, routing, router_weight, gate_weight, up_weight, down_weight, cotangent):
    return layer(tokens, routing.T, router_weight.T, gate_weight[0], up_weight[0], down_weight[0], cotangent)


def layer(tokens, routing, router, wg, wu, wd, cotangent):
    groups = lax.axis_size("ep")
    shares = lax.axis_size("tp")
    chips = shares // 2
    toks, width = tokens.shape
    top = routing.shape[0]
    experts = router.shape[0]
    hidden = wg.shape[1]
    capacity = 7 * toks * top // (4 * experts)
    slots = -(-capacity // 8) * 8
    span = slots + 8
    count = groups * slots
    cols = width // shares
    half = width // 2
    unit = 2 * count * half * hidden
    q = lax.axis_index("tp").astype(jnp.int32).reshape(1)

    def swap(value, bit, axis="tp"):
        size = lax.axis_size(axis)
        return lax.ppermute(value, axis, [(i, i ^ bit) for i in range(size)])

    def exchange(value):
        return lax.all_to_all(value, "ep", split_axis=0, concat_axis=0, tiled=True)

    def spread(value):
        far = [value] + [swap(value, 2 * j) for j in range(1, chips)]
        return [part for piece in far for part in (piece, swap(piece, 1))]

    rows_send, aff, place = call(
        functools.partial(route_kernel, slots),
        (shape(experts, span, cols), shape(experts, toks, dtype=F32), shape(experts, toks, dtype=F32)),
        True, q, tokens, routing, router,
    )
    rows_got = exchange(rows_send)
    cots_send = call(
        functools.partial(cots_kernel, slots), shape(experts, slots, half),
        True, q, cotangent, place, flops=2 * count * toks * half,
    )
    cots_send, rows_got = lax.optimization_barrier((cots_send, rows_got))
    cots_got = exchange(cots_send)

    x_parts = spread(rows_got)
    hid, up_factor, gate_factor = call(
        functools.partial(gate_up_kernel, slots, shares),
        (shape(groups, slots, hidden), shape(groups, slots, hidden, dtype=F32), shape(groups, slots, hidden, dtype=F32)),
        True, q, *x_parts, wg, wu, flops=4 * unit,
        scratch=[pltpu.VMEM((groups * span, hidden), F32)] * 2,
    )
    hid = hid.reshape(count, hidden)
    up_factor = up_factor.reshape(count, hidden)
    gate_factor = gate_factor.reshape(count, hidden)

    z_own = cots_got.reshape(count, half)
    z_far = swap(z_own, 1)
    back = call(
        functools.partial(back_kernel, 0), shape(count, hidden, dtype=F32),
        True, q, z_own, wd, flops=unit,
    )
    gg, gu, odd, term = call(
        functools.partial(middle_kernel, slots, shares),
        (
            shape(groups, span, hidden),
            shape(groups, span, hidden),
            shape(chips, count, cols),
            shape(8, -(-count // 1024) * 128, dtype=F32),
        ),
        True, q, back, z_far, wd, hid, up_factor, gate_factor, wg, wu, flops=3 * unit,
    )
    term_got = swap(term, 1)
    core_got = swap(odd, 1)
    even = call(
        functools.partial(even_kernel, slots, shares), shape(chips, groups, slots, cols, dtype=F32),
        True, q, gg, gu, wg, wu, flops=2 * unit,
    ).reshape(chips, count, cols)
    term = term + term_got
    bit = 2
    while 2 * bit < shares:
        term = term + swap(term, bit)
        bit *= 2
    term_got = swap(term, bit)
    chip_send = call(add_core_kernel, shape(chips - 1, count, cols), False, even, core_got)
    chip_got = [swap(chip_send[j], 2 * (j + 1)) for j in range(chips - 1)]
    terms = call(
        functools.partial(term_kernel, slots), shape(groups, 8, 128, dtype=F32), False, term, term_got,
    )
    terms = exchange(terms)
    home_send = call(add_chip_kernel, shape(count, cols), False, even, core_got, *chip_got)
    home_got = exchange(home_send.reshape(groups, slots, cols)).reshape(count, cols)

    grad_spec = pl.BlockSpec((cols, hidden), lambda r, q: (q[0] ^ r, 0))
    gate_grad, up_grad, norms = pl.pallas_call(
        functools.partial(grads_kernel, shares),
        out_shape=(shape(width, hidden), shape(width, hidden), shape(shares, 2, cols, dtype=F32)),
        grid_spec=pltpu.PrefetchScalarGridSpec(
            num_scalar_prefetch=1,
            grid=(shares,),
            in_specs=[VMEM] * (shares + 2),
            out_specs=(grad_spec, grad_spec, pl.BlockSpec((1, 2, cols), lambda r, q: (q[0] ^ r, 0, 0))),
        ),
        compiler_params=params(),
        cost_estimate=cost(4 * unit, 0),
        name="grads",
    )(q, *x_parts, gg, gu)
    down_grad, down_norms = pl.pallas_call(
        functools.partial(down_kernel, slots),
        out_shape=(shape(hidden, width), shape(2, 1, hidden, dtype=F32)),
        grid_spec=pltpu.PrefetchScalarGridSpec(
            num_scalar_prefetch=1,
            grid=(2,),
            in_specs=[VMEM] * 4,
            out_specs=(
                pl.BlockSpec((hidden, half), lambda h, q: (0, (q[0] % 2) ^ h)),
                pl.BlockSpec((1, 1, hidden), lambda h, q: (h, 0, 0)),
            ),
        ),
        compiler_params=params(),
        cost_estimate=cost(2 * unit, 0),
        name="down",
    )(q, z_own, z_far, rows_got, hid)
    norms = norms.transpose(1, 0, 2).reshape(2, width)
    bit = 1
    while bit < shares:
        norms = norms + swap(norms, bit)
        bit *= 2
    down_rows = (down_norms[0] + down_norms[1]).reshape(1, hidden)

    d_logits, router_sum = call(
        functools.partial(router_kernel, slots),
        (shape(experts, toks, dtype=F32), shape(experts, cols, dtype=F32)),
        True, q, terms, place, aff, tokens,
    )
    bit = 1
    while bit < groups:
        router_sum = router_sum + swap(router_sum, bit, "ep")
        bit *= 2
    router_rows = jnp.sum(router_sum * router_sum, axis=0)
    token_part = call(home_kernel, shape(toks, cols), True, q, home_got, place, d_logits, router)
    token_grad = call(assemble_kernel, shape(toks, width), True, q, *spread(token_part))
    return (
        token_grad,
        router_sum.T,
        router_rows,
        gate_grad[None],
        up_grad[None],
        down_grad[None],
        norms[0:1],
        norms[1:2],
        down_rows,
    )


def solution(mesh):
    return jax.shard_map(
        per_device,
        mesh=mesh,
        in_specs=(
            P("ep", None),
            P("ep", None),
            P(),
            P("ep", None, "tp"),
            P("ep", None, "tp"),
            P("ep", "tp", None),
            P("ep", None),
        ),
        out_specs=(
            P("ep", None),
            P("tp", None),
            P("tp"),
            P("ep", None, "tp"),
            P("ep", None, "tp"),
            P("ep", "tp", None),
            P("ep", None),
            P("ep", None),
            P("ep", "tp"),
        ),
        check_vma=False,
    )
```

time: 256 us -> 129 us (0.50)
  blocking collectives: 55 us -> 0 us
  matrix products: 33.1 us -> 0 us
  waiting for transfers between devices: 90.1 us -> 59.5 us
  Pallas kernels: 0 us -> 23.9 us
  local copies, waits for them, and re-layouts: 30 us -> 11.3 us
  between operations: 14.3 us -> 0.87 us
  other arithmetic: 6.23 us -> 1.8 us
  starting transfers between devices: 26.2 us -> 30.5 us
    psum x2 -> x0, blocking collectives: 48.5 us -> none  [the longest x1 37.5 us: per_device(): router_grad = lax.psum(router_part, 'ep')]
    all_to_all x5 -> x4, waiting for transfers between devices: 74.4 us -> 38.5 us  [exchange(): return lax.all_to_all(value, 'ep', split_axis=0, concat_axis=0, tiled=True)]
    dot_general x11 -> x0, matrix products: 33.1 us -> none  [the longest x1 5.52 us: expert_backward(): lax.dot_general(cots_in, w_down, (((1,), (1,)), ((), ())), preferred_elem...]
    pallas_call x0 -> x14, Pallas kernels: none -> 23.9 us  [the longest x12 15 us: call(): pl.pallas_call(kernel, out_shape=outs, in_specs=([SMEM] if scalar else []...]
    ppermute x0 -> x16, waiting for transfers between devices: none -> 21.1 us  [swap(): return lax.ppermute(value, axis, [(i, i ^ bit) for i in range(size)])]
    reduce_scatter x1 -> x0, waiting for transfers between devices: 15.6 us -> none  [per_device(): lax.psum_scatter(partial_value, 'tp', scatter_dimension=2, tiled=True)]
    gather x10 -> x0, local copies, waits for them, and re-layouts: 14.5 us -> none  [the longest x1 3.2 us: per_device(): tok_pad[source_tok].reshape(local_experts, groups, capacity, model_width)]
    ppermute x0 -> x16, starting transfers between devices: none -> 12.3 us  [swap(): return lax.ppermute(value, axis, [(i, i ^ bit) for i in range(size)])]
  transfers between devices with their start and end apart: 6 -> 20, of which waited for: 4 -> 12; matrix products, arithmetic and copies ran while one was open for 17% -> 2% of each run, Pallas kernels for 0% -> 15%
where the time goes in v1:
time: 129 us; the launch traced here: 128 us
  waiting for transfers between devices  59.5 us (46%)
  starting transfers between devices  30.5 us (24%)
  Pallas kernels  23.9 us (19%)
  local copies, waits for them, and re-layouts  11.3 us (9%)
  other arithmetic  1.8 us (1%)
    all_to_all x4, waiting for transfers between devices, exchange(): return lax.all_to_all(value, 'ep', split_axis=0, concat_axis=0, tiled=True)  38.5 us
    ppermute x16, waiting for transfers between devices, swap(): return lax.ppermute(value, axis, [(i, i ^ bit) for i in range(size)])  21.1 us
    all_to_all x4, starting transfers between devices, exchange(): return lax.all_to_all(value, 'ep', split_axis=0, concat_axis=0, tiled=True)  18.2 us
    pallas_call x12, Pallas kernels, call(): pl.pallas_call(kernel, out_shape=outs, in_specs=([SMEM] if scalar else []...  15 us
    ppermute x16, starting transfers between devices, swap(): return lax.ppermute(value, axis, [(i, i ^ bit) for i in range(size)])  12.3 us
    unnamed x50, local copies, waits for them, and re-layouts  10.7 us
    pallas_call x1, Pallas kernels, layer(): pl.pallas_call(functools.partial(grads_kernel, shares), out_shape=(shape(...  5.73 us
    pallas_call x1, Pallas kernels, layer(): pl.pallas_call(functools.partial(down_kernel, slots), out_shape=(shape(hi...  3.15 us
  transfers between devices with their start and end apart: 20, of which 12 were waited for; matrix products, arithmetic and copies ran while one was open for 2% of the time, Pallas kernels for 15%

profile of v1, /device:TPU:0, one launch (start us, length us, event | category | flops | bytes accessed | tf_op | source)
XLA Modules:
  0.0 127.9 jit_solution(11880108056460981943)
XLA Ops:
  0.6 0.0 copy-start.7
  0.7 1.0 copy-done.7
  1.7 0.8 copy-done.18
  2.5 0.7 copy-done.20
  3.1 1.3 %shard_map.142 = (bf16[8,64,512]{2,1,0:T(8,128)(2,1)}, f32[8,128]{1,0:T(8,128)S(1)}, f32[8,128]{1,0:T(8,128)S(1)}) custom-call(s32[1]{0:T(128)} %bitcast.q_ref, bf16[128,2048]{1,0:T(8,128)(2,1)S(1)} %copy-done.7, s32[2,128]{1,0:T(2,128)S(1)} %bitcast.46, bf16[8,2048]{1,0:T(8,128)(2,1)S(1)} %bitcast.42), custom_call_target="tpu_custom_call" | custom-call | tf_op jit(solution)/shard_map/pallas_call | solution.py:265
  4.5 7.4 %all-to-all-start = ((bf16[8,64,512]{2,1,0:T(8,128)(2,1)}), bf16[8,64,512]{2,1,0:T(8,128)(2,1)S(1)}, u32[]{:S(2)}, u32[]{:S(2)}) async-start(bf16[8,64,512]{2,1,0:T(8,128)(2,1)} %get-tuple-element.29), calls=%async_computation | async-start | bytes 1048576 | tf_op jit(solution)/shard_map/all_to_all | solution.py:306
  11.9 1.0 copy-done.13
  12.9 1.3 %shard_map.143 = bf16[8,56,1024]{2,1,0:T(8,128)(2,1)} custom-call(s32[1]{0:T(128)} %bitcast.q_ref, bf16[128,2048]{1,0:T(8,128)(2,1)S(1)} %copy-done.13, f32[8,128]{1,0:T(8,128)S(1)} %get-tuple-element.28.place_ref), custom_call_target="tpu_custom_call" | custom-call | flops 117440512 | tf_op jit(solution)/shard_map/pallas_call | solution.py:265
  14.2 12.1 %all-to-all-done.refs_0_.x_ref = bf16[8,64,512]{2,1,0:T(8,128)(2,1)S(1)} async-done(((bf16[8,64,512]{2,1,0:T(8,128)(2,1)}), bf16[8,64,512]{2,1,0:T(8,128)(2,1)S(1)}, u32[]{:S(2)}, u32[]{:S(2)}) %all-to-all-start) | async-done | bytes 524320 | tf_op jit(solution)/shard_map/all_to_all | solution.py:306
  26.4 3.6 %all-to-all-start.1 = ((bf16[8,56,1024]{2,1,0:T(8,128)(2,1)}), bf16[8,56,1024]{2,1,0:T(8,128)(2,1)S(1)}, u32[]{:S(2)}, u32[]{:S(2)}) async-start(bf16[8,56,1024]{2,1,0:T(8,128)(2,1)} %shard_map.143), calls=%async_computation.1 | async-start | bytes 1835008 | tf_op jit(solution)/shard_map/all_to_all | solution.py:306
  30.0 1.5 %collective-permute-start.2 = (bf16[8,64,512]{2,1,0:T(8,128)(2,1)S(1)}, bf16[8,64,512]{2,1,0:T(8,128)(2,1)}, u32[]{:S(2)}, u32[]{:S(2)}) collective-permute-start(bf16[8,64,512]{2,1,0:T(8,128)(2,1)S(1)} %all-to-all-done.refs_0_.x_ref), channel_id=1, source_target_pairs={{0,2},{1,3},{2,0},{3,1},{4,6},{5,7},{6,4},{7,5},{8,10},{9,11},{10,... | collective-permute-start | bytes 1572872 | tf_op jit(solution)/shard_map/ppermute | solution.py:303
  31.6 21.6 %all-to-all-done.1 = bf16[8,56,1024]{2,1,0:T(8,128)(2,1)S(1)} async-done(((bf16[8,56,1024]{2,1,0:T(8,128)(2,1)}), bf16[8,56,1024]{2,1,0:T(8,128)(2,1)S(1)}, u32[]{:S(2)}, u32[]{:S(2)}) %all-to-all-start.1) | async-done | bytes 917536 | tf_op jit(solution)/shard_map/all_to_all | solution.py:306
  53.2 0.0 collective-permute-start
  53.2 0.5 collective-permute-start.1
  53.7 0.0 collective-permute-done.2.refs_2_
  53.7 0.0 collective-permute-start.3
  53.7 2.7 %collective-permute-done.1.refs_1_ = bf16[8,64,512]{2,1,0:T(8,128)(2,1)S(1)} collective-permute-done((bf16[8,64,512]{2,1,0:T(8,128)(2,1)S(1)}, bf16[8,64,512]{2,1,0:T(8,128)(2,1)S(1)}, u32[]{:S(2)}, u32[]{:S(2)}) %collective-permute-start.1) | collective-permute-done | bytes 524320 | tf_op jit(solution)/shard_map/ppermute | solution.py:303
  56.4 0.7 collective-permute-done.3.refs_3_
  57.1 1.8 %copy-done.2 = bf16[1,2048,512]{2,1,0:T(8,128)(2,1)S(1)} copy-done((bf16[1,2048,512]{2,1,0:T(8,128)(2,1)S(1)}, bf16[1,2048,512]{2,1,0:T(8,128)(2,1)}, u32[]{:S(2)}) %copy-start.2) | copy-done | bytes 2097176
  58.9 3.7 %shard_map.145 = (bf16[8,56,512]{2,1,0:T(8,128)(2,1)S(1)}, f32[8,56,512]{2,1,0:T(8,128)S(1)}, f32[8,56,512]{2,1,0:T(8,128)S(1)}) custom-call(s32[1]{0:T(128)} %bitcast.q_ref, bf16[8,64,512]{2,1,0:T(8,128)(2,1)S(1)} %all-to-all-done.refs_0_.x_ref, bf16[8,64,512]{2,1,0:T(8,128)(2,1)S(1)} %collective-permute-done.1.refs_1_, ...), custom_call_target="tpu_custom_call" | custom-call | flops 1879048192 | tf_op jit(solution)/shard_map/pallas_call | solution.py:265
  62.7 0.0 copy-start.3
  62.7 0.7 shard_map.144.back_ref
  63.4 0.0 collective-permute-done.z_ref.far_ref
  63.4 1.2 copy-done.3
  64.6 1.8 %shard_map.146 = (bf16[8,64,512]{2,1,0:T(8,128)(2,1)S(1)}, bf16[8,64,512]{2,1,0:T(8,128)(2,1)S(1)}, bf16[2,448,512]{2,1,0:T(8,128)(2,1)S(1)}, f32[8,128]{1,0:T(8,128)S(1)}) custom-call(s32[1]{0:T(128)} %bitcast.q_ref, f32[448,512]{1,0:T(8,128)S(1)} %shard_map.144.back_ref, bf16[448,1024]{1,0:T(8,128)(2,1)S(1)} %collective-permute-done.z_ref.far_ref, ...), custom_call_target="tpu_custom_call" | custom-call | flops 1409286144 | tf_op jit(solution)/shard_map/pallas_call | solution.py:265
  66.4 0.2 collective-permute-start.4
  66.6 1.3 %shard_map.147 = f32[2,8,56,512]{3,2,1,0:T(8,128)S(1)} custom-call(s32[1]{0:T(128)} %bitcast.q_ref, bf16[8,64,512]{2,1,0:T(8,128)(2,1)S(1)} %get-tuple-element.35.gg_ref.refs_4_, bf16[8,64,512]{2,1,0:T(8,128)(2,1)S(1)} %get-tuple-element.36.gu_ref.refs_5_, bf16[2048,512]{1,0:T(8,128)(2,1)S(1)} %bitcast.28, bf16[2048,512]{1,0:T(8,128)(2,1)S(1)} %bitcast.31), custom_call_target="tpu_custom_call" | custom-call | flops 939524096 | tf_op jit(solution)/shard_map/pallas_call | solution.py:265
  67.9 1.0 collective-permute-done.4.got_ref.core_ref
  69.0 0.8 shard_map.148
  69.8 1.5 %collective-permute-start.5 = (bf16[448,512]{1,0:T(8,128)(2,1)}, bf16[448,512]{1,0:T(8,128)(2,1)}, u32[]{:S(2)}, u32[]{:S(2)}) collective-permute-start(bf16[448,512]{1,0:T(8,128)(2,1)} %bitcast.11), channel_id=1, source_target_pairs={{0,2},{1,3},{2,0},{3,1},{4,6},{5,7},{6,4},{7,5},{8,10},{9,11},{10,... | collective-permute-start | bytes 1376264 | tf_op jit(solution)/shard_map/ppermute | solution.py:303
  71.3 0.0 collective-permute-start.6
  71.3 1.2 collective-permute-done.6
  72.5 0.5 collective-permute-start.7
  73.0 9.7 %collective-permute-done.7.got_ref = f32[8,128]{1,0:T(8,128)S(1)} collective-permute-done((f32[8,128]{1,0:T(8,128)S(1)}, f32[8,128]{1,0:T(8,128)S(1)}, u32[]{:S(2)}, u32[]{:S(2)}) %collective-permute-start.7) | collective-permute-done | bytes 4128 | tf_op jit(solution)/shard_map/ppermute | solution.py:303
  82.7 0.7 shard_map.150
  83.4 3.6 %all-to-all-start.3 = ((f32[8,8,128]{2,1,0:T(8,128)}), f32[8,8,128]{2,1,0:T(8,128)S(1)}, u32[]{:S(2)}, u32[]{:S(2)}) async-start(f32[8,8,128]{2,1,0:T(8,128)} %shard_map.150), calls=%async_computation.3 | async-start | bytes 65536 | tf_op jit(solution)/shard_map/all_to_all | solution.py:306
  87.1 0.0 collective-permute-done.5.refs_0_
  87.1 1.9 %shard_map.149 = bf16[448,512]{1,0:T(8,128)(2,1)} custom-call(f32[2,448,512]{2,1,0:T(8,128)S(1)} %bitcast.25, bf16[2,448,512]{2,1,0:T(8,128)(2,1)S(1)} %collective-permute-done.4.got_ref.core_ref, bf16[448,512]{1,0:T(8,128)(2,1)} %collective-permute-done.5.refs_0_), custom_call_target="tpu_custom_call" | custom-call | tf_op jit(solution)/shard_map/pallas_call | solution.py:265
  89.0 4.8 %all-to-all-done.3.term_ref = f32[8,8,128]{2,1,0:T(8,128)S(1)} async-done(((f32[8,8,128]{2,1,0:T(8,128)}), f32[8,8,128]{2,1,0:T(8,128)S(1)}, u32[]{:S(2)}, u32[]{:S(2)}) %all-to-all-start.3) | async-done | bytes 32800 | tf_op jit(solution)/shard_map/all_to_all | solution.py:306
  93.8 3.5 %all-to-all-start.2 = ((bf16[8,56,512]{2,1,0:T(8,128)(2,1)}), bf16[8,56,512]{2,1,0:T(8,128)(2,1)S(1)}, u32[]{:S(2)}, u32[]{:S(2)}) async-start(bf16[8,56,512]{2,1,0:T(8,128)(2,1)} %bitcast.12), calls=%async_computation.2 | async-start | bytes 917504 | tf_op jit(solution)/shard_map/all_to_all | solution.py:306
  97.2 1.0 copy-done.12
  98.3 1.0 copy-done.15
  99.3 1.0 copy-done.22
  100.4 1.0 copy-done.24
  101.4 5.7 %grads.1 = (bf16[2048,512]{1,0:T(8,128)(2,1)}, bf16[2048,512]{1,0:T(8,128)(2,1)}, f32[4,2,512]{2,1,0:T(2,128)S(1)}) custom-call(s32[1]{0:T(128)} %bitcast.q_ref, bf16[8,64,512]{2,1,0:T(8,128)(2,1)S(1)} %copy-done.15, bf16[8,64,512]{2,1,0:T(8,128)(2,1)S(1)} %copy-done.22, bf16[8,64,512]{2,1,0:T(8,128)(2,1)} %collective-permute-done.2.refs_2_, ...), custom_call_target="tpu_custom_call" | custom-call | flops 1879048192 | tf_op jit(solution)/shard_map/grads/pallas_call | solution.py:374
  107.2 0.3 shard_map.151
  107.5 1.9 %collective-permute-start.11 = (f32[8,512]{1,0:T(8,128)S(1)}, f32[8,512]{1,0:T(8,128)S(1)}, u32[]{:S(2)}, u32[]{:S(2)}) collective-permute-start(f32[8,512]{1,0:T(8,128)S(1)} %get-tuple-element.41), channel_id=1, source_target_pairs={{0,4},{4,0},{8,12},{12,8},{16,20},{20,16},{24,28},{28,24},{1,5},{5... | collective-permute-start | bytes 49160 | tf_op jit(solution)/shard_map/ppermute | solution.py:303
  109.4 3.1 %down.1 = (bf16[512,2048]{1,0:T(8,128)(2,1)}, f32[2,1,512]{2,1,0:T(1,128)S(1)}) custom-call(s32[1]{0:T(128)} %bitcast.q_ref, bf16[448,1024]{1,0:T(8,128)(2,1)S(1)} %bitcast.36, bf16[448,1024]{1,0:T(8,128)(2,1)S(1)} %copy-done.10, bf16[8,64,512]{2,1,0:T(8,128)(2,1)S(1)} %copy-done.15, bf16[448,512]{1,0:T(8,128)(2,1)S(1)} %bitcast.41), custom_call_target="tpu_custom_call" | custom-call | flops 939524096 | tf_op jit(solution)/shard_map/down/pallas_call | solution.py:387
  112.5 0.0 collective-permute-done.14
  112.5 1.6 %collective-permute-start.15 = (f32[2,2048]{1,0:T(2,128)S(1)}, f32[2,2048]{1,0:T(2,128)S(1)}, u32[]{:S(2)}, u32[]{:S(2)}) collective-permute-start(f32[2,2048]{1,0:T(2,128)S(1)} %add.36), channel_id=1, source_target_pairs={{0,2},{1,3},{2,0},{3,1},{4,6},{5,7},{6,4},{7,5},{8,10},{9,11},{10,... | collective-permute-start | bytes 49160 | tf_op jit(solution)/shard_map/ppermute | solution.py:303
  114.1 0.0 collective-permute-done.11
  114.2 1.5 %collective-permute-start.12 = (f32[8,512]{1,0:T(8,128)S(1)}, f32[8,512]{1,0:T(8,128)S(1)}, u32[]{:S(2)}, u32[]{:S(2)}) collective-permute-start(f32[8,512]{1,0:T(8,128)S(1)} %add.33), channel_id=1, source_target_pairs={{0,8},{4,12},{8,0},{12,4},{16,24},{20,28},{24,16},{28,20},{1,9},{5... | collective-permute-start | bytes 49160 | tf_op jit(solution)/shard_map/ppermute | solution.py:303
  115.7 0.6 add_bitcast_fusion.1
  116.3 0.1 collective-permute-done.15
  116.4 1.6 %collective-permute-done.12 = f32[8,512]{1,0:T(8,128)S(1)} collective-permute-done((f32[8,512]{1,0:T(8,128)S(1)}, f32[8,512]{1,0:T(8,128)S(1)}, u32[]{:S(2)}, u32[]{:S(2)}) %collective-permute-start.12) | collective-permute-done | bytes 16416 | tf_op jit(solution)/shard_map/ppermute | solution.py:303
  118.0 2.4 %collective-permute-start.13 = (f32[8,512]{1,0:T(8,128)S(1)}, f32[8,512]{1,0:T(8,128)S(1)}, u32[]{:S(2)}, u32[]{:S(2)}) collective-permute-start(f32[8,512]{1,0:T(8,128)S(1)} %add.34), channel_id=1, source_target_pairs={{0,16},{4,20},{8,24},{12,28},{16,0},{20,4},{24,8},{28,12},{1,17},{... | collective-permute-start | bytes 49160 | tf_op jit(solution)/shard_map/ppermute | solution.py:303
  120.4 0.0 all-to-all-done.2
  120.4 0.3 shard_map.152.refs_0_
  120.7 0.6 collective-permute-start.9
  121.2 0.6 fusion
  121.8 3.9 %collective-permute-done.9.refs_2_ = bf16[128,512]{1,0:T(8,128)(2,1)S(1)} collective-permute-done((bf16[128,512]{1,0:T(8,128)(2,1)S(1)}, bf16[128,512]{1,0:T(8,128)(2,1)S(1)}, u32[]{:S(2)}, u32[]{:S(2)}) %collective-permute-start.9) | collective-permute-done | bytes 131104 | tf_op jit(solution)/shard_map/ppermute | solution.py:303
  125.7 1.2 multiply_reduce_fusion
  126.9 0.1 collective-permute-done.10.refs_3_
  127.1 0.8 shard_map.153
  (48 shorter events, 0.1 us)
Async XLA Ops:
  0.6 1.0 copy-start.7
  1.7 0.8 copy-start.18
  2.4 0.7 copy-start.20
  4.5 52.7 %copy-start = (bf16[1,2048,512]{2,1,0:T(8,128)(2,1)S(1)}, bf16[1,2048,512]{2,1,0:T(8,128)(2,1)}, u32[]{:S(2)}) copy-start(bf16[1,2048,512]{2,1,0:T(8,128)(2,1)} %param.10) | copy-start | bytes 6291460
  4.5 21.9 %all-to-all-start = ((bf16[8,64,512]{2,1,0:T(8,128)(2,1)}), bf16[8,64,512]{2,1,0:T(8,128)(2,1)S(1)}, u32[]{:S(2)}, u32[]{:S(2)}) async-start(bf16[8,64,512]{2,1,0:T(8,128)(2,1)} %get-tuple-element.29), calls=%async_computation | async-start | bytes 1048576 | tf_op jit(solution)/shard_map/all_to_all | solution.py:306
  11.9 1.0 copy-start.13
  26.4 36.3 %copy-start.14 = (bf16[8,64,512]{2,1,0:T(8,128)(2,1)}, bf16[8,64,512]{2,1,0:T(8,128)(2,1)S(1)}, u32[]{:S(2)}) copy-start(bf16[8,64,512]{2,1,0:T(8,128)(2,1)S(1)} %all-to-all-done.refs_0_.x_ref) | copy-start | bytes 1572868
  26.4 26.8 %all-to-all-start.1 = ((bf16[8,56,1024]{2,1,0:T(8,128)(2,1)}), bf16[8,56,1024]{2,1,0:T(8,128)(2,1)S(1)}, u32[]{:S(2)}, u32[]{:S(2)}) async-start(bf16[8,56,1024]{2,1,0:T(8,128)(2,1)} %shard_map.143), calls=%async_computation.1 | async-start | bytes 1835008 | tf_op jit(solution)/shard_map/all_to_all | solution.py:306
  30.0 23.7 %collective-permute-start.2 = (bf16[8,64,512]{2,1,0:T(8,128)(2,1)S(1)}, bf16[8,64,512]{2,1,0:T(8,128)(2,1)}, u32[]{:S(2)}, u32[]{:S(2)}) collective-permute-start(bf16[8,64,512]{2,1,0:T(8,128)(2,1)S(1)} %all-to-all-done.refs_0_.x_ref), channel_id=1, source_target_pairs={{0,2},{1,3},{2,0},{3,1},{4,6},{5,7},{6,4},{7,5},{8,10},{9,11},{10,... | collective-permute-start | bytes 1572872 | tf_op jit(solution)/shard_map/ppermute | solution.py:303
  53.2 9.5 %copy-start.5 = (bf16[8,56,1024]{2,1,0:T(8,128)(2,1)}, bf16[8,56,1024]{2,1,0:T(8,128)(2,1)S(1)}, u32[]{:S(2)}) copy-start(bf16[8,56,1024]{2,1,0:T(8,128)(2,1)S(1)} %all-to-all-done.1) | copy-start | bytes 2752516
  53.2 10.2 %collective-permute-start = (bf16[448,1024]{1,0:T(8,128)(2,1)S(1)}, bf16[448,1024]{1,0:T(8,128)(2,1)S(1)}, u32[]{:S(2)}, u32[]{:S(2)}) collective-permute-start(bf16[448,1024]{1,0:T(8,128)(2,1)S(1)} %bitcast.34), channel_id=1, source_target_pairs={{0,1},{1,0},{2,3},{3,2},{4,5},{5,4},{6,7},{7,6},{8,9},{9,8},{10,11... | collective-permute-start | bytes 2752520 | tf_op jit(solution)/shard_map/ppermute | solution.py:303
  53.2 3.2 %collective-permute-start.1 = (bf16[8,64,512]{2,1,0:T(8,128)(2,1)S(1)}, bf16[8,64,512]{2,1,0:T(8,128)(2,1)S(1)}, u32[]{:S(2)}, u32[]{:S(2)}) collective-permute-start(bf16[8,64,512]{2,1,0:T(8,128)(2,1)S(1)} %all-to-all-done.refs_0_.x_ref), channel_id=1, source_target_pairs={{0,1},{1,0},{2,3},{3,2},{4,5},{5,4},{6,7},{7,6},{8,9},{9,8},{10,11... | collective-permute-start | bytes 1572872 | tf_op jit(solution)/shard_map/ppermute | solution.py:303
  53.7 3.5 %collective-permute-start.3 = (bf16[8,64,512]{2,1,0:T(8,128)(2,1)}, bf16[8,64,512]{2,1,0:T(8,128)(2,1)S(1)}, u32[]{:S(2)}, u32[]{:S(2)}) collective-permute-start(bf16[8,64,512]{2,1,0:T(8,128)(2,1)} %collective-permute-done.2.refs_2_), channel_id=1, source_target_pairs={{0,1},{1,0},{2,3},{3,2},{4,5},{5,4},{6,7},{7,6},{8,9},{9,8},{10,11... | collective-permute-start | bytes 1572872 | tf_op jit(solution)/shard_map/ppermute | solution.py:303
  56.4 6.3 %copy-start.21 = (bf16[8,64,512]{2,1,0:T(8,128)(2,1)}, bf16[8,64,512]{2,1,0:T(8,128)(2,1)S(1)}, u32[]{:S(2)}) copy-start(bf16[8,64,512]{2,1,0:T(8,128)(2,1)S(1)} %collective-permute-done.1.refs_1_) | copy-start | bytes 1572868
  57.1 5.5 %copy-start.23 = (bf16[8,64,512]{2,1,0:T(8,128)(2,1)}, bf16[8,64,512]{2,1,0:T(8,128)(2,1)S(1)}, u32[]{:S(2)}) copy-start(bf16[8,64,512]{2,1,0:T(8,128)(2,1)S(1)} %collective-permute-done.3.refs_3_) | copy-start | bytes 1572868
  57.1 1.8 %copy-start.2 = (bf16[1,2048,512]{2,1,0:T(8,128)(2,1)S(1)}, bf16[1,2048,512]{2,1,0:T(8,128)(2,1)}, u32[]{:S(2)}) copy-start(bf16[1,2048,512]{2,1,0:T(8,128)(2,1)} %param.11) | copy-start | bytes 6291460
  58.9 3.8 %copy-start.4 = (bf16[1,512,2048]{2,1,0:T(8,128)(2,1)S(1)}, bf16[1,512,2048]{2,1,0:T(8,128)(2,1)}, u32[]{:S(2)}) copy-start(bf16[1,512,2048]{2,1,0:T(8,128)(2,1)} %param.12) | copy-start | bytes 6291460
  62.7 3.7 %copy-start.16 = (bf16[8,56,512]{2,1,0:T(8,128)(2,1)}, bf16[8,56,512]{2,1,0:T(8,128)(2,1)S(1)}, u32[]{:S(2)}) copy-start(bf16[8,56,512]{2,1,0:T(8,128)(2,1)S(1)} %get-tuple-element.32) | copy-start | bytes 1376260
  62.7 1.9 %copy-start.3 = (bf16[1,2048,512]{2,1,0:T(8,128)(2,1)S(1)}, bf16[1,2048,512]{2,1,0:T(8,128)(2,1)}, u32[]{:S(2)}) copy-start(bf16[1,2048,512]{2,1,0:T(8,128)(2,1)} %param.11) | copy-start | bytes 6291460
  63.4 3.0 %copy-start.9 = (bf16[448,1024]{1,0:T(8,128)(2,1)}, bf16[448,1024]{1,0:T(8,128)(2,1)S(1)}, u32[]{:S(2)}) copy-start(bf16[448,1024]{1,0:T(8,128)(2,1)S(1)} %collective-permute-done.z_ref.far_ref) | copy-start | bytes 2752516
  64.6 2.1 %copy-start.1 = (bf16[1,2048,512]{2,1,0:T(8,128)(2,1)S(1)}, bf16[1,2048,512]{2,1,0:T(8,128)(2,1)}, u32[]{:S(2)}) copy-start(bf16[1,2048,512]{2,1,0:T(8,128)(2,1)} %param.10) | copy-start | bytes 6291460
  66.4 1.5 %copy-start.11 = (bf16[8,64,512]{2,1,0:T(8,128)(2,1)}, bf16[8,64,512]{2,1,0:T(8,128)(2,1)S(1)}, u32[]{:S(2)}) copy-start(bf16[8,64,512]{2,1,0:T(8,128)(2,1)S(1)} %get-tuple-element.36.gu_ref.refs_5_) | copy-start | bytes 1572868
  66.4 2.5 %collective-permute-start.4 = (bf16[2,448,512]{2,1,0:T(8,128)(2,1)S(1)}, bf16[2,448,512]{2,1,0:T(8,128)(2,1)S(1)}, u32[]{:S(2)}, u32[]{:S(2)}) collective-permute-start(bf16[2,448,512]{2,1,0:T(8,128)(2,1)S(1)} %get-tuple-element.37), channel_id=1, source_target_pairs={{0,1},{1,0},{2,3},{3,2},{4,5},{5,4},{6,7},{7,6},{8,9},{9,8},{10,11... | collective-permute-start | bytes 2752520 | tf_op jit(solution)/shard_map/ppermute | solution.py:303
  69.8 17.3 %collective-permute-start.5 = (bf16[448,512]{1,0:T(8,128)(2,1)}, bf16[448,512]{1,0:T(8,128)(2,1)}, u32[]{:S(2)}, u32[]{:S(2)}) collective-permute-start(bf16[448,512]{1,0:T(8,128)(2,1)} %bitcast.11), channel_id=1, source_target_pairs={{0,2},{1,3},{2,0},{3,1},{4,6},{5,7},{6,4},{7,5},{8,10},{9,11},{10,... | collective-permute-start | bytes 1376264 | tf_op jit(solution)/shard_map/ppermute | solution.py:303
  71.3 1.2 collective-permute-start.6
  72.5 10.2 %collective-permute-start.7 = (f32[8,128]{1,0:T(8,128)S(1)}, f32[8,128]{1,0:T(8,128)S(1)}, u32[]{:S(2)}, u32[]{:S(2)}) collective-permute-start(f32[8,128]{1,0:T(8,128)S(1)} %add.32.own_ref), channel_id=1, source_target_pairs={{0,2},{1,3},{2,0},{3,1},{4,6},{5,7},{6,4},{7,5},{8,10},{9,11},{10,... | collective-permute-start | bytes 12296 | tf_op jit(solution)/shard_map/ppermute | solution.py:303
  83.4 10.3 %all-to-all-start.3 = ((f32[8,8,128]{2,1,0:T(8,128)}), f32[8,8,128]{2,1,0:T(8,128)S(1)}, u32[]{:S(2)}, u32[]{:S(2)}) async-start(f32[8,8,128]{2,1,0:T(8,128)} %shard_map.150), calls=%async_computation.3 | async-start | bytes 65536 | tf_op jit(solution)/shard_map/all_to_all | solution.py:306
  93.8 26.6 %all-to-all-start.2 = ((bf16[8,56,512]{2,1,0:T(8,128)(2,1)}), bf16[8,56,512]{2,1,0:T(8,128)(2,1)S(1)}, u32[]{:S(2)}, u32[]{:S(2)}) async-start(bf16[8,56,512]{2,1,0:T(8,128)(2,1)} %bitcast.12), calls=%async_computation.2 | async-start | bytes 917504 | tf_op jit(solution)/shard_map/all_to_all | solution.py:306
  97.2 1.0 copy-start.12
  98.3 1.0 copy-start.15
  99.3 1.0 copy-start.22
  100.4 1.0 copy-start.24
  101.4 5.7 %copy-start.8 = (bf16[128,2048]{1,0:T(8,128)(2,1)S(1)}, bf16[128,2048]{1,0:T(8,128)(2,1)}, u32[]{:S(2)}) copy-start(bf16[128,2048]{1,0:T(8,128)(2,1)} %tok_ref.3) | copy-start | bytes 1572868
  101.4 8.0 %copy-start.6 = (bf16[8,56,1024]{2,1,0:T(8,128)(2,1)S(1)}, bf16[8,56,1024]{2,1,0:T(8,128)(2,1)}, u32[]{:S(2)}) copy-start(bf16[8,56,1024]{2,1,0:T(8,128)(2,1)} %copy-done.5) | copy-start | bytes 2752516
  101.4 8.0 %copy-start.10 = (bf16[448,1024]{1,0:T(8,128)(2,1)S(1)}, bf16[448,1024]{1,0:T(8,128)(2,1)}, u32[]{:S(2)}) copy-start(bf16[448,1024]{1,0:T(8,128)(2,1)} %copy-done.9) | copy-start | bytes 2752516
  101.4 8.0 %copy-start.17 = (bf16[8,56,512]{2,1,0:T(8,128)(2,1)S(1)}, bf16[8,56,512]{2,1,0:T(8,128)(2,1)}, u32[]{:S(2)}) copy-start(bf16[8,56,512]{2,1,0:T(8,128)(2,1)} %copy-done.16) | copy-start | bytes 1376260
  107.1 5.4 %collective-permute-start.14 = (f32[2,2048]{1,0:T(2,128)S(1)}, f32[2,2048]{1,0:T(2,128)S(1)}, u32[]{:S(2)}, u32[]{:S(2)}) collective-permute-start(f32[2,2048]{1,0:T(2,128)S(1)} %bitcast.44), channel_id=1, source_target_pairs={{0,1},{1,0},{2,3},{3,2},{4,5},{5,4},{6,7},{7,6},{8,9},{9,8},{10,11... | collective-permute-start | bytes 49160 | tf_op jit(solution)/shard_map/ppermute | solution.py:303
  107.2 13.2 %copy-start.19 = (bf16[2048,8]{0,1:T(8,128)(2,1)S(1)}, bf16[2048,8]{0,1:T(8,128)(2,1)}, u32[]{:S(2)}) copy-start(bf16[2048,8]{0,1:T(8,128)(2,1)} %param.9) | copy-start | bytes 98308
  107.5 6.7 %collective-permute-start.11 = (f32[8,512]{1,0:T(8,128)S(1)}, f32[8,512]{1,0:T(8,128)S(1)}, u32[]{:S(2)}, u32[]{:S(2)}) collective-permute-start(f32[8,512]{1,0:T(8,128)S(1)} %get-tuple-element.41), channel_id=1, source_target_pairs={{0,4},{4,0},{8,12},{12,8},{16,20},{20,16},{24,28},{28,24},{1,5},{5... | collective-permute-start | bytes 49160 | tf_op jit(solution)/shard_map/ppermute | solution.py:303
  112.5 3.8 %collective-permute-start.15 = (f32[2,2048]{1,0:T(2,128)S(1)}, f32[2,2048]{1,0:T(2,128)S(1)}, u32[]{:S(2)}, u32[]{:S(2)}) collective-permute-start(f32[2,2048]{1,0:T(2,128)S(1)} %add.36), channel_id=1, source_target_pairs={{0,2},{1,3},{2,0},{3,1},{4,6},{5,7},{6,4},{7,5},{8,10},{9,11},{10,... | collective-permute-start | bytes 49160 | tf_op jit(solution)/shard_map/ppermute | solution.py:303
  114.2 3.8 %collective-permute-start.12 = (f32[8,512]{1,0:T(8,128)S(1)}, f32[8,512]{1,0:T(8,128)S(1)}, u32[]{:S(2)}, u32[]{:S(2)}) collective-permute-start(f32[8,512]{1,0:T(8,128)S(1)} %add.33), channel_id=1, source_target_pairs={{0,8},{4,12},{8,0},{12,4},{16,24},{20,28},{24,16},{28,20},{1,9},{5... | collective-permute-start | bytes 49160 | tf_op jit(solution)/shard_map/ppermute | solution.py:303
  118.0 7.8 %collective-permute-start.13 = (f32[8,512]{1,0:T(8,128)S(1)}, f32[8,512]{1,0:T(8,128)S(1)}, u32[]{:S(2)}, u32[]{:S(2)}) collective-permute-start(f32[8,512]{1,0:T(8,128)S(1)} %add.34), channel_id=1, source_target_pairs={{0,16},{4,20},{8,24},{12,28},{16,0},{20,4},{24,8},{28,12},{1,17},{... | collective-permute-start | bytes 49160 | tf_op jit(solution)/shard_map/ppermute | solution.py:303
  120.7 5.0 %collective-permute-start.9 = (bf16[128,512]{1,0:T(8,128)(2,1)S(1)}, bf16[128,512]{1,0:T(8,128)(2,1)S(1)}, u32[]{:S(2)}, u32[]{:S(2)}) collective-permute-start(bf16[128,512]{1,0:T(8,128)(2,1)S(1)} %shard_map.152.refs_0_), channel_id=1, source_target_pairs={{0,2},{1,3},{2,0},{3,1},{4,6},{5,7},{6,4},{7,5},{8,10},{9,11},{10,... | collective-permute-start | bytes 393224 | tf_op jit(solution)/shard_map/ppermute | solution.py:303
  121.8 5.1 %collective-permute-start.8 = (bf16[128,512]{1,0:T(8,128)(2,1)S(1)}, bf16[128,512]{1,0:T(8,128)(2,1)S(1)}, u32[]{:S(2)}, u32[]{:S(2)}) collective-permute-start(bf16[128,512]{1,0:T(8,128)(2,1)S(1)} %shard_map.152.refs_0_), channel_id=1, source_target_pairs={{0,1},{1,0},{2,3},{3,2},{4,5},{5,4},{6,7},{7,6},{8,9},{9,8},{10,11... | collective-permute-start | bytes 393224 | tf_op jit(solution)/shard_map/ppermute | solution.py:303
  125.7 1.3 %collective-permute-start.10 = (bf16[128,512]{1,0:T(8,128)(2,1)S(1)}, bf16[128,512]{1,0:T(8,128)(2,1)S(1)}, u32[]{:S(2)}, u32[]{:S(2)}) collective-permute-start(bf16[128,512]{1,0:T(8,128)(2,1)S(1)} %collective-permute-done.9.refs_2_), channel_id=1, source_target_pairs={{0,1},{1,0},{2,3},{3,2},{4,5},{5,4},{6,7},{7,6},{8,9},{9,8},{10,11... | collective-permute-start | bytes 393224 | tf_op jit(solution)/shard_map/ppermute | solution.py:303

commit v2 on v1

--- a/solution.py
+++ b/solution.py
@@ -12,18 +12,32 @@
 F32 = jnp.float32
 VMEM = pl.BlockSpec(memory_space=pltpu.VMEM)
 SMEM = pl.BlockSpec(memory_space=pltpu.SMEM)
+HBM = pl.BlockSpec(memory_space=pltpu.HBM)
 
 
 def dot(a, b, ca=1, cb=0):
     return lax.dot_general(a, b, (((ca,), (cb,)), ((), ())), preferred_element_type=F32)
 
 
-def params(mib=40):
-    return pltpu.CompilerParams(vmem_limit_bytes=mib * 1024 * 1024)
+ALONE = 67043328
+SHARED = 16 * 1024 * 1024
+JOIN = 1
+BACK = 1
+
+
+def params(limit=SHARED):
+    return pltpu.CompilerParams(vmem_limit_bytes=limit)
 
 
 def cost(flops, bytes_accessed):
     return pl.CostEstimate(flops=flops, bytes_accessed=bytes_accessed, transcendentals=0)
+
+
+def fetch(sems, *pairs):
+    copies = [pltpu.make_async_copy(src, dst, sems.at[i]) for i, (src, dst) in enumerate(pairs)]
+    for copy in copies:
+        copy.start()
+    return copies
 
 
 def one_hot(place, slots):
@@ -32,11 +46,17 @@
     return [(rows == place[e : e + 1, :]).astype(F32) for e in range(experts)]
 
 
-def route_kernel(slots, q_ref, tok_ref, routing_ref, router_ref, rows_ref, aff_ref, place_ref):
+def route_kernel(
+    slots, tok_hbm, routing_hbm, router_hbm, rows_ref, aff_ref, place_ref,
+    tok_ref, routing_ref, router_ref, sems,
+):
+    copies = fetch(sems, (tok_hbm, tok_ref), (routing_hbm, routing_ref), (router_hbm, router_ref))
     toks = tok_ref.shape[0]
     experts = router_ref.shape[0]
     cols = rows_ref.shape[2]
-    start = pl.multiple_of(q_ref[0] * cols, 128)
+    start = pl.multiple_of(lax.axis_index("tp") * cols, 128)
+    for copy in copies:
+        copy.wait()
     aff = jax.nn.sigmoid(dot(router_ref[...], tok_ref[...], 1, 1))
     ids = lax.broadcasted_iota(jnp.int32, (experts, toks), 0)
     routed = routing_ref[...]
@@ -65,23 +85,35 @@
         rows_ref[e] = block.astype(BF16)
 
 
-def cots_kernel(slots, q_ref, cot_ref, place_ref, cots_ref):
-    cols = cots_ref.shape[2]
-    start = pl.multiple_of((q_ref[0] % 2) * cols, 128)
-    hot = one_hot(place_ref[...], slots)
+def cots_kernel(slots, cot_hbm, place_ref, *refs):
+    cot_ref, sems = refs[-2:]
+    experts, toks = place_ref.shape
+    cols = cot_ref.shape[1]
+    start = pl.multiple_of((lax.axis_index("tp") % 2) * cols, 128)
+    copies = fetch(sems, (cot_hbm.at[:, pl.ds(start, cols)], cot_ref))
+    rows = lax.broadcasted_iota(jnp.int32, (slots, toks), 0).astype(F32)
+    hot = [
+        (rows == place_ref[pl.ds(lax.axis_index("ep") ^ k, 1), :]).astype(F32) for k in range(experts)
+    ]
     full = jnp.concatenate(hot, axis=0).astype(BF16)
-    sent = dot(full, cot_ref[:, pl.ds(start, cols)])
-    for e in range(len(hot)):
-        cots_ref[e] = sent[e * slots : (e + 1) * slots, :].astype(BF16)
-
-
-def gate_up_kernel(slots, shares, q_ref, *refs):
+    copies[0].wait()
+    sent = dot(full, cot_ref[...])
+    for k in range(experts):
+        refs[k][...] = sent[k * slots : (k + 1) * slots, :].astype(BF16)
+
+
+def join_kernel(*refs):
+    for k, ref in enumerate(refs[:-1]):
+        refs[-1][lax.axis_index("ep") ^ k] = ref[...]
+
+
+def gate_up_kernel(slots, shares, *refs):
     x_refs = refs[:shares]
     wg_ref, wu_ref, hid_ref, up_ref, gate_ref, acc_g, acc_u = refs[shares:]
     groups, span, cols = x_refs[0].shape
     for r in range(shares):
         x = x_refs[r][...].reshape(groups * span, cols)
-        rows = pl.ds(pl.multiple_of((q_ref[0] ^ r) * cols, 128), cols)
+        rows = pl.ds(pl.multiple_of((lax.axis_index("tp") ^ r) * cols, 128), cols)
         part_g = dot(x, wg_ref[rows, :])
         part_u = dot(x, wu_ref[rows, :])
         if r == 0:
@@ -107,27 +139,27 @@
     return jnp.concatenate([tile[:, g : g + 1] for g in range(slots // 8)], axis=0)
 
 
-def back_kernel(half, q_ref, z_ref, wd_ref, back_ref):
+def back_kernel(half, z_ref, wd_ref, back_ref):
     cols = z_ref.shape[1]
-    start = pl.multiple_of(((q_ref[0] % 2) ^ half) * cols, 128)
+    start = pl.multiple_of(((lax.axis_index("tp") % 2) ^ half) * cols, 128)
     back_ref[...] = dot(z_ref[...], wd_ref[:, pl.ds(start, cols)], 1, 1)
 
 
-def slot_parts(q_ref, first, gg, gu, wg_ref, wu_ref, shares):
+def slot_parts(first, gg, gu, wg_ref, wu_ref, shares):
     cols = wg_ref.shape[0] // shares
-    start = pl.multiple_of((q_ref[0] ^ first) * cols, 128)
+    start = pl.multiple_of((lax.axis_index("tp") ^ first) * cols, 128)
     return dot(gg, wg_ref[pl.ds(start, cols), :], 1, 1) + dot(
         gu, wu_ref[pl.ds(start, cols), :], 1, 1
     )
 
 
 def middle_kernel(
-    slots, shares, q_ref, back_ref, z_ref, wd_ref, hid_ref, up_ref, gate_ref,
-    wg_ref, wu_ref, gg_ref, gu_ref, odd_ref, term_ref,
+    slots, shares, back_ref, z_ref, wd_ref, hid_ref, up_ref, gate_ref,
+    wg_ref, wu_ref, gg_ref, gu_ref, home_ref, chip_ref, term_ref,
 ):
     cols = z_ref.shape[1]
     groups = gg_ref.shape[0]
-    start = pl.multiple_of(((q_ref[0] % 2) ^ 1) * cols, 128)
+    start = pl.multiple_of(((lax.axis_index("tp") % 2) ^ 1) * cols, 128)
     back = back_ref[...] + dot(z_ref[...], wd_ref[:, pl.ds(start, cols)], 1, 1)
     term = jnp.sum(hid_ref[...].astype(F32) * back, axis=1, keepdims=True)
     gu = back * up_ref[...]
@@ -145,38 +177,36 @@
     gg = gg.astype(BF16)
     gu = gu.astype(BF16)
     for j in range(shares // 2):
-        part = slot_parts(q_ref, 2 * j + 1, gg, gu, wg_ref, wu_ref, shares)
-        odd_ref[j] = part.astype(BF16)
-
-
-def even_kernel(slots, shares, q_ref, gg_ref, gu_ref, wg_ref, wu_ref, even_ref):
+        part = slot_parts(2 * j + 1, gg, gu, wg_ref, wu_ref, shares)
+        if j == 0:
+            home_ref[...] = part.astype(BF16)
+        else:
+            chip_ref[j - 1] = part.astype(BF16)
+
+
+def even_kernel(slots, shares, gg_ref, gu_ref, wg_ref, wu_ref, home_ref, chip_ref):
     groups, span, hidden = gg_ref.shape
     gg = gg_ref[...].reshape(groups * span, hidden)
     gu = gu_ref[...].reshape(groups * span, hidden)
     for j in range(shares // 2):
-        part = slot_parts(q_ref, 2 * j, gg, gu, wg_ref, wu_ref, shares)
+        part = slot_parts(2 * j, gg, gu, wg_ref, wu_ref, shares)
         for e in range(groups):
-            even_ref[j, e] = part[e * span : e * span + slots, :]
+            block = part[e * span : e * span + slots, :]
+            if j == 0:
+                home_ref[e * slots : (e + 1) * slots, :] = block
+            else:
+                chip_ref[j - 1, e * slots : (e + 1) * slots, :] = block
 
 
 def add_core_kernel(own_ref, got_ref, out_ref):
-    for j in range(out_ref.shape[0]):
-        out_ref[j] = (own_ref[j + 1] + got_ref[j + 1].astype(F32)).astype(BF16)
+    out_ref[...] = (own_ref[...] + got_ref[...].astype(F32)).astype(BF16)
 
 
 def add_chip_kernel(own_ref, core_ref, *refs):
-    total = own_ref[0] + core_ref[0].astype(F32)
+    total = own_ref[...] + core_ref[...].astype(F32)
     for chip_ref in refs[:-1]:
         total = total + chip_ref[...].astype(F32)
     refs[-1][...] = total.astype(BF16)
-
-
-def term_kernel(slots, own_ref, got_ref, out_ref):
-    total = (own_ref[...] + got_ref[...]).astype(BF16).astype(F32)
-    count = slots // 8
-    out_ref[...] = jnp.zeros(out_ref.shape, F32)
-    for b in range(out_ref.shape[0]):
-        out_ref[b, :, :count] = total[:, b * count : (b + 1) * count]
 
 
 def grads_kernel(shares, q_ref, *refs):
@@ -218,59 +248,76 @@
             rows_out[0] = square_rows(down)
 
 
-def router_kernel(slots, q_ref, term_ref, place_ref, aff_ref, tok_ref, logit_out, part_out):
+def router_kernel(slots, term_ref, place_ref, aff_ref, tok_ref, router_ref, base_out, part_out):
     experts, toks = place_ref.shape
     cols = part_out.shape[1]
-    start = pl.multiple_of(q_ref[0] * cols, 128)
+    start = pl.multiple_of(lax.axis_index("tp") * cols, 128)
     place = place_ref[...]
     aff = aff_ref[...]
-    hot = one_hot(place, slots)
-    rows = []
-    for e in range(experts):
-        tile = term_ref[e]
+    slot = lax.broadcasted_iota(jnp.int32, (slots, toks), 0).astype(F32)
+    lanes = term_ref.shape[2]
+    own = lax.axis_index("ep")
+    row = lax.broadcasted_iota(jnp.int32, (experts, toks), 0)
+    term = jnp.zeros((experts, toks), F32)
+    for r in range(experts):
+        tile = pltpu.roll(term_ref[r], lanes - own * (slots // 8), 1)
+        hot = (slot == place_ref[pl.ds(own ^ r, 1), :]).astype(F32)
         total = jnp.zeros((8, toks), F32)
         for g in range(slots // 8):
-            total = total + hot[e][8 * g : 8 * g + 8, :] * tile[:, g : g + 1]
-        rows.append(jnp.sum(total, axis=0, keepdims=True))
-    term = jnp.concatenate(rows, axis=0)
+            total = total + hot[8 * g : 8 * g + 8, :] * tile[:, g : g + 1]
+        term = jnp.where(row == (own ^ r), jnp.sum(total, axis=0, keepdims=True), term)
     named = (place >= 0).astype(F32)
     chosen = named * aff
     total_aff = jnp.sum(chosen, axis=0, keepdims=True)
     weights = chosen / total_aff
     d_chosen = (term - jnp.sum(term * weights, axis=0, keepdims=True)) / total_aff
     d_logit = named * d_chosen * aff * (1.0 - aff)
-    logit_out[...] = d_logit
+    base_out[...] = dot(d_logit.T.astype(BF16), router_ref[:, pl.ds(start, cols)])
     part_out[...] = dot(d_logit.astype(BF16), tok_ref[:, pl.ds(start, cols)])
 
 
-def home_kernel(q_ref, got_ref, place_ref, logit_ref, router_ref, token_out):
-    cols = got_ref.shape[1]
-    start = pl.multiple_of(q_ref[0] * cols, 128)
-    experts = place_ref.shape[0]
-    full = jnp.concatenate(one_hot(place_ref[...], got_ref.shape[0] // experts), axis=0).astype(BF16)
-    back = dot(full, got_ref[...], 0, 0)
-    router_back = dot(logit_ref[...].T.astype(BF16), router_ref[:, pl.ds(start, cols)])
-    token_out[...] = (back + router_back).astype(BF16)
-
-
-def assemble_kernel(q_ref, *refs):
-    out_ref = refs[-1]
-    for r, ref in enumerate(refs[:-1]):
+def slot_map_kernel(slots, place_ref, hot_ref):
+    hot_ref[...] = jnp.concatenate(one_hot(place_ref[...], slots), axis=0).astype(BF16)
+
+
+def home_kernel(got_hbm, hot_hbm, base_hbm, token_out, got_ref, hot_ref, base_ref, sems):
+    copies = fetch(sems, (hot_hbm, hot_ref), (got_hbm, got_ref), (base_hbm, base_ref))
+    for copy in copies:
+        copy.wait()
+    token_out[...] = (dot(hot_ref[...], got_ref[...], 0, 0) + base_ref[...]).astype(BF16)
+
+
+def assemble_kernel(*refs):
+    out_hbm, sems = refs[-2:]
+    pairs = []
+    for r, ref in enumerate(refs[:-2]):
         cols = ref.shape[1]
-        out_ref[:, pl.ds(pl.multiple_of((q_ref[0] ^ r) * cols, 128), cols)] = ref[...]
-
-
-def call(kernel, outs, scalar, *args, flops=0, nbytes=0, scratch=()):
+        start = pl.multiple_of((lax.axis_index("tp") ^ r) * cols, 128)
+        pairs.append((ref, out_hbm.at[:, pl.ds(start, cols)]))
+    for copy in fetch(sems, *pairs):
+        copy.wait()
+
+
+def call(kernel, outs, scalar, *args, flops=0, nbytes=0, scratch=(), hbm=(), out_hbm=False, limit=SHARED):
     single = not isinstance(outs, tuple)
+    ins = [HBM if i in hbm else VMEM for i in range(int(scalar), len(args))]
+    out = HBM if out_hbm else VMEM
     return pl.pallas_call(
         kernel,
         out_shape=outs,
-        in_specs=([SMEM] if scalar else []) + [VMEM] * (len(args) - int(scalar)),
-        out_specs=VMEM if single else tuple(VMEM for _ in outs),
+        in_specs=([SMEM] if scalar else []) + ins,
+        out_specs=out if single else tuple(out for _ in outs),
         scratch_shapes=list(scratch),
-        compiler_params=params(),
+        compiler_params=params(limit),
         cost_estimate=cost(flops, nbytes),
     )(*args)
+
+
+DMAS = pltpu.SemaphoreType.DMA
+
+
+def buffer(*dims, dtype=BF16):
+    return pltpu.VMEM(dims, dtype)
 
 
 def shape(*dims, dtype=BF16):
@@ -312,62 +359,71 @@
     rows_send, aff, place = call(
         functools.partial(route_kernel, slots),
         (shape(experts, span, cols), shape(experts, toks, dtype=F32), shape(experts, toks, dtype=F32)),
-        True, q, tokens, routing, router,
+        False, tokens, routing, router, hbm=(0, 1, 2), limit=ALONE,
+        scratch=[buffer(toks, width), buffer(top, toks, dtype=jnp.int32), buffer(experts, width), DMAS((3,))],
     )
     rows_got = exchange(rows_send)
-    cots_send = call(
-        functools.partial(cots_kernel, slots), shape(experts, slots, half),
-        True, q, cotangent, place, flops=2 * count * toks * half,
-    )
-    cots_send, rows_got = lax.optimization_barrier((cots_send, rows_got))
-    cots_got = exchange(cots_send)
+    pieces = call(
+        functools.partial(cots_kernel, slots), tuple(shape(slots, half) for _ in range(experts)),
+        False, cotangent, place, flops=2 * count * toks * half, hbm=(0,), limit=ALONE,
+        scratch=[buffer(toks, half), DMAS((1,))],
+    )
+    pieces = list(pieces)
+    for k in range(experts - 1, 0, -1):
+        pieces[k] = swap(pieces[k], k, "ep")
+
+    hot = call(functools.partial(slot_map_kernel, slots), shape(count, toks), False, place)
 
     x_parts = spread(rows_got)
     hid, up_factor, gate_factor = call(
         functools.partial(gate_up_kernel, slots, shares),
         (shape(groups, slots, hidden), shape(groups, slots, hidden, dtype=F32), shape(groups, slots, hidden, dtype=F32)),
-        True, q, *x_parts, wg, wu, flops=4 * unit,
+        False, *x_parts, wg, wu, flops=4 * unit,
         scratch=[pltpu.VMEM((groups * span, hidden), F32)] * 2,
     )
     hid = hid.reshape(count, hidden)
     up_factor = up_factor.reshape(count, hidden)
     gate_factor = gate_factor.reshape(count, hidden)
 
-    z_own = cots_got.reshape(count, half)
+    z_own = call(join_kernel, shape(groups, slots, half), False, *pieces, flops=JOIN * unit).reshape(count, half)
     z_far = swap(z_own, 1)
     back = call(
         functools.partial(back_kernel, 0), shape(count, hidden, dtype=F32),
-        True, q, z_own, wd, flops=unit,
-    )
-    gg, gu, odd, term = call(
+        False, z_own, wd, flops=BACK * unit,
+    )
+    gg, gu, odd_home, odd_chip, term = call(
         functools.partial(middle_kernel, slots, shares),
         (
             shape(groups, span, hidden),
             shape(groups, span, hidden),
-            shape(chips, count, cols),
+            shape(count, cols),
+            shape(chips - 1, count, cols),
             shape(8, -(-count // 1024) * 128, dtype=F32),
         ),
-        True, q, back, z_far, wd, hid, up_factor, gate_factor, wg, wu, flops=3 * unit,
+        False, back, z_far, wd, hid, up_factor, gate_factor, wg, wu, flops=3 * unit,
     )
     term_got = swap(term, 1)
-    core_got = swap(odd, 1)
-    even = call(
-        functools.partial(even_kernel, slots, shares), shape(chips, groups, slots, cols, dtype=F32),
-        True, q, gg, gu, wg, wu, flops=2 * unit,
-    ).reshape(chips, count, cols)
+    core_chip = swap(odd_chip, 1)
+    core_home = swap(odd_home, 1)
+    even_home, even_chip = call(
+        functools.partial(even_kernel, slots, shares),
+        (shape(count, cols, dtype=F32), shape(chips - 1, count, cols, dtype=F32)),
+        False, gg, gu, wg, wu, flops=2 * unit,
+    )
     term = term + term_got
     bit = 2
     while 2 * bit < shares:
         term = term + swap(term, bit)
         bit *= 2
     term_got = swap(term, bit)
-    chip_send = call(add_core_kernel, shape(chips - 1, count, cols), False, even, core_got)
+    chip_send = call(add_core_kernel, shape(chips - 1, count, cols), False, even_chip, core_chip)
     chip_got = [swap(chip_send[j], 2 * (j + 1)) for j in range(chips - 1)]
-    terms = call(
-        functools.partial(term_kernel, slots), shape(groups, 8, 128, dtype=F32), False, term, term_got,
-    )
-    terms = exchange(terms)
-    home_send = call(add_chip_kernel, shape(count, cols), False, even, core_got, *chip_got)
+    terms = (term + term_got).astype(BF16).astype(F32)[None]
+    bit = 1
+    while bit < groups:
+        terms = jnp.concatenate([terms, swap(terms, bit, "ep")], axis=0)
+        bit *= 2
+    home_send = call(add_chip_kernel, shape(count, cols), False, even_home, core_home, *chip_got)
     home_got = exchange(home_send.reshape(groups, slots, cols)).reshape(count, cols)
 
     grad_spec = pl.BlockSpec((cols, hidden), lambda r, q: (q[0] ^ r, 0))
@@ -401,24 +457,29 @@
         name="down",
     )(q, z_own, z_far, rows_got, hid)
     norms = norms.transpose(1, 0, 2).reshape(2, width)
-    bit = 1
-    while bit < shares:
-        norms = norms + swap(norms, bit)
-        bit *= 2
+    norms = spread(norms)
+    while len(norms) > 1:
+        norms = [a + b for a, b in zip(norms[::2], norms[1::2])]
+    norms = norms[0]
     down_rows = (down_norms[0] + down_norms[1]).reshape(1, hidden)
 
-    d_logits, router_sum = call(
+    token_base, router_sum = call(
         functools.partial(router_kernel, slots),
-        (shape(experts, toks, dtype=F32), shape(experts, cols, dtype=F32)),
-        True, q, terms, place, aff, tokens,
+        (shape(toks, cols, dtype=F32), shape(experts, cols, dtype=F32)),
+        False, terms, place, aff, tokens, router,
     )
     bit = 1
     while bit < groups:
         router_sum = router_sum + swap(router_sum, bit, "ep")
         bit *= 2
     router_rows = jnp.sum(router_sum * router_sum, axis=0)
-    token_part = call(home_kernel, shape(toks, cols), True, q, home_got, place, d_logits, router)
-    token_grad = call(assemble_kernel, shape(toks, width), True, q, *spread(token_part))
+    token_part = call(
+        home_kernel, shape(toks, cols), False, home_got, hot, token_base, hbm=(0, 1, 2), limit=ALONE,
+        scratch=[buffer(count, cols), buffer(count, toks), buffer(toks, cols, dtype=F32), DMAS((3,))],
+    )
+    token_grad = call(
+        assemble_kernel, shape(toks, width), False, *spread(token_part), out_hbm=True, scratch=[DMAS((shares,))],
+    )
     return (
         token_grad,
         router_sum.T,

time: 129 us -> 123 us (0.953)
  waiting for transfers between devices: 59.5 us -> 21.9 us
  blocking collectives: 0 us -> 21.9 us
  Pallas kernels: 23.9 us -> 29.5 us
  starting transfers between devices: 30.5 us -> 33.3 us
  other arithmetic: 1.8 us -> 3.76 us
    all_to_all x4 -> x1, waiting for transfers between devices: 38.5 us -> 0.01 us  [exchange(): return lax.all_to_all(value, 'ep', split_axis=0, concat_axis=0, tiled=True)]
    all_to_all x0 -> x1, blocking collectives: none -> 21.9 us  [exchange(): return lax.all_to_all(value, 'ep', split_axis=0, concat_axis=0, tiled=True)]
    ppermute x16 -> x28, starting transfers between devices: 12.3 us -> 28.8 us  [swap(): return lax.ppermute(value, axis, [(i, i ^ bit) for i in range(size)])]
    all_to_all x4 -> x1, starting transfers between devices: 18.2 us -> 4.43 us  [exchange(): return lax.all_to_all(value, 'ep', split_axis=0, concat_axis=0, tiled=True)]
    pallas_call x12 -> x13, Pallas kernels: 15 us -> 19.7 us  [call(): pl.pallas_call(kernel, out_shape=outs, in_specs=([SMEM] if scalar else []...]
    unnamed x50 -> x40, local copies, waits for them, and re-layouts: 10.7 us -> 9.26 us
    ppermute x16 -> x28, waiting for transfers between devices: 21.1 us -> 21.9 us  [swap(): return lax.ppermute(value, axis, [(i, i ^ bit) for i in range(size)])]
  transfers between devices with their start and end apart: 20 -> 29, of which waited for: 12 -> 11; matrix products, arithmetic and copies ran while one was open for 2% -> 4% of each run, Pallas kernels for 15% -> 20%
where the time goes in v2:
time: 123 us; the launch traced here: 122 us
  starting transfers between devices  33.3 us (27%)
  Pallas kernels  29.5 us (24%)
  blocking collectives  21.9 us (18%)
  waiting for transfers between devices  21.9 us (18%)
  local copies, waits for them, and re-layouts  10.7 us (9%)
  other arithmetic  3.76 us (3%)
    ppermute x28, starting transfers between devices, swap(): return lax.ppermute(value, axis, [(i, i ^ bit) for i in range(size)])  28.8 us
    all_to_all x1, blocking collectives, exchange(): return lax.all_to_all(value, 'ep', split_axis=0, concat_axis=0, tiled=True)  21.9 us
    ppermute x28, waiting for transfers between devices, swap(): return lax.ppermute(value, axis, [(i, i ^ bit) for i in range(size)])  21.9 us
    pallas_call x13, Pallas kernels, call(): pl.pallas_call(kernel, out_shape=outs, in_specs=([SMEM] if scalar else []...  19.7 us
    unnamed x40, local copies, waits for them, and re-layouts  9.26 us
    pallas_call x1, Pallas kernels, layer(): pl.pallas_call(functools.partial(grads_kernel, shares), out_shape=(shape(...  5.65 us
    all_to_all x1, starting transfers between devices, exchange(): return lax.all_to_all(value, 'ep', split_axis=0, concat_axis=0, tiled=True)  4.43 us
    pallas_call x1, Pallas kernels, layer(): pl.pallas_call(functools.partial(down_kernel, slots), out_shape=(shape(hi...  4.13 us
  transfers between devices with their start and end apart: 29, of which 11 were waited for; matrix products, arithmetic and copies ran while one was open for 4% of the time, Pallas kernels for 20%

profile of v2, /device:TPU:0, one launch (start us, length us, event | category | flops | bytes accessed | tf_op | source)
XLA Modules:
  0.0 122.0 jit_solution(221690172884489323)
XLA Ops:
  0.6 2.4 %shard_map.142 = (bf16[8,64,512]{2,1,0:T(8,128)(2,1)}, f32[8,128]{1,0:T(8,128)}, f32[8,128]{1,0:T(8,128)}) custom-call(bf16[128,2048]{1,0:T(8,128)(2,1)} %tok_ref.1, s32[2,128]{1,0:T(2,128)} %bitcast.48, bf16[8,2048]{1,0:T(8,128)(2,1)} %bitcast.43), custom_call_target="tpu_custom_call" | custom-call | tf_op jit(solution)/shard_map/pallas_call | solution.py:305
  3.1 21.9 %all_to_all.10.refs_0_.x_ref = bf16[8,64,512]{2,1,0:T(8,128)(2,1)} all-to-all(bf16[8,64,512]{2,1,0:T(8,128)(2,1)} %get-tuple-element.46), channel_id=1, replica_groups=mesh['ep'=8,'tp'=4] {'ep'}, dimensions={0} | all-to-all | bytes 1048576 | tf_op jit(solution)/shard_map/all_to_all | solution.py:353
  25.0 1.5 %collective-permute-start.9 = (bf16[8,64,512]{2,1,0:T(8,128)(2,1)}, bf16[8,64,512]{2,1,0:T(8,128)(2,1)}, u32[]{:S(2)}, u32[]{:S(2)}) collective-permute-start(bf16[8,64,512]{2,1,0:T(8,128)(2,1)} %all_to_all.10.refs_0_.x_ref), channel_id=1, source_target_pairs={{0,2},{1,3},{2,0},{3,1},{4,6},{5,7},{6,4},{7,5},{8,10},{9,11},{10,... | collective-permute-start | bytes 1572872 | tf_op jit(solution)/shard_map/ppermute | solution.py:350
  26.5 2.8 %shard_map.143 = (bf16[56,1024]{1,0:T(8,128)(2,1)}, bf16[56,1024]{1,0:T(8,128)(2,1)}, bf16[56,1024]{1,0:T(8,128)(2,1)}, bf16[56,1024]{1,0:T(8,128)(2,1)}, bf16[5...) custom-call(bf16[128,2048]{1,0:T(8,128)(2,1)} %cot_hbm.1, ...), custom_call_target="tpu_custom_call" | custom-call | flops 117440512 | tf_op jit(solution)/shard_map/pallas_call | solution.py:305
  29.4 1.5 %collective-permute-start = (bf16[56,1024]{1,0:T(8,128)(2,1)}, bf16[56,1024]{1,0:T(8,128)(2,1)S(1)}, u32[]{:S(2)}, u32[]{:S(2)}) collective-permute-start(bf16[56,1024]{1,0:T(8,128)(2,1)} %get-tuple-element.39), channel_id=1, source_target_pairs={{0,4},{4,0},{8,12},{12,8},{16,20},{20,16},{24,28},{28,24},{1,5},{5... | collective-permute-start | bytes 344072 | tf_op jit(solution)/shard_map/ppermute | solution.py:350
  30.9 2.1 %collective-permute-start.2 = (bf16[56,1024]{1,0:T(8,128)(2,1)}, bf16[56,1024]{1,0:T(8,128)(2,1)S(1)}, u32[]{:S(2)}, u32[]{:S(2)}) collective-permute-start(bf16[56,1024]{1,0:T(8,128)(2,1)} %get-tuple-element.41), channel_id=1, source_target_pairs={{0,12},{4,8},{8,4},{12,0},{16,28},{20,24},{24,20},{28,16},{1,13},{... | collective-permute-start | bytes 344072 | tf_op jit(solution)/shard_map/ppermute | solution.py:350
  32.9 1.1 collective-permute-start.3
  34.0 1.5 %collective-permute-done.refs_1_ = bf16[56,1024]{1,0:T(8,128)(2,1)S(1)} collective-permute-done((bf16[56,1024]{1,0:T(8,128)(2,1)}, bf16[56,1024]{1,0:T(8,128)(2,1)S(1)}, u32[]{:S(2)}, u32[]{:S(2)}) %collective-permute-start) | collective-permute-done | bytes 114720 | tf_op jit(solution)/shard_map/ppermute | solution.py:350
  35.5 1.2 collective-permute-start.4
  36.7 0.1 collective-permute-done.1.refs_2_
  36.8 2.4 %collective-permute-start.5 = (bf16[56,1024]{1,0:T(8,128)(2,1)}, bf16[56,1024]{1,0:T(8,128)(2,1)S(1)}, u32[]{:S(2)}, u32[]{:S(2)}) collective-permute-start(bf16[56,1024]{1,0:T(8,128)(2,1)} %get-tuple-element.44), channel_id=1, source_target_pairs={{0,24},{4,28},{8,16},{12,20},{16,8},{20,12},{24,0},{28,4},{1,25},{... | collective-permute-start | bytes 344072 | tf_op jit(solution)/shard_map/ppermute | solution.py:350
  39.2 0.8 collective-permute-done.2.refs_3_
  39.9 2.5 %collective-permute-start.6 = (bf16[56,1024]{1,0:T(8,128)(2,1)}, bf16[56,1024]{1,0:T(8,128)(2,1)S(1)}, u32[]{:S(2)}, u32[]{:S(2)}) collective-permute-start(bf16[56,1024]{1,0:T(8,128)(2,1)} %get-tuple-element.45), channel_id=1, source_target_pairs={{0,28},{4,24},{8,20},{12,16},{16,12},{20,8},{24,4},{28,0},{1,29},{... | collective-permute-start | bytes 344072 | tf_op jit(solution)/shard_map/ppermute | solution.py:350
  42.5 6.3 %collective-permute-done.3.refs_4_ = bf16[56,1024]{1,0:T(8,128)(2,1)S(1)} collective-permute-done((bf16[56,1024]{1,0:T(8,128)(2,1)}, bf16[56,1024]{1,0:T(8,128)(2,1)S(1)}, u32[]{:S(2)}, u32[]{:S(2)}) %collective-permute-start.3) | collective-permute-done | bytes 114720 | tf_op jit(solution)/shard_map/ppermute | solution.py:350
  48.8 3.4 %collective-permute-done.4.refs_5_ = bf16[56,1024]{1,0:T(8,128)(2,1)S(1)} collective-permute-done((bf16[56,1024]{1,0:T(8,128)(2,1)}, bf16[56,1024]{1,0:T(8,128)(2,1)S(1)}, u32[]{:S(2)}, u32[]{:S(2)}) %collective-permute-start.4) | collective-permute-done | bytes 114720 | tf_op jit(solution)/shard_map/ppermute | solution.py:350
  52.3 0.9 copy-done.13
  53.2 0.1 shard_map.144
  53.3 0.5 collective-permute-start.8
  53.8 0.1 collective-permute-start.10
  53.9 2.0 %copy-done.2 = bf16[1,512,2048]{2,1,0:T(8,128)(2,1)S(1)} copy-done((bf16[1,512,2048]{2,1,0:T(8,128)(2,1)S(1)}, bf16[1,512,2048]{2,1,0:T(8,128)(2,1)}, u32[]{:S(2)}) %copy-start.2) | copy-done | bytes 2097176
  55.9 0.7 shard_map.145.back_ref
  56.6 0.7 collective-permute-done.10.refs_3_
  57.3 4.0 %shard_map.146 = (bf16[8,56,512]{2,1,0:T(8,128)(2,1)S(1)}, f32[8,56,512]{2,1,0:T(8,128)S(1)}, f32[8,56,512]{2,1,0:T(8,128)S(1)}) custom-call(bf16[8,64,512]{2,1,0:T(8,128)(2,1)} %all_to_all.10.refs_0_.x_ref, bf16[8,64,512]{2,1,0:T(8,128)(2,1)S(1)} %collective-permute-done.8.refs_1_, bf16[8,64,512]{2,1,0:T(8,128)(2,1)} %collective-permute-done.9.refs_2_, ...), custom_call_target="tpu_custom_call" | custom-call | flops 1879048192 | tf_op jit(solution)/shard_map/pallas_call | solution.py:305
  61.3 2.1 %shard_map.147 = (bf16[8,64,512]{2,1,0:T(8,128)(2,1)S(1)}, bf16[8,64,512]{2,1,0:T(8,128)(2,1)S(1)}, bf16[448,512]{1,0:T(8,128)(2,1)}, bf16[1,448,512]{2,1,0:T(8,128)(2,1)S(1)}, f32[8,128]{1,0:T(8,128)S(1)}) custom-call(f32[448,512]{1,0:T(8,128)S(1)} %shard_map.145.back_ref, bf16[448,1024]{1,0:T(8,128)(2,1)S(1)} %collective-permute-done.7.z_ref.far_ref, ...), custom_call_target="tpu_custom_call" | custom-call | flops 1409286144 | tf_op jit(solution)/shard_map/pallas_call | solution.py:305
  63.4 0.1 collective-permute-start.12
  63.6 0.4 collective-permute-start.14
  64.0 0.1 collective-permute-start.11
  64.1 1.2 collective-permute-done.14
  65.3 0.5 collective-permute-start.15
  65.8 1.3 %shard_map.148 = (f32[448,512]{1,0:T(8,128)S(1)}, f32[1,448,512]{2,1,0:T(8,128)S(1)}) custom-call(bf16[8,64,512]{2,1,0:T(8,128)(2,1)S(1)} %get-tuple-element.50.gg_ref.refs_4_, bf16[8,64,512]{2,1,0:T(8,128)(2,1)S(1)} %get-tuple-element.51.gu_ref.refs_5_, bf16[2048,512]{1,0:T(8,128)(2,1)S(1)} %bitcast.30, bf16[2048,512]{1,0:T(8,128)(2,1)S(1)} %bitcast.33), custom_call_target="tpu_custom_call" | custom-call | flops 939524096 | tf_op jit(solution)/shard_map/pallas_call | solution.py:305
  67.1 0.9 shard_map.149
  68.0 1.5 %collective-permute-start.13 = (bf16[448,512]{1,0:T(8,128)(2,1)}, bf16[448,512]{1,0:T(8,128)(2,1)}, u32[]{:S(2)}, u32[]{:S(2)}) collective-permute-start(bf16[448,512]{1,0:T(8,128)(2,1)} %bitcast.9), channel_id=1, source_target_pairs={{0,2},{1,3},{2,0},{3,1},{4,6},{5,7},{6,4},{7,5},{8,10},{9,11},{10,... | collective-permute-start | bytes 1376264 | tf_op jit(solution)/shard_map/ppermute | solution.py:350
  69.5 0.5 collective-permute-start.16
  70.0 0.6 copy-done.8
  70.6 2.5 %collective-permute-done.16 = f32[1,8,128]{2,1,0:T(8,128)S(1)} collective-permute-done((f32[1,8,128]{2,1,0:T(8,128)S(1)}, f32[1,8,128]{2,1,0:T(8,128)S(1)}, u32[]{:S(2)}, u32[]{:S(2)}) %collective-permute-start.16) | collective-permute-done | bytes 4128 | tf_op jit(solution)/shard_map/ppermute | solution.py:350
  73.1 3.4 %collective-permute-start.17 = (f32[2,8,128]{2,1,0:T(8,128)S(1)}, f32[2,8,128]{2,1,0:T(8,128)S(1)}, u32[]{:S(2)}, u32[]{:S(2)}) collective-permute-start(f32[2,8,128]{2,1,0:T(8,128)S(1)} %pad_maximum_fusion.2), channel_id=1, source_target_pairs={{0,8},{4,12},{8,0},{12,4},{16,24},{20,28},{24,16},{28,20},{1,9},{5... | collective-permute-start | bytes 24584 | tf_op jit(solution)/shard_map/ppermute | solution.py:350
  76.5 1.0 copy-done.6
  77.5 1.0 copy-done.17
  78.6 1.0 copy-done.19
  79.6 5.6 %grads.1 = (bf16[2048,512]{1,0:T(8,128)(2,1)}, bf16[2048,512]{1,0:T(8,128)(2,1)}, f32[4,2,512]{2,1,0:T(2,128)S(1)}) custom-call(s32[1]{0:T(128)} %bitcast.15.q_ref, bf16[8,64,512]{2,1,0:T(8,128)(2,1)} %all_to_all.10.refs_0_.x_ref, bf16[8,64,512]{2,1,0:T(8,128)(2,1)S(1)} %copy-done.17, bf16[8,64,512]{2,1,0:T(8,128)(2,1)} %collective-permute-done.9.refs_2_, ...), custom_call_target="tpu_custom_call" | custom-call | flops 1879048192 | tf_op jit(solution)/shard_map/grads/pallas_call | solution.py:430
  85.3 0.5 collective-permute-start.26
  85.8 0.5 collective-permute-start.18
  86.2 2.1 %shard_map.150 = bf16[448,512]{1,0:T(8,128)(2,1)} custom-call(f32[448,512]{1,0:T(8,128)S(1)} %get-tuple-element.52.own_ref, bf16[448,512]{1,0:T(8,128)(2,1)} %collective-permute-done.11.core_ref, bf16[448,512]{1,0:T(8,128)(2,1)} %collective-permute-done.13.refs_0_), custom_call_target="tpu_custom_call" | custom-call | tf_op jit(solution)/shard_map/pallas_call | solution.py:305
  88.3 4.4 %all-to-all-start.1 = ((bf16[8,56,512]{2,1,0:T(8,128)(2,1)}), bf16[8,56,512]{2,1,0:T(8,128)(2,1)}, u32[]{:S(2)}, u32[]{:S(2)}) async-start(bf16[8,56,512]{2,1,0:T(8,128)(2,1)} %bitcast.10), calls=%async_computation.1 | async-start | bytes 917504 | tf_op jit(solution)/shard_map/all_to_all | solution.py:353
  92.8 1.0 copy-done.10
  93.8 4.1 %down.1 = (bf16[512,2048]{1,0:T(8,128)(2,1)}, f32[2,1,512]{2,1,0:T(1,128)S(1)}) custom-call(s32[1]{0:T(128)} %bitcast.15.q_ref, bf16[448,1024]{1,0:T(8,128)(2,1)S(1)} %bitcast.38, bf16[448,1024]{1,0:T(8,128)(2,1)S(1)} %collective-permute-done.7.z_ref.far_ref, bf16[8,64,512]{2,1,0:T(8,128)(2,1)} %all_to_all.10.refs_0_.x_ref, bf16[448,512]{1,0:T(8,128)(2,1)S(1)} %bitcast.42), custom_call_target="tpu_custom_call" | custom-call | flops 939524096 | tf_op jit(solution)/shard_map/down/pallas_call | solution.py:443
  97.9 0.2 collective-permute-start.27
  98.1 0.5 shard_map.152
  98.6 0.7 copy-done.11
  99.3 1.7 %collective-permute-start.22 = (f32[8,512]{1,0:T(8,128)S(1)}, f32[8,512]{1,0:T(8,128)S(1)}, u32[]{:S(2)}, u32[]{:S(2)}) collective-permute-start(f32[8,512]{1,0:T(8,128)S(1)} %get-tuple-element.59), channel_id=1, source_target_pairs={{0,4},{4,0},{8,12},{12,8},{16,20},{20,16},{24,28},{28,24},{1,5},{5... | collective-permute-start | bytes 49160 | tf_op jit(solution)/shard_map/ppermute | solution.py:350
  101.0 0.6 add_bitcast_fusion.1
  101.6 1.7 %collective-permute-done.22 = f32[8,512]{1,0:T(8,128)S(1)} collective-permute-done((f32[8,512]{1,0:T(8,128)S(1)}, f32[8,512]{1,0:T(8,128)S(1)}, u32[]{:S(2)}, u32[]{:S(2)}) %collective-permute-start.22) | collective-permute-done | bytes 16416 | tf_op jit(solution)/shard_map/ppermute | solution.py:350
  103.3 1.7 %collective-permute-start.23 = (f32[8,512]{1,0:T(8,128)S(1)}, f32[8,512]{1,0:T(8,128)S(1)}, u32[]{:S(2)}, u32[]{:S(2)}) collective-permute-start(f32[8,512]{1,0:T(8,128)S(1)} %add.40), channel_id=1, source_target_pairs={{0,8},{4,12},{8,0},{12,4},{16,24},{20,28},{24,16},{28,20},{1,9},{5... | collective-permute-start | bytes 49160 | tf_op jit(solution)/shard_map/ppermute | solution.py:350
  105.0 0.6 add_add_fusion
  105.6 1.4 %collective-permute-done.23 = f32[8,512]{1,0:T(8,128)S(1)} collective-permute-done((f32[8,512]{1,0:T(8,128)S(1)}, f32[8,512]{1,0:T(8,128)S(1)}, u32[]{:S(2)}, u32[]{:S(2)}) %collective-permute-start.23) | collective-permute-done | bytes 16416 | tf_op jit(solution)/shard_map/ppermute | solution.py:350
  107.0 0.6 add.41
  107.6 3.3 %collective-permute-start.24 = (f32[8,512]{1,0:T(8,128)}, f32[8,512]{1,0:T(8,128)}, u32[]{:S(2)}, u32[]{:S(2)}) collective-permute-start(f32[8,512]{1,0:T(8,128)} %add.41), channel_id=1, source_target_pairs={{0,16},{4,20},{8,24},{12,28},{16,0},{20,4},{24,8},{28,12},{1,17},{... | collective-permute-start | bytes 49160 | tf_op jit(solution)/shard_map/ppermute | solution.py:350
  110.9 2.1 %shard_map.153.refs_0_ = bf16[128,512]{1,0:T(8,128)(2,1)} custom-call(bf16[448,512]{1,0:T(8,128)(2,1)} %bitcast.11.got_hbm, bf16[448,128]{1,0:T(8,128)(2,1)} %copy-done.8, f32[128,512]{1,0:T(8,128)} %copy-done.11), custom_call_target="tpu_custom_call" | custom-call | tf_op jit(solution)/shard_map/pallas_call | solution.py:305
  113.0 1.6 %collective-permute-start.20 = (bf16[128,512]{1,0:T(8,128)(2,1)}, bf16[128,512]{1,0:T(8,128)(2,1)S(1)}, u32[]{:S(2)}, u32[]{:S(2)}) collective-permute-start(bf16[128,512]{1,0:T(8,128)(2,1)} %shard_map.153.refs_0_), channel_id=1, source_target_pairs={{0,2},{1,3},{2,0},{3,1},{4,6},{5,7},{6,4},{7,5},{8,10},{9,11},{10,... | collective-permute-start | bytes 393224 | tf_op jit(solution)/shard_map/ppermute | solution.py:350
  114.6 1.4 %fusion.2 = (f32[1,2048]{1,0:T(1,128)}, f32[1,2048]{1,0:T(1,128)}) fusion(f32[2,2048]{1,0:T(2,128)} %add_add_fusion), kind=kLoop, calls=%fused_computation.10 | loop fusion | bytes 32768 | tf_op jit(solution)/shard_map/slice | solution.py:491
  116.0 2.2 %collective-permute-done.20.refs_2_ = bf16[128,512]{1,0:T(8,128)(2,1)S(1)} collective-permute-done((bf16[128,512]{1,0:T(8,128)(2,1)}, bf16[128,512]{1,0:T(8,128)(2,1)S(1)}, u32[]{:S(2)}, u32[]{:S(2)}) %collective-permute-start.20) | collective-permute-done | bytes 131104 | tf_op jit(solution)/shard_map/ppermute | solution.py:350
  118.2 1.9 %multiply_reduce_fusion = (f32[512]{0:T(512)}, f32[512,8]{0,1:T(8,128)}) fusion(f32[8,512]{1,0:T(8,128)} %add.41, f32[8,512]{1,0:T(8,128)} %collective-permute-done.24), kind=kLoop, calls=%fused_computation.3 | loop fusion | flops 11776 | bytes 51200 | tf_op jit(solution)/shard_map/reduce_sum | solution.py:475
  120.2 0.9 copy-done.7
  121.1 0.8 shard_map.154
  (61 shorter events, 0.2 us)
Async XLA Ops:
  25.0 28.8 %collective-permute-start.9 = (bf16[8,64,512]{2,1,0:T(8,128)(2,1)}, bf16[8,64,512]{2,1,0:T(8,128)(2,1)}, u32[]{:S(2)}, u32[]{:S(2)}) collective-permute-start(bf16[8,64,512]{2,1,0:T(8,128)(2,1)} %all_to_all.10.refs_0_.x_ref), channel_id=1, source_target_pairs={{0,2},{1,3},{2,0},{3,1},{4,6},{5,7},{6,4},{7,5},{8,10},{9,11},{10,... | collective-permute-start | bytes 1572872 | tf_op jit(solution)/shard_map/ppermute | solution.py:350
  29.4 6.2 %collective-permute-start = (bf16[56,1024]{1,0:T(8,128)(2,1)}, bf16[56,1024]{1,0:T(8,128)(2,1)S(1)}, u32[]{:S(2)}, u32[]{:S(2)}) collective-permute-start(bf16[56,1024]{1,0:T(8,128)(2,1)} %get-tuple-element.39), channel_id=1, source_target_pairs={{0,4},{4,0},{8,12},{12,8},{16,20},{20,16},{24,28},{28,24},{1,5},{5... | collective-permute-start | bytes 344072 | tf_op jit(solution)/shard_map/ppermute | solution.py:350
  30.9 6.0 %collective-permute-start.1 = (bf16[56,1024]{1,0:T(8,128)(2,1)}, bf16[56,1024]{1,0:T(8,128)(2,1)S(1)}, u32[]{:S(2)}, u32[]{:S(2)}) collective-permute-start(bf16[56,1024]{1,0:T(8,128)(2,1)} %get-tuple-element.40), channel_id=1, source_target_pairs={{0,8},{4,12},{8,0},{12,4},{16,24},{20,28},{24,16},{28,20},{1,9},{5... | collective-permute-start | bytes 344072 | tf_op jit(solution)/shard_map/ppermute | solution.py:350
  30.9 9.1 %collective-permute-start.2 = (bf16[56,1024]{1,0:T(8,128)(2,1)}, bf16[56,1024]{1,0:T(8,128)(2,1)S(1)}, u32[]{:S(2)}, u32[]{:S(2)}) collective-permute-start(bf16[56,1024]{1,0:T(8,128)(2,1)} %get-tuple-element.41), channel_id=1, source_target_pairs={{0,12},{4,8},{8,4},{12,0},{16,28},{20,24},{24,20},{28,16},{1,13},{... | collective-permute-start | bytes 344072 | tf_op jit(solution)/shard_map/ppermute | solution.py:350
  32.9 15.9 %collective-permute-start.3 = (bf16[56,1024]{1,0:T(8,128)(2,1)}, bf16[56,1024]{1,0:T(8,128)(2,1)S(1)}, u32[]{:S(2)}, u32[]{:S(2)}) collective-permute-start(bf16[56,1024]{1,0:T(8,128)(2,1)} %get-tuple-element.42), channel_id=1, source_target_pairs={{0,16},{4,20},{8,24},{12,28},{16,0},{20,4},{24,8},{28,12},{1,17},{... | collective-permute-start | bytes 344072 | tf_op jit(solution)/shard_map/ppermute | solution.py:350
  35.5 16.7 %collective-permute-start.4 = (bf16[56,1024]{1,0:T(8,128)(2,1)}, bf16[56,1024]{1,0:T(8,128)(2,1)S(1)}, u32[]{:S(2)}, u32[]{:S(2)}) collective-permute-start(bf16[56,1024]{1,0:T(8,128)(2,1)} %get-tuple-element.43), channel_id=1, source_target_pairs={{0,20},{4,16},{8,28},{12,24},{16,4},{20,0},{24,12},{28,8},{1,21},{... | collective-permute-start | bytes 344072 | tf_op jit(solution)/shard_map/ppermute | solution.py:350
  36.8 15.5 %collective-permute-start.5 = (bf16[56,1024]{1,0:T(8,128)(2,1)}, bf16[56,1024]{1,0:T(8,128)(2,1)S(1)}, u32[]{:S(2)}, u32[]{:S(2)}) collective-permute-start(bf16[56,1024]{1,0:T(8,128)(2,1)} %get-tuple-element.44), channel_id=1, source_target_pairs={{0,24},{4,28},{8,16},{12,20},{16,8},{20,12},{24,0},{28,4},{1,25},{... | collective-permute-start | bytes 344072 | tf_op jit(solution)/shard_map/ppermute | solution.py:350
  39.9 12.3 %collective-permute-start.6 = (bf16[56,1024]{1,0:T(8,128)(2,1)}, bf16[56,1024]{1,0:T(8,128)(2,1)S(1)}, u32[]{:S(2)}, u32[]{:S(2)}) collective-permute-start(bf16[56,1024]{1,0:T(8,128)(2,1)} %get-tuple-element.45), channel_id=1, source_target_pairs={{0,28},{4,24},{8,20},{12,16},{16,12},{20,8},{24,4},{28,0},{1,29},{... | collective-permute-start | bytes 344072 | tf_op jit(solution)/shard_map/ppermute | solution.py:350
  52.3 0.9 copy-start.13
  53.2 4.1 %copy-start.1 = (bf16[1,2048,512]{2,1,0:T(8,128)(2,1)S(1)}, bf16[1,2048,512]{2,1,0:T(8,128)(2,1)}, u32[]{:S(2)}) copy-start(bf16[1,2048,512]{2,1,0:T(8,128)(2,1)} %param.11) | copy-start | bytes 6291460
  53.3 4.1 %copy-start = (bf16[1,2048,512]{2,1,0:T(8,128)(2,1)S(1)}, bf16[1,2048,512]{2,1,0:T(8,128)(2,1)}, u32[]{:S(2)}) copy-start(bf16[1,2048,512]{2,1,0:T(8,128)(2,1)} %param.10) | copy-start | bytes 6291460
  53.3 8.1 %collective-permute-start.7 = (bf16[448,1024]{1,0:T(8,128)(2,1)S(1)}, bf16[448,1024]{1,0:T(8,128)(2,1)S(1)}, u32[]{:S(2)}, u32[]{:S(2)}) collective-permute-start(bf16[448,1024]{1,0:T(8,128)(2,1)S(1)} %bitcast.36), channel_id=1, source_target_pairs={{0,1},{1,0},{2,3},{3,2},{4,5},{5,4},{6,7},{7,6},{8,9},{9,8},{10,11... | collective-permute-start | bytes 2752520 | tf_op jit(solution)/shard_map/ppermute | solution.py:350
  53.3 3.2 %collective-permute-start.8 = (bf16[8,64,512]{2,1,0:T(8,128)(2,1)}, bf16[8,64,512]{2,1,0:T(8,128)(2,1)S(1)}, u32[]{:S(2)}, u32[]{:S(2)}) collective-permute-start(bf16[8,64,512]{2,1,0:T(8,128)(2,1)} %all_to_all.10.refs_0_.x_ref), channel_id=1, source_target_pairs={{0,1},{1,0},{2,3},{3,2},{4,5},{5,4},{6,7},{7,6},{8,9},{9,8},{10,11... | collective-permute-start | bytes 1572872 | tf_op jit(solution)/shard_map/ppermute | solution.py:350
  53.8 3.5 %collective-permute-start.10 = (bf16[8,64,512]{2,1,0:T(8,128)(2,1)}, bf16[8,64,512]{2,1,0:T(8,128)(2,1)S(1)}, u32[]{:S(2)}, u32[]{:S(2)}) collective-permute-start(bf16[8,64,512]{2,1,0:T(8,128)(2,1)} %collective-permute-done.9.refs_2_), channel_id=1, source_target_pairs={{0,1},{1,0},{2,3},{3,2},{4,5},{5,4},{6,7},{7,6},{8,9},{9,8},{10,11... | collective-permute-start | bytes 1572872 | tf_op jit(solution)/shard_map/ppermute | solution.py:350
  53.9 2.0 %copy-start.2 = (bf16[1,512,2048]{2,1,0:T(8,128)(2,1)S(1)}, bf16[1,512,2048]{2,1,0:T(8,128)(2,1)}, u32[]{:S(2)}) copy-start(bf16[1,512,2048]{2,1,0:T(8,128)(2,1)} %param.12) | copy-start | bytes 6291460
  56.6 4.7 %copy-start.16 = (bf16[8,64,512]{2,1,0:T(8,128)(2,1)}, bf16[8,64,512]{2,1,0:T(8,128)(2,1)S(1)}, u32[]{:S(2)}) copy-start(bf16[8,64,512]{2,1,0:T(8,128)(2,1)S(1)} %collective-permute-done.8.refs_1_) | copy-start | bytes 1572868
  57.3 4.0 %copy-start.18 = (bf16[8,64,512]{2,1,0:T(8,128)(2,1)}, bf16[8,64,512]{2,1,0:T(8,128)(2,1)S(1)}, u32[]{:S(2)}) copy-start(bf16[8,64,512]{2,1,0:T(8,128)(2,1)S(1)} %collective-permute-done.10.refs_3_) | copy-start | bytes 1572868
  57.3 4.0 %copy-start.3 = (bf16[1,512,2048]{2,1,0:T(8,128)(2,1)S(1)}, bf16[1,512,2048]{2,1,0:T(8,128)(2,1)}, u32[]{:S(2)}) copy-start(bf16[1,512,2048]{2,1,0:T(8,128)(2,1)} %param.12) | copy-start | bytes 6291460
  61.3 2.1 %copy-start.9 = (bf16[8,56,512]{2,1,0:T(8,128)(2,1)}, bf16[8,56,512]{2,1,0:T(8,128)(2,1)S(1)}, u32[]{:S(2)}) copy-start(bf16[8,56,512]{2,1,0:T(8,128)(2,1)S(1)} %get-tuple-element.47) | copy-start | bytes 1376260
  63.4 3.6 %copy-start.5 = (bf16[8,64,512]{2,1,0:T(8,128)(2,1)}, bf16[8,64,512]{2,1,0:T(8,128)(2,1)S(1)}, u32[]{:S(2)}) copy-start(bf16[8,64,512]{2,1,0:T(8,128)(2,1)S(1)} %get-tuple-element.51.gu_ref.refs_5_) | copy-start | bytes 1572868
  63.4 3.6 %collective-permute-start.12 = (bf16[1,448,512]{2,1,0:T(8,128)(2,1)S(1)}, bf16[1,448,512]{2,1,0:T(8,128)(2,1)S(1)}, u32[]{:S(2)}, u32[]{:S(2)}) collective-permute-start(bf16[1,448,512]{2,1,0:T(8,128)(2,1)S(1)} %get-tuple-element.55), channel_id=1, source_target_pairs={{0,1},{1,0},{2,3},{3,2},{4,5},{5,4},{6,7},{7,6},{8,9},{9,8},{10,11... | collective-permute-start | bytes 1376264 | tf_op jit(solution)/shard_map/ppermute | solution.py:350
  63.6 1.7 %collective-permute-start.14 = (f32[8,128]{1,0:T(8,128)S(1)}, f32[8,128]{1,0:T(8,128)S(1)}, u32[]{:S(2)}, u32[]{:S(2)}) collective-permute-start(f32[8,128]{1,0:T(8,128)S(1)} %get-tuple-element.56), channel_id=1, source_target_pairs={{0,1},{1,0},{2,3},{3,2},{4,5},{5,4},{6,7},{7,6},{8,9},{9,8},{10,11... | collective-permute-start | bytes 12296 | tf_op jit(solution)/shard_map/ppermute | solution.py:350
  64.0 22.3 %collective-permute-start.11 = (bf16[448,512]{1,0:T(8,128)(2,1)}, bf16[448,512]{1,0:T(8,128)(2,1)}, u32[]{:S(2)}, u32[]{:S(2)}) collective-permute-start(bf16[448,512]{1,0:T(8,128)(2,1)} %get-tuple-element.53), channel_id=1, source_target_pairs={{0,1},{1,0},{2,3},{3,2},{4,5},{5,4},{6,7},{7,6},{8,9},{9,8},{10,11... | collective-permute-start | bytes 1376264 | tf_op jit(solution)/shard_map/ppermute | solution.py:350
  65.3 4.2 %collective-permute-start.15 = (f32[8,128]{1,0:T(8,128)S(1)}, f32[8,128]{1,0:T(8,128)S(1)}, u32[]{:S(2)}, u32[]{:S(2)}) collective-permute-start(f32[8,128]{1,0:T(8,128)S(1)} %add.38), channel_id=1, source_target_pairs={{0,2},{1,3},{2,0},{3,1},{4,6},{5,7},{6,4},{7,5},{8,10},{9,11},{10,... | collective-permute-start | bytes 12296 | tf_op jit(solution)/shard_map/ppermute | solution.py:350
  65.8 4.2 %copy-start.14 = (f32[8,128]{1,0:T(8,128)S(1)}, f32[8,128]{1,0:T(8,128)}, u32[]{:S(2)}) copy-start(f32[8,128]{1,0:T(8,128)} %get-tuple-element.37.place_ref) | copy-start | bytes 12292
  68.0 18.3 %collective-permute-start.13 = (bf16[448,512]{1,0:T(8,128)(2,1)}, bf16[448,512]{1,0:T(8,128)(2,1)}, u32[]{:S(2)}, u32[]{:S(2)}) collective-permute-start(bf16[448,512]{1,0:T(8,128)(2,1)} %bitcast.9), channel_id=1, source_target_pairs={{0,2},{1,3},{2,0},{3,1},{4,6},{5,7},{6,4},{7,5},{8,10},{9,11},{10,... | collective-permute-start | bytes 1376264 | tf_op jit(solution)/shard_map/ppermute | solution.py:350
  69.5 3.6 %collective-permute-start.16 = (f32[1,8,128]{2,1,0:T(8,128)S(1)}, f32[1,8,128]{2,1,0:T(8,128)S(1)}, u32[]{:S(2)}, u32[]{:S(2)}) collective-permute-start(f32[1,8,128]{2,1,0:T(8,128)S(1)} %fusion.1), channel_id=1, source_target_pairs={{0,4},{4,0},{8,12},{12,8},{16,20},{20,16},{24,28},{28,24},{1,5},{5... | collective-permute-start | bytes 12296 | tf_op jit(solution)/shard_map/ppermute | solution.py:350
  70.0 0.6 copy-start.8
  73.1 12.7 %collective-permute-start.17 = (f32[2,8,128]{2,1,0:T(8,128)S(1)}, f32[2,8,128]{2,1,0:T(8,128)S(1)}, u32[]{:S(2)}, u32[]{:S(2)}) collective-permute-start(f32[2,8,128]{2,1,0:T(8,128)S(1)} %pad_maximum_fusion.2), channel_id=1, source_target_pairs={{0,8},{4,12},{8,0},{12,4},{16,24},{20,28},{24,16},{28,20},{1,9},{5... | collective-permute-start | bytes 24584 | tf_op jit(solution)/shard_map/ppermute | solution.py:350
  76.5 1.0 copy-start.6
  77.5 1.0 copy-start.17
  78.6 1.0 copy-start.19
  85.3 12.7 %collective-permute-start.26 = (f32[2,2048]{1,0:T(2,128)S(1)}, f32[2,2048]{1,0:T(2,128)S(1)}, u32[]{:S(2)}, u32[]{:S(2)}) collective-permute-start(f32[2,2048]{1,0:T(2,128)S(1)} %bitcast.45), channel_id=1, source_target_pairs={{0,2},{1,3},{2,0},{3,1},{4,6},{5,7},{6,4},{7,5},{8,10},{9,11},{10,... | collective-permute-start | bytes 49160 | tf_op jit(solution)/shard_map/ppermute | solution.py:350
  85.8 19.3 %collective-permute-start.25 = (f32[2,2048]{1,0:T(2,128)S(1)}, f32[2,2048]{1,0:T(2,128)S(1)}, u32[]{:S(2)}, u32[]{:S(2)}) collective-permute-start(f32[2,2048]{1,0:T(2,128)S(1)} %bitcast.46), channel_id=1, source_target_pairs={{0,1},{1,0},{2,3},{3,2},{4,5},{5,4},{6,7},{7,6},{8,9},{9,8},{10,11... | collective-permute-start | bytes 49160 | tf_op jit(solution)/shard_map/ppermute | solution.py:350
  85.8 12.3 %collective-permute-start.18 = (f32[4,8,128]{2,1,0:T(8,128)S(1)}, f32[4,8,128]{2,1,0:T(8,128)S(1)}, u32[]{:S(2)}, u32[]{:S(2)}) collective-permute-start(f32[4,8,128]{2,1,0:T(8,128)S(1)} %pad_maximum_fusion.1), channel_id=1, source_target_pairs={{0,16},{4,20},{8,24},{12,28},{16,0},{20,4},{24,8},{28,12},{1,17},{... | collective-permute-start | bytes 49160 | tf_op jit(solution)/shard_map/ppermute | solution.py:350
  88.3 9.8 %copy-start.4 = (bf16[128,2048]{1,0:T(8,128)(2,1)S(1)}, bf16[128,2048]{1,0:T(8,128)(2,1)}, u32[]{:S(2)}) copy-start(bf16[128,2048]{1,0:T(8,128)(2,1)} %tok_ref.1) | copy-start | bytes 1572868
  88.3 9.8 %copy-start.12 = (bf16[2048,8]{0,1:T(8,128)(2,1)S(1)}, bf16[2048,8]{0,1:T(8,128)(2,1)}, u32[]{:S(2)}) copy-start(bf16[2048,8]{0,1:T(8,128)(2,1)} %param.9) | copy-start | bytes 98308
  88.3 9.8 %copy-start.15 = (f32[8,128]{1,0:T(8,128)S(1)}, f32[8,128]{1,0:T(8,128)}, u32[]{:S(2)}) copy-start(f32[8,128]{1,0:T(8,128)} %get-tuple-element.57.aff_ref) | copy-start | bytes 12292
  88.3 22.6 %all-to-all-start.1 = ((bf16[8,56,512]{2,1,0:T(8,128)(2,1)}), bf16[8,56,512]{2,1,0:T(8,128)(2,1)}, u32[]{:S(2)}, u32[]{:S(2)}) async-start(bf16[8,56,512]{2,1,0:T(8,128)(2,1)} %bitcast.10), calls=%async_computation.1 | async-start | bytes 917504 | tf_op jit(solution)/shard_map/all_to_all | solution.py:353
  92.7 1.0 copy-start.10
  97.9 7.1 %collective-permute-start.27 = (f32[2,2048]{1,0:T(2,128)S(1)}, f32[2,2048]{1,0:T(2,128)S(1)}, u32[]{:S(2)}, u32[]{:S(2)}) collective-permute-start(f32[2,2048]{1,0:T(2,128)S(1)} %collective-permute-done.26), channel_id=1, source_target_pairs={{0,1},{1,0},{2,3},{3,2},{4,5},{5,4},{6,7},{7,6},{8,9},{9,8},{10,11... | collective-permute-start | bytes 49160 | tf_op jit(solution)/shard_map/ppermute | solution.py:350
  98.6 0.7 copy-start.11
  99.3 4.0 %collective-permute-start.22 = (f32[8,512]{1,0:T(8,128)S(1)}, f32[8,512]{1,0:T(8,128)S(1)}, u32[]{:S(2)}, u32[]{:S(2)}) collective-permute-start(f32[8,512]{1,0:T(8,128)S(1)} %get-tuple-element.59), channel_id=1, source_target_pairs={{0,4},{4,0},{8,12},{12,8},{16,20},{20,16},{24,28},{28,24},{1,5},{5... | collective-permute-start | bytes 49160 | tf_op jit(solution)/shard_map/ppermute | solution.py:350
  103.3 3.7 %collective-permute-start.23 = (f32[8,512]{1,0:T(8,128)S(1)}, f32[8,512]{1,0:T(8,128)S(1)}, u32[]{:S(2)}, u32[]{:S(2)}) collective-permute-start(f32[8,512]{1,0:T(8,128)S(1)} %add.40), channel_id=1, source_target_pairs={{0,8},{4,12},{8,0},{12,4},{16,24},{20,28},{24,16},{28,20},{1,9},{5... | collective-permute-start | bytes 49160 | tf_op jit(solution)/shard_map/ppermute | solution.py:350
  107.6 10.6 %collective-permute-start.24 = (f32[8,512]{1,0:T(8,128)}, f32[8,512]{1,0:T(8,128)}, u32[]{:S(2)}, u32[]{:S(2)}) collective-permute-start(f32[8,512]{1,0:T(8,128)} %add.41), channel_id=1, source_target_pairs={{0,16},{4,20},{8,24},{12,28},{16,0},{20,4},{24,8},{28,12},{1,17},{... | collective-permute-start | bytes 49160 | tf_op jit(solution)/shard_map/ppermute | solution.py:350
  113.0 5.2 %collective-permute-start.20 = (bf16[128,512]{1,0:T(8,128)(2,1)}, bf16[128,512]{1,0:T(8,128)(2,1)S(1)}, u32[]{:S(2)}, u32[]{:S(2)}) collective-permute-start(bf16[128,512]{1,0:T(8,128)(2,1)} %shard_map.153.refs_0_), channel_id=1, source_target_pairs={{0,2},{1,3},{2,0},{3,1},{4,6},{5,7},{6,4},{7,5},{8,10},{9,11},{10,... | collective-permute-start | bytes 393224 | tf_op jit(solution)/shard_map/ppermute | solution.py:350
  116.0 4.2 %collective-permute-start.19 = (bf16[128,512]{1,0:T(8,128)(2,1)}, bf16[128,512]{1,0:T(8,128)(2,1)S(1)}, u32[]{:S(2)}, u32[]{:S(2)}) collective-permute-start(bf16[128,512]{1,0:T(8,128)(2,1)} %shard_map.153.refs_0_), channel_id=1, source_target_pairs={{0,1},{1,0},{2,3},{3,2},{4,5},{5,4},{6,7},{7,6},{8,9},{9,8},{10,11... | collective-permute-start | bytes 393224 | tf_op jit(solution)/shard_map/ppermute | solution.py:350
  118.2 1.9 %collective-permute-start.21 = (bf16[128,512]{1,0:T(8,128)(2,1)S(1)}, bf16[128,512]{1,0:T(8,128)(2,1)S(1)}, u32[]{:S(2)}, u32[]{:S(2)}) collective-permute-start(bf16[128,512]{1,0:T(8,128)(2,1)S(1)} %collective-permute-done.20.refs_2_), channel_id=1, source_target_pairs={{0,1},{1,0},{2,3},{3,2},{4,5},{5,4},{6,7},{7,6},{8,9},{9,8},{10,11... | collective-permute-start | bytes 393224 | tf_op jit(solution)/shard_map/ppermute | solution.py:350
  120.2 0.9 copy-start.7

commit v3 on v2

--- a/solution.py
+++ b/solution.py
@@ -21,8 +21,7 @@
 
 ALONE = 67043328
 SHARED = 16 * 1024 * 1024
-JOIN = 1
-BACK = 1
+COEF_LANE = 64
 
 
 def params(limit=SHARED):
@@ -75,12 +74,24 @@
     hot = one_hot(place, slots)
     full = jnp.concatenate(hot, axis=0).astype(BF16)
     sent = dot(full, tok_ref[:, pl.ds(start, cols)])
-    lane = lax.broadcasted_iota(jnp.int32, (8, cols), 1)
+    slope = named * aff * (1.0 - aff) / jnp.sum(chosen, axis=0, keepdims=True)
+    row = lax.broadcasted_iota(jnp.int32, (experts, toks), 0)
+    lane = lax.broadcasted_iota(jnp.int32, (8, 128), 1)
     for e in range(experts):
-        column = jnp.sum(hot[e] * weights[e : e + 1, :], axis=1, keepdims=True)
-        tile = jnp.zeros((8, cols), F32)
+        own = weights[e : e + 1, :]
+        others = jnp.sum(jnp.where(row == e, 0.0, weights), axis=0, keepdims=True)
+        factors = jnp.where(row == e, others, -own) * slope
+        table = jnp.concatenate([factors, own, jnp.zeros((127 - experts, toks), F32)], axis=0)
+        values = dot(hot[e].astype(BF16), table.astype(BF16), 1, 1)
+        tile = jnp.zeros((8, 128), F32)
         for g in range(slots // 8):
-            tile = jnp.where(lane == g, column[8 * g : 8 * g + 8, :], tile)
+            part = values[8 * g : 8 * g + 8, :]
+            tile = jnp.where(lane == g, part[:, experts : experts + 1], tile)
+            shift = COEF_LANE + g * experts
+            moved = pltpu.roll(part, shift, 1)
+            tile = jnp.where((lane >= shift) & (lane < shift + experts), moved, tile)
+        if cols > 128:
+            tile = jnp.concatenate([tile, jnp.zeros((8, cols - 128), F32)], axis=1)
         block = jnp.concatenate([sent[e * slots : (e + 1) * slots, :], tile], axis=0)
         rows_ref[e] = block.astype(BF16)
 
@@ -102,9 +113,17 @@
         refs[k][...] = sent[k * slots : (k + 1) * slots, :].astype(BF16)
 
 
+def half_of(groups):
+    me = lax.axis_index("ep")
+    return me // (groups // 2), me % (groups // 2)
+
+
 def join_kernel(*refs):
-    for k, ref in enumerate(refs[:-1]):
-        refs[-1][lax.axis_index("ep") ^ k] = ref[...]
+    out_ref = refs[-1]
+    count = out_ref.shape[0]
+    _, place = half_of(2 * count)
+    for k in range(count):
+        out_ref[place ^ k] = refs[k][...]
 
 
 def gate_up_kernel(slots, shares, *refs):
@@ -139,10 +158,13 @@
     return jnp.concatenate([tile[:, g : g + 1] for g in range(slots // 8)], axis=0)
 
 
-def back_kernel(half, z_ref, wd_ref, back_ref):
-    cols = z_ref.shape[1]
-    start = pl.multiple_of(((lax.axis_index("tp") % 2) ^ half) * cols, 128)
-    back_ref[...] = dot(z_ref[...], wd_ref[:, pl.ds(start, cols)], 1, 1)
+def back_kernel(groups, near_hbm, far_hbm, wd_hbm, back_ref):
+    cols = near_hbm.shape[1]
+    side, _ = half_of(groups)
+    start = pl.multiple_of((lax.axis_index("tp") % 2) * cols, 128)
+    wd = wd_hbm[:, pl.ds(start, cols)]
+    back_ref[side] = dot(near_hbm[...], wd, 1, 1)
+    back_ref[1 - side] = dot(far_hbm[...], wd, 1, 1)
 
 
 def slot_parts(first, gg, gu, wg_ref, wu_ref, shares):
@@ -154,21 +176,26 @@
 
 
 def middle_kernel(
-    slots, shares, back_ref, z_ref, wd_ref, hid_ref, up_ref, gate_ref,
-    wg_ref, wu_ref, gg_ref, gu_ref, home_ref, chip_ref, term_ref,
+    slots, shares, back_ref, near_ref, far_ref, wd_ref, hid_ref, up_ref, gate_ref, wg_ref, wu_ref,
+    g_ref, home_ref, chip_ref, term_ref, sum_ref,
 ):
-    cols = z_ref.shape[1]
-    groups = gg_ref.shape[0]
+    cols = near_ref.shape[1]
+    groups = g_ref.shape[0]
+    side, _ = half_of(groups)
     start = pl.multiple_of(((lax.axis_index("tp") % 2) ^ 1) * cols, 128)
-    back = back_ref[...] + dot(z_ref[...], wd_ref[:, pl.ds(start, cols)], 1, 1)
+    wd = wd_ref[:, pl.ds(start, cols)]
+    sum_ref[side] = back_ref[side] + dot(near_ref[...], wd, 1, 1)
+    sum_ref[1 - side] = back_ref[1 - side] + dot(far_ref[...], wd, 1, 1)
+    back = sum_ref[...].reshape(hid_ref.shape)
+    hidden = hid_ref.shape[1]
     term = jnp.sum(hid_ref[...].astype(F32) * back, axis=1, keepdims=True)
     gu = back * up_ref[...]
     gg = back * gate_ref[...]
     pad = jnp.zeros((8, gu.shape[1]), F32)
     for e in range(groups):
         at = slice(e * slots, (e + 1) * slots)
-        gu_ref[e] = jnp.concatenate([gu[at], pad], axis=0).astype(BF16)
-        gg_ref[e] = jnp.concatenate([gg[at], pad], axis=0).astype(BF16)
+        g_ref[e, :, :hidden] = jnp.concatenate([gg[at], pad], axis=0).astype(BF16)
+        g_ref[e, :, hidden:] = jnp.concatenate([gu[at], pad], axis=0).astype(BF16)
     lane = lax.broadcasted_iota(jnp.int32, term_ref.shape, 1)
     tile = jnp.zeros(term_ref.shape, F32)
     for c in range(term.shape[0] // 8):
@@ -184,10 +211,10 @@
             chip_ref[j - 1] = part.astype(BF16)
 
 
-def even_kernel(slots, shares, gg_ref, gu_ref, wg_ref, wu_ref, home_ref, chip_ref):
-    groups, span, hidden = gg_ref.shape
-    gg = gg_ref[...].reshape(groups * span, hidden)
-    gu = gu_ref[...].reshape(groups * span, hidden)
+def even_kernel(slots, shares, g_ref, wg_ref, wu_ref, home_ref, chip_ref):
+    groups, span, double = g_ref.shape
+    both = g_ref[...].reshape(groups * span, double)
+    gg, gu = both[:, : double // 2], both[:, double // 2 :]
     for j in range(shares // 2):
         part = slot_parts(2 * j, gg, gu, wg_ref, wu_ref, shares)
         for e in range(groups):
@@ -202,25 +229,29 @@
     out_ref[...] = (own_ref[...] + got_ref[...].astype(F32)).astype(BF16)
 
 
-def add_chip_kernel(own_ref, core_ref, *refs):
+def add_chip_kernel(own_ref, core_ref, tile_ref, *refs):
     total = own_ref[...] + core_ref[...].astype(F32)
     for chip_ref in refs[:-1]:
         total = total + chip_ref[...].astype(F32)
-    refs[-1][...] = total.astype(BF16)
+    out_ref = refs[-1]
+    slots = out_ref.shape[1] - 8
+    for e in range(out_ref.shape[0]):
+        block = jnp.concatenate([total[e * slots : (e + 1) * slots], tile_ref[e]], axis=0)
+        out_ref[e] = block.astype(BF16)
 
 
 def grads_kernel(shares, q_ref, *refs):
     x_refs = refs[:shares]
-    gg_ref, gu_ref, gate_out, up_out, rows_out = refs[shares:]
+    g_ref, gate_out, up_out, rows_out = refs[shares:]
     groups, span, cols = x_refs[0].shape
-    hidden = gg_ref.shape[2]
+    double = g_ref.shape[2]
     for r in range(shares):
 
         @pl.when(pl.program_id(0) == r)
         def _(x_ref=x_refs[r]):
             x = x_ref[...].reshape(groups * span, cols)
-            gate = dot(x, gg_ref[...].reshape(groups * span, hidden), 0, 0)
-            up = dot(x, gu_ref[...].reshape(groups * span, hidden), 0, 0)
+            both = dot(x, g_ref[...].reshape(groups * span, double), 0, 0)
+            gate, up = both[:, : double // 2], both[:, double // 2 :]
             gate_out[...] = gate.astype(BF16)
             up_out[...] = up.astype(BF16)
             rows_out[0, 0:1, :] = square_rows(gate)
@@ -235,56 +266,98 @@
     return jnp.sum(folded.T, axis=0, keepdims=True)
 
 
-def down_kernel(slots, q_ref, own_ref, far_ref, x_ref, hid_ref, down_out, rows_out):
+def down_kernel(slots, q_ref, *refs):
+    x_ref, hid_ref, down_out, rows_out = refs[4:]
     groups = x_ref.shape[0]
-    for h, z_ref in enumerate((own_ref, far_ref)):
+    side, _ = half_of(groups)
+    for h in range(2):
 
         @pl.when(pl.program_id(0) == h)
-        def _(z_ref=z_ref):
-            scale = jnp.concatenate([scale_column(x_ref, e, slots) for e in range(groups)], axis=0)
-            weighted = (scale * z_ref[...].astype(F32)).astype(BF16)
-            down = dot(hid_ref[...], weighted, 0, 0)
+        def _(pair=refs[2 * h : 2 * h + 2]):
+            down = 0.0
+            for z_ref, at in zip(pair, (side, 1 - side)):
+                scale = [scale_column(x_ref, at * (groups // 2) + e, slots) for e in range(groups // 2)]
+                scale = jnp.concatenate(scale, axis=0)
+                weighted = (scale * z_ref[...].astype(F32)).astype(BF16)
+                down = down + dot(hid_ref[at], weighted, 0, 0)
             down_out[...] = down.astype(BF16)
             rows_out[0] = square_rows(down)
 
 
-def router_kernel(slots, term_ref, place_ref, aff_ref, tok_ref, router_ref, base_out, part_out):
-    experts, toks = place_ref.shape
-    cols = part_out.shape[1]
+def add_kernel(a_ref, b_ref, out_ref):
+    out_ref[...] = a_ref[...] + b_ref[...]
+
+
+def terms_kernel(slots, a_ref, b_ref, x_ref, tile_ref, part_ref):
+    term = (a_ref[...] + b_ref[...]).astype(BF16).astype(F32)
+    groups, span, cols = x_ref.shape
+    experts = part_ref.shape[0]
+    count = slots // 8
+    lanes = term.shape[1]
+    lane = lax.broadcasted_iota(jnp.int32, (8, lanes), 1)
+    blocks = []
+    for b in range(groups):
+        moved = pltpu.roll(term, (lanes - b * count) % lanes, 1)
+        moved = jnp.where(lane < count, moved, 0.0)[:, :128]
+        if cols > 128:
+            moved = jnp.concatenate([moved, jnp.zeros((8, cols - 128), F32)], axis=1)
+        tile_ref[b] = moved
+        spare = x_ref[b, slots:, :128].astype(F32)
+        for g in range(count):
+            factors = pltpu.roll(spare, 128 - COEF_LANE - g * experts, 1)
+            c = b * count + g
+            blocks.append(term[:, c : c + 1] * factors)
+        blocks.append(jnp.zeros((8, 128), F32))
+    table = jnp.concatenate(blocks, axis=0)
+    table = jnp.where(lax.broadcasted_iota(jnp.int32, table.shape, 1) < experts, table, 0.0)
+    high = table.astype(BF16)
+    low = (table - high.astype(F32)).astype(BF16)
+    x = x_ref[...].reshape(groups * span, cols)
+    part_ref[...] = (dot(high, x, 0, 0) + dot(low, x, 0, 0))[:experts]
+
+
+def last_sum_kernel(a_ref, b_ref, sum_ref, rows_ref):
+    total = a_ref[...] + b_ref[...]
+    sum_ref[...] = total
+    rows_ref[...] = jnp.sum(total * total, axis=0, keepdims=True)
+
+
+def slot_map_kernel(slots, place_ref, hot_ref):
+    hot_ref[...] = jnp.concatenate(one_hot(place_ref[...], slots), axis=0).astype(BF16)
+
+
+def home_kernel(
+    slots, got_hbm, hot_hbm, place_hbm, aff_hbm, router_hbm, token_out,
+    got_ref, hot_ref, place_ref, aff_ref, router_ref, sems,
+):
+    experts, span, cols = got_ref.shape
+    toks = place_ref.shape[1]
     start = pl.multiple_of(lax.axis_index("tp") * cols, 128)
+    copies = fetch(
+        sems, (place_hbm, place_ref), (aff_hbm, aff_ref), (got_hbm, got_ref),
+        (router_hbm.at[:, pl.ds(start, cols)], router_ref), (hot_hbm, hot_ref),
+    )
+    for copy in copies:
+        copy.wait()
     place = place_ref[...]
     aff = aff_ref[...]
-    slot = lax.broadcasted_iota(jnp.int32, (slots, toks), 0).astype(F32)
-    lanes = term_ref.shape[2]
-    own = lax.axis_index("ep")
-    row = lax.broadcasted_iota(jnp.int32, (experts, toks), 0)
-    term = jnp.zeros((experts, toks), F32)
-    for r in range(experts):
-        tile = pltpu.roll(term_ref[r], lanes - own * (slots // 8), 1)
-        hot = (slot == place_ref[pl.ds(own ^ r, 1), :]).astype(F32)
+    back = dot(hot_ref[...], got_ref[...].reshape(experts * span, cols), 0, 0)
+    hot = one_hot(place, slots)
+    rows = []
+    for e in range(experts):
+        tile = got_ref[e, slots:, :128].astype(F32)
         total = jnp.zeros((8, toks), F32)
         for g in range(slots // 8):
-            total = total + hot[8 * g : 8 * g + 8, :] * tile[:, g : g + 1]
-        term = jnp.where(row == (own ^ r), jnp.sum(total, axis=0, keepdims=True), term)
+            total = total + hot[e][8 * g : 8 * g + 8, :] * tile[:, g : g + 1]
+        rows.append(jnp.sum(total, axis=0, keepdims=True))
+    term = jnp.concatenate(rows, axis=0)
     named = (place >= 0).astype(F32)
     chosen = named * aff
     total_aff = jnp.sum(chosen, axis=0, keepdims=True)
     weights = chosen / total_aff
     d_chosen = (term - jnp.sum(term * weights, axis=0, keepdims=True)) / total_aff
     d_logit = named * d_chosen * aff * (1.0 - aff)
-    base_out[...] = dot(d_logit.T.astype(BF16), router_ref[:, pl.ds(start, cols)])
-    part_out[...] = dot(d_logit.astype(BF16), tok_ref[:, pl.ds(start, cols)])
-
-
-def slot_map_kernel(slots, place_ref, hot_ref):
-    hot_ref[...] = jnp.concatenate(one_hot(place_ref[...], slots), axis=0).astype(BF16)
-
-
-def home_kernel(got_hbm, hot_hbm, base_hbm, token_out, got_ref, hot_ref, base_ref, sems):
-    copies = fetch(sems, (hot_hbm, hot_ref), (got_hbm, got_ref), (base_hbm, base_ref))
-    for copy in copies:
-        copy.wait()
-    token_out[...] = (dot(hot_ref[...], got_ref[...], 0, 0) + base_ref[...]).astype(BF16)
+    token_out[...] = (back + dot(d_logit.T.astype(BF16), router_ref[...])).astype(BF16)
 
 
 def assemble_kernel(*refs):
@@ -372,7 +445,7 @@
     for k in range(experts - 1, 0, -1):
         pieces[k] = swap(pieces[k], k, "ep")
 
-    hot = call(functools.partial(slot_map_kernel, slots), shape(count, toks), False, place)
+    hot = call(functools.partial(slot_map_kernel, span), shape(groups * span, toks), False, place)
 
     x_parts = spread(rows_got)
     hid, up_factor, gate_factor = call(
@@ -385,22 +458,25 @@
     up_factor = up_factor.reshape(count, hidden)
     gate_factor = gate_factor.reshape(count, hidden)
 
-    z_own = call(join_kernel, shape(groups, slots, half), False, *pieces, flops=JOIN * unit).reshape(count, half)
-    z_far = swap(z_own, 1)
+    side = groups // 2
+    near = call(join_kernel, shape(side, slots, half), False, *pieces[:side], wg, wu).reshape(count // 2, half)
+    near_got = swap(near, 1)
+    far = call(join_kernel, shape(side, slots, half), False, *pieces[side:]).reshape(count // 2, half)
+    far_got = swap(far, 1)
     back = call(
-        functools.partial(back_kernel, 0), shape(count, hidden, dtype=F32),
-        False, z_own, wd, flops=BACK * unit,
-    )
-    gg, gu, odd_home, odd_chip, term = call(
+        functools.partial(back_kernel, groups), shape(2, count // 2, hidden, dtype=F32),
+        False, near, far, wd, flops=unit,
+    )
+    g, odd_home, odd_chip, term = call(
         functools.partial(middle_kernel, slots, shares),
         (
-            shape(groups, span, hidden),
-            shape(groups, span, hidden),
+            shape(groups, span, 2 * hidden),
             shape(count, cols),
             shape(chips - 1, count, cols),
             shape(8, -(-count // 1024) * 128, dtype=F32),
         ),
-        False, back, z_far, wd, hid, up_factor, gate_factor, wg, wu, flops=3 * unit,
+        False, back, near_got, far_got, wd, hid, up_factor, gate_factor, wg, wu, flops=3 * unit,
+        scratch=[buffer(2, count // 2, hidden, dtype=F32)],
     )
     term_got = swap(term, 1)
     core_chip = swap(odd_chip, 1)
@@ -408,23 +484,38 @@
     even_home, even_chip = call(
         functools.partial(even_kernel, slots, shares),
         (shape(count, cols, dtype=F32), shape(chips - 1, count, cols, dtype=F32)),
-        False, gg, gu, wg, wu, flops=2 * unit,
-    )
-    term = term + term_got
+        False, g, wg, wu, flops=2 * unit,
+    )
+
+    def add(a, b, kernel=add_kernel, lead=()):
+        return call(kernel, shape(*lead, *a.shape, dtype=F32), False, a, b)
+
+    term = add(term, term_got)
     bit = 2
     while 2 * bit < shares:
-        term = term + swap(term, bit)
+        term = add(term, swap(term, bit))
         bit *= 2
     term_got = swap(term, bit)
     chip_send = call(add_core_kernel, shape(chips - 1, count, cols), False, even_chip, core_chip)
     chip_got = [swap(chip_send[j], 2 * (j + 1)) for j in range(chips - 1)]
-    terms = (term + term_got).astype(BF16).astype(F32)[None]
+    tiles, router_sum = call(
+        functools.partial(terms_kernel, slots),
+        (shape(groups, 8, cols, dtype=F32), shape(experts, cols, dtype=F32)),
+        False, term, term_got, rows_got,
+    )
     bit = 1
-    while bit < groups:
-        terms = jnp.concatenate([terms, swap(terms, bit, "ep")], axis=0)
+    while 2 * bit < groups:
+        router_got = swap(router_sum, bit, "ep")
+        router_sum = add(router_sum, router_got)
         bit *= 2
-    home_send = call(add_chip_kernel, shape(count, cols), False, even_home, core_home, *chip_got)
-    home_got = exchange(home_send.reshape(groups, slots, cols)).reshape(count, cols)
+    router_got = swap(router_sum, bit, "ep")
+    router_sum, router_rows = call(
+        last_sum_kernel, (shape(experts, cols, dtype=F32), shape(1, cols, dtype=F32)),
+        False, router_sum, router_got,
+    )
+    router_rows = router_rows.reshape(cols)
+    home_send = call(add_chip_kernel, shape(groups, span, cols), False, even_home, core_home, tiles, *chip_got)
+    home_got = exchange(home_send)
 
     grad_spec = pl.BlockSpec((cols, hidden), lambda r, q: (q[0] ^ r, 0))
     gate_grad, up_grad, norms = pl.pallas_call(
@@ -433,29 +524,29 @@
         grid_spec=pltpu.PrefetchScalarGridSpec(
             num_scalar_prefetch=1,
             grid=(shares,),
-            in_specs=[VMEM] * (shares + 2),
+            in_specs=[VMEM] * (shares + 1),
             out_specs=(grad_spec, grad_spec, pl.BlockSpec((1, 2, cols), lambda r, q: (q[0] ^ r, 0, 0))),
         ),
         compiler_params=params(),
         cost_estimate=cost(4 * unit, 0),
         name="grads",
-    )(q, *x_parts, gg, gu)
+    )(q, *x_parts, g)
     down_grad, down_norms = pl.pallas_call(
         functools.partial(down_kernel, slots),
         out_shape=(shape(hidden, width), shape(2, 1, hidden, dtype=F32)),
         grid_spec=pltpu.PrefetchScalarGridSpec(
             num_scalar_prefetch=1,
             grid=(2,),
-            in_specs=[VMEM] * 4,
+            in_specs=[VMEM] * 6,
             out_specs=(
                 pl.BlockSpec((hidden, half), lambda h, q: (0, (q[0] % 2) ^ h)),
                 pl.BlockSpec((1, 1, hidden), lambda h, q: (h, 0, 0)),
             ),
         ),
-        compiler_params=params(),
+        compiler_params=params(ALONE),
         cost_estimate=cost(2 * unit, 0),
         name="down",
-    )(q, z_own, z_far, rows_got, hid)
+    )(q, near, far, near_got, far_got, rows_got, hid.reshape(2, count // 2, hidden))
     norms = norms.transpose(1, 0, 2).reshape(2, width)
     norms = spread(norms)
     while len(norms) > 1:
@@ -463,19 +554,17 @@
     norms = norms[0]
     down_rows = (down_norms[0] + down_norms[1]).reshape(1, hidden)
 
-    token_base, router_sum = call(
-        functools.partial(router_kernel, slots),
-        (shape(toks, cols, dtype=F32), shape(experts, cols, dtype=F32)),
-        False, terms, place, aff, tokens, router,
-    )
-    bit = 1
-    while bit < groups:
-        router_sum = router_sum + swap(router_sum, bit, "ep")
-        bit *= 2
-    router_rows = jnp.sum(router_sum * router_sum, axis=0)
     token_part = call(
-        home_kernel, shape(toks, cols), False, home_got, hot, token_base, hbm=(0, 1, 2), limit=ALONE,
-        scratch=[buffer(count, cols), buffer(count, toks), buffer(toks, cols, dtype=F32), DMAS((3,))],
+        functools.partial(home_kernel, slots), shape(toks, cols),
+        False, home_got, hot, place, aff, router, hbm=range(5), limit=ALONE,
+        scratch=[
+            buffer(groups, span, cols),
+            buffer(groups * span, toks),
+            buffer(experts, toks, dtype=F32),
+            buffer(experts, toks, dtype=F32),
+            buffer(experts, cols),
+            DMAS((5,)),
+        ],
     )
     token_grad = call(
         assemble_kernel, shape(toks, width), False, *spread(token_part), out_hbm=True, scratch=[DMAS((shares,))],

time: 123 us -> 130 us (1.057)
  waiting for transfers between devices: 21.9 us -> 33.1 us
  starting transfers between devices: 33.3 us -> 29.7 us
  Pallas kernels: 29.5 us -> 31.4 us
  other arithmetic: 3.76 us -> 2.05 us
    ppermute x28 -> x26, waiting for transfers between devices: 21.9 us -> 33.1 us  [swap(): return lax.ppermute(value, axis, [(i, i ^ bit) for i in range(size)])]
    ppermute x28 -> x26, starting transfers between devices: 28.8 us -> 25.4 us  [swap(): return lax.ppermute(value, axis, [(i, i ^ bit) for i in range(size)])]
    reduce_sum x1 -> x0, other arithmetic: 1.92 us -> none  [layer(): router_rows = jnp.sum(router_sum * router_sum, axis=0)]
    pallas_call x13 -> x18, Pallas kernels: 19.7 us -> 21 us  [call(): pl.pallas_call(kernel, out_shape=outs, in_specs=([SMEM] if scalar else []...]
    unnamed x40 -> x32, local copies, waits for them, and re-layouts: 9.26 us -> 9 us
  transfers between devices with their start and end apart: 29 -> 27, of which waited for: 11 -> 8; matrix products, arithmetic and copies ran while one was open for 4% -> 2% of each run, Pallas kernels for 20% -> 19%
where the time goes in v3:
time: 130 us; the launch traced here: 129 us
  waiting for transfers between devices  33.1 us (25%)
  Pallas kernels  31.4 us (24%)
  starting transfers between devices  29.7 us (23%)
  blocking collectives  21.9 us (17%)
  local copies, waits for them, and re-layouts  9.62 us (7%)
  other arithmetic  2.05 us (2%)
    ppermute x26, waiting for transfers between devices, swap(): return lax.ppermute(value, axis, [(i, i ^ bit) for i in range(size)])  33.1 us
    ppermute x26, starting transfers between devices, swap(): return lax.ppermute(value, axis, [(i, i ^ bit) for i in range(size)])  25.4 us
    all_to_all x1, blocking collectives, exchange(): return lax.all_to_all(value, 'ep', split_axis=0, concat_axis=0, tiled=True)  21.9 us
    pallas_call x18, Pallas kernels, call(): pl.pallas_call(kernel, out_shape=outs, in_specs=([SMEM] if scalar else []...  21 us
    unnamed x32, local copies, waits for them, and re-layouts  9 us
    pallas_call x1, Pallas kernels, layer(): pl.pallas_call(functools.partial(grads_kernel, shares), out_shape=(shape(...  5.7 us
    pallas_call x1, Pallas kernels, layer(): pl.pallas_call(functools.partial(down_kernel, slots), out_shape=(shape(hi...  4.75 us
    all_to_all x1, starting transfers between devices, exchange(): return lax.all_to_all(value, 'ep', split_axis=0, concat_axis=0, tiled=True)  4.32 us
  transfers between devices with their start and end apart: 27, of which 8 were waited for; matrix products, arithmetic and copies ran while one was open for 2% of the time, Pallas kernels for 19%

profile of v3, /device:TPU:0, one launch (start us, length us, event | category | flops | bytes accessed | tf_op | source)
XLA Modules:
  0.0 129.0 jit_solution(6676570580432271583)
XLA Ops:
  0.6 2.6 %shard_map.142 = (bf16[8,64,512]{2,1,0:T(8,128)(2,1)}, f32[8,128]{1,0:T(8,128)}, f32[8,128]{1,0:T(8,128)}) custom-call(bf16[128,2048]{1,0:T(8,128)(2,1)} %tok_hbm.1, s32[2,128]{1,0:T(2,128)} %bitcast.46, bf16[8,2048]{1,0:T(8,128)(2,1)} %bitcast.44), custom_call_target="tpu_custom_call" | custom-call | tf_op jit(solution)/shard_map/pallas_call | solution.py:378
  3.2 21.9 %all_to_all.10.refs_0_.x_ref.refs_4_ = bf16[8,64,512]{2,1,0:T(8,128)(2,1)} all-to-all(bf16[8,64,512]{2,1,0:T(8,128)(2,1)} %get-tuple-element.47), channel_id=1, replica_groups=mesh['ep'=8,'tp'=4] {'ep'}, dimensions={0} | all-to-all | bytes 1048576 | tf_op jit(solution)/shard_map/all_to_all | solution.py:426
  25.1 1.5 %collective-permute-start.10 = (bf16[8,64,512]{2,1,0:T(8,128)(2,1)}, bf16[8,64,512]{2,1,0:T(8,128)(2,1)}, u32[]{:S(2)}, u32[]{:S(2)}) collective-permute-start(bf16[8,64,512]{2,1,0:T(8,128)(2,1)} %all_to_all.10.refs_0_.x_ref.refs_4_), channel_id=1, source_target_pairs={{0,2},{1,3},{2,0},{3,1},{4,6},{5,7},{6,4},{7,5},{8,10},{9,11},{10,... | collective-permute-start | bytes 1572872 | tf_op jit(solution)/shard_map/ppermute | solution.py:423
  26.6 2.8 %shard_map.143 = (bf16[56,1024]{1,0:T(8,128)(2,1)}, bf16[56,1024]{1,0:T(8,128)(2,1)}, bf16[56,1024]{1,0:T(8,128)(2,1)}, bf16[56,1024]{1,0:T(8,128)(2,1)}, bf16[5...) custom-call(bf16[128,2048]{1,0:T(8,128)(2,1)} %cot_hbm.1, ...), custom_call_target="tpu_custom_call" | custom-call | flops 117440512 | tf_op jit(solution)/shard_map/pallas_call | solution.py:378
  29.5 1.1 collective-permute-start.3
  30.6 0.0 collective-permute-start.9
  30.6 7.3 %collective-permute-done.10.refs_2_ = bf16[8,64,512]{2,1,0:T(8,128)(2,1)} collective-permute-done((bf16[8,64,512]{2,1,0:T(8,128)(2,1)}, bf16[8,64,512]{2,1,0:T(8,128)(2,1)}, u32[]{:S(2)}, u32[]{:S(2)}) %collective-permute-start.10) | collective-permute-done | bytes 524320 | tf_op jit(solution)/shard_map/ppermute | solution.py:423
  38.0 1.0 collective-permute-start.4
  39.0 1.8 %collective-permute-start.5 = (bf16[56,1024]{1,0:T(8,128)(2,1)}, bf16[56,1024]{1,0:T(8,128)(2,1)S(1)}, u32[]{:S(2)}, u32[]{:S(2)}) collective-permute-start(bf16[56,1024]{1,0:T(8,128)(2,1)} %get-tuple-element.45), channel_id=1, source_target_pairs={{0,24},{4,28},{8,16},{12,20},{16,8},{20,12},{24,0},{28,4},{1,25},{... | collective-permute-start | bytes 344072 | tf_op jit(solution)/shard_map/ppermute | solution.py:423
  40.9 3.3 %collective-permute-start.6 = (bf16[56,1024]{1,0:T(8,128)(2,1)}, bf16[56,1024]{1,0:T(8,128)(2,1)S(1)}, u32[]{:S(2)}, u32[]{:S(2)}) collective-permute-start(bf16[56,1024]{1,0:T(8,128)(2,1)} %get-tuple-element.46), channel_id=1, source_target_pairs={{0,28},{4,24},{8,20},{12,16},{16,12},{20,8},{24,4},{28,0},{1,29},{... | collective-permute-start | bytes 344072 | tf_op jit(solution)/shard_map/ppermute | solution.py:423
  44.1 9.1 %collective-permute-done.4.refs_1_ = bf16[56,1024]{1,0:T(8,128)(2,1)S(1)} collective-permute-done((bf16[56,1024]{1,0:T(8,128)(2,1)}, bf16[56,1024]{1,0:T(8,128)(2,1)S(1)}, u32[]{:S(2)}, u32[]{:S(2)}) %collective-permute-start.4) | collective-permute-done | bytes 114720 | tf_op jit(solution)/shard_map/ppermute | solution.py:423
  53.2 0.2 collective-permute-start
  53.5 1.6 %collective-permute-start.1 = (bf16[56,1024]{1,0:T(8,128)(2,1)}, bf16[56,1024]{1,0:T(8,128)(2,1)S(1)}, u32[]{:S(2)}, u32[]{:S(2)}) collective-permute-start(bf16[56,1024]{1,0:T(8,128)(2,1)} %get-tuple-element.41), channel_id=1, source_target_pairs={{0,8},{4,12},{8,0},{12,4},{16,24},{20,28},{24,16},{28,20},{1,9},{5... | collective-permute-start | bytes 344072 | tf_op jit(solution)/shard_map/ppermute | solution.py:423
  55.0 0.0 collective-permute-done.6.refs_3_
  55.0 3.4 %collective-permute-start.2 = (bf16[56,1024]{1,0:T(8,128)(2,1)}, bf16[56,1024]{1,0:T(8,128)(2,1)S(1)}, u32[]{:S(2)}, u32[]{:S(2)}) collective-permute-start(bf16[56,1024]{1,0:T(8,128)(2,1)} %get-tuple-element.42), channel_id=1, source_target_pairs={{0,12},{4,8},{8,4},{12,0},{16,28},{20,24},{24,20},{28,16},{1,13},{... | collective-permute-start | bytes 344072 | tf_op jit(solution)/shard_map/ppermute | solution.py:423
  58.5 0.1 collective-permute-start.8
  58.6 3.5 %collective-permute-done.2.refs_3_ = bf16[56,1024]{1,0:T(8,128)(2,1)S(1)} collective-permute-done((bf16[56,1024]{1,0:T(8,128)(2,1)}, bf16[56,1024]{1,0:T(8,128)(2,1)S(1)}, u32[]{:S(2)}, u32[]{:S(2)}) %collective-permute-start.2) | collective-permute-done | bytes 114720 | tf_op jit(solution)/shard_map/ppermute | solution.py:423
  62.2 1.6 %copy-done = bf16[1,2048,512]{2,1,0:T(8,128)(2,1)S(1)} copy-done((bf16[1,2048,512]{2,1,0:T(8,128)(2,1)S(1)}, bf16[1,2048,512]{2,1,0:T(8,128)(2,1)}, u32[]{:S(2)}) %copy-start) | copy-done | bytes 2097176
  63.7 1.6 %copy-done.2 = bf16[1,2048,512]{2,1,0:T(8,128)(2,1)S(1)} copy-done((bf16[1,2048,512]{2,1,0:T(8,128)(2,1)S(1)}, bf16[1,2048,512]{2,1,0:T(8,128)(2,1)}, u32[]{:S(2)}) %copy-start.2) | copy-done | bytes 2097176
  65.3 0.9 copy-done.12
  66.3 0.0 copy-start.1
  66.3 0.1 collective-permute-start.7
  66.4 1.6 %copy-done.4 = bf16[1,512,2048]{2,1,0:T(8,128)(2,1)S(1)} copy-done((bf16[1,512,2048]{2,1,0:T(8,128)(2,1)S(1)}, bf16[1,512,2048]{2,1,0:T(8,128)(2,1)}, u32[]{:S(2)}) %copy-start.4) | copy-done | bytes 2097176
  68.0 0.8 shard_map.146.back_ref
  68.8 0.4 copy-done.1
  69.3 3.7 %shard_map.147 = (bf16[8,56,512]{2,1,0:T(8,128)(2,1)S(1)}, f32[8,56,512]{2,1,0:T(8,128)S(1)}, f32[8,56,512]{2,1,0:T(8,128)S(1)}) custom-call(bf16[8,64,512]{2,1,0:T(8,128)(2,1)} %all_to_all.10.refs_0_.x_ref.refs_4_, bf16[8,64,512]{2,1,0:T(8,128)(2,1)S(1)} %collective-permute-done.9.refs_1_, bf16[8,64,512]{2,1,0:T(8,128)(2,1)} %collective-permute-done.10.refs_2_, ...), custom_call_target="tpu_custom_call" | custom-call | flops 1879048192 | tf_op jit(solution)/shard_map/pallas_call | solution.py:378
  73.0 2.1 %shard_map.148 = (bf16[8,64,1024]{2,1,0:T(8,128)(2,1)S(1)}, bf16[448,512]{1,0:T(8,128)(2,1)S(1)}, bf16[1,448,512]{2,1,0:T(8,128)(2,1)S(1)}, f32[8,128]{1,0:T(8,128)S(1)}) custom-call(f32[2,224,512]{2,1,0:T(8,128)S(1)} %shard_map.146.back_ref, bf16[224,1024]{1,0:T(8,128)(2,1)S(1)} %collective-permute-done.7.near_ref.refs_2_, ...), custom_call_target="tpu_custom_call" | custom-call | flops 1409286144 | tf_op jit(solution)/shard_map/pallas_call | solution.py:378
  75.1 0.1 collective-permute-start.15
  75.2 0.5 collective-permute-start.12
  75.7 1.3 shard_map.149
  77.0 0.0 collective-permute-done.15.got_ref
  77.0 0.1 shard_map.152
  77.1 0.0 copy-start.13
  77.1 1.6 %collective-permute-start.16 = (bf16[448,512]{1,0:T(8,128)(2,1)S(1)}, bf16[448,512]{1,0:T(8,128)(2,1)S(1)}, u32[]{:S(2)}, u32[]{:S(2)}) collective-permute-start(bf16[448,512]{1,0:T(8,128)(2,1)S(1)} %bitcast.41), channel_id=1, source_target_pairs={{0,2},{1,3},{2,0},{3,1},{4,6},{5,7},{6,4},{7,5},{8,10},{9,11},{10,... | collective-permute-start | bytes 1376264 | tf_op jit(solution)/shard_map/ppermute | solution.py:423
  78.7 1.2 collective-permute-done.13.b_ref
  79.9 0.5 collective-permute-start.14
  80.4 9.5 %collective-permute-done.14.b_ref = f32[8,128]{1,0:T(8,128)S(1)} collective-permute-done((f32[8,128]{1,0:T(8,128)S(1)}, f32[8,128]{1,0:T(8,128)S(1)}, u32[]{:S(2)}, u32[]{:S(2)}) %collective-permute-start.14) | collective-permute-done | bytes 4128 | tf_op jit(solution)/shard_map/ppermute | solution.py:423
  89.8 1.5 %shard_map.151 = (f32[8,8,512]{2,1,0:T(8,128)S(1)}, f32[8,512]{1,0:T(8,128)S(1)}) custom-call(f32[8,128]{1,0:T(8,128)S(1)} %shard_map.150.a_ref, f32[8,128]{1,0:T(8,128)S(1)} %collective-permute-done.14.b_ref, bf16[8,64,512]{2,1,0:T(8,128)(2,1)} %all_to_all.10.refs_0_.x_ref.refs_4_), custom_call_target="tpu_custom_call" | custom-call | tf_op jit(solution)/shard_map/pallas_call | solution.py:378
  91.4 0.0 copy-start.14
  91.4 0.6 copy-done.14
  92.0 0.9 shard_map.153
  92.9 4.3 %all-to-all-start.1 = ((bf16[8,64,512]{2,1,0:T(8,128)(2,1)}), bf16[8,64,512]{2,1,0:T(8,128)(2,1)}, u32[]{:S(2)}, u32[]{:S(2)}) async-start(bf16[8,64,512]{2,1,0:T(8,128)(2,1)} %shard_map.153), calls=%async_computation.1 | async-start | bytes 1048576 | tf_op jit(solution)/shard_map/all_to_all | solution.py:426
  97.3 0.6 copy-done.7
  98.0 5.7 %grads.1 = (bf16[2048,512]{1,0:T(8,128)(2,1)}, bf16[2048,512]{1,0:T(8,128)(2,1)}, f32[4,2,512]{2,1,0:T(2,128)}) custom-call(s32[1]{0:T(128)} %bitcast.13.q_ref, bf16[8,64,512]{2,1,0:T(8,128)(2,1)} %all_to_all.10.refs_0_.x_ref.refs_4_, bf16[8,64,512]{2,1,0:T(8,128)(2,1)S(1)} %collective-permute-done.9.refs_1_, ...), custom_call_target="tpu_custom_call" | custom-call | flops 1879048192 | tf_op jit(solution)/shard_map/grads/pallas_call | solution.py:521
  103.7 1.5 %collective-permute-start.24 = (f32[2,2048]{1,0:T(2,128)}, f32[2,2048]{1,0:T(2,128)}, u32[]{:S(2)}, u32[]{:S(2)}) collective-permute-start(f32[2,2048]{1,0:T(2,128)} %bitcast.19), channel_id=1, source_target_pairs={{0,2},{1,3},{2,0},{3,1},{4,6},{5,7},{6,4},{7,5},{8,10},{9,11},{10,... | collective-permute-start | bytes 49160 | tf_op jit(solution)/shard_map/ppermute | solution.py:423
  105.2 4.8 %down.1 = (bf16[512,2048]{1,0:T(8,128)(2,1)}, f32[2,1,512]{2,1,0:T(1,128)}) custom-call(s32[1]{0:T(128)} %bitcast.13.q_ref, bf16[224,1024]{1,0:T(8,128)(2,1)} %bitcast.35, bf16[224,1024]{1,0:T(8,128)(2,1)} %bitcast.38, bf16[224,1024]{1,0:T(8,128)(2,1)} %copy-done.10, bf16[224,1024]{1,0:T(8,128)(2,1)} %copy-done.9, ...), custom_call_target="tpu_custom_call" | custom-call | flops 939524096 | tf_op jit(solution)/shard_map/down/pallas_call | solution.py:534
  109.9 1.9 %collective-permute-start.20 = (f32[8,512]{1,0:T(8,128)}, f32[8,512]{1,0:T(8,128)S(1)}, u32[]{:S(2)}, u32[]{:S(2)}) collective-permute-start(f32[8,512]{1,0:T(8,128)} %copy-done.14), channel_id=1, source_target_pairs={{0,4},{4,0},{8,12},{12,8},{16,20},{20,16},{24,28},{28,24},{1,5},{5... | collective-permute-start | bytes 49160 | tf_op jit(solution)/shard_map/ppermute | solution.py:423
  111.8 0.2 collective-permute-start.25
  112.1 1.3 add_bitcast_fusion
  113.4 0.5 collective-permute-done.20.b_ref
  113.9 0.7 copy-done.15
  114.6 0.6 shard_map.157.a_ref
  115.2 2.2 %collective-permute-start.21 = (f32[8,512]{1,0:T(8,128)}, f32[8,512]{1,0:T(8,128)}, u32[]{:S(2)}, u32[]{:S(2)}) collective-permute-start(f32[8,512]{1,0:T(8,128)} %shard_map.157.a_ref), channel_id=1, source_target_pairs={{0,8},{4,12},{8,0},{12,4},{16,24},{20,28},{24,16},{28,20},{1,9},{5... | collective-permute-start | bytes 49160 | tf_op jit(solution)/shard_map/ppermute | solution.py:423
  117.4 2.3 %shard_map.155.refs_0_ = bf16[128,512]{1,0:T(8,128)(2,1)} custom-call(bf16[8,64,512]{2,1,0:T(8,128)(2,1)} %all-to-all-done.1.got_hbm, bf16[512,128]{1,0:T(8,128)(2,1)} %copy-done.7, f32[8,128]{1,0:T(8,128)} %get-tuple-element.38.place_ref.place_hbm, f32[8,128]{1,0:T(8,128)} %get-tuple-element.58.aff_hbm, bf16[8,2048]{1,0:T(8,128)(2,1)} %bitcast.45), custom_call_target="tpu_custom_call" | custom-call | tf_op jit(solution)/shard_map/pallas_call | solution.py:378
  119.7 0.6 collective-permute-start.18
  120.3 0.8 add_add_fusion
  121.1 0.7 shard_map.158.a_ref
  121.8 2.1 %collective-permute-start.22 = (f32[8,512]{1,0:T(8,128)S(1)}, f32[8,512]{1,0:T(8,128)S(1)}, u32[]{:S(2)}, u32[]{:S(2)}) collective-permute-start(f32[8,512]{1,0:T(8,128)S(1)} %shard_map.158.a_ref), channel_id=1, source_target_pairs={{0,16},{4,20},{8,24},{12,28},{16,0},{20,4},{24,8},{28,12},{1,17},{... | collective-permute-start | bytes 49160 | tf_op jit(solution)/shard_map/ppermute | solution.py:423
  123.9 1.0 collective-permute-done.18.refs_2_
  124.9 0.6 fusion
  125.5 0.9 collective-permute-done.22.b_ref
  126.5 0.6 shard_map.159
  127.1 0.9 copy-done.8
  128.0 0.8 shard_map.156
  (46 shorter events, 0.2 us)
Async XLA Ops:
  25.1 12.9 %collective-permute-start.10 = (bf16[8,64,512]{2,1,0:T(8,128)(2,1)}, bf16[8,64,512]{2,1,0:T(8,128)(2,1)}, u32[]{:S(2)}, u32[]{:S(2)}) collective-permute-start(bf16[8,64,512]{2,1,0:T(8,128)(2,1)} %all_to_all.10.refs_0_.x_ref.refs_4_), channel_id=1, source_target_pairs={{0,2},{1,3},{2,0},{3,1},{4,6},{5,7},{6,4},{7,5},{8,10},{9,11},{10,... | collective-permute-start | bytes 1572872 | tf_op jit(solution)/shard_map/ppermute | solution.py:423
  29.5 11.4 %collective-permute-start.3 = (bf16[56,1024]{1,0:T(8,128)(2,1)}, bf16[56,1024]{1,0:T(8,128)(2,1)S(1)}, u32[]{:S(2)}, u32[]{:S(2)}) collective-permute-start(bf16[56,1024]{1,0:T(8,128)(2,1)} %get-tuple-element.43), channel_id=1, source_target_pairs={{0,16},{4,20},{8,24},{12,28},{16,0},{20,4},{24,8},{28,12},{1,17},{... | collective-permute-start | bytes 344072 | tf_op jit(solution)/shard_map/ppermute | solution.py:423
  30.6 38.2 %collective-permute-start.9 = (bf16[8,64,512]{2,1,0:T(8,128)(2,1)}, bf16[8,64,512]{2,1,0:T(8,128)(2,1)S(1)}, u32[]{:S(2)}, u32[]{:S(2)}) collective-permute-start(bf16[8,64,512]{2,1,0:T(8,128)(2,1)} %all_to_all.10.refs_0_.x_ref.refs_4_), channel_id=1, source_target_pairs={{0,1},{1,0},{2,3},{3,2},{4,5},{5,4},{6,7},{7,6},{8,9},{9,8},{10,11... | collective-permute-start | bytes 1572872 | tf_op jit(solution)/shard_map/ppermute | solution.py:423
  38.0 30.8 %collective-permute-start.11 = (bf16[8,64,512]{2,1,0:T(8,128)(2,1)}, bf16[8,64,512]{2,1,0:T(8,128)(2,1)S(1)}, u32[]{:S(2)}, u32[]{:S(2)}) collective-permute-start(bf16[8,64,512]{2,1,0:T(8,128)(2,1)} %collective-permute-done.10.refs_2_), channel_id=1, source_target_pairs={{0,1},{1,0},{2,3},{3,2},{4,5},{5,4},{6,7},{7,6},{8,9},{9,8},{10,11... | collective-permute-start | bytes 1572872 | tf_op jit(solution)/shard_map/ppermute | solution.py:423
  38.0 15.2 %collective-permute-start.4 = (bf16[56,1024]{1,0:T(8,128)(2,1)}, bf16[56,1024]{1,0:T(8,128)(2,1)S(1)}, u32[]{:S(2)}, u32[]{:S(2)}) collective-permute-start(bf16[56,1024]{1,0:T(8,128)(2,1)} %get-tuple-element.44), channel_id=1, source_target_pairs={{0,20},{4,16},{8,28},{12,24},{16,4},{20,0},{24,12},{28,8},{1,21},{... | collective-permute-start | bytes 344072 | tf_op jit(solution)/shard_map/ppermute | solution.py:423
  39.0 14.5 %collective-permute-start.5 = (bf16[56,1024]{1,0:T(8,128)(2,1)}, bf16[56,1024]{1,0:T(8,128)(2,1)S(1)}, u32[]{:S(2)}, u32[]{:S(2)}) collective-permute-start(bf16[56,1024]{1,0:T(8,128)(2,1)} %get-tuple-element.45), channel_id=1, source_target_pairs={{0,24},{4,28},{8,16},{12,20},{16,8},{20,12},{24,0},{28,4},{1,25},{... | collective-permute-start | bytes 344072 | tf_op jit(solution)/shard_map/ppermute | solution.py:423
  40.9 14.2 %collective-permute-start.6 = (bf16[56,1024]{1,0:T(8,128)(2,1)}, bf16[56,1024]{1,0:T(8,128)(2,1)S(1)}, u32[]{:S(2)}, u32[]{:S(2)}) collective-permute-start(bf16[56,1024]{1,0:T(8,128)(2,1)} %get-tuple-element.46), channel_id=1, source_target_pairs={{0,28},{4,24},{8,20},{12,16},{16,12},{20,8},{24,4},{28,0},{1,29},{... | collective-permute-start | bytes 344072 | tf_op jit(solution)/shard_map/ppermute | solution.py:423
  53.2 5.3 %collective-permute-start = (bf16[56,1024]{1,0:T(8,128)(2,1)}, bf16[56,1024]{1,0:T(8,128)(2,1)S(1)}, u32[]{:S(2)}, u32[]{:S(2)}) collective-permute-start(bf16[56,1024]{1,0:T(8,128)(2,1)} %get-tuple-element.40), channel_id=1, source_target_pairs={{0,4},{4,0},{8,12},{12,8},{16,20},{20,16},{24,28},{28,24},{1,5},{5... | collective-permute-start | bytes 344072 | tf_op jit(solution)/shard_map/ppermute | solution.py:423
  53.5 5.1 %collective-permute-start.1 = (bf16[56,1024]{1,0:T(8,128)(2,1)}, bf16[56,1024]{1,0:T(8,128)(2,1)S(1)}, u32[]{:S(2)}, u32[]{:S(2)}) collective-permute-start(bf16[56,1024]{1,0:T(8,128)(2,1)} %get-tuple-element.41), channel_id=1, source_target_pairs={{0,8},{4,12},{8,0},{12,4},{16,24},{20,28},{24,16},{28,20},{1,9},{5... | collective-permute-start | bytes 344072 | tf_op jit(solution)/shard_map/ppermute | solution.py:423
  55.0 7.1 %collective-permute-start.2 = (bf16[56,1024]{1,0:T(8,128)(2,1)}, bf16[56,1024]{1,0:T(8,128)(2,1)S(1)}, u32[]{:S(2)}, u32[]{:S(2)}) collective-permute-start(bf16[56,1024]{1,0:T(8,128)(2,1)} %get-tuple-element.42), channel_id=1, source_target_pairs={{0,12},{4,8},{8,4},{12,0},{16,28},{20,24},{24,20},{28,16},{1,13},{... | collective-permute-start | bytes 344072 | tf_op jit(solution)/shard_map/ppermute | solution.py:423
  58.5 7.9 %copy-start.6 = (bf16[4,56,1024]{2,1,0:T(8,128)(2,1)}, bf16[4,56,1024]{2,1,0:T(8,128)(2,1)S(1)}, u32[]{:S(2)}) copy-start(bf16[4,56,1024]{2,1,0:T(8,128)(2,1)S(1)} %shard_map.145) | copy-start | bytes 1376260
  58.5 14.5 %collective-permute-start.8 = (bf16[224,1024]{1,0:T(8,128)(2,1)S(1)}, bf16[224,1024]{1,0:T(8,128)(2,1)S(1)}, u32[]{:S(2)}, u32[]{:S(2)}) collective-permute-start(bf16[224,1024]{1,0:T(8,128)(2,1)S(1)} %bitcast.36), channel_id=1, source_target_pairs={{0,1},{1,0},{2,3},{3,2},{4,5},{5,4},{6,7},{7,6},{8,9},{9,8},{10,11... | collective-permute-start | bytes 1376264 | tf_op jit(solution)/shard_map/ppermute | solution.py:423
  62.2 1.6 %copy-start = (bf16[1,2048,512]{2,1,0:T(8,128)(2,1)S(1)}, bf16[1,2048,512]{2,1,0:T(8,128)(2,1)}, u32[]{:S(2)}) copy-start(bf16[1,2048,512]{2,1,0:T(8,128)(2,1)} %param.10) | copy-start | bytes 6291460
  63.7 1.6 %copy-start.2 = (bf16[1,2048,512]{2,1,0:T(8,128)(2,1)S(1)}, bf16[1,2048,512]{2,1,0:T(8,128)(2,1)}, u32[]{:S(2)}) copy-start(bf16[1,2048,512]{2,1,0:T(8,128)(2,1)} %param.11) | copy-start | bytes 6291460
  65.3 0.9 copy-start.12
  66.2 1.8 %copy-start.4 = (bf16[1,512,2048]{2,1,0:T(8,128)(2,1)S(1)}, bf16[1,512,2048]{2,1,0:T(8,128)(2,1)}, u32[]{:S(2)}) copy-start(bf16[1,512,2048]{2,1,0:T(8,128)(2,1)} %param.12) | copy-start | bytes 6291460
  66.2 2.6 %copy-start.3 = (bf16[1,2048,512]{2,1,0:T(8,128)(2,1)S(1)}, bf16[1,2048,512]{2,1,0:T(8,128)(2,1)}, u32[]{:S(2)}) copy-start(bf16[1,2048,512]{2,1,0:T(8,128)(2,1)} %param.11) | copy-start | bytes 6291460
  66.3 6.7 %copy-start.5 = (bf16[4,56,1024]{2,1,0:T(8,128)(2,1)}, bf16[4,56,1024]{2,1,0:T(8,128)(2,1)S(1)}, u32[]{:S(2)}) copy-start(bf16[4,56,1024]{2,1,0:T(8,128)(2,1)S(1)} %shard_map.144) | copy-start | bytes 1376260
  66.3 3.0 %copy-start.1 = (bf16[1,2048,512]{2,1,0:T(8,128)(2,1)S(1)}, bf16[1,2048,512]{2,1,0:T(8,128)(2,1)}, u32[]{:S(2)}) copy-start(bf16[1,2048,512]{2,1,0:T(8,128)(2,1)} %param.10) | copy-start | bytes 6291460
  66.3 6.7 %collective-permute-start.7 = (bf16[224,1024]{1,0:T(8,128)(2,1)S(1)}, bf16[224,1024]{1,0:T(8,128)(2,1)S(1)}, u32[]{:S(2)}, u32[]{:S(2)}) collective-permute-start(bf16[224,1024]{1,0:T(8,128)(2,1)S(1)} %bitcast.33), channel_id=1, source_target_pairs={{0,1},{1,0},{2,3},{3,2},{4,5},{5,4},{6,7},{7,6},{8,9},{9,8},{10,11... | collective-permute-start | bytes 1376264 | tf_op jit(solution)/shard_map/ppermute | solution.py:423
  73.0 2.1 %copy-start.11 = (bf16[8,56,512]{2,1,0:T(8,128)(2,1)}, bf16[8,56,512]{2,1,0:T(8,128)(2,1)S(1)}, u32[]{:S(2)}) copy-start(bf16[8,56,512]{2,1,0:T(8,128)(2,1)S(1)} %get-tuple-element.48) | copy-start | bytes 1376260
  73.0 2.1 %copy-start.9 = (bf16[224,1024]{1,0:T(8,128)(2,1)}, bf16[224,1024]{1,0:T(8,128)(2,1)S(1)}, u32[]{:S(2)}) copy-start(bf16[224,1024]{1,0:T(8,128)(2,1)S(1)} %collective-permute-done.8.far_ref.refs_3_) | copy-start | bytes 1376260
  73.0 2.1 %copy-start.10 = (bf16[224,1024]{1,0:T(8,128)(2,1)}, bf16[224,1024]{1,0:T(8,128)(2,1)S(1)}, u32[]{:S(2)}) copy-start(bf16[224,1024]{1,0:T(8,128)(2,1)S(1)} %collective-permute-done.7.near_ref.refs_2_) | copy-start | bytes 1376260
  75.1 1.9 %collective-permute-start.15 = (bf16[1,448,512]{2,1,0:T(8,128)(2,1)S(1)}, bf16[1,448,512]{2,1,0:T(8,128)(2,1)S(1)}, u32[]{:S(2)}, u32[]{:S(2)}) collective-permute-start(bf16[1,448,512]{2,1,0:T(8,128)(2,1)S(1)} %get-tuple-element.57), channel_id=1, source_target_pairs={{0,1},{1,0},{2,3},{3,2},{4,5},{5,4},{6,7},{7,6},{8,9},{9,8},{10,11... | collective-permute-start | bytes 1376264 | tf_op jit(solution)/shard_map/ppermute | solution.py:423
  75.2 16.8 %collective-permute-start.12 = (bf16[448,512]{1,0:T(8,128)(2,1)S(1)}, bf16[448,512]{1,0:T(8,128)(2,1)S(1)}, u32[]{:S(2)}, u32[]{:S(2)}) collective-permute-start(bf16[448,512]{1,0:T(8,128)(2,1)S(1)} %get-tuple-element.53), channel_id=1, source_target_pairs={{0,1},{1,0},{2,3},{3,2},{4,5},{5,4},{6,7},{7,6},{8,9},{9,8},{10,11... | collective-permute-start | bytes 1376264 | tf_op jit(solution)/shard_map/ppermute | solution.py:423
  77.1 20.2 %copy-start.13 = (f32[8,128]{1,0:T(8,128)S(1)}, f32[8,128]{1,0:T(8,128)}, u32[]{:S(2)}) copy-start(f32[8,128]{1,0:T(8,128)} %get-tuple-element.38.place_ref.place_hbm) | copy-start | bytes 12292
  77.1 14.9 %collective-permute-start.16 = (bf16[448,512]{1,0:T(8,128)(2,1)S(1)}, bf16[448,512]{1,0:T(8,128)(2,1)S(1)}, u32[]{:S(2)}, u32[]{:S(2)}) collective-permute-start(bf16[448,512]{1,0:T(8,128)(2,1)S(1)} %bitcast.41), channel_id=1, source_target_pairs={{0,2},{1,3},{2,0},{3,1},{4,6},{5,7},{6,4},{7,5},{8,10},{9,11},{10,... | collective-permute-start | bytes 1376264 | tf_op jit(solution)/shard_map/ppermute | solution.py:423
  78.7 1.2 collective-permute-start.13
  79.9 10.0 %collective-permute-start.14 = (f32[8,128]{1,0:T(8,128)S(1)}, f32[8,128]{1,0:T(8,128)S(1)}, u32[]{:S(2)}, u32[]{:S(2)}) collective-permute-start(f32[8,128]{1,0:T(8,128)S(1)} %shard_map.150.a_ref), channel_id=1, source_target_pairs={{0,2},{1,3},{2,0},{3,1},{4,6},{5,7},{6,4},{7,5},{8,10},{9,11},{10,... | collective-permute-start | bytes 12296 | tf_op jit(solution)/shard_map/ppermute | solution.py:423
  91.4 0.6 copy-start.14
  92.9 24.5 %all-to-all-start.1 = ((bf16[8,64,512]{2,1,0:T(8,128)(2,1)}), bf16[8,64,512]{2,1,0:T(8,128)(2,1)}, u32[]{:S(2)}, u32[]{:S(2)}) async-start(bf16[8,64,512]{2,1,0:T(8,128)(2,1)} %shard_map.153), calls=%async_computation.1 | async-start | bytes 1048576 | tf_op jit(solution)/shard_map/all_to_all | solution.py:426
  97.3 0.7 copy-start.7
  103.7 8.2 %collective-permute-start.24 = (f32[2,2048]{1,0:T(2,128)}, f32[2,2048]{1,0:T(2,128)}, u32[]{:S(2)}, u32[]{:S(2)}) collective-permute-start(f32[2,2048]{1,0:T(2,128)} %bitcast.19), channel_id=1, source_target_pairs={{0,2},{1,3},{2,0},{3,1},{4,6},{5,7},{6,4},{7,5},{8,10},{9,11},{10,... | collective-permute-start | bytes 49160 | tf_op jit(solution)/shard_map/ppermute | solution.py:423
  105.2 15.1 %collective-permute-start.23 = (f32[2,2048]{1,0:T(2,128)}, f32[2,2048]{1,0:T(2,128)}, u32[]{:S(2)}, u32[]{:S(2)}) collective-permute-start(f32[2,2048]{1,0:T(2,128)} %bitcast.19), channel_id=1, source_target_pairs={{0,1},{1,0},{2,3},{3,2},{4,5},{5,4},{6,7},{7,6},{8,9},{9,8},{10,11... | collective-permute-start | bytes 49160 | tf_op jit(solution)/shard_map/ppermute | solution.py:423
  109.9 3.9 %collective-permute-start.20 = (f32[8,512]{1,0:T(8,128)}, f32[8,512]{1,0:T(8,128)S(1)}, u32[]{:S(2)}, u32[]{:S(2)}) collective-permute-start(f32[8,512]{1,0:T(8,128)} %copy-done.14), channel_id=1, source_target_pairs={{0,4},{4,0},{8,12},{12,8},{16,20},{20,16},{24,28},{28,24},{1,5},{5... | collective-permute-start | bytes 49160 | tf_op jit(solution)/shard_map/ppermute | solution.py:423
  111.8 8.4 %collective-permute-start.25 = (f32[2,2048]{1,0:T(2,128)}, f32[2,2048]{1,0:T(2,128)}, u32[]{:S(2)}, u32[]{:S(2)}) collective-permute-start(f32[2,2048]{1,0:T(2,128)} %collective-permute-done.24), channel_id=1, source_target_pairs={{0,1},{1,0},{2,3},{3,2},{4,5},{5,4},{6,7},{7,6},{8,9},{9,8},{10,11... | collective-permute-start | bytes 49160 | tf_op jit(solution)/shard_map/ppermute | solution.py:423
  113.9 0.7 copy-start.15
  115.2 5.9 %collective-permute-start.21 = (f32[8,512]{1,0:T(8,128)}, f32[8,512]{1,0:T(8,128)}, u32[]{:S(2)}, u32[]{:S(2)}) collective-permute-start(f32[8,512]{1,0:T(8,128)} %shard_map.157.a_ref), channel_id=1, source_target_pairs={{0,8},{4,12},{8,0},{12,4},{16,24},{20,28},{24,16},{28,20},{1,9},{5... | collective-permute-start | bytes 49160 | tf_op jit(solution)/shard_map/ppermute | solution.py:423
  119.7 5.2 %collective-permute-start.18 = (bf16[128,512]{1,0:T(8,128)(2,1)}, bf16[128,512]{1,0:T(8,128)(2,1)S(1)}, u32[]{:S(2)}, u32[]{:S(2)}) collective-permute-start(bf16[128,512]{1,0:T(8,128)(2,1)} %shard_map.155.refs_0_), channel_id=1, source_target_pairs={{0,2},{1,3},{2,0},{3,1},{4,6},{5,7},{6,4},{7,5},{8,10},{9,11},{10,... | collective-permute-start | bytes 393224 | tf_op jit(solution)/shard_map/ppermute | solution.py:423
  121.8 4.6 %collective-permute-start.22 = (f32[8,512]{1,0:T(8,128)S(1)}, f32[8,512]{1,0:T(8,128)S(1)}, u32[]{:S(2)}, u32[]{:S(2)}) collective-permute-start(f32[8,512]{1,0:T(8,128)S(1)} %shard_map.158.a_ref), channel_id=1, source_target_pairs={{0,16},{4,20},{8,24},{12,28},{16,0},{20,4},{24,8},{28,12},{1,17},{... | collective-permute-start | bytes 49160 | tf_op jit(solution)/shard_map/ppermute | solution.py:423
  123.9 3.2 %collective-permute-start.17 = (bf16[128,512]{1,0:T(8,128)(2,1)}, bf16[128,512]{1,0:T(8,128)(2,1)S(1)}, u32[]{:S(2)}, u32[]{:S(2)}) collective-permute-start(bf16[128,512]{1,0:T(8,128)(2,1)} %shard_map.155.refs_0_), channel_id=1, source_target_pairs={{0,1},{1,0},{2,3},{3,2},{4,5},{5,4},{6,7},{7,6},{8,9},{9,8},{10,11... | collective-permute-start | bytes 393224 | tf_op jit(solution)/shard_map/ppermute | solution.py:423
  124.9 2.2 %collective-permute-start.19 = (bf16[128,512]{1,0:T(8,128)(2,1)S(1)}, bf16[128,512]{1,0:T(8,128)(2,1)S(1)}, u32[]{:S(2)}, u32[]{:S(2)}) collective-permute-start(bf16[128,512]{1,0:T(8,128)(2,1)S(1)} %collective-permute-done.18.refs_2_), channel_id=1, source_target_pairs={{0,1},{1,0},{2,3},{3,2},{4,5},{5,4},{6,7},{7,6},{8,9},{9,8},{10,11... | collective-permute-start | bytes 393224 | tf_op jit(solution)/shard_map/ppermute | solution.py:423
  127.1 0.9 copy-start.8

commit v4 on v3

--- a/solution.py
+++ b/solution.py
@@ -21,6 +21,7 @@
 
 ALONE = 67043328
 SHARED = 16 * 1024 * 1024
+GRADS_ROOM = 4500000
 COEF_LANE = 64
 
 
@@ -126,23 +127,40 @@
         out_ref[place ^ k] = refs[k][...]
 
 
-def gate_up_kernel(slots, shares, *refs):
-    x_refs = refs[:shares]
-    wg_ref, wu_ref, hid_ref, up_ref, gate_ref, acc_g, acc_u = refs[shares:]
+def add_parts(tokens_of, x_refs, wg_ref, wu_ref, acc_g, acc_u, fresh):
     groups, span, cols = x_refs[0].shape
-    for r in range(shares):
-        x = x_refs[r][...].reshape(groups * span, cols)
+    for r, x_ref in zip(tokens_of, x_refs):
+        x = x_ref[...].reshape(groups * span, cols)
         rows = pl.ds(pl.multiple_of((lax.axis_index("tp") ^ r) * cols, 128), cols)
         part_g = dot(x, wg_ref[rows, :])
         part_u = dot(x, wu_ref[rows, :])
-        if r == 0:
-            acc_g[...] = part_g
-            acc_u[...] = part_u
-        else:
-            acc_g[...] += part_g
-            acc_u[...] += part_u
+        acc_g[...] = part_g if fresh else acc_g[...] + part_g
+        acc_u[...] = part_u if fresh else acc_u[...] + part_u
+        fresh = False
+
+
+def first_parts_kernel(which, *refs):
+    count = len(which)
+    add_parts(which, refs[:count], *refs[count:], True)
+
+
+def more_parts_kernel(which, got_g, got_u, *refs):
+    count = len(which)
+    acc_g, acc_u = refs[-2:]
+    acc_g[...] = got_g[...]
+    acc_u[...] = got_u[...]
+    add_parts(which, refs[:count], *refs[count:], False)
+
+
+def gate_up_kernel(slots, which, got_g, got_u, own_ref, *refs):
+    count = len(which)
+    wg_ref, wu_ref, hid_ref, up_ref, gate_ref, acc_g, acc_u = refs[count:]
+    groups, span, _ = own_ref.shape
+    acc_g[...] = got_g[...]
+    acc_u[...] = got_u[...]
+    add_parts(which, refs[:count], wg_ref, wu_ref, acc_g, acc_u, False)
     for e in range(groups):
-        scale = scale_column(x_refs[0], e, slots)
+        scale = scale_column(own_ref, e, slots)
         at = slice(e * span, e * span + slots)
         pre_gate = acc_g[at, :]
         pre_up = acc_u[at, :]
@@ -281,7 +299,10 @@
                 weighted = (scale * z_ref[...].astype(F32)).astype(BF16)
                 down = down + dot(hid_ref[at], weighted, 0, 0)
             down_out[...] = down.astype(BF16)
-            rows_out[0] = square_rows(down)
+            if h == 0:
+                rows_out[...] = square_rows(down)
+            else:
+                rows_out[...] += square_rows(down)
 
 
 def add_kernel(a_ref, b_ref, out_ref):
@@ -327,8 +348,8 @@
 
 
 def home_kernel(
-    slots, got_hbm, hot_hbm, place_hbm, aff_hbm, router_hbm, token_out,
-    got_ref, hot_ref, place_ref, aff_ref, router_ref, sems,
+    slots, got_hbm, hot_hbm, place_hbm, aff_hbm, router_hbm, token_out, whole_hbm,
+    got_ref, hot_ref, place_ref, aff_ref, router_ref, own_ref, sems,
 ):
     experts, span, cols = got_ref.shape
     toks = place_ref.shape[1]
@@ -357,15 +378,18 @@
     weights = chosen / total_aff
     d_chosen = (term - jnp.sum(term * weights, axis=0, keepdims=True)) / total_aff
     d_logit = named * d_chosen * aff * (1.0 - aff)
-    token_out[...] = (back + dot(d_logit.T.astype(BF16), router_ref[...])).astype(BF16)
+    own_ref[...] = (back + dot(d_logit.T.astype(BF16), router_ref[...])).astype(BF16)
+    copies = fetch(sems, (own_ref, token_out), (own_ref, whole_hbm.at[:, pl.ds(start, cols)]))
+    for copy in copies:
+        copy.wait()
 
 
 def assemble_kernel(*refs):
     out_hbm, sems = refs[-2:]
     pairs = []
-    for r, ref in enumerate(refs[:-2]):
+    for r, ref in enumerate(refs[1:-2]):
         cols = ref.shape[1]
-        start = pl.multiple_of((lax.axis_index("tp") ^ r) * cols, 128)
+        start = pl.multiple_of((lax.axis_index("tp") ^ (r + 1)) * cols, 128)
         pairs.append((ref, out_hbm.at[:, pl.ds(start, cols)]))
     for copy in fetch(sems, *pairs):
         copy.wait()
@@ -448,10 +472,20 @@
     hot = call(functools.partial(slot_map_kernel, span), shape(groups * span, toks), False, place)
 
     x_parts = spread(rows_got)
+    sums = tuple(shape(groups * span, hidden, dtype=F32) for _ in range(2))
+    chip_parts, core_parts = list(range(2, shares, 2)), list(range(3, shares, 2))
+    pre = call(
+        functools.partial(first_parts_kernel, (0, 1)), sums,
+        False, *x_parts[:2], wg, wu, flops=unit,
+    )
+    pre = call(
+        functools.partial(more_parts_kernel, chip_parts), sums,
+        False, *pre, *[x_parts[r] for r in chip_parts], wg, wu, flops=unit,
+    )
     hid, up_factor, gate_factor = call(
-        functools.partial(gate_up_kernel, slots, shares),
+        functools.partial(gate_up_kernel, slots, core_parts),
         (shape(groups, slots, hidden), shape(groups, slots, hidden, dtype=F32), shape(groups, slots, hidden, dtype=F32)),
-        False, *x_parts, wg, wu, flops=4 * unit,
+        False, *pre, x_parts[0], *[x_parts[r] for r in core_parts], wg, wu, flops=2 * unit,
         scratch=[pltpu.VMEM((groups * span, hidden), F32)] * 2,
     )
     hid = hid.reshape(count, hidden)
@@ -459,9 +493,13 @@
     gate_factor = gate_factor.reshape(count, hidden)
 
     side = groups // 2
-    near = call(join_kernel, shape(side, slots, half), False, *pieces[:side], wg, wu).reshape(count // 2, half)
+    near = call(
+        join_kernel, shape(side, slots, half), False, *pieces[:side],
+    ).reshape(count // 2, half)
     near_got = swap(near, 1)
-    far = call(join_kernel, shape(side, slots, half), False, *pieces[side:]).reshape(count // 2, half)
+    far = call(
+        join_kernel, shape(side, slots, half), False, *pieces[side:],
+    ).reshape(count // 2, half)
     far_got = swap(far, 1)
     back = call(
         functools.partial(back_kernel, groups), shape(2, count // 2, hidden, dtype=F32),
@@ -514,7 +552,9 @@
         False, router_sum, router_got,
     )
     router_rows = router_rows.reshape(cols)
-    home_send = call(add_chip_kernel, shape(groups, span, cols), False, even_home, core_home, tiles, *chip_got)
+    home_send = call(
+        add_chip_kernel, shape(groups, span, cols), False, even_home, core_home, tiles, *chip_got,
+    )
     home_got = exchange(home_send)
 
     grad_spec = pl.BlockSpec((cols, hidden), lambda r, q: (q[0] ^ r, 0))
@@ -527,20 +567,20 @@
             in_specs=[VMEM] * (shares + 1),
             out_specs=(grad_spec, grad_spec, pl.BlockSpec((1, 2, cols), lambda r, q: (q[0] ^ r, 0, 0))),
         ),
-        compiler_params=params(),
+        compiler_params=params(ALONE - GRADS_ROOM),
         cost_estimate=cost(4 * unit, 0),
         name="grads",
     )(q, *x_parts, g)
-    down_grad, down_norms = pl.pallas_call(
+    down_grad, down_rows = pl.pallas_call(
         functools.partial(down_kernel, slots),
-        out_shape=(shape(hidden, width), shape(2, 1, hidden, dtype=F32)),
+        out_shape=(shape(hidden, width), shape(1, hidden, dtype=F32)),
         grid_spec=pltpu.PrefetchScalarGridSpec(
             num_scalar_prefetch=1,
             grid=(2,),
             in_specs=[VMEM] * 6,
             out_specs=(
                 pl.BlockSpec((hidden, half), lambda h, q: (0, (q[0] % 2) ^ h)),
-                pl.BlockSpec((1, 1, hidden), lambda h, q: (h, 0, 0)),
+                pl.BlockSpec((1, hidden), lambda h, q: (0, 0)),
             ),
         ),
         compiler_params=params(ALONE),
@@ -552,23 +592,31 @@
     while len(norms) > 1:
         norms = [a + b for a, b in zip(norms[::2], norms[1::2])]
     norms = norms[0]
-    down_rows = (down_norms[0] + down_norms[1]).reshape(1, hidden)
-
-    token_part = call(
-        functools.partial(home_kernel, slots), shape(toks, cols),
-        False, home_got, hot, place, aff, router, hbm=range(5), limit=ALONE,
+
+    token_part, token_grad = call(
+        functools.partial(home_kernel, slots), (shape(toks, cols), shape(toks, width)),
+        False, home_got, hot, place, aff, router, hbm=range(5), limit=ALONE, out_hbm=True,
         scratch=[
             buffer(groups, span, cols),
             buffer(groups * span, toks),
             buffer(experts, toks, dtype=F32),
             buffer(experts, toks, dtype=F32),
             buffer(experts, cols),
+            buffer(toks, cols),
             DMAS((5,)),
         ],
     )
-    token_grad = call(
-        assemble_kernel, shape(toks, width), False, *spread(token_part), out_hbm=True, scratch=[DMAS((shares,))],
-    )
+    token_parts = spread(token_part)[1:]
+    token_grad = pl.pallas_call(
+        assemble_kernel,
+        out_shape=shape(toks, width),
+        in_specs=[HBM] + [VMEM] * (shares - 1),
+        out_specs=HBM,
+        scratch_shapes=[DMAS((shares - 1,))],
+        input_output_aliases={0: 0},
+        compiler_params=params(),
+        name="assemble",
+    )(token_grad, *token_parts)
     return (
         token_grad,
         router_sum.T,

time: 130 us -> 121 us (0.931)
  waiting for transfers between devices: 33.1 us -> 27.2 us
  local copies, waits for them, and re-layouts: 9.62 us -> 4.23 us
  Pallas kernels: 31.4 us -> 36 us
    ppermute x26, waiting for transfers between devices: 33.1 us -> 27.2 us  [swap(): return lax.ppermute(value, axis, [(i, i ^ bit) for i in range(size)])]
    unnamed x32 -> x30, local copies, waits for them, and re-layouts: 9 us -> 3.62 us
    pallas_call x18 -> x19, Pallas kernels: 21 us -> 24.1 us  [call(): pl.pallas_call(kernel, out_shape=outs, in_specs=([SMEM] if scalar else []...]
  transfers between devices with their start and end apart: 27 -> 27, of which waited for: 8 -> 9; matrix products, arithmetic and copies ran while one was open for 2% -> 1% of each run, Pallas kernels for 19% -> 25%
where the time goes in v4:
time: 121 us; the launch traced here: 120 us
  Pallas kernels  36 us (30%)
  starting transfers between devices  29 us (24%)
  waiting for transfers between devices  27.2 us (22%)
  blocking collectives  21.9 us (18%)
  local copies, waits for them, and re-layouts  4.23 us (3%)
    ppermute x26, waiting for transfers between devices, swap(): return lax.ppermute(value, axis, [(i, i ^ bit) for i in range(size)])  27.2 us
    ppermute x26, starting transfers between devices, swap(): return lax.ppermute(value, axis, [(i, i ^ bit) for i in range(size)])  24.4 us
    pallas_call x19, Pallas kernels, call(): pl.pallas_call(kernel, out_shape=outs, in_specs=([SMEM] if scalar else []...  24.1 us
    all_to_all x1, blocking collectives, exchange(): return lax.all_to_all(value, 'ep', split_axis=0, concat_axis=0, tiled=True)  21.9 us
    pallas_call x1, Pallas kernels, layer(): pl.pallas_call(functools.partial(grads_kernel, shares), out_shape=(shape(...  6.37 us
    pallas_call x1, Pallas kernels, layer(): pl.pallas_call(functools.partial(down_kernel, slots), out_shape=(shape(hi...  4.71 us
    all_to_all x1, starting transfers between devices, exchange(): return lax.all_to_all(value, 'ep', split_axis=0, concat_axis=0, tiled=True)  4.58 us
    unnamed x30, local copies, waits for them, and re-layouts  3.62 us
  transfers between devices with their start and end apart: 27, of which 9 were waited for; matrix products, arithmetic and copies ran while one was open for 1% of the time, Pallas kernels for 25%

profile of v4, /device:TPU:0, one launch (start us, length us, event | category | flops | bytes accessed | tf_op | source)
XLA Modules:
  0.0 120.3 jit_solution(9374124800957359321)
XLA Ops:
  0.6 2.6 %shard_map.142 = (bf16[8,64,512]{2,1,0:T(8,128)(2,1)}, f32[8,128]{1,0:T(8,128)}, f32[8,128]{1,0:T(8,128)}) custom-call(bf16[128,2048]{1,0:T(8,128)(2,1)} %tok_hbm.1, s32[2,128]{1,0:T(2,128)} %bitcast.49, bf16[8,2048]{1,0:T(8,128)(2,1)} %bitcast.44), custom_call_target="tpu_custom_call" | custom-call | tf_op jit(solution)/shard_map/pallas_call | solution.py:402
  3.2 21.9 %all_to_all.10.refs_0_.own_ref.x_ref.refs_4_ = bf16[8,64,512]{2,1,0:T(8,128)(2,1)} all-to-all(bf16[8,64,512]{2,1,0:T(8,128)(2,1)} %get-tuple-element.53), channel_id=1, replica_groups=mesh['ep'=8,'tp'=4] {'ep'}, dimensions={0} | all-to-all | bytes 1048576 | tf_op jit(solution)/shard_map/all_to_all | solution.py:450
  25.1 1.5 %collective-permute-start.10 = (bf16[8,64,512]{2,1,0:T(8,128)(2,1)}, bf16[8,64,512]{2,1,0:T(8,128)(2,1)}, u32[]{:S(2)}, u32[]{:S(2)}) collective-permute-start(bf16[8,64,512]{2,1,0:T(8,128)(2,1)} %all_to_all.10.refs_0_.own_ref.x_ref.refs_4_), channel_id=1, source_target_pairs={{0,2},{1,3},{2,0},{3,1},{4,6},{5,7},{6,4},{7,5},{8,10},{9,11},{10,... | collective-permute-start | bytes 1572872 | tf_op jit(solution)/shard_map/ppermute | solution.py:447
  26.6 2.8 %shard_map.143 = (bf16[56,1024]{1,0:T(8,128)(2,1)}, bf16[56,1024]{1,0:T(8,128)(2,1)}, bf16[56,1024]{1,0:T(8,128)(2,1)}, bf16[56,1024]{1,0:T(8,128)(2,1)}, bf16[5...) custom-call(bf16[128,2048]{1,0:T(8,128)(2,1)} %cot_hbm.1, ...), custom_call_target="tpu_custom_call" | custom-call | flops 117440512 | tf_op jit(solution)/shard_map/pallas_call | solution.py:402
  29.5 1.1 collective-permute-start.3
  30.6 2.7 %collective-permute-start.4 = (bf16[56,1024]{1,0:T(8,128)(2,1)}, bf16[56,1024]{1,0:T(8,128)(2,1)S(1)}, u32[]{:S(2)}, u32[]{:S(2)}) collective-permute-start(bf16[56,1024]{1,0:T(8,128)(2,1)} %get-tuple-element.50), channel_id=1, source_target_pairs={{0,20},{4,16},{8,28},{12,24},{16,4},{20,0},{24,12},{28,8},{1,21},{... | collective-permute-start | bytes 344072 | tf_op jit(solution)/shard_map/ppermute | solution.py:447
  33.4 1.5 %collective-permute-start.5 = (bf16[56,1024]{1,0:T(8,128)(2,1)}, bf16[56,1024]{1,0:T(8,128)(2,1)S(1)}, u32[]{:S(2)}, u32[]{:S(2)}) collective-permute-start(bf16[56,1024]{1,0:T(8,128)(2,1)} %get-tuple-element.51), channel_id=1, source_target_pairs={{0,24},{4,28},{8,16},{12,20},{16,8},{20,12},{24,0},{28,4},{1,25},{... | collective-permute-start | bytes 344072 | tf_op jit(solution)/shard_map/ppermute | solution.py:447
  34.8 7.5 %collective-permute-done.3.refs_0_ = bf16[56,1024]{1,0:T(8,128)(2,1)S(1)} collective-permute-done((bf16[56,1024]{1,0:T(8,128)(2,1)}, bf16[56,1024]{1,0:T(8,128)(2,1)S(1)}, u32[]{:S(2)}, u32[]{:S(2)}) %collective-permute-start.3) | collective-permute-done | bytes 114720 | tf_op jit(solution)/shard_map/ppermute | solution.py:447
  42.3 1.9 %collective-permute-start.6 = (bf16[56,1024]{1,0:T(8,128)(2,1)}, bf16[56,1024]{1,0:T(8,128)(2,1)S(1)}, u32[]{:S(2)}, u32[]{:S(2)}) collective-permute-start(bf16[56,1024]{1,0:T(8,128)(2,1)} %get-tuple-element.52), channel_id=1, source_target_pairs={{0,28},{4,24},{8,20},{12,16},{16,12},{20,8},{24,4},{28,0},{1,29},{... | collective-permute-start | bytes 344072 | tf_op jit(solution)/shard_map/ppermute | solution.py:447
  44.2 0.0 collective-permute-done.10.refs_0_.refs_2_
  44.2 0.0 collective-permute-start.11
  44.2 2.6 %collective-permute-done.4.refs_1_ = bf16[56,1024]{1,0:T(8,128)(2,1)S(1)} collective-permute-done((bf16[56,1024]{1,0:T(8,128)(2,1)}, bf16[56,1024]{1,0:T(8,128)(2,1)S(1)}, u32[]{:S(2)}, u32[]{:S(2)}) %collective-permute-start.4) | collective-permute-done | bytes 114720 | tf_op jit(solution)/shard_map/ppermute | solution.py:447
  46.8 0.0 collective-permute-start
  46.8 2.3 %collective-permute-start.1 = (bf16[56,1024]{1,0:T(8,128)(2,1)}, bf16[56,1024]{1,0:T(8,128)(2,1)S(1)}, u32[]{:S(2)}, u32[]{:S(2)}) collective-permute-start(bf16[56,1024]{1,0:T(8,128)(2,1)} %get-tuple-element.47), channel_id=1, source_target_pairs={{0,8},{4,12},{8,0},{12,4},{16,24},{20,28},{24,16},{28,20},{1,9},{5... | collective-permute-start | bytes 344072 | tf_op jit(solution)/shard_map/ppermute | solution.py:447
  49.1 1.2 collective-permute-done.6.refs_3_
  50.2 2.3 %collective-permute-start.2 = (bf16[56,1024]{1,0:T(8,128)(2,1)}, bf16[56,1024]{1,0:T(8,128)(2,1)S(1)}, u32[]{:S(2)}, u32[]{:S(2)}) collective-permute-start(bf16[56,1024]{1,0:T(8,128)(2,1)} %get-tuple-element.48), channel_id=1, source_target_pairs={{0,12},{4,8},{8,4},{12,0},{16,28},{20,24},{24,20},{28,16},{1,13},{... | collective-permute-start | bytes 344072 | tf_op jit(solution)/shard_map/ppermute | solution.py:447
  52.6 0.0 collective-permute-done.refs_1_
  52.6 0.1 collective-permute-start.8
  52.7 1.1 collective-permute-done.1.refs_2_
  53.8 2.3 %collective-permute-done.2.refs_3_ = bf16[56,1024]{1,0:T(8,128)(2,1)S(1)} collective-permute-done((bf16[56,1024]{1,0:T(8,128)(2,1)}, bf16[56,1024]{1,0:T(8,128)(2,1)S(1)}, u32[]{:S(2)}, u32[]{:S(2)}) %collective-permute-start.2) | collective-permute-done | bytes 114720 | tf_op jit(solution)/shard_map/ppermute | solution.py:447
  56.1 0.9 copy-done.13
  57.1 0.0 copy-start
  57.1 0.1 collective-permute-start.7
  57.2 0.0 copy-start.2
  57.2 1.8 %copy-done.2 = bf16[1,512,2048]{2,1,0:T(8,128)(2,1)S(1)} copy-done((bf16[1,512,2048]{2,1,0:T(8,128)(2,1)S(1)}, bf16[1,512,2048]{2,1,0:T(8,128)(2,1)}, u32[]{:S(2)}) %copy-start.2) | copy-done | bytes 2097176
  59.0 0.8 shard_map.146.back_ref
  59.8 0.2 copy-done
  60.0 2.3 %shard_map.147 = (f32[512,512]{1,0:T(8,128)S(1)}, f32[512,512]{1,0:T(8,128)S(1)}) custom-call(bf16[8,64,512]{2,1,0:T(8,128)(2,1)} %all_to_all.10.refs_0_.own_ref.x_ref.refs_4_, bf16[8,64,512]{2,1,0:T(8,128)(2,1)S(1)} %collective-permute-done.9.refs_1_, bf16[2048,512]{1,0:T(8,128)(2,1)S(1)} %bitcast.21, bf16[2048,512]{1,0:T(8,128)(2,1)S(1)} %bitcast.26), custom_call_target="tpu_custom_call" | custom-call | flops 469762048 | tf_op jit(solution)/shard_map/pallas_call | solution.py:402
  62.3 1.8 %shard_map.148 = (f32[512,512]{1,0:T(8,128)S(1)}, f32[512,512]{1,0:T(8,128)S(1)}) custom-call(f32[512,512]{1,0:T(8,128)S(1)} %get-tuple-element.54.got_g, f32[512,512]{1,0:T(8,128)S(1)} %get-tuple-element.55.got_u, bf16[8,64,512]{2,1,0:T(8,128)(2,1)} %collective-permute-done.10.refs_0_.refs_2_, bf16[2048,512]{1,0:T(8,128)(2,1)S(1)} %bitcast.22, ...), custom_call_target="tpu_custom_call" | custom-call | flops 469762048 | tf_op jit(solution)/shard_map/pallas_call | solution.py:402
  64.1 0.0 copy-start.3
  64.1 2.2 %shard_map.149 = (bf16[8,56,512]{2,1,0:T(8,128)(2,1)S(1)}, f32[8,56,512]{2,1,0:T(8,128)S(1)}, f32[8,56,512]{2,1,0:T(8,128)S(1)}) custom-call(f32[512,512]{1,0:T(8,128)S(1)} %get-tuple-element.56.got_g, f32[512,512]{1,0:T(8,128)S(1)} %get-tuple-element.57.got_u, bf16[8,64,512]{2,1,0:T(8,128)(2,1)} %all_to_all.10.refs_0_.own_ref.x_ref.refs_4_, ...), custom_call_target="tpu_custom_call" | custom-call | flops 939524096 | tf_op jit(solution)/shard_map/pallas_call | solution.py:402
  66.4 2.1 %shard_map.150 = (bf16[8,64,1024]{2,1,0:T(8,128)(2,1)S(1)}, bf16[448,512]{1,0:T(8,128)(2,1)S(1)}, bf16[1,448,512]{2,1,0:T(8,128)(2,1)S(1)}, f32[8,128]{1,0:T(8,128)S(1)}) custom-call(f32[2,224,512]{2,1,0:T(8,128)S(1)} %shard_map.146.back_ref, bf16[224,1024]{1,0:T(8,128)(2,1)S(1)} %collective-permute-done.7.near_ref.refs_2_, ...), custom_call_target="tpu_custom_call" | custom-call | flops 1409286144 | tf_op jit(solution)/shard_map/pallas_call | solution.py:402
  68.5 0.0 copy-start.6
  68.5 0.3 collective-permute-start.15
  68.9 0.3 collective-permute-start.12
  69.1 1.3 %shard_map.151 = (f32[448,512]{1,0:T(8,128)S(1)}, f32[1,448,512]{2,1,0:T(8,128)S(1)}) custom-call(bf16[8,64,1024]{2,1,0:T(8,128)(2,1)S(1)} %get-tuple-element.61.g_ref.refs_4_, bf16[2048,512]{1,0:T(8,128)(2,1)S(1)} %bitcast.25, bf16[2048,512]{1,0:T(8,128)(2,1)S(1)} %bitcast.30), custom_call_target="tpu_custom_call" | custom-call | flops 939524096 | tf_op jit(solution)/shard_map/pallas_call | solution.py:402
  70.4 0.0 collective-permute-done.15.got_ref
  70.4 0.1 shard_map.154
  70.6 0.6 collective-permute-start.16
  71.1 1.2 collective-permute-done.13.b_ref
  72.3 1.5 %collective-permute-start.14 = (f32[8,128]{1,0:T(8,128)S(1)}, f32[8,128]{1,0:T(8,128)S(1)}, u32[]{:S(2)}, u32[]{:S(2)}) collective-permute-start(f32[8,128]{1,0:T(8,128)S(1)} %shard_map.152.a_ref), channel_id=1, source_target_pairs={{0,2},{1,3},{2,0},{3,1},{4,6},{5,7},{6,4},{7,5},{8,10},{9,11},{10,... | collective-permute-start | bytes 12296 | tf_op jit(solution)/shard_map/ppermute | solution.py:447
  73.8 9.6 %collective-permute-done.14.b_ref = f32[8,128]{1,0:T(8,128)S(1)} collective-permute-done((f32[8,128]{1,0:T(8,128)S(1)}, f32[8,128]{1,0:T(8,128)S(1)}, u32[]{:S(2)}, u32[]{:S(2)}) %collective-permute-start.14) | collective-permute-done | bytes 4128 | tf_op jit(solution)/shard_map/ppermute | solution.py:447
  83.4 2.1 %shard_map.153 = (f32[8,8,512]{2,1,0:T(8,128)S(1)}, f32[8,512]{1,0:T(8,128)}) custom-call(f32[8,128]{1,0:T(8,128)S(1)} %shard_map.152.a_ref, f32[8,128]{1,0:T(8,128)S(1)} %collective-permute-done.14.b_ref, bf16[8,64,512]{2,1,0:T(8,128)(2,1)} %all_to_all.10.refs_0_.own_ref.x_ref.refs_4_), custom_call_target="tpu_custom_call" | custom-call | tf_op jit(solution)/shard_map/pallas_call | solution.py:402
  85.5 1.0 shard_map.155
  86.5 4.6 %all-to-all-start.1 = ((bf16[8,64,512]{2,1,0:T(8,128)(2,1)}), bf16[8,64,512]{2,1,0:T(8,128)(2,1)}, u32[]{:S(2)}, u32[]{:S(2)}) async-start(bf16[8,64,512]{2,1,0:T(8,128)(2,1)} %shard_map.155), calls=%async_computation.1 | async-start | bytes 1048576 | tf_op jit(solution)/shard_map/all_to_all | solution.py:450
  91.1 6.4 %grads.1 = (bf16[2048,512]{1,0:T(8,128)(2,1)}, bf16[2048,512]{1,0:T(8,128)(2,1)}, f32[4,2,512]{2,1,0:T(2,128)}) custom-call(s32[1]{0:T(128)} %bitcast.13.q_ref, bf16[8,64,512]{2,1,0:T(8,128)(2,1)} %all_to_all.10.refs_0_.own_ref.x_ref.refs_4_, bf16[8,64,512]{2,1,0:T(8,128)(2,1)} %copy-done.8, bf16[8,64,512]{2,1,0:T(8,128)(2,1)} %collective-permute-done.10.refs_0_.refs_2_, ...), custom_call_target="tpu_custom_call" | custom-call | flops 1879048192 | tf_op jit(solution)/shard_map/grads/pallas_call | solution.py:561
  97.4 0.5 collective-permute-start.24
  98.0 0.6 copy-done.9
  98.6 2.8 %collective-permute-start.20 = (f32[8,512]{1,0:T(8,128)}, f32[8,512]{1,0:T(8,128)}, u32[]{:S(2)}, u32[]{:S(2)}) collective-permute-start(f32[8,512]{1,0:T(8,128)} %get-tuple-element.71.a_ref), channel_id=1, source_target_pairs={{0,4},{4,0},{8,12},{12,8},{16,20},{20,16},{24,28},{28,24},{1,5},{5... | collective-permute-start | bytes 49160 | tf_op jit(solution)/shard_map/ppermute | solution.py:447
  101.5 0.0 collective-permute-done.24
  101.5 0.2 collective-permute-start.25
  101.7 4.7 %down.1 = (bf16[512,2048]{1,0:T(8,128)(2,1)}, f32[1,512]{1,0:T(1,128)}) custom-call(s32[1]{0:T(128)} %bitcast.13.q_ref, bf16[224,1024]{1,0:T(8,128)(2,1)} %bitcast.38, bf16[224,1024]{1,0:T(8,128)(2,1)} %bitcast.35, bf16[224,1024]{1,0:T(8,128)(2,1)} %copy-done.11, bf16[224,1024]{1,0:T(8,128)(2,1)} %copy-done.10, ...), custom_call_target="tpu_custom_call" | custom-call | flops 939524096 | tf_op jit(solution)/shard_map/down/pallas_call | solution.py:574
  106.4 1.3 %shard_map.158.a_ref = f32[8,512]{1,0:T(8,128)} custom-call(f32[8,512]{1,0:T(8,128)} %get-tuple-element.71.a_ref, f32[8,512]{1,0:T(8,128)} %collective-permute-done.20.b_ref), custom_call_target="tpu_custom_call" | custom-call | tf_op jit(solution)/shard_map/pallas_call | solution.py:402
  107.8 1.9 %collective-permute-start.21 = (f32[8,512]{1,0:T(8,128)}, f32[8,512]{1,0:T(8,128)}, u32[]{:S(2)}, u32[]{:S(2)}) collective-permute-start(f32[8,512]{1,0:T(8,128)} %shard_map.158.a_ref), channel_id=1, source_target_pairs={{0,8},{4,12},{8,0},{12,4},{16,24},{20,28},{24,16},{28,20},{1,9},{5... | collective-permute-start | bytes 49160 | tf_op jit(solution)/shard_map/ppermute | solution.py:447
  109.6 2.3 %shard_map.157 = (bf16[128,512]{1,0:T(8,128)(2,1)}, bf16[128,2048]{1,0:T(8,128)(2,1)}) custom-call(bf16[8,64,512]{2,1,0:T(8,128)(2,1)} %all-to-all-done.1.got_hbm, bf16[512,128]{1,0:T(8,128)(2,1)} %copy-done.9, f32[8,128]{1,0:T(8,128)} %get-tuple-element.44.place_ref.place_hbm, f32[8,128]{1,0:T(8,128)} %get-tuple-element.68.aff_hbm, bf16[8,2048]{1,0:T(8,128)(2,1)} %bitcast.45), custom_call_target="tpu_custom_call" | custom-call | tf_op jit(solution)/shard_map/pallas_call | solution.py:402
  112.0 0.6 collective-permute-start.18
  112.5 0.8 add_add_fusion
  113.3 0.7 shard_map.159.a_ref
  114.1 2.3 %collective-permute-start.22 = (f32[8,512]{1,0:T(8,128)S(1)}, f32[8,512]{1,0:T(8,128)S(1)}, u32[]{:S(2)}, u32[]{:S(2)}) collective-permute-start(f32[8,512]{1,0:T(8,128)S(1)} %shard_map.159.a_ref), channel_id=1, source_target_pairs={{0,16},{4,20},{8,24},{12,28},{16,0},{20,4},{24,8},{28,12},{1,17},{... | collective-permute-start | bytes 49160 | tf_op jit(solution)/shard_map/ppermute | solution.py:447
  116.4 1.5 %collective-permute-done.18.refs_2_ = bf16[128,512]{1,0:T(8,128)(2,1)S(1)} collective-permute-done((bf16[128,512]{1,0:T(8,128)(2,1)}, bf16[128,512]{1,0:T(8,128)(2,1)S(1)}, u32[]{:S(2)}, u32[]{:S(2)}) %collective-permute-start.18) | collective-permute-done | bytes 131104 | tf_op jit(solution)/shard_map/ppermute | solution.py:447
  117.9 0.6 fusion
  118.5 0.2 collective-permute-done.22.b_ref
  118.7 0.6 shard_map.160
  119.3 0.8 assemble.1
  (45 shorter events, 0.2 us)
Async XLA Ops:
  25.1 19.1 %collective-permute-start.10 = (bf16[8,64,512]{2,1,0:T(8,128)(2,1)}, bf16[8,64,512]{2,1,0:T(8,128)(2,1)}, u32[]{:S(2)}, u32[]{:S(2)}) collective-permute-start(bf16[8,64,512]{2,1,0:T(8,128)(2,1)} %all_to_all.10.refs_0_.own_ref.x_ref.refs_4_), channel_id=1, source_target_pairs={{0,2},{1,3},{2,0},{3,1},{4,6},{5,7},{6,4},{7,5},{8,10},{9,11},{10,... | collective-permute-start | bytes 1572872 | tf_op jit(solution)/shard_map/ppermute | solution.py:447
  29.5 12.9 %collective-permute-start.3 = (bf16[56,1024]{1,0:T(8,128)(2,1)}, bf16[56,1024]{1,0:T(8,128)(2,1)S(1)}, u32[]{:S(2)}, u32[]{:S(2)}) collective-permute-start(bf16[56,1024]{1,0:T(8,128)(2,1)} %get-tuple-element.49), channel_id=1, source_target_pairs={{0,16},{4,20},{8,24},{12,28},{16,0},{20,4},{24,8},{28,12},{1,17},{... | collective-permute-start | bytes 344072 | tf_op jit(solution)/shard_map/ppermute | solution.py:447
  30.6 29.2 %collective-permute-start.9 = (bf16[8,64,512]{2,1,0:T(8,128)(2,1)}, bf16[8,64,512]{2,1,0:T(8,128)(2,1)S(1)}, u32[]{:S(2)}, u32[]{:S(2)}) collective-permute-start(bf16[8,64,512]{2,1,0:T(8,128)(2,1)} %all_to_all.10.refs_0_.own_ref.x_ref.refs_4_), channel_id=1, source_target_pairs={{0,1},{1,0},{2,3},{3,2},{4,5},{5,4},{6,7},{7,6},{8,9},{9,8},{10,11... | collective-permute-start | bytes 1572872 | tf_op jit(solution)/shard_map/ppermute | solution.py:447
  30.6 16.1 %collective-permute-start.4 = (bf16[56,1024]{1,0:T(8,128)(2,1)}, bf16[56,1024]{1,0:T(8,128)(2,1)S(1)}, u32[]{:S(2)}, u32[]{:S(2)}) collective-permute-start(bf16[56,1024]{1,0:T(8,128)(2,1)} %get-tuple-element.50), channel_id=1, source_target_pairs={{0,20},{4,16},{8,28},{12,24},{16,4},{20,0},{24,12},{28,8},{1,21},{... | collective-permute-start | bytes 344072 | tf_op jit(solution)/shard_map/ppermute | solution.py:447
  33.4 13.4 %collective-permute-start.5 = (bf16[56,1024]{1,0:T(8,128)(2,1)}, bf16[56,1024]{1,0:T(8,128)(2,1)S(1)}, u32[]{:S(2)}, u32[]{:S(2)}) collective-permute-start(bf16[56,1024]{1,0:T(8,128)(2,1)} %get-tuple-element.51), channel_id=1, source_target_pairs={{0,24},{4,28},{8,16},{12,20},{16,8},{20,12},{24,0},{28,4},{1,25},{... | collective-permute-start | bytes 344072 | tf_op jit(solution)/shard_map/ppermute | solution.py:447
  42.3 7.9 %collective-permute-start.6 = (bf16[56,1024]{1,0:T(8,128)(2,1)}, bf16[56,1024]{1,0:T(8,128)(2,1)S(1)}, u32[]{:S(2)}, u32[]{:S(2)}) collective-permute-start(bf16[56,1024]{1,0:T(8,128)(2,1)} %get-tuple-element.52), channel_id=1, source_target_pairs={{0,28},{4,24},{8,20},{12,16},{16,12},{20,8},{24,4},{28,0},{1,29},{... | collective-permute-start | bytes 344072 | tf_op jit(solution)/shard_map/ppermute | solution.py:447
  44.2 19.9 %collective-permute-start.11 = (bf16[8,64,512]{2,1,0:T(8,128)(2,1)}, bf16[8,64,512]{2,1,0:T(8,128)(2,1)S(1)}, u32[]{:S(2)}, u32[]{:S(2)}) collective-permute-start(bf16[8,64,512]{2,1,0:T(8,128)(2,1)} %collective-permute-done.10.refs_0_.refs_2_), channel_id=1, source_target_pairs={{0,1},{1,0},{2,3},{3,2},{4,5},{5,4},{6,7},{7,6},{8,9},{9,8},{10,11... | collective-permute-start | bytes 1572872 | tf_op jit(solution)/shard_map/ppermute | solution.py:447
  46.8 5.8 %collective-permute-start = (bf16[56,1024]{1,0:T(8,128)(2,1)}, bf16[56,1024]{1,0:T(8,128)(2,1)S(1)}, u32[]{:S(2)}, u32[]{:S(2)}) collective-permute-start(bf16[56,1024]{1,0:T(8,128)(2,1)} %get-tuple-element.46), channel_id=1, source_target_pairs={{0,4},{4,0},{8,12},{12,8},{16,20},{20,16},{24,28},{28,24},{1,5},{5... | collective-permute-start | bytes 344072 | tf_op jit(solution)/shard_map/ppermute | solution.py:447
  46.8 7.0 %collective-permute-start.1 = (bf16[56,1024]{1,0:T(8,128)(2,1)}, bf16[56,1024]{1,0:T(8,128)(2,1)S(1)}, u32[]{:S(2)}, u32[]{:S(2)}) collective-permute-start(bf16[56,1024]{1,0:T(8,128)(2,1)} %get-tuple-element.47), channel_id=1, source_target_pairs={{0,8},{4,12},{8,0},{12,4},{16,24},{20,28},{24,16},{28,20},{1,9},{5... | collective-permute-start | bytes 344072 | tf_op jit(solution)/shard_map/ppermute | solution.py:447
  50.2 5.9 %collective-permute-start.2 = (bf16[56,1024]{1,0:T(8,128)(2,1)}, bf16[56,1024]{1,0:T(8,128)(2,1)S(1)}, u32[]{:S(2)}, u32[]{:S(2)}) collective-permute-start(bf16[56,1024]{1,0:T(8,128)(2,1)} %get-tuple-element.48), channel_id=1, source_target_pairs={{0,12},{4,8},{8,4},{12,0},{16,28},{20,24},{24,20},{28,16},{1,13},{... | collective-permute-start | bytes 344072 | tf_op jit(solution)/shard_map/ppermute | solution.py:447
  52.6 7.2 %copy-start.4 = (bf16[4,56,1024]{2,1,0:T(8,128)(2,1)}, bf16[4,56,1024]{2,1,0:T(8,128)(2,1)S(1)}, u32[]{:S(2)}) copy-start(bf16[4,56,1024]{2,1,0:T(8,128)(2,1)S(1)} %shard_map.145) | copy-start | bytes 1376260
  52.6 13.8 %collective-permute-start.8 = (bf16[224,1024]{1,0:T(8,128)(2,1)S(1)}, bf16[224,1024]{1,0:T(8,128)(2,1)S(1)}, u32[]{:S(2)}, u32[]{:S(2)}) collective-permute-start(bf16[224,1024]{1,0:T(8,128)(2,1)S(1)} %bitcast.33), channel_id=1, source_target_pairs={{0,1},{1,0},{2,3},{3,2},{4,5},{5,4},{6,7},{7,6},{8,9},{9,8},{10,11... | collective-permute-start | bytes 1376264 | tf_op jit(solution)/shard_map/ppermute | solution.py:447
  56.1 0.9 copy-start.13
  57.0 2.8 %copy-start.1 = (bf16[1,2048,512]{2,1,0:T(8,128)(2,1)S(1)}, bf16[1,2048,512]{2,1,0:T(8,128)(2,1)}, u32[]{:S(2)}) copy-start(bf16[1,2048,512]{2,1,0:T(8,128)(2,1)} %param.11) | copy-start | bytes 6291460
  57.1 5.3 %copy-start.5 = (bf16[4,56,1024]{2,1,0:T(8,128)(2,1)}, bf16[4,56,1024]{2,1,0:T(8,128)(2,1)S(1)}, u32[]{:S(2)}) copy-start(bf16[4,56,1024]{2,1,0:T(8,128)(2,1)S(1)} %shard_map.144) | copy-start | bytes 1376260
  57.1 3.0 %copy-start = (bf16[1,2048,512]{2,1,0:T(8,128)(2,1)S(1)}, bf16[1,2048,512]{2,1,0:T(8,128)(2,1)}, u32[]{:S(2)}) copy-start(bf16[1,2048,512]{2,1,0:T(8,128)(2,1)} %param.10) | copy-start | bytes 6291460
  57.1 9.3 %collective-permute-start.7 = (bf16[224,1024]{1,0:T(8,128)(2,1)S(1)}, bf16[224,1024]{1,0:T(8,128)(2,1)S(1)}, u32[]{:S(2)}, u32[]{:S(2)}) collective-permute-start(bf16[224,1024]{1,0:T(8,128)(2,1)S(1)} %bitcast.36), channel_id=1, source_target_pairs={{0,1},{1,0},{2,3},{3,2},{4,5},{5,4},{6,7},{7,6},{8,9},{9,8},{10,11... | collective-permute-start | bytes 1376264 | tf_op jit(solution)/shard_map/ppermute | solution.py:447
  57.2 1.8 %copy-start.2 = (bf16[1,512,2048]{2,1,0:T(8,128)(2,1)S(1)}, bf16[1,512,2048]{2,1,0:T(8,128)(2,1)}, u32[]{:S(2)}) copy-start(bf16[1,512,2048]{2,1,0:T(8,128)(2,1)} %param.12) | copy-start | bytes 6291460
  59.8 2.5 %copy-start.8 = (bf16[8,64,512]{2,1,0:T(8,128)(2,1)}, bf16[8,64,512]{2,1,0:T(8,128)(2,1)S(1)}, u32[]{:S(2)}) copy-start(bf16[8,64,512]{2,1,0:T(8,128)(2,1)S(1)} %collective-permute-done.9.refs_1_) | copy-start | bytes 1572868
  64.1 2.3 %copy-start.7 = (bf16[8,64,512]{2,1,0:T(8,128)(2,1)}, bf16[8,64,512]{2,1,0:T(8,128)(2,1)S(1)}, u32[]{:S(2)}) copy-start(bf16[8,64,512]{2,1,0:T(8,128)(2,1)S(1)} %collective-permute-done.11.refs_0_.refs_3_) | copy-start | bytes 1572868
  64.1 2.3 %copy-start.3 = (bf16[1,512,2048]{2,1,0:T(8,128)(2,1)S(1)}, bf16[1,512,2048]{2,1,0:T(8,128)(2,1)}, u32[]{:S(2)}) copy-start(bf16[1,512,2048]{2,1,0:T(8,128)(2,1)} %param.12) | copy-start | bytes 6291460
  66.4 2.1 %copy-start.12 = (bf16[8,56,512]{2,1,0:T(8,128)(2,1)}, bf16[8,56,512]{2,1,0:T(8,128)(2,1)S(1)}, u32[]{:S(2)}) copy-start(bf16[8,56,512]{2,1,0:T(8,128)(2,1)S(1)} %get-tuple-element.58) | copy-start | bytes 1376260
  66.4 2.1 %copy-start.10 = (bf16[224,1024]{1,0:T(8,128)(2,1)}, bf16[224,1024]{1,0:T(8,128)(2,1)S(1)}, u32[]{:S(2)}) copy-start(bf16[224,1024]{1,0:T(8,128)(2,1)S(1)} %collective-permute-done.8.far_ref.refs_3_) | copy-start | bytes 1376260
  66.4 2.1 %copy-start.11 = (bf16[224,1024]{1,0:T(8,128)(2,1)}, bf16[224,1024]{1,0:T(8,128)(2,1)S(1)}, u32[]{:S(2)}) copy-start(bf16[224,1024]{1,0:T(8,128)(2,1)S(1)} %collective-permute-done.7.near_ref.refs_2_) | copy-start | bytes 1376260
  68.5 1.9 %copy-start.6 = (bf16[8,64,1024]{2,1,0:T(8,128)(2,1)}, bf16[8,64,1024]{2,1,0:T(8,128)(2,1)S(1)}, u32[]{:S(2)}) copy-start(bf16[8,64,1024]{2,1,0:T(8,128)(2,1)S(1)} %get-tuple-element.61.g_ref.refs_4_) | copy-start | bytes 3145732
  68.5 1.9 %collective-permute-start.15 = (bf16[1,448,512]{2,1,0:T(8,128)(2,1)S(1)}, bf16[1,448,512]{2,1,0:T(8,128)(2,1)S(1)}, u32[]{:S(2)}, u32[]{:S(2)}) collective-permute-start(bf16[1,448,512]{2,1,0:T(8,128)(2,1)S(1)} %get-tuple-element.67), channel_id=1, source_target_pairs={{0,1},{1,0},{2,3},{3,2},{4,5},{5,4},{6,7},{7,6},{8,9},{9,8},{10,11... | collective-permute-start | bytes 1376264 | tf_op jit(solution)/shard_map/ppermute | solution.py:447
  68.9 16.6 %collective-permute-start.12 = (bf16[448,512]{1,0:T(8,128)(2,1)S(1)}, bf16[448,512]{1,0:T(8,128)(2,1)S(1)}, u32[]{:S(2)}, u32[]{:S(2)}) collective-permute-start(bf16[448,512]{1,0:T(8,128)(2,1)S(1)} %get-tuple-element.63), channel_id=1, source_target_pairs={{0,1},{1,0},{2,3},{3,2},{4,5},{5,4},{6,7},{7,6},{8,9},{9,8},{10,11... | collective-permute-start | bytes 1376264 | tf_op jit(solution)/shard_map/ppermute | solution.py:447
  70.6 14.9 %collective-permute-start.16 = (bf16[448,512]{1,0:T(8,128)(2,1)S(1)}, bf16[448,512]{1,0:T(8,128)(2,1)S(1)}, u32[]{:S(2)}, u32[]{:S(2)}) collective-permute-start(bf16[448,512]{1,0:T(8,128)(2,1)S(1)} %bitcast.41), channel_id=1, source_target_pairs={{0,2},{1,3},{2,0},{3,1},{4,6},{5,7},{6,4},{7,5},{8,10},{9,11},{10,... | collective-permute-start | bytes 1376264 | tf_op jit(solution)/shard_map/ppermute | solution.py:447
  71.1 1.2 collective-permute-start.13
  72.3 11.1 %collective-permute-start.14 = (f32[8,128]{1,0:T(8,128)S(1)}, f32[8,128]{1,0:T(8,128)S(1)}, u32[]{:S(2)}, u32[]{:S(2)}) collective-permute-start(f32[8,128]{1,0:T(8,128)S(1)} %shard_map.152.a_ref), channel_id=1, source_target_pairs={{0,2},{1,3},{2,0},{3,1},{4,6},{5,7},{6,4},{7,5},{8,10},{9,11},{10,... | collective-permute-start | bytes 12296 | tf_op jit(solution)/shard_map/ppermute | solution.py:447
  86.5 23.2 %all-to-all-start.1 = ((bf16[8,64,512]{2,1,0:T(8,128)(2,1)}), bf16[8,64,512]{2,1,0:T(8,128)(2,1)}, u32[]{:S(2)}, u32[]{:S(2)}) async-start(bf16[8,64,512]{2,1,0:T(8,128)(2,1)} %shard_map.155), calls=%async_computation.1 | async-start | bytes 1048576 | tf_op jit(solution)/shard_map/all_to_all | solution.py:450
  91.1 6.9 %copy-start.14 = (f32[8,128]{1,0:T(8,128)S(1)}, f32[8,128]{1,0:T(8,128)}, u32[]{:S(2)}) copy-start(f32[8,128]{1,0:T(8,128)} %get-tuple-element.44.place_ref.place_hbm) | copy-start | bytes 12292
  97.4 4.1 %collective-permute-start.24 = (f32[2,2048]{1,0:T(2,128)}, f32[2,2048]{1,0:T(2,128)}, u32[]{:S(2)}, u32[]{:S(2)}) collective-permute-start(f32[2,2048]{1,0:T(2,128)} %bitcast.46), channel_id=1, source_target_pairs={{0,2},{1,3},{2,0},{3,1},{4,6},{5,7},{6,4},{7,5},{8,10},{9,11},{10,... | collective-permute-start | bytes 49160 | tf_op jit(solution)/shard_map/ppermute | solution.py:447
  98.0 0.7 copy-start.9
  98.6 13.9 %collective-permute-start.23 = (f32[2,2048]{1,0:T(2,128)}, f32[2,2048]{1,0:T(2,128)}, u32[]{:S(2)}, u32[]{:S(2)}) collective-permute-start(f32[2,2048]{1,0:T(2,128)} %bitcast.47), channel_id=1, source_target_pairs={{0,1},{1,0},{2,3},{3,2},{4,5},{5,4},{6,7},{7,6},{8,9},{9,8},{10,11... | collective-permute-start | bytes 49160 | tf_op jit(solution)/shard_map/ppermute | solution.py:447
  98.6 7.8 %collective-permute-start.20 = (f32[8,512]{1,0:T(8,128)}, f32[8,512]{1,0:T(8,128)}, u32[]{:S(2)}, u32[]{:S(2)}) collective-permute-start(f32[8,512]{1,0:T(8,128)} %get-tuple-element.71.a_ref), channel_id=1, source_target_pairs={{0,4},{4,0},{8,12},{12,8},{16,20},{20,16},{24,28},{28,24},{1,5},{5... | collective-permute-start | bytes 49160 | tf_op jit(solution)/shard_map/ppermute | solution.py:447
  101.5 11.0 %collective-permute-start.25 = (f32[2,2048]{1,0:T(2,128)}, f32[2,2048]{1,0:T(2,128)}, u32[]{:S(2)}, u32[]{:S(2)}) collective-permute-start(f32[2,2048]{1,0:T(2,128)} %collective-permute-done.24), channel_id=1, source_target_pairs={{0,1},{1,0},{2,3},{3,2},{4,5},{5,4},{6,7},{7,6},{8,9},{9,8},{10,11... | collective-permute-start | bytes 49160 | tf_op jit(solution)/shard_map/ppermute | solution.py:447
  107.8 5.5 %collective-permute-start.21 = (f32[8,512]{1,0:T(8,128)}, f32[8,512]{1,0:T(8,128)}, u32[]{:S(2)}, u32[]{:S(2)}) collective-permute-start(f32[8,512]{1,0:T(8,128)} %shard_map.158.a_ref), channel_id=1, source_target_pairs={{0,8},{4,12},{8,0},{12,4},{16,24},{20,28},{24,16},{28,20},{1,9},{5... | collective-permute-start | bytes 49160 | tf_op jit(solution)/shard_map/ppermute | solution.py:447
  112.0 5.9 %collective-permute-start.18 = (bf16[128,512]{1,0:T(8,128)(2,1)}, bf16[128,512]{1,0:T(8,128)(2,1)S(1)}, u32[]{:S(2)}, u32[]{:S(2)}) collective-permute-start(bf16[128,512]{1,0:T(8,128)(2,1)} %get-tuple-element.70), channel_id=1, source_target_pairs={{0,2},{1,3},{2,0},{3,1},{4,6},{5,7},{6,4},{7,5},{8,10},{9,11},{10,... | collective-permute-start | bytes 393224 | tf_op jit(solution)/shard_map/ppermute | solution.py:447
  114.1 4.6 %collective-permute-start.22 = (f32[8,512]{1,0:T(8,128)S(1)}, f32[8,512]{1,0:T(8,128)S(1)}, u32[]{:S(2)}, u32[]{:S(2)}) collective-permute-start(f32[8,512]{1,0:T(8,128)S(1)} %shard_map.159.a_ref), channel_id=1, source_target_pairs={{0,16},{4,20},{8,24},{12,28},{16,0},{20,4},{24,8},{28,12},{1,17},{... | collective-permute-start | bytes 49160 | tf_op jit(solution)/shard_map/ppermute | solution.py:447
  116.4 3.0 %collective-permute-start.17 = (bf16[128,512]{1,0:T(8,128)(2,1)}, bf16[128,512]{1,0:T(8,128)(2,1)S(1)}, u32[]{:S(2)}, u32[]{:S(2)}) collective-permute-start(bf16[128,512]{1,0:T(8,128)(2,1)} %get-tuple-element.70), channel_id=1, source_target_pairs={{0,1},{1,0},{2,3},{3,2},{4,5},{5,4},{6,7},{7,6},{8,9},{9,8},{10,11... | collective-permute-start | bytes 393224 | tf_op jit(solution)/shard_map/ppermute | solution.py:447
  117.9 1.5 %collective-permute-start.19 = (bf16[128,512]{1,0:T(8,128)(2,1)S(1)}, bf16[128,512]{1,0:T(8,128)(2,1)S(1)}, u32[]{:S(2)}, u32[]{:S(2)}) collective-permute-start(bf16[128,512]{1,0:T(8,128)(2,1)S(1)} %collective-permute-done.18.refs_2_), channel_id=1, source_target_pairs={{0,1},{1,0},{2,3},{3,2},{4,5},{5,4},{6,7},{7,6},{8,9},{9,8},{10,11... | collective-permute-start | bytes 393224 | tf_op jit(solution)/shard_map/ppermute | solution.py:447

commit v5 on v4

--- a/solution.py
+++ b/solution.py
@@ -47,7 +47,7 @@
 
 
 def route_kernel(
-    slots, tok_hbm, routing_hbm, router_hbm, rows_ref, aff_ref, place_ref,
+    slots, tok_hbm, routing_hbm, router_hbm, rows_ref, place_ref,
     tok_ref, routing_ref, router_ref, sems,
 ):
     copies = fetch(sems, (tok_hbm, tok_ref), (routing_hbm, routing_ref), (router_hbm, router_ref))
@@ -70,7 +70,6 @@
     place = jnp.where(named > 0, position, -1.0)
     chosen = named * aff
     weights = chosen / jnp.sum(chosen, axis=0, keepdims=True)
-    aff_ref[...] = aff
     place_ref[...] = place
     hot = one_hot(place, slots)
     full = jnp.concatenate(hot, axis=0).astype(BF16)
@@ -247,15 +246,16 @@
     out_ref[...] = (own_ref[...] + got_ref[...].astype(F32)).astype(BF16)
 
 
-def add_chip_kernel(own_ref, core_ref, tile_ref, *refs):
+def add_chip_kernel(own_ref, core_ref, table_ref, router_ref, *refs):
+    out_ref = refs[-1]
+    experts = router_ref.shape[0]
+    cols = out_ref.shape[1]
+    start = pl.multiple_of(lax.axis_index("tp") * cols, 128)
     total = own_ref[...] + core_ref[...].astype(F32)
+    total = total + dot(table_ref[...][:, :experts].astype(BF16), router_ref[:, pl.ds(start, cols)])
     for chip_ref in refs[:-1]:
         total = total + chip_ref[...].astype(F32)
-    out_ref = refs[-1]
-    slots = out_ref.shape[1] - 8
-    for e in range(out_ref.shape[0]):
-        block = jnp.concatenate([total[e * slots : (e + 1) * slots], tile_ref[e]], axis=0)
-        out_ref[e] = block.astype(BF16)
+    out_ref[...] = total.astype(BF16)
 
 
 def grads_kernel(shares, q_ref, *refs):
@@ -309,20 +309,13 @@
     out_ref[...] = a_ref[...] + b_ref[...]
 
 
-def terms_kernel(slots, a_ref, b_ref, x_ref, tile_ref, part_ref):
+def terms_kernel(slots, a_ref, b_ref, x_ref, table_ref, part_ref):
     term = (a_ref[...] + b_ref[...]).astype(BF16).astype(F32)
     groups, span, cols = x_ref.shape
     experts = part_ref.shape[0]
     count = slots // 8
-    lanes = term.shape[1]
-    lane = lax.broadcasted_iota(jnp.int32, (8, lanes), 1)
     blocks = []
     for b in range(groups):
-        moved = pltpu.roll(term, (lanes - b * count) % lanes, 1)
-        moved = jnp.where(lane < count, moved, 0.0)[:, :128]
-        if cols > 128:
-            moved = jnp.concatenate([moved, jnp.zeros((8, cols - 128), F32)], axis=1)
-        tile_ref[b] = moved
         spare = x_ref[b, slots:, :128].astype(F32)
         for g in range(count):
             factors = pltpu.roll(spare, 128 - COEF_LANE - g * experts, 1)
@@ -331,6 +324,8 @@
         blocks.append(jnp.zeros((8, 128), F32))
     table = jnp.concatenate(blocks, axis=0)
     table = jnp.where(lax.broadcasted_iota(jnp.int32, table.shape, 1) < experts, table, 0.0)
+    for b in range(groups):
+        table_ref[b * slots : (b + 1) * slots, :] = table[b * span : b * span + slots, :]
     high = table.astype(BF16)
     low = (table - high.astype(F32)).astype(BF16)
     x = x_ref[...].reshape(groups * span, cols)
@@ -347,38 +342,12 @@
     hot_ref[...] = jnp.concatenate(one_hot(place_ref[...], slots), axis=0).astype(BF16)
 
 
-def home_kernel(
-    slots, got_hbm, hot_hbm, place_hbm, aff_hbm, router_hbm, token_out, whole_hbm,
-    got_ref, hot_ref, place_ref, aff_ref, router_ref, own_ref, sems,
-):
-    experts, span, cols = got_ref.shape
-    toks = place_ref.shape[1]
+def home_kernel(got_hbm, hot_hbm, token_out, whole_hbm, got_ref, hot_ref, own_ref, sems):
+    cols = got_ref.shape[1]
     start = pl.multiple_of(lax.axis_index("tp") * cols, 128)
-    copies = fetch(
-        sems, (place_hbm, place_ref), (aff_hbm, aff_ref), (got_hbm, got_ref),
-        (router_hbm.at[:, pl.ds(start, cols)], router_ref), (hot_hbm, hot_ref),
-    )
-    for copy in copies:
+    for copy in fetch(sems, (got_hbm, got_ref), (hot_hbm, hot_ref)):
         copy.wait()
-    place = place_ref[...]
-    aff = aff_ref[...]
-    back = dot(hot_ref[...], got_ref[...].reshape(experts * span, cols), 0, 0)
-    hot = one_hot(place, slots)
-    rows = []
-    for e in range(experts):
-        tile = got_ref[e, slots:, :128].astype(F32)
-        total = jnp.zeros((8, toks), F32)
-        for g in range(slots // 8):
-            total = total + hot[e][8 * g : 8 * g + 8, :] * tile[:, g : g + 1]
-        rows.append(jnp.sum(total, axis=0, keepdims=True))
-    term = jnp.concatenate(rows, axis=0)
-    named = (place >= 0).astype(F32)
-    chosen = named * aff
-    total_aff = jnp.sum(chosen, axis=0, keepdims=True)
-    weights = chosen / total_aff
-    d_chosen = (term - jnp.sum(term * weights, axis=0, keepdims=True)) / total_aff
-    d_logit = named * d_chosen * aff * (1.0 - aff)
-    own_ref[...] = (back + dot(d_logit.T.astype(BF16), router_ref[...])).astype(BF16)
+    own_ref[...] = dot(hot_ref[...], got_ref[...], 0, 0).astype(BF16)
     copies = fetch(sems, (own_ref, token_out), (own_ref, whole_hbm.at[:, pl.ds(start, cols)]))
     for copy in copies:
         copy.wait()
@@ -453,9 +422,9 @@
         far = [value] + [swap(value, 2 * j) for j in range(1, chips)]
         return [part for piece in far for part in (piece, swap(piece, 1))]
 
-    rows_send, aff, place = call(
+    rows_send, place = call(
         functools.partial(route_kernel, slots),
-        (shape(experts, span, cols), shape(experts, toks, dtype=F32), shape(experts, toks, dtype=F32)),
+        (shape(experts, span, cols), shape(experts, toks, dtype=F32)),
         False, tokens, routing, router, hbm=(0, 1, 2), limit=ALONE,
         scratch=[buffer(toks, width), buffer(top, toks, dtype=jnp.int32), buffer(experts, width), DMAS((3,))],
     )
@@ -469,7 +438,7 @@
     for k in range(experts - 1, 0, -1):
         pieces[k] = swap(pieces[k], k, "ep")
 
-    hot = call(functools.partial(slot_map_kernel, span), shape(groups * span, toks), False, place)
+    hot = call(functools.partial(slot_map_kernel, slots), shape(count, toks), False, place)
 
     x_parts = spread(rows_got)
     sums = tuple(shape(groups * span, hidden, dtype=F32) for _ in range(2))
@@ -536,9 +505,9 @@
     term_got = swap(term, bit)
     chip_send = call(add_core_kernel, shape(chips - 1, count, cols), False, even_chip, core_chip)
     chip_got = [swap(chip_send[j], 2 * (j + 1)) for j in range(chips - 1)]
-    tiles, router_sum = call(
+    table, router_sum = call(
         functools.partial(terms_kernel, slots),
-        (shape(groups, 8, cols, dtype=F32), shape(experts, cols, dtype=F32)),
+        (shape(count, 128, dtype=F32), shape(experts, cols, dtype=F32)),
         False, term, term_got, rows_got,
     )
     bit = 1
@@ -553,9 +522,9 @@
     )
     router_rows = router_rows.reshape(cols)
     home_send = call(
-        add_chip_kernel, shape(groups, span, cols), False, even_home, core_home, tiles, *chip_got,
-    )
-    home_got = exchange(home_send)
+        add_chip_kernel, shape(count, cols), False, even_home, core_home, table, router, *chip_got,
+    )
+    home_got = exchange(home_send.reshape(groups, slots, cols)).reshape(count, cols)
 
     grad_spec = pl.BlockSpec((cols, hidden), lambda r, q: (q[0] ^ r, 0))
     gate_grad, up_grad, norms = pl.pallas_call(
@@ -594,17 +563,9 @@
     norms = norms[0]
 
     token_part, token_grad = call(
-        functools.partial(home_kernel, slots), (shape(toks, cols), shape(toks, width)),
-        False, home_got, hot, place, aff, router, hbm=range(5), limit=ALONE, out_hbm=True,
-        scratch=[
-            buffer(groups, span, cols),
-            buffer(groups * span, toks),
-            buffer(experts, toks, dtype=F32),
-            buffer(experts, toks, dtype=F32),
-            buffer(experts, cols),
-            buffer(toks, cols),
-            DMAS((5,)),
-        ],
+        home_kernel, (shape(toks, cols), shape(toks, width)),
+        False, home_got, hot, hbm=(0, 1), limit=ALONE, out_hbm=True,
+        scratch=[buffer(count, cols), buffer(count, toks), buffer(toks, cols), DMAS((2,))],
     )
     token_parts = spread(token_part)[1:]
     token_grad = pl.pallas_call(

time: 121 us -> 121 us (level)
    unnamed x30 -> x32, local copies, waits for them, and re-layouts: 3.62 us -> 3.62 us
  transfers between devices with their start and end apart: 27 -> 27, of which waited for: 9 -> 9; matrix products, arithmetic and copies ran while one was open for 1% -> 1% of each run, Pallas kernels for 25% -> 24%
where the time goes in v5:
time: 121 us; the launch traced here: 120 us
  Pallas kernels  35.8 us (30%)
  starting transfers between devices  28.9 us (24%)
  waiting for transfers between devices  27.2 us (22%)
  blocking collectives  21.9 us (18%)
  local copies, waits for them, and re-layouts  4.24 us (4%)
    ppermute x26, waiting for transfers between devices, swap(): return lax.ppermute(value, axis, [(i, i ^ bit) for i in range(size)])  27.2 us
    ppermute x26, starting transfers between devices, swap(): return lax.ppermute(value, axis, [(i, i ^ bit) for i in range(size)])  24.4 us
    pallas_call x19, Pallas kernels, call(): pl.pallas_call(kernel, out_shape=outs, in_specs=([SMEM] if scalar else []...  23.9 us
    all_to_all x1, blocking collectives, exchange(): return lax.all_to_all(value, 'ep', split_axis=0, concat_axis=0, tiled=True)  21.9 us
    pallas_call x1, Pallas kernels, layer(): pl.pallas_call(functools.partial(grads_kernel, shares), out_shape=(shape(...  6.37 us
    pallas_call x1, Pallas kernels, layer(): pl.pallas_call(functools.partial(down_kernel, slots), out_shape=(shape(hi...  4.72 us
    all_to_all x1, starting transfers between devices, exchange(): return lax.all_to_all(value, 'ep', split_axis=0, concat_axis=0, tiled=True)  4.57 us
    unnamed x32, local copies, waits for them, and re-layouts  3.62 us
  transfers between devices with their start and end apart: 27, of which 9 were waited for; matrix products, arithmetic and copies ran while one was open for 1% of the time, Pallas kernels for 24%

profile of v5, /device:TPU:0, one launch (start us, length us, event | category | flops | bytes accessed | tf_op | source)
XLA Modules:
  0.0 120.0 jit_solution(10354045678337332141)
XLA Ops:
  0.6 2.6 %shard_map.142 = (bf16[8,64,512]{2,1,0:T(8,128)(2,1)}, f32[8,128]{1,0:T(8,128)}) custom-call(bf16[128,2048]{1,0:T(8,128)(2,1)} %tok_hbm.1, s32[2,128]{1,0:T(2,128)} %bitcast.51, bf16[8,2048]{1,0:T(8,128)(2,1)} %bitcast.46), custom_call_target="tpu_custom_call" | custom-call | tf_op jit(solution)/shard_map/pallas_call | solution.py:371
  3.2 21.9 %all_to_all.10.refs_0_.own_ref.x_ref.refs_4_ = bf16[8,64,512]{2,1,0:T(8,128)(2,1)} all-to-all(bf16[8,64,512]{2,1,0:T(8,128)(2,1)} %get-tuple-element.52), channel_id=1, replica_groups=mesh['ep'=8,'tp'=4] {'ep'}, dimensions={0} | all-to-all | bytes 1048576 | tf_op jit(solution)/shard_map/all_to_all | solution.py:419
  25.1 1.5 %collective-permute-start.10 = (bf16[8,64,512]{2,1,0:T(8,128)(2,1)}, bf16[8,64,512]{2,1,0:T(8,128)(2,1)}, u32[]{:S(2)}, u32[]{:S(2)}) collective-permute-start(bf16[8,64,512]{2,1,0:T(8,128)(2,1)} %all_to_all.10.refs_0_.own_ref.x_ref.refs_4_), channel_id=1, source_target_pairs={{0,2},{1,3},{2,0},{3,1},{4,6},{5,7},{6,4},{7,5},{8,10},{9,11},{10,... | collective-permute-start | bytes 1572872 | tf_op jit(solution)/shard_map/ppermute | solution.py:416
  26.6 2.8 %shard_map.143 = (bf16[56,1024]{1,0:T(8,128)(2,1)}, bf16[56,1024]{1,0:T(8,128)(2,1)}, bf16[56,1024]{1,0:T(8,128)(2,1)}, bf16[56,1024]{1,0:T(8,128)(2,1)}, bf16[5...) custom-call(bf16[128,2048]{1,0:T(8,128)(2,1)} %cot_hbm.1, ...), custom_call_target="tpu_custom_call" | custom-call | flops 117440512 | tf_op jit(solution)/shard_map/pallas_call | solution.py:371
  29.5 1.1 collective-permute-start.3
  30.6 0.0 collective-permute-start.9
  30.6 2.7 %collective-permute-start.4 = (bf16[56,1024]{1,0:T(8,128)(2,1)}, bf16[56,1024]{1,0:T(8,128)(2,1)S(1)}, u32[]{:S(2)}, u32[]{:S(2)}) collective-permute-start(bf16[56,1024]{1,0:T(8,128)(2,1)} %get-tuple-element.49), channel_id=1, source_target_pairs={{0,20},{4,16},{8,28},{12,24},{16,4},{20,0},{24,12},{28,8},{1,21},{... | collective-permute-start | bytes 344072 | tf_op jit(solution)/shard_map/ppermute | solution.py:416
  33.3 1.5 %collective-permute-start.5 = (bf16[56,1024]{1,0:T(8,128)(2,1)}, bf16[56,1024]{1,0:T(8,128)(2,1)S(1)}, u32[]{:S(2)}, u32[]{:S(2)}) collective-permute-start(bf16[56,1024]{1,0:T(8,128)(2,1)} %get-tuple-element.50), channel_id=1, source_target_pairs={{0,24},{4,28},{8,16},{12,20},{16,8},{20,12},{24,0},{28,4},{1,25},{... | collective-permute-start | bytes 344072 | tf_op jit(solution)/shard_map/ppermute | solution.py:416
  34.8 7.5 %collective-permute-done.3.refs_0_ = bf16[56,1024]{1,0:T(8,128)(2,1)S(1)} collective-permute-done((bf16[56,1024]{1,0:T(8,128)(2,1)}, bf16[56,1024]{1,0:T(8,128)(2,1)S(1)}, u32[]{:S(2)}, u32[]{:S(2)}) %collective-permute-start.3) | collective-permute-done | bytes 114720 | tf_op jit(solution)/shard_map/ppermute | solution.py:416
  42.3 1.9 %collective-permute-start.6 = (bf16[56,1024]{1,0:T(8,128)(2,1)}, bf16[56,1024]{1,0:T(8,128)(2,1)S(1)}, u32[]{:S(2)}, u32[]{:S(2)}) collective-permute-start(bf16[56,1024]{1,0:T(8,128)(2,1)} %get-tuple-element.51), channel_id=1, source_target_pairs={{0,28},{4,24},{8,20},{12,16},{16,12},{20,8},{24,4},{28,0},{1,29},{... | collective-permute-start | bytes 344072 | tf_op jit(solution)/shard_map/ppermute | solution.py:416
  44.2 0.0 collective-permute-done.10.refs_0_.refs_2_
  44.2 2.6 %collective-permute-done.4.refs_1_ = bf16[56,1024]{1,0:T(8,128)(2,1)S(1)} collective-permute-done((bf16[56,1024]{1,0:T(8,128)(2,1)}, bf16[56,1024]{1,0:T(8,128)(2,1)S(1)}, u32[]{:S(2)}, u32[]{:S(2)}) %collective-permute-start.4) | collective-permute-done | bytes 114720 | tf_op jit(solution)/shard_map/ppermute | solution.py:416
  46.8 2.3 %collective-permute-start.1 = (bf16[56,1024]{1,0:T(8,128)(2,1)}, bf16[56,1024]{1,0:T(8,128)(2,1)S(1)}, u32[]{:S(2)}, u32[]{:S(2)}) collective-permute-start(bf16[56,1024]{1,0:T(8,128)(2,1)} %get-tuple-element.46), channel_id=1, source_target_pairs={{0,8},{4,12},{8,0},{12,4},{16,24},{20,28},{24,16},{28,20},{1,9},{5... | collective-permute-start | bytes 344072 | tf_op jit(solution)/shard_map/ppermute | solution.py:416
  49.0 1.2 collective-permute-done.6.refs_3_
  50.2 2.3 %collective-permute-start.2 = (bf16[56,1024]{1,0:T(8,128)(2,1)}, bf16[56,1024]{1,0:T(8,128)(2,1)S(1)}, u32[]{:S(2)}, u32[]{:S(2)}) collective-permute-start(bf16[56,1024]{1,0:T(8,128)(2,1)} %get-tuple-element.47), channel_id=1, source_target_pairs={{0,12},{4,8},{8,4},{12,0},{16,28},{20,24},{24,20},{28,16},{1,13},{... | collective-permute-start | bytes 344072 | tf_op jit(solution)/shard_map/ppermute | solution.py:416
  52.6 0.0 collective-permute-done.refs_1_
  52.6 0.1 collective-permute-start.8
  52.7 1.1 collective-permute-done.1.refs_2_
  53.8 2.3 %collective-permute-done.2.refs_3_ = bf16[56,1024]{1,0:T(8,128)(2,1)S(1)} collective-permute-done((bf16[56,1024]{1,0:T(8,128)(2,1)}, bf16[56,1024]{1,0:T(8,128)(2,1)S(1)}, u32[]{:S(2)}, u32[]{:S(2)}) %collective-permute-start.2) | collective-permute-done | bytes 114720 | tf_op jit(solution)/shard_map/ppermute | solution.py:416
  56.1 0.9 copy-done.14
  57.1 0.0 copy-start
  57.1 0.1 collective-permute-start.7
  57.2 0.0 copy-start.2
  57.2 1.8 %copy-done.2 = bf16[1,512,2048]{2,1,0:T(8,128)(2,1)S(1)} copy-done((bf16[1,512,2048]{2,1,0:T(8,128)(2,1)S(1)}, bf16[1,512,2048]{2,1,0:T(8,128)(2,1)}, u32[]{:S(2)}) %copy-start.2) | copy-done | bytes 2097176
  59.0 0.8 shard_map.146.back_ref
  59.8 0.0 copy-start.8
  59.8 0.2 copy-done
  60.0 2.3 %shard_map.147 = (f32[512,512]{1,0:T(8,128)S(1)}, f32[512,512]{1,0:T(8,128)S(1)}) custom-call(bf16[8,64,512]{2,1,0:T(8,128)(2,1)} %all_to_all.10.refs_0_.own_ref.x_ref.refs_4_, bf16[8,64,512]{2,1,0:T(8,128)(2,1)S(1)} %collective-permute-done.9.refs_1_, bf16[2048,512]{1,0:T(8,128)(2,1)S(1)} %bitcast.23, bf16[2048,512]{1,0:T(8,128)(2,1)S(1)} %bitcast.28), custom_call_target="tpu_custom_call" | custom-call | flops 469762048 | tf_op jit(solution)/shard_map/pallas_call | solution.py:371
  62.3 1.8 %shard_map.148 = (f32[512,512]{1,0:T(8,128)S(1)}, f32[512,512]{1,0:T(8,128)S(1)}) custom-call(f32[512,512]{1,0:T(8,128)S(1)} %get-tuple-element.53.got_g, f32[512,512]{1,0:T(8,128)S(1)} %get-tuple-element.54.got_u, bf16[8,64,512]{2,1,0:T(8,128)(2,1)} %collective-permute-done.10.refs_0_.refs_2_, bf16[2048,512]{1,0:T(8,128)(2,1)S(1)} %bitcast.24, ...), custom_call_target="tpu_custom_call" | custom-call | flops 469762048 | tf_op jit(solution)/shard_map/pallas_call | solution.py:371
  64.1 0.0 copy-start.3
  64.1 2.2 %shard_map.149 = (bf16[8,56,512]{2,1,0:T(8,128)(2,1)S(1)}, f32[8,56,512]{2,1,0:T(8,128)S(1)}, f32[8,56,512]{2,1,0:T(8,128)S(1)}) custom-call(f32[512,512]{1,0:T(8,128)S(1)} %get-tuple-element.55.got_g, f32[512,512]{1,0:T(8,128)S(1)} %get-tuple-element.56.got_u, bf16[8,64,512]{2,1,0:T(8,128)(2,1)} %all_to_all.10.refs_0_.own_ref.x_ref.refs_4_, ...), custom_call_target="tpu_custom_call" | custom-call | flops 939524096 | tf_op jit(solution)/shard_map/pallas_call | solution.py:371
  66.4 2.1 %shard_map.150 = (bf16[8,64,1024]{2,1,0:T(8,128)(2,1)S(1)}, bf16[448,512]{1,0:T(8,128)(2,1)S(1)}, bf16[1,448,512]{2,1,0:T(8,128)(2,1)S(1)}, f32[8,128]{1,0:T(8,128)S(1)}) custom-call(f32[2,224,512]{2,1,0:T(8,128)S(1)} %shard_map.146.back_ref, bf16[224,1024]{1,0:T(8,128)(2,1)S(1)} %collective-permute-done.7.near_ref.refs_2_, ...), custom_call_target="tpu_custom_call" | custom-call | flops 1409286144 | tf_op jit(solution)/shard_map/pallas_call | solution.py:371
  68.5 0.0 copy-start.6
  68.5 0.3 collective-permute-start.15
  68.9 0.3 collective-permute-start.12
  69.1 1.3 %shard_map.151 = (f32[448,512]{1,0:T(8,128)S(1)}, f32[1,448,512]{2,1,0:T(8,128)S(1)}) custom-call(bf16[8,64,1024]{2,1,0:T(8,128)(2,1)S(1)} %get-tuple-element.60.g_ref.refs_4_, bf16[2048,512]{1,0:T(8,128)(2,1)S(1)} %bitcast.27, bf16[2048,512]{1,0:T(8,128)(2,1)S(1)} %bitcast.32), custom_call_target="tpu_custom_call" | custom-call | flops 939524096 | tf_op jit(solution)/shard_map/pallas_call | solution.py:371
  70.4 0.0 copy-start.13
  70.4 0.1 shard_map.154
  70.6 0.6 collective-permute-start.16
  71.1 1.2 collective-permute-done.13.b_ref
  72.3 1.5 %collective-permute-start.14 = (f32[8,128]{1,0:T(8,128)S(1)}, f32[8,128]{1,0:T(8,128)S(1)}, u32[]{:S(2)}, u32[]{:S(2)}) collective-permute-start(f32[8,128]{1,0:T(8,128)S(1)} %shard_map.152.a_ref), channel_id=1, source_target_pairs={{0,2},{1,3},{2,0},{3,1},{4,6},{5,7},{6,4},{7,5},{8,10},{9,11},{10,... | collective-permute-start | bytes 12296 | tf_op jit(solution)/shard_map/ppermute | solution.py:416
  73.8 9.6 %collective-permute-done.14.b_ref = f32[8,128]{1,0:T(8,128)S(1)} collective-permute-done((f32[8,128]{1,0:T(8,128)S(1)}, f32[8,128]{1,0:T(8,128)S(1)}, u32[]{:S(2)}, u32[]{:S(2)}) %collective-permute-start.14) | collective-permute-done | bytes 4128 | tf_op jit(solution)/shard_map/ppermute | solution.py:416
  83.4 2.1 %shard_map.153 = (f32[448,128]{1,0:T(8,128)S(1)}, f32[8,512]{1,0:T(8,128)}) custom-call(f32[8,128]{1,0:T(8,128)S(1)} %shard_map.152.a_ref, f32[8,128]{1,0:T(8,128)S(1)} %collective-permute-done.14.b_ref, bf16[8,64,512]{2,1,0:T(8,128)(2,1)} %all_to_all.10.refs_0_.own_ref.x_ref.refs_4_), custom_call_target="tpu_custom_call" | custom-call | tf_op jit(solution)/shard_map/pallas_call | solution.py:371
  85.5 1.1 shard_map.155
  86.6 4.6 %all-to-all-start.1 = ((bf16[8,56,512]{2,1,0:T(8,128)(2,1)}), bf16[8,56,512]{2,1,0:T(8,128)(2,1)}, u32[]{:S(2)}, u32[]{:S(2)}) async-start(bf16[8,56,512]{2,1,0:T(8,128)(2,1)} %bitcast.11), calls=%async_computation.1 | async-start | bytes 917504 | tf_op jit(solution)/shard_map/all_to_all | solution.py:419
  91.2 6.4 %grads.1 = (bf16[2048,512]{1,0:T(8,128)(2,1)}, bf16[2048,512]{1,0:T(8,128)(2,1)}, f32[4,2,512]{2,1,0:T(2,128)}) custom-call(s32[1]{0:T(128)} %bitcast.15.q_ref, bf16[8,64,512]{2,1,0:T(8,128)(2,1)} %all_to_all.10.refs_0_.own_ref.x_ref.refs_4_, bf16[8,64,512]{2,1,0:T(8,128)(2,1)} %copy-done.8, bf16[8,64,512]{2,1,0:T(8,128)(2,1)} %collective-permute-done.10.refs_0_.refs_2_, ...), custom_call_target="tpu_custom_call" | custom-call | flops 1879048192 | tf_op jit(solution)/shard_map/grads/pallas_call | solution.py:530
  97.6 0.5 collective-permute-start.24
  98.1 0.6 copy-done.9
  98.8 2.8 %collective-permute-start.20 = (f32[8,512]{1,0:T(8,128)}, f32[8,512]{1,0:T(8,128)}, u32[]{:S(2)}, u32[]{:S(2)}) collective-permute-start(f32[8,512]{1,0:T(8,128)} %get-tuple-element.69.a_ref), channel_id=1, source_target_pairs={{0,4},{4,0},{8,12},{12,8},{16,20},{20,16},{24,28},{28,24},{1,5},{5... | collective-permute-start | bytes 49160 | tf_op jit(solution)/shard_map/ppermute | solution.py:416
  101.6 0.0 collective-permute-done.24
  101.6 0.2 collective-permute-start.25
  101.8 4.7 %down.1 = (bf16[512,2048]{1,0:T(8,128)(2,1)}, f32[1,512]{1,0:T(1,128)}) custom-call(s32[1]{0:T(128)} %bitcast.15.q_ref, bf16[224,1024]{1,0:T(8,128)(2,1)} %bitcast.40, bf16[224,1024]{1,0:T(8,128)(2,1)} %bitcast.37, bf16[224,1024]{1,0:T(8,128)(2,1)} %copy-done.11, bf16[224,1024]{1,0:T(8,128)(2,1)} %copy-done.10, ...), custom_call_target="tpu_custom_call" | custom-call | flops 939524096 | tf_op jit(solution)/shard_map/down/pallas_call | solution.py:543
  106.5 1.3 %shard_map.158.a_ref = f32[8,512]{1,0:T(8,128)} custom-call(f32[8,512]{1,0:T(8,128)} %get-tuple-element.69.a_ref, f32[8,512]{1,0:T(8,128)} %collective-permute-done.20.b_ref), custom_call_target="tpu_custom_call" | custom-call | tf_op jit(solution)/shard_map/pallas_call | solution.py:371
  107.9 1.9 %collective-permute-start.21 = (f32[8,512]{1,0:T(8,128)}, f32[8,512]{1,0:T(8,128)}, u32[]{:S(2)}, u32[]{:S(2)}) collective-permute-start(f32[8,512]{1,0:T(8,128)} %shard_map.158.a_ref), channel_id=1, source_target_pairs={{0,8},{4,12},{8,0},{12,4},{16,24},{20,28},{24,16},{28,20},{1,9},{5... | collective-permute-start | bytes 49160 | tf_op jit(solution)/shard_map/ppermute | solution.py:416
  109.7 2.0 %shard_map.157 = (bf16[128,512]{1,0:T(8,128)(2,1)}, bf16[128,2048]{1,0:T(8,128)(2,1)}) custom-call(bf16[448,512]{1,0:T(8,128)(2,1)} %bitcast.12.got_hbm, bf16[448,128]{1,0:T(8,128)(2,1)} %copy-done.9), custom_call_target="tpu_custom_call" | custom-call | tf_op jit(solution)/shard_map/pallas_call | solution.py:371
  111.7 0.6 collective-permute-start.18
  112.3 0.8 add_add_fusion
  113.1 0.7 shard_map.159.a_ref
  113.9 2.3 %collective-permute-start.22 = (f32[8,512]{1,0:T(8,128)S(1)}, f32[8,512]{1,0:T(8,128)S(1)}, u32[]{:S(2)}, u32[]{:S(2)}) collective-permute-start(f32[8,512]{1,0:T(8,128)S(1)} %shard_map.159.a_ref), channel_id=1, source_target_pairs={{0,16},{4,20},{8,24},{12,28},{16,0},{20,4},{24,8},{28,12},{1,17},{... | collective-permute-start | bytes 49160 | tf_op jit(solution)/shard_map/ppermute | solution.py:416
  116.2 1.5 %collective-permute-done.18.refs_2_ = bf16[128,512]{1,0:T(8,128)(2,1)S(1)} collective-permute-done((bf16[128,512]{1,0:T(8,128)(2,1)}, bf16[128,512]{1,0:T(8,128)(2,1)S(1)}, u32[]{:S(2)}, u32[]{:S(2)}) %collective-permute-start.18) | collective-permute-done | bytes 131104 | tf_op jit(solution)/shard_map/ppermute | solution.py:416
  117.7 0.6 fusion
  118.3 0.2 collective-permute-done.22.b_ref
  118.5 0.6 shard_map.160
  119.1 0.8 assemble.1
  (47 shorter events, 0.2 us)
Async XLA Ops:
  25.1 19.1 %collective-permute-start.10 = (bf16[8,64,512]{2,1,0:T(8,128)(2,1)}, bf16[8,64,512]{2,1,0:T(8,128)(2,1)}, u32[]{:S(2)}, u32[]{:S(2)}) collective-permute-start(bf16[8,64,512]{2,1,0:T(8,128)(2,1)} %all_to_all.10.refs_0_.own_ref.x_ref.refs_4_), channel_id=1, source_target_pairs={{0,2},{1,3},{2,0},{3,1},{4,6},{5,7},{6,4},{7,5},{8,10},{9,11},{10,... | collective-permute-start | bytes 1572872 | tf_op jit(solution)/shard_map/ppermute | solution.py:416
  29.5 12.9 %collective-permute-start.3 = (bf16[56,1024]{1,0:T(8,128)(2,1)}, bf16[56,1024]{1,0:T(8,128)(2,1)S(1)}, u32[]{:S(2)}, u32[]{:S(2)}) collective-permute-start(bf16[56,1024]{1,0:T(8,128)(2,1)} %get-tuple-element.48), channel_id=1, source_target_pairs={{0,16},{4,20},{8,24},{12,28},{16,0},{20,4},{24,8},{28,12},{1,17},{... | collective-permute-start | bytes 344072 | tf_op jit(solution)/shard_map/ppermute | solution.py:416
  30.6 29.2 %collective-permute-start.9 = (bf16[8,64,512]{2,1,0:T(8,128)(2,1)}, bf16[8,64,512]{2,1,0:T(8,128)(2,1)S(1)}, u32[]{:S(2)}, u32[]{:S(2)}) collective-permute-start(bf16[8,64,512]{2,1,0:T(8,128)(2,1)} %all_to_all.10.refs_0_.own_ref.x_ref.refs_4_), channel_id=1, source_target_pairs={{0,1},{1,0},{2,3},{3,2},{4,5},{5,4},{6,7},{7,6},{8,9},{9,8},{10,11... | collective-permute-start | bytes 1572872 | tf_op jit(solution)/shard_map/ppermute | solution.py:416
  30.6 16.1 %collective-permute-start.4 = (bf16[56,1024]{1,0:T(8,128)(2,1)}, bf16[56,1024]{1,0:T(8,128)(2,1)S(1)}, u32[]{:S(2)}, u32[]{:S(2)}) collective-permute-start(bf16[56,1024]{1,0:T(8,128)(2,1)} %get-tuple-element.49), channel_id=1, source_target_pairs={{0,20},{4,16},{8,28},{12,24},{16,4},{20,0},{24,12},{28,8},{1,21},{... | collective-permute-start | bytes 344072 | tf_op jit(solution)/shard_map/ppermute | solution.py:416
  33.3 13.4 %collective-permute-start.5 = (bf16[56,1024]{1,0:T(8,128)(2,1)}, bf16[56,1024]{1,0:T(8,128)(2,1)S(1)}, u32[]{:S(2)}, u32[]{:S(2)}) collective-permute-start(bf16[56,1024]{1,0:T(8,128)(2,1)} %get-tuple-element.50), channel_id=1, source_target_pairs={{0,24},{4,28},{8,16},{12,20},{16,8},{20,12},{24,0},{28,4},{1,25},{... | collective-permute-start | bytes 344072 | tf_op jit(solution)/shard_map/ppermute | solution.py:416
  42.3 7.9 %collective-permute-start.6 = (bf16[56,1024]{1,0:T(8,128)(2,1)}, bf16[56,1024]{1,0:T(8,128)(2,1)S(1)}, u32[]{:S(2)}, u32[]{:S(2)}) collective-permute-start(bf16[56,1024]{1,0:T(8,128)(2,1)} %get-tuple-element.51), channel_id=1, source_target_pairs={{0,28},{4,24},{8,20},{12,16},{16,12},{20,8},{24,4},{28,0},{1,29},{... | collective-permute-start | bytes 344072 | tf_op jit(solution)/shard_map/ppermute | solution.py:416
  44.2 19.9 %collective-permute-start.11 = (bf16[8,64,512]{2,1,0:T(8,128)(2,1)}, bf16[8,64,512]{2,1,0:T(8,128)(2,1)S(1)}, u32[]{:S(2)}, u32[]{:S(2)}) collective-permute-start(bf16[8,64,512]{2,1,0:T(8,128)(2,1)} %collective-permute-done.10.refs_0_.refs_2_), channel_id=1, source_target_pairs={{0,1},{1,0},{2,3},{3,2},{4,5},{5,4},{6,7},{7,6},{8,9},{9,8},{10,11... | collective-permute-start | bytes 1572872 | tf_op jit(solution)/shard_map/ppermute | solution.py:416
  46.8 5.8 %collective-permute-start = (bf16[56,1024]{1,0:T(8,128)(2,1)}, bf16[56,1024]{1,0:T(8,128)(2,1)S(1)}, u32[]{:S(2)}, u32[]{:S(2)}) collective-permute-start(bf16[56,1024]{1,0:T(8,128)(2,1)} %get-tuple-element.45), channel_id=1, source_target_pairs={{0,4},{4,0},{8,12},{12,8},{16,20},{20,16},{24,28},{28,24},{1,5},{5... | collective-permute-start | bytes 344072 | tf_op jit(solution)/shard_map/ppermute | solution.py:416
  46.8 7.0 %collective-permute-start.1 = (bf16[56,1024]{1,0:T(8,128)(2,1)}, bf16[56,1024]{1,0:T(8,128)(2,1)S(1)}, u32[]{:S(2)}, u32[]{:S(2)}) collective-permute-start(bf16[56,1024]{1,0:T(8,128)(2,1)} %get-tuple-element.46), channel_id=1, source_target_pairs={{0,8},{4,12},{8,0},{12,4},{16,24},{20,28},{24,16},{28,20},{1,9},{5... | collective-permute-start | bytes 344072 | tf_op jit(solution)/shard_map/ppermute | solution.py:416
  50.2 5.9 %collective-permute-start.2 = (bf16[56,1024]{1,0:T(8,128)(2,1)}, bf16[56,1024]{1,0:T(8,128)(2,1)S(1)}, u32[]{:S(2)}, u32[]{:S(2)}) collective-permute-start(bf16[56,1024]{1,0:T(8,128)(2,1)} %get-tuple-element.47), channel_id=1, source_target_pairs={{0,12},{4,8},{8,4},{12,0},{16,28},{20,24},{24,20},{28,16},{1,13},{... | collective-permute-start | bytes 344072 | tf_op jit(solution)/shard_map/ppermute | solution.py:416
  52.6 7.2 %copy-start.4 = (bf16[4,56,1024]{2,1,0:T(8,128)(2,1)}, bf16[4,56,1024]{2,1,0:T(8,128)(2,1)S(1)}, u32[]{:S(2)}) copy-start(bf16[4,56,1024]{2,1,0:T(8,128)(2,1)S(1)} %shard_map.145) | copy-start | bytes 1376260
  52.6 13.8 %collective-permute-start.8 = (bf16[224,1024]{1,0:T(8,128)(2,1)S(1)}, bf16[224,1024]{1,0:T(8,128)(2,1)S(1)}, u32[]{:S(2)}, u32[]{:S(2)}) collective-permute-start(bf16[224,1024]{1,0:T(8,128)(2,1)S(1)} %bitcast.35), channel_id=1, source_target_pairs={{0,1},{1,0},{2,3},{3,2},{4,5},{5,4},{6,7},{7,6},{8,9},{9,8},{10,11... | collective-permute-start | bytes 1376264 | tf_op jit(solution)/shard_map/ppermute | solution.py:416
  56.1 0.9 copy-start.14
  57.0 2.8 %copy-start.1 = (bf16[1,2048,512]{2,1,0:T(8,128)(2,1)S(1)}, bf16[1,2048,512]{2,1,0:T(8,128)(2,1)}, u32[]{:S(2)}) copy-start(bf16[1,2048,512]{2,1,0:T(8,128)(2,1)} %param.11) | copy-start | bytes 6291460
  57.1 5.3 %copy-start.5 = (bf16[4,56,1024]{2,1,0:T(8,128)(2,1)}, bf16[4,56,1024]{2,1,0:T(8,128)(2,1)S(1)}, u32[]{:S(2)}) copy-start(bf16[4,56,1024]{2,1,0:T(8,128)(2,1)S(1)} %shard_map.144) | copy-start | bytes 1376260
  57.1 3.0 %copy-start = (bf16[1,2048,512]{2,1,0:T(8,128)(2,1)S(1)}, bf16[1,2048,512]{2,1,0:T(8,128)(2,1)}, u32[]{:S(2)}) copy-start(bf16[1,2048,512]{2,1,0:T(8,128)(2,1)} %param.10) | copy-start | bytes 6291460
  57.1 9.3 %collective-permute-start.7 = (bf16[224,1024]{1,0:T(8,128)(2,1)S(1)}, bf16[224,1024]{1,0:T(8,128)(2,1)S(1)}, u32[]{:S(2)}, u32[]{:S(2)}) collective-permute-start(bf16[224,1024]{1,0:T(8,128)(2,1)S(1)} %bitcast.38), channel_id=1, source_target_pairs={{0,1},{1,0},{2,3},{3,2},{4,5},{5,4},{6,7},{7,6},{8,9},{9,8},{10,11... | collective-permute-start | bytes 1376264 | tf_op jit(solution)/shard_map/ppermute | solution.py:416
  57.2 1.8 %copy-start.2 = (bf16[1,512,2048]{2,1,0:T(8,128)(2,1)S(1)}, bf16[1,512,2048]{2,1,0:T(8,128)(2,1)}, u32[]{:S(2)}) copy-start(bf16[1,512,2048]{2,1,0:T(8,128)(2,1)} %param.12) | copy-start | bytes 6291460
  59.8 2.5 %copy-start.8 = (bf16[8,64,512]{2,1,0:T(8,128)(2,1)}, bf16[8,64,512]{2,1,0:T(8,128)(2,1)S(1)}, u32[]{:S(2)}) copy-start(bf16[8,64,512]{2,1,0:T(8,128)(2,1)S(1)} %collective-permute-done.9.refs_1_) | copy-start | bytes 1572868
  64.1 2.3 %copy-start.7 = (bf16[8,64,512]{2,1,0:T(8,128)(2,1)}, bf16[8,64,512]{2,1,0:T(8,128)(2,1)S(1)}, u32[]{:S(2)}) copy-start(bf16[8,64,512]{2,1,0:T(8,128)(2,1)S(1)} %collective-permute-done.11.refs_0_.refs_3_) | copy-start | bytes 1572868
  64.1 2.3 %copy-start.3 = (bf16[1,512,2048]{2,1,0:T(8,128)(2,1)S(1)}, bf16[1,512,2048]{2,1,0:T(8,128)(2,1)}, u32[]{:S(2)}) copy-start(bf16[1,512,2048]{2,1,0:T(8,128)(2,1)} %param.12) | copy-start | bytes 6291460
  66.4 2.1 %copy-start.12 = (bf16[8,56,512]{2,1,0:T(8,128)(2,1)}, bf16[8,56,512]{2,1,0:T(8,128)(2,1)S(1)}, u32[]{:S(2)}) copy-start(bf16[8,56,512]{2,1,0:T(8,128)(2,1)S(1)} %get-tuple-element.57) | copy-start | bytes 1376260
  66.4 2.1 %copy-start.10 = (bf16[224,1024]{1,0:T(8,128)(2,1)}, bf16[224,1024]{1,0:T(8,128)(2,1)S(1)}, u32[]{:S(2)}) copy-start(bf16[224,1024]{1,0:T(8,128)(2,1)S(1)} %collective-permute-done.8.far_ref.refs_3_) | copy-start | bytes 1376260
  66.4 2.1 %copy-start.11 = (bf16[224,1024]{1,0:T(8,128)(2,1)}, bf16[224,1024]{1,0:T(8,128)(2,1)S(1)}, u32[]{:S(2)}) copy-start(bf16[224,1024]{1,0:T(8,128)(2,1)S(1)} %collective-permute-done.7.near_ref.refs_2_) | copy-start | bytes 1376260
  68.5 1.9 %copy-start.6 = (bf16[8,64,1024]{2,1,0:T(8,128)(2,1)}, bf16[8,64,1024]{2,1,0:T(8,128)(2,1)S(1)}, u32[]{:S(2)}) copy-start(bf16[8,64,1024]{2,1,0:T(8,128)(2,1)S(1)} %get-tuple-element.60.g_ref.refs_4_) | copy-start | bytes 3145732
  68.5 1.9 %collective-permute-start.15 = (bf16[1,448,512]{2,1,0:T(8,128)(2,1)S(1)}, bf16[1,448,512]{2,1,0:T(8,128)(2,1)S(1)}, u32[]{:S(2)}, u32[]{:S(2)}) collective-permute-start(bf16[1,448,512]{2,1,0:T(8,128)(2,1)S(1)} %get-tuple-element.66), channel_id=1, source_target_pairs={{0,1},{1,0},{2,3},{3,2},{4,5},{5,4},{6,7},{7,6},{8,9},{9,8},{10,11... | collective-permute-start | bytes 1376264 | tf_op jit(solution)/shard_map/ppermute | solution.py:416
  68.9 16.7 %collective-permute-start.12 = (bf16[448,512]{1,0:T(8,128)(2,1)S(1)}, bf16[448,512]{1,0:T(8,128)(2,1)S(1)}, u32[]{:S(2)}, u32[]{:S(2)}) collective-permute-start(bf16[448,512]{1,0:T(8,128)(2,1)S(1)} %get-tuple-element.62), channel_id=1, source_target_pairs={{0,1},{1,0},{2,3},{3,2},{4,5},{5,4},{6,7},{7,6},{8,9},{9,8},{10,11... | collective-permute-start | bytes 1376264 | tf_op jit(solution)/shard_map/ppermute | solution.py:416
  70.4 15.1 %copy-start.13 = (bf16[2048,8]{0,1:T(8,128)(2,1)S(1)}, bf16[2048,8]{0,1:T(8,128)(2,1)}, u32[]{:S(2)}) copy-start(bf16[2048,8]{0,1:T(8,128)(2,1)} %param.9) | copy-start | bytes 98308
  70.6 15.0 %collective-permute-start.16 = (bf16[448,512]{1,0:T(8,128)(2,1)S(1)}, bf16[448,512]{1,0:T(8,128)(2,1)S(1)}, u32[]{:S(2)}, u32[]{:S(2)}) collective-permute-start(bf16[448,512]{1,0:T(8,128)(2,1)S(1)} %bitcast.43), channel_id=1, source_target_pairs={{0,2},{1,3},{2,0},{3,1},{4,6},{5,7},{6,4},{7,5},{8,10},{9,11},{10,... | collective-permute-start | bytes 1376264 | tf_op jit(solution)/shard_map/ppermute | solution.py:416
  71.1 1.2 collective-permute-start.13
  72.3 11.1 %collective-permute-start.14 = (f32[8,128]{1,0:T(8,128)S(1)}, f32[8,128]{1,0:T(8,128)S(1)}, u32[]{:S(2)}, u32[]{:S(2)}) collective-permute-start(f32[8,128]{1,0:T(8,128)S(1)} %shard_map.152.a_ref), channel_id=1, source_target_pairs={{0,2},{1,3},{2,0},{3,1},{4,6},{5,7},{6,4},{7,5},{8,10},{9,11},{10,... | collective-permute-start | bytes 12296 | tf_op jit(solution)/shard_map/ppermute | solution.py:416
  86.6 23.1 %all-to-all-start.1 = ((bf16[8,56,512]{2,1,0:T(8,128)(2,1)}), bf16[8,56,512]{2,1,0:T(8,128)(2,1)}, u32[]{:S(2)}, u32[]{:S(2)}) async-start(bf16[8,56,512]{2,1,0:T(8,128)(2,1)} %bitcast.11), calls=%async_computation.1 | async-start | bytes 917504 | tf_op jit(solution)/shard_map/all_to_all | solution.py:419
  91.2 6.9 %copy-start.15 = (f32[8,128]{1,0:T(8,128)S(1)}, f32[8,128]{1,0:T(8,128)}, u32[]{:S(2)}) copy-start(f32[8,128]{1,0:T(8,128)} %get-tuple-element.43.place_ref) | copy-start | bytes 12292
  97.6 4.1 %collective-permute-start.24 = (f32[2,2048]{1,0:T(2,128)}, f32[2,2048]{1,0:T(2,128)}, u32[]{:S(2)}, u32[]{:S(2)}) collective-permute-start(f32[2,2048]{1,0:T(2,128)} %bitcast.48), channel_id=1, source_target_pairs={{0,2},{1,3},{2,0},{3,1},{4,6},{5,7},{6,4},{7,5},{8,10},{9,11},{10,... | collective-permute-start | bytes 49160 | tf_op jit(solution)/shard_map/ppermute | solution.py:416
  98.1 0.6 copy-start.9
  98.8 13.6 %collective-permute-start.23 = (f32[2,2048]{1,0:T(2,128)}, f32[2,2048]{1,0:T(2,128)}, u32[]{:S(2)}, u32[]{:S(2)}) collective-permute-start(f32[2,2048]{1,0:T(2,128)} %bitcast.49), channel_id=1, source_target_pairs={{0,1},{1,0},{2,3},{3,2},{4,5},{5,4},{6,7},{7,6},{8,9},{9,8},{10,11... | collective-permute-start | bytes 49160 | tf_op jit(solution)/shard_map/ppermute | solution.py:416
  98.8 7.8 %collective-permute-start.20 = (f32[8,512]{1,0:T(8,128)}, f32[8,512]{1,0:T(8,128)}, u32[]{:S(2)}, u32[]{:S(2)}) collective-permute-start(f32[8,512]{1,0:T(8,128)} %get-tuple-element.69.a_ref), channel_id=1, source_target_pairs={{0,4},{4,0},{8,12},{12,8},{16,20},{20,16},{24,28},{28,24},{1,5},{5... | collective-permute-start | bytes 49160 | tf_op jit(solution)/shard_map/ppermute | solution.py:416
  101.6 10.7 %collective-permute-start.25 = (f32[2,2048]{1,0:T(2,128)}, f32[2,2048]{1,0:T(2,128)}, u32[]{:S(2)}, u32[]{:S(2)}) collective-permute-start(f32[2,2048]{1,0:T(2,128)} %collective-permute-done.24), channel_id=1, source_target_pairs={{0,1},{1,0},{2,3},{3,2},{4,5},{5,4},{6,7},{7,6},{8,9},{9,8},{10,11... | collective-permute-start | bytes 49160 | tf_op jit(solution)/shard_map/ppermute | solution.py:416
  107.9 5.2 %collective-permute-start.21 = (f32[8,512]{1,0:T(8,128)}, f32[8,512]{1,0:T(8,128)}, u32[]{:S(2)}, u32[]{:S(2)}) collective-permute-start(f32[8,512]{1,0:T(8,128)} %shard_map.158.a_ref), channel_id=1, source_target_pairs={{0,8},{4,12},{8,0},{12,4},{16,24},{20,28},{24,16},{28,20},{1,9},{5... | collective-permute-start | bytes 49160 | tf_op jit(solution)/shard_map/ppermute | solution.py:416
  111.7 5.9 %collective-permute-start.18 = (bf16[128,512]{1,0:T(8,128)(2,1)}, bf16[128,512]{1,0:T(8,128)(2,1)S(1)}, u32[]{:S(2)}, u32[]{:S(2)}) collective-permute-start(bf16[128,512]{1,0:T(8,128)(2,1)} %get-tuple-element.68), channel_id=1, source_target_pairs={{0,2},{1,3},{2,0},{3,1},{4,6},{5,7},{6,4},{7,5},{8,10},{9,11},{10,... | collective-permute-start | bytes 393224 | tf_op jit(solution)/shard_map/ppermute | solution.py:416
  113.9 4.6 %collective-permute-start.22 = (f32[8,512]{1,0:T(8,128)S(1)}, f32[8,512]{1,0:T(8,128)S(1)}, u32[]{:S(2)}, u32[]{:S(2)}) collective-permute-start(f32[8,512]{1,0:T(8,128)S(1)} %shard_map.159.a_ref), channel_id=1, source_target_pairs={{0,16},{4,20},{8,24},{12,28},{16,0},{20,4},{24,8},{28,12},{1,17},{... | collective-permute-start | bytes 49160 | tf_op jit(solution)/shard_map/ppermute | solution.py:416
  116.2 2.9 %collective-permute-start.17 = (bf16[128,512]{1,0:T(8,128)(2,1)}, bf16[128,512]{1,0:T(8,128)(2,1)S(1)}, u32[]{:S(2)}, u32[]{:S(2)}) collective-permute-start(bf16[128,512]{1,0:T(8,128)(2,1)} %get-tuple-element.68), channel_id=1, source_target_pairs={{0,1},{1,0},{2,3},{3,2},{4,5},{5,4},{6,7},{7,6},{8,9},{9,8},{10,11... | collective-permute-start | bytes 393224 | tf_op jit(solution)/shard_map/ppermute | solution.py:416
  117.6 1.5 %collective-permute-start.19 = (bf16[128,512]{1,0:T(8,128)(2,1)S(1)}, bf16[128,512]{1,0:T(8,128)(2,1)S(1)}, u32[]{:S(2)}, u32[]{:S(2)}) collective-permute-start(bf16[128,512]{1,0:T(8,128)(2,1)S(1)} %collective-permute-done.18.refs_2_), channel_id=1, source_target_pairs={{0,1},{1,0},{2,3},{3,2},{4,5},{5,4},{6,7},{7,6},{8,9},{9,8},{10,11... | collective-permute-start | bytes 393224 | tf_op jit(solution)/shard_map/ppermute | solution.py:416

commit v6 on v5

--- a/solution.py
+++ b/solution.py
@@ -175,13 +175,14 @@
     return jnp.concatenate([tile[:, g : g + 1] for g in range(slots // 8)], axis=0)
 
 
-def back_kernel(groups, near_hbm, far_hbm, wd_hbm, back_ref):
-    cols = near_hbm.shape[1]
+def back_kernel(groups, near_ref, far_ref, near_got, wd_ref, back_ref):
+    cols = near_ref.shape[1]
     side, _ = half_of(groups)
-    start = pl.multiple_of((lax.axis_index("tp") % 2) * cols, 128)
-    wd = wd_hbm[:, pl.ds(start, cols)]
-    back_ref[side] = dot(near_hbm[...], wd, 1, 1)
-    back_ref[1 - side] = dot(far_hbm[...], wd, 1, 1)
+    core = lax.axis_index("tp") % 2
+    own = wd_ref[:, pl.ds(pl.multiple_of(core * cols, 128), cols)]
+    other = wd_ref[:, pl.ds(pl.multiple_of((core ^ 1) * cols, 128), cols)]
+    back_ref[1 - side] = dot(far_ref[...], own, 1, 1)
+    back_ref[side] = dot(near_ref[...], own, 1, 1) + dot(near_got[...], other, 1, 1)
 
 
 def slot_parts(first, gg, gu, wg_ref, wu_ref, shares):
@@ -193,15 +194,15 @@
 
 
 def middle_kernel(
-    slots, shares, back_ref, near_ref, far_ref, wd_ref, hid_ref, up_ref, gate_ref, wg_ref, wu_ref,
-    g_ref, home_ref, chip_ref, term_ref, sum_ref,
+    slots, shares, back_ref, far_ref, wd_ref, hid_ref, up_ref, gate_ref, wg_ref, wu_ref,
+    g_ref, chip_ref, term_ref, sum_ref,
 ):
-    cols = near_ref.shape[1]
+    cols = far_ref.shape[1]
     groups = g_ref.shape[0]
     side, _ = half_of(groups)
     start = pl.multiple_of(((lax.axis_index("tp") % 2) ^ 1) * cols, 128)
     wd = wd_ref[:, pl.ds(start, cols)]
-    sum_ref[side] = back_ref[side] + dot(near_ref[...], wd, 1, 1)
+    sum_ref[side] = back_ref[side]
     sum_ref[1 - side] = back_ref[1 - side] + dot(far_ref[...], wd, 1, 1)
     back = sum_ref[...].reshape(hid_ref.shape)
     hidden = hid_ref.shape[1]
@@ -220,42 +221,48 @@
     term_ref[...] = tile
     gg = gg.astype(BF16)
     gu = gu.astype(BF16)
-    for j in range(shares // 2):
-        part = slot_parts(2 * j + 1, gg, gu, wg_ref, wu_ref, shares)
-        if j == 0:
-            home_ref[...] = part.astype(BF16)
-        else:
-            chip_ref[j - 1] = part.astype(BF16)
-
-
-def even_kernel(slots, shares, g_ref, wg_ref, wu_ref, home_ref, chip_ref):
+    for j in range(1, shares // 2):
+        chip_ref[j - 1] = slot_parts(2 * j + 1, gg, gu, wg_ref, wu_ref, shares).astype(BF16)
+
+
+def even_kernel(slots, shares, g_ref, wg_ref, wu_ref, chip_ref):
     groups, span, double = g_ref.shape
     both = g_ref[...].reshape(groups * span, double)
     gg, gu = both[:, : double // 2], both[:, double // 2 :]
-    for j in range(shares // 2):
+    for j in range(1, shares // 2):
         part = slot_parts(2 * j, gg, gu, wg_ref, wu_ref, shares)
         for e in range(groups):
+            chip_ref[j - 1, e * slots : (e + 1) * slots, :] = part[e * span : e * span + slots, :]
+
+
+def rest_kernel(slots, shares, g_ref, wg_ref, wu_ref, odd_ref, even_ref):
+    groups, span, double = g_ref.shape
+    both = g_ref[...].reshape(groups * span, double)
+    gg, gu = both[:, : double // 2], both[:, double // 2 :]
+    for r, out_ref in enumerate((even_ref, odd_ref)):
+        part = slot_parts(r, gg, gu, wg_ref, wu_ref, shares)
+        for e in range(groups):
             block = part[e * span : e * span + slots, :]
-            if j == 0:
-                home_ref[e * slots : (e + 1) * slots, :] = block
-            else:
-                chip_ref[j - 1, e * slots : (e + 1) * slots, :] = block
+            out_ref[e] = block.astype(out_ref.dtype)
 
 
 def add_core_kernel(own_ref, got_ref, out_ref):
     out_ref[...] = (own_ref[...] + got_ref[...].astype(F32)).astype(BF16)
 
 
-def add_chip_kernel(own_ref, core_ref, table_ref, router_ref, *refs):
-    out_ref = refs[-1]
+def base_kernel(own_ref, core_ref, table_ref, router_ref, out_ref):
     experts = router_ref.shape[0]
     cols = out_ref.shape[1]
     start = pl.multiple_of(lax.axis_index("tp") * cols, 128)
     total = own_ref[...] + core_ref[...].astype(F32)
-    total = total + dot(table_ref[...][:, :experts].astype(BF16), router_ref[:, pl.ds(start, cols)])
+    out_ref[...] = total + dot(table_ref[...][:, :experts].astype(BF16), router_ref[:, pl.ds(start, cols)])
+
+
+def add_chip_kernel(base_ref, *refs):
+    total = base_ref[...]
     for chip_ref in refs[:-1]:
         total = total + chip_ref[...].astype(F32)
-    out_ref[...] = total.astype(BF16)
+    refs[-1][...] = total.astype(BF16)
 
 
 def grads_kernel(shares, q_ref, *refs):
@@ -462,37 +469,37 @@
     gate_factor = gate_factor.reshape(count, hidden)
 
     side = groups // 2
-    near = call(
-        join_kernel, shape(side, slots, half), False, *pieces[:side],
-    ).reshape(count // 2, half)
+    near = call(join_kernel, shape(side, slots, half), False, *pieces[:side]).reshape(count // 2, half)
     near_got = swap(near, 1)
-    far = call(
-        join_kernel, shape(side, slots, half), False, *pieces[side:],
-    ).reshape(count // 2, half)
+    far = call(join_kernel, shape(side, slots, half), False, *pieces[side:]).reshape(count // 2, half)
     far_got = swap(far, 1)
     back = call(
         functools.partial(back_kernel, groups), shape(2, count // 2, hidden, dtype=F32),
-        False, near, far, wd, flops=unit,
-    )
-    g, odd_home, odd_chip, term = call(
+        False, near, far, near_got, wd, flops=unit,
+    )
+    g, odd_chip, term = call(
         functools.partial(middle_kernel, slots, shares),
         (
             shape(groups, span, 2 * hidden),
-            shape(count, cols),
             shape(chips - 1, count, cols),
             shape(8, -(-count // 1024) * 128, dtype=F32),
         ),
-        False, back, near_got, far_got, wd, hid, up_factor, gate_factor, wg, wu, flops=3 * unit,
+        False, back, far_got, wd, hid, up_factor, gate_factor, wg, wu, flops=3 * unit,
         scratch=[buffer(2, count // 2, hidden, dtype=F32)],
     )
     term_got = swap(term, 1)
     core_chip = swap(odd_chip, 1)
-    core_home = swap(odd_home, 1)
-    even_home, even_chip = call(
-        functools.partial(even_kernel, slots, shares),
-        (shape(count, cols, dtype=F32), shape(chips - 1, count, cols, dtype=F32)),
+    even_chip = call(
+        functools.partial(even_kernel, slots, shares), shape(chips - 1, count, cols, dtype=F32),
+        False, g, wg, wu, flops=unit,
+    )
+    odd_home, even_home = call(
+        functools.partial(rest_kernel, slots, shares),
+        (shape(groups, slots, cols), shape(groups, slots, cols, dtype=F32)),
         False, g, wg, wu, flops=2 * unit,
     )
+    even_home = even_home.reshape(count, cols)
+    core_home = swap(odd_home.reshape(count, cols), 1)
 
     def add(a, b, kernel=add_kernel, lead=()):
         return call(kernel, shape(*lead, *a.shape, dtype=F32), False, a, b)
@@ -521,9 +528,8 @@
         False, router_sum, router_got,
     )
     router_rows = router_rows.reshape(cols)
-    home_send = call(
-        add_chip_kernel, shape(count, cols), False, even_home, core_home, table, router, *chip_got,
-    )
+    base = call(base_kernel, shape(count, cols, dtype=F32), False, even_home, core_home, table, router)
+    home_send = call(add_chip_kernel, shape(count, cols), False, base, *chip_got)
     home_got = exchange(home_send.reshape(groups, slots, cols)).reshape(count, cols)
 
     grad_spec = pl.BlockSpec((cols, hidden), lambda r, q: (q[0] ^ r, 0))

time: 121 us -> 122 us (level)
  waiting for transfers between devices: 27.2 us -> 25.2 us
  starting transfers between devices: 28.9 us -> 30.6 us
    ppermute x26, waiting for transfers between devices: 27.2 us -> 25.2 us  [swap(): return lax.ppermute(value, axis, [(i, i ^ bit) for i in range(size)])]
    ppermute x26, starting transfers between devices: 24.4 us -> 26.3 us  [swap(): return lax.ppermute(value, axis, [(i, i ^ bit) for i in range(size)])]
    pallas_call x19 -> x21, Pallas kernels: 23.9 us -> 24.1 us  [call(): pl.pallas_call(kernel, out_shape=outs, in_specs=([SMEM] if scalar else []...]
  transfers between devices with their start and end apart: 27 -> 27, of which waited for: 9 -> 9; matrix products, arithmetic and copies ran while one was open for 1% -> 1% of each run, Pallas kernels for 24% -> 25%
where the time goes in v6:
time: 122 us; the launch traced here: 121 us
  Pallas kernels  36 us (30%)
  starting transfers between devices  30.6 us (25%)
  waiting for transfers between devices  25.2 us (21%)
  blocking collectives  21.9 us (18%)
  local copies, waits for them, and re-layouts  5.29 us (4%)
    ppermute x26, starting transfers between devices, swap(): return lax.ppermute(value, axis, [(i, i ^ bit) for i in range(size)])  26.3 us
    ppermute x26, waiting for transfers between devices, swap(): return lax.ppermute(value, axis, [(i, i ^ bit) for i in range(size)])  25.2 us
    pallas_call x21, Pallas kernels, call(): pl.pallas_call(kernel, out_shape=outs, in_specs=([SMEM] if scalar else []...  24.1 us
    all_to_all x1, blocking collectives, exchange(): return lax.all_to_all(value, 'ep', split_axis=0, concat_axis=0, tiled=True)  21.9 us
    pallas_call x1, Pallas kernels, layer(): pl.pallas_call(functools.partial(grads_kernel, shares), out_shape=(shape(...  6.38 us
    pallas_call x1, Pallas kernels, layer(): pl.pallas_call(functools.partial(down_kernel, slots), out_shape=(shape(hi...  4.71 us
    unnamed x32, local copies, waits for them, and re-layouts  4.68 us
    all_to_all x1, starting transfers between devices, exchange(): return lax.all_to_all(value, 'ep', split_axis=0, concat_axis=0, tiled=True)  4.29 us
  transfers between devices with their start and end apart: 27, of which 9 were waited for; matrix products, arithmetic and copies ran while one was open for 1% of the time, Pallas kernels for 25%

profile of v6, /device:TPU:0, one launch (start us, length us, event | category | flops | bytes accessed | tf_op | source)
XLA Modules:
  0.0 121.0 jit_solution(94806605114693761)
XLA Ops:
  0.6 2.6 %shard_map.142 = (bf16[8,64,512]{2,1,0:T(8,128)(2,1)}, f32[8,128]{1,0:T(8,128)}) custom-call(bf16[128,2048]{1,0:T(8,128)(2,1)} %tok_hbm.1, s32[2,128]{1,0:T(2,128)} %bitcast.57, bf16[8,2048]{1,0:T(8,128)(2,1)} %bitcast.51), custom_call_target="tpu_custom_call" | custom-call | tf_op jit(solution)/shard_map/pallas_call | solution.py:378
  3.2 21.9 %all_to_all.10.refs_0_.own_ref.x_ref.refs_4_ = bf16[8,64,512]{2,1,0:T(8,128)(2,1)} all-to-all(bf16[8,64,512]{2,1,0:T(8,128)(2,1)} %get-tuple-element.51), channel_id=1, replica_groups=mesh['ep'=8,'tp'=4] {'ep'}, dimensions={0} | all-to-all | bytes 1048576 | tf_op jit(solution)/shard_map/all_to_all | solution.py:426
  25.1 1.5 %collective-permute-start.10 = (bf16[8,64,512]{2,1,0:T(8,128)(2,1)}, bf16[8,64,512]{2,1,0:T(8,128)(2,1)}, u32[]{:S(2)}, u32[]{:S(2)}) collective-permute-start(bf16[8,64,512]{2,1,0:T(8,128)(2,1)} %all_to_all.10.refs_0_.own_ref.x_ref.refs_4_), channel_id=1, source_target_pairs={{0,2},{1,3},{2,0},{3,1},{4,6},{5,7},{6,4},{7,5},{8,10},{9,11},{10,... | collective-permute-start | bytes 1572872 | tf_op jit(solution)/shard_map/ppermute | solution.py:423
  26.6 2.8 %shard_map.143 = (bf16[56,1024]{1,0:T(8,128)(2,1)}, bf16[56,1024]{1,0:T(8,128)(2,1)}, bf16[56,1024]{1,0:T(8,128)(2,1)}, bf16[56,1024]{1,0:T(8,128)(2,1)}, bf16[5...) custom-call(bf16[128,2048]{1,0:T(8,128)(2,1)} %cot_hbm.1, ...), custom_call_target="tpu_custom_call" | custom-call | flops 117440512 | tf_op jit(solution)/shard_map/pallas_call | solution.py:378
  29.5 1.5 %collective-permute-start = (bf16[56,1024]{1,0:T(8,128)(2,1)}, bf16[56,1024]{1,0:T(8,128)(2,1)S(1)}, u32[]{:S(2)}, u32[]{:S(2)}) collective-permute-start(bf16[56,1024]{1,0:T(8,128)(2,1)} %get-tuple-element.44), channel_id=1, source_target_pairs={{0,4},{4,0},{8,12},{12,8},{16,20},{20,16},{24,28},{28,24},{1,5},{5... | collective-permute-start | bytes 344072 | tf_op jit(solution)/shard_map/ppermute | solution.py:423
  31.0 2.1 %collective-permute-start.2 = (bf16[56,1024]{1,0:T(8,128)(2,1)}, bf16[56,1024]{1,0:T(8,128)(2,1)S(1)}, u32[]{:S(2)}, u32[]{:S(2)}) collective-permute-start(bf16[56,1024]{1,0:T(8,128)(2,1)} %get-tuple-element.46), channel_id=1, source_target_pairs={{0,12},{4,8},{8,4},{12,0},{16,28},{20,24},{24,20},{28,16},{1,13},{... | collective-permute-start | bytes 344072 | tf_op jit(solution)/shard_map/ppermute | solution.py:423
  33.0 2.6 %collective-permute-done.refs_1_ = bf16[56,1024]{1,0:T(8,128)(2,1)S(1)} collective-permute-done((bf16[56,1024]{1,0:T(8,128)(2,1)}, bf16[56,1024]{1,0:T(8,128)(2,1)S(1)}, u32[]{:S(2)}, u32[]{:S(2)}) %collective-permute-start) | collective-permute-done | bytes 114720 | tf_op jit(solution)/shard_map/ppermute | solution.py:423
  35.7 0.8 collective-permute-start.3
  36.4 3.1 %collective-permute-start.4 = (bf16[56,1024]{1,0:T(8,128)(2,1)}, bf16[56,1024]{1,0:T(8,128)(2,1)S(1)}, u32[]{:S(2)}, u32[]{:S(2)}) collective-permute-start(bf16[56,1024]{1,0:T(8,128)(2,1)} %get-tuple-element.48), channel_id=1, source_target_pairs={{0,20},{4,16},{8,28},{12,24},{16,4},{20,0},{24,12},{28,8},{1,21},{... | collective-permute-start | bytes 344072 | tf_op jit(solution)/shard_map/ppermute | solution.py:423
  39.5 0.9 copy-done.14
  40.5 0.1 collective-permute-start.7
  40.5 0.5 collective-permute-start.11
  41.0 4.4 %collective-permute-done.3.refs_0_ = bf16[56,1024]{1,0:T(8,128)(2,1)S(1)} collective-permute-done((bf16[56,1024]{1,0:T(8,128)(2,1)}, bf16[56,1024]{1,0:T(8,128)(2,1)S(1)}, u32[]{:S(2)}, u32[]{:S(2)}) %collective-permute-start.3) | collective-permute-done | bytes 114720 | tf_op jit(solution)/shard_map/ppermute | solution.py:423
  45.4 3.5 %collective-permute-start.5 = (bf16[56,1024]{1,0:T(8,128)(2,1)}, bf16[56,1024]{1,0:T(8,128)(2,1)S(1)}, u32[]{:S(2)}, u32[]{:S(2)}) collective-permute-start(bf16[56,1024]{1,0:T(8,128)(2,1)} %get-tuple-element.49), channel_id=1, source_target_pairs={{0,24},{4,28},{8,16},{12,20},{16,8},{20,12},{24,0},{28,4},{1,25},{... | collective-permute-start | bytes 344072 | tf_op jit(solution)/shard_map/ppermute | solution.py:423
  49.0 3.1 %collective-permute-start.6 = (bf16[56,1024]{1,0:T(8,128)(2,1)}, bf16[56,1024]{1,0:T(8,128)(2,1)S(1)}, u32[]{:S(2)}, u32[]{:S(2)}) collective-permute-start(bf16[56,1024]{1,0:T(8,128)(2,1)} %get-tuple-element.50), channel_id=1, source_target_pairs={{0,28},{4,24},{8,20},{12,16},{16,12},{20,8},{24,4},{28,0},{1,29},{... | collective-permute-start | bytes 344072 | tf_op jit(solution)/shard_map/ppermute | solution.py:423
  52.0 0.7 collective-permute-done.5.refs_2_
  52.7 4.1 %collective-permute-done.6.refs_3_ = bf16[56,1024]{1,0:T(8,128)(2,1)S(1)} collective-permute-done((bf16[56,1024]{1,0:T(8,128)(2,1)}, bf16[56,1024]{1,0:T(8,128)(2,1)S(1)}, u32[]{:S(2)}, u32[]{:S(2)}) %collective-permute-start.6) | collective-permute-done | bytes 114720 | tf_op jit(solution)/shard_map/ppermute | solution.py:423
  56.8 0.1 collective-permute-start.8
  56.9 0.0 copy-start.2
  56.9 1.8 %copy-done.2 = bf16[1,512,2048]{2,1,0:T(8,128)(2,1)S(1)} copy-done((bf16[1,512,2048]{2,1,0:T(8,128)(2,1)S(1)}, bf16[1,512,2048]{2,1,0:T(8,128)(2,1)}, u32[]{:S(2)}) %copy-start.2) | copy-done | bytes 2097176
  58.8 1.1 shard_map.146.back_ref
  59.9 0.0 copy-start.8
  59.9 0.4 copy-done
  60.4 0.8 copy-done.1
  61.2 2.3 %shard_map.147 = (f32[512,512]{1,0:T(8,128)S(1)}, f32[512,512]{1,0:T(8,128)S(1)}) custom-call(bf16[8,64,512]{2,1,0:T(8,128)(2,1)} %all_to_all.10.refs_0_.own_ref.x_ref.refs_4_, bf16[8,64,512]{2,1,0:T(8,128)(2,1)S(1)} %collective-permute-done.9.refs_1_, bf16[2048,512]{1,0:T(8,128)(2,1)S(1)} %bitcast.25, bf16[2048,512]{1,0:T(8,128)(2,1)S(1)} %bitcast.31), custom_call_target="tpu_custom_call" | custom-call | flops 469762048 | tf_op jit(solution)/shard_map/pallas_call | solution.py:378
  63.5 1.8 %shard_map.148 = (f32[512,512]{1,0:T(8,128)S(1)}, f32[512,512]{1,0:T(8,128)S(1)}) custom-call(f32[512,512]{1,0:T(8,128)S(1)} %get-tuple-element.52.got_g, f32[512,512]{1,0:T(8,128)S(1)} %get-tuple-element.53.got_u, bf16[8,64,512]{2,1,0:T(8,128)(2,1)} %collective-permute-done.10.refs_0_.refs_2_, bf16[2048,512]{1,0:T(8,128)(2,1)S(1)} %bitcast.26, ...), custom_call_target="tpu_custom_call" | custom-call | flops 469762048 | tf_op jit(solution)/shard_map/pallas_call | solution.py:378
  65.2 0.0 copy-start.3
  65.3 2.2 %shard_map.149 = (bf16[8,56,512]{2,1,0:T(8,128)(2,1)S(1)}, f32[8,56,512]{2,1,0:T(8,128)S(1)}, f32[8,56,512]{2,1,0:T(8,128)S(1)}) custom-call(f32[512,512]{1,0:T(8,128)S(1)} %get-tuple-element.54.got_g, f32[512,512]{1,0:T(8,128)S(1)} %get-tuple-element.55.got_u, bf16[8,64,512]{2,1,0:T(8,128)(2,1)} %all_to_all.10.refs_0_.own_ref.x_ref.refs_4_, ...), custom_call_target="tpu_custom_call" | custom-call | flops 939524096 | tf_op jit(solution)/shard_map/pallas_call | solution.py:378
  67.5 1.2 %shard_map.150 = (bf16[8,64,1024]{2,1,0:T(8,128)(2,1)S(1)}, bf16[1,448,512]{2,1,0:T(8,128)(2,1)S(1)}, f32[8,128]{1,0:T(8,128)S(1)}) custom-call(f32[2,224,512]{2,1,0:T(8,128)S(1)} %shard_map.146.back_ref, bf16[224,1024]{1,0:T(8,128)(2,1)S(1)} %collective-permute-done.8.far_ref.refs_3_, bf16[512,2048]{1,0:T(8,128)(2,1)S(1)} %bitcast.38, ...), custom_call_target="tpu_custom_call" | custom-call | flops 1409286144 | tf_op jit(solution)/shard_map/pallas_call | solution.py:378
  68.8 0.0 copy-start.4
  68.8 0.5 collective-permute-start.15
  69.3 1.3 %shard_map.151 = (bf16[8,56,512]{2,1,0:T(8,128)(2,1)S(1)}, f32[8,56,512]{2,1,0:T(8,128)S(1)}) custom-call(bf16[8,64,1024]{2,1,0:T(8,128)(2,1)S(1)} %get-tuple-element.59.g_ref.refs_4_, bf16[2048,512]{1,0:T(8,128)(2,1)S(1)} %bitcast.29, bf16[2048,512]{1,0:T(8,128)(2,1)S(1)} %bitcast.35), custom_call_target="tpu_custom_call" | custom-call | flops 939524096 | tf_op jit(solution)/shard_map/pallas_call | solution.py:378
  70.6 0.2 collective-permute-start.12
  70.8 0.7 shard_map.155.own_ref
  71.5 0.0 copy-start.13
  71.5 0.1 shard_map.156
  71.6 0.6 collective-permute-start.16
  72.2 0.1 collective-permute-start.13
  72.3 1.0 collective-permute-done.13.b_ref
  73.3 1.5 %collective-permute-start.14 = (f32[8,128]{1,0:T(8,128)S(1)}, f32[8,128]{1,0:T(8,128)S(1)}, u32[]{:S(2)}, u32[]{:S(2)}) collective-permute-start(f32[8,128]{1,0:T(8,128)S(1)} %shard_map.152.a_ref), channel_id=1, source_target_pairs={{0,2},{1,3},{2,0},{3,1},{4,6},{5,7},{6,4},{7,5},{8,10},{9,11},{10,... | collective-permute-start | bytes 12296 | tf_op jit(solution)/shard_map/ppermute | solution.py:423
  74.9 9.7 %collective-permute-done.14.b_ref = f32[8,128]{1,0:T(8,128)S(1)} collective-permute-done((f32[8,128]{1,0:T(8,128)S(1)}, f32[8,128]{1,0:T(8,128)S(1)}, u32[]{:S(2)}, u32[]{:S(2)}) %collective-permute-start.14) | collective-permute-done | bytes 4128 | tf_op jit(solution)/shard_map/ppermute | solution.py:423
  84.6 2.1 %shard_map.153 = (f32[448,128]{1,0:T(8,128)S(1)}, f32[8,512]{1,0:T(8,128)}) custom-call(f32[8,128]{1,0:T(8,128)S(1)} %shard_map.152.a_ref, f32[8,128]{1,0:T(8,128)S(1)} %collective-permute-done.14.b_ref, bf16[8,64,512]{2,1,0:T(8,128)(2,1)} %all_to_all.10.refs_0_.own_ref.x_ref.refs_4_), custom_call_target="tpu_custom_call" | custom-call | tf_op jit(solution)/shard_map/pallas_call | solution.py:378
  86.7 0.3 shard_map.154.base_ref
  87.0 0.9 shard_map.157
  87.9 4.3 %all-to-all-start.1 = ((bf16[8,56,512]{2,1,0:T(8,128)(2,1)}), bf16[8,56,512]{2,1,0:T(8,128)(2,1)}, u32[]{:S(2)}, u32[]{:S(2)}) async-start(bf16[8,56,512]{2,1,0:T(8,128)(2,1)} %bitcast.13), calls=%async_computation.1 | async-start | bytes 917504 | tf_op jit(solution)/shard_map/all_to_all | solution.py:426
  92.2 0.0 copy-start.15
  92.2 6.4 %grads.1 = (bf16[2048,512]{1,0:T(8,128)(2,1)}, bf16[2048,512]{1,0:T(8,128)(2,1)}, f32[4,2,512]{2,1,0:T(2,128)}) custom-call(s32[1]{0:T(128)} %bitcast.17.q_ref, bf16[8,64,512]{2,1,0:T(8,128)(2,1)} %all_to_all.10.refs_0_.own_ref.x_ref.refs_4_, bf16[8,64,512]{2,1,0:T(8,128)(2,1)} %copy-done.8, bf16[8,64,512]{2,1,0:T(8,128)(2,1)} %collective-permute-done.10.refs_0_.refs_2_, ...), custom_call_target="tpu_custom_call" | custom-call | flops 1879048192 | tf_op jit(solution)/shard_map/grads/pallas_call | solution.py:536
  98.6 0.5 collective-permute-start.24
  99.1 0.6 copy-done.10
  99.8 1.9 %collective-permute-start.20 = (f32[8,512]{1,0:T(8,128)}, f32[8,512]{1,0:T(8,128)}, u32[]{:S(2)}, u32[]{:S(2)}) collective-permute-start(f32[8,512]{1,0:T(8,128)} %get-tuple-element.67.a_ref), channel_id=1, source_target_pairs={{0,4},{4,0},{8,12},{12,8},{16,20},{20,16},{24,28},{28,24},{1,5},{5... | collective-permute-start | bytes 49160 | tf_op jit(solution)/shard_map/ppermute | solution.py:423
  101.7 0.9 collective-permute-done.24
  102.6 4.7 %down.1 = (bf16[512,2048]{1,0:T(8,128)(2,1)}, f32[1,512]{1,0:T(1,128)}) custom-call(s32[1]{0:T(128)} %bitcast.17.q_ref, bf16[224,1024]{1,0:T(8,128)(2,1)} %bitcast.41, bf16[224,1024]{1,0:T(8,128)(2,1)} %bitcast.44, bf16[224,1024]{1,0:T(8,128)(2,1)} %copy-done.9, bf16[224,1024]{1,0:T(8,128)(2,1)} %copy-done.11, ...), custom_call_target="tpu_custom_call" | custom-call | flops 939524096 | tf_op jit(solution)/shard_map/down/pallas_call | solution.py:549
  107.3 1.3 %shard_map.160.a_ref = f32[8,512]{1,0:T(8,128)} custom-call(f32[8,512]{1,0:T(8,128)} %get-tuple-element.67.a_ref, f32[8,512]{1,0:T(8,128)} %collective-permute-done.20.b_ref), custom_call_target="tpu_custom_call" | custom-call | tf_op jit(solution)/shard_map/pallas_call | solution.py:378
  108.7 1.9 %collective-permute-start.21 = (f32[8,512]{1,0:T(8,128)}, f32[8,512]{1,0:T(8,128)}, u32[]{:S(2)}, u32[]{:S(2)}) collective-permute-start(f32[8,512]{1,0:T(8,128)} %shard_map.160.a_ref), channel_id=1, source_target_pairs={{0,8},{4,12},{8,0},{12,4},{16,24},{20,28},{24,16},{28,20},{1,9},{5... | collective-permute-start | bytes 49160 | tf_op jit(solution)/shard_map/ppermute | solution.py:423
  110.6 2.0 %shard_map.159 = (bf16[128,512]{1,0:T(8,128)(2,1)}, bf16[128,2048]{1,0:T(8,128)(2,1)}) custom-call(bf16[448,512]{1,0:T(8,128)(2,1)} %bitcast.14.got_hbm, bf16[448,128]{1,0:T(8,128)(2,1)} %copy-done.10), custom_call_target="tpu_custom_call" | custom-call | tf_op jit(solution)/shard_map/pallas_call | solution.py:378
  112.6 0.6 collective-permute-start.18
  113.2 0.8 add_add_fusion
  114.0 0.7 shard_map.161.a_ref
  114.7 2.4 %collective-permute-start.22 = (f32[8,512]{1,0:T(8,128)S(1)}, f32[8,512]{1,0:T(8,128)S(1)}, u32[]{:S(2)}, u32[]{:S(2)}) collective-permute-start(f32[8,512]{1,0:T(8,128)S(1)} %shard_map.161.a_ref), channel_id=1, source_target_pairs={{0,16},{4,20},{8,24},{12,28},{16,0},{20,4},{24,8},{28,12},{1,17},{... | collective-permute-start | bytes 49160 | tf_op jit(solution)/shard_map/ppermute | solution.py:423
  117.1 1.4 %collective-permute-done.18.refs_2_ = bf16[128,512]{1,0:T(8,128)(2,1)S(1)} collective-permute-done((bf16[128,512]{1,0:T(8,128)(2,1)}, bf16[128,512]{1,0:T(8,128)(2,1)S(1)}, u32[]{:S(2)}, u32[]{:S(2)}) %collective-permute-start.18) | collective-permute-done | bytes 131104 | tf_op jit(solution)/shard_map/ppermute | solution.py:423
  118.5 0.6 fusion
  119.2 0.2 collective-permute-done.22.b_ref
  119.4 0.6 shard_map.162
  120.0 0.8 assemble.1
  (49 shorter events, 0.2 us)
Async XLA Ops:
  25.1 15.4 %collective-permute-start.10 = (bf16[8,64,512]{2,1,0:T(8,128)(2,1)}, bf16[8,64,512]{2,1,0:T(8,128)(2,1)}, u32[]{:S(2)}, u32[]{:S(2)}) collective-permute-start(bf16[8,64,512]{2,1,0:T(8,128)(2,1)} %all_to_all.10.refs_0_.own_ref.x_ref.refs_4_), channel_id=1, source_target_pairs={{0,2},{1,3},{2,0},{3,1},{4,6},{5,7},{6,4},{7,5},{8,10},{9,11},{10,... | collective-permute-start | bytes 1572872 | tf_op jit(solution)/shard_map/ppermute | solution.py:423
  29.5 6.2 %collective-permute-start = (bf16[56,1024]{1,0:T(8,128)(2,1)}, bf16[56,1024]{1,0:T(8,128)(2,1)S(1)}, u32[]{:S(2)}, u32[]{:S(2)}) collective-permute-start(bf16[56,1024]{1,0:T(8,128)(2,1)} %get-tuple-element.44), channel_id=1, source_target_pairs={{0,4},{4,0},{8,12},{12,8},{16,20},{20,16},{24,28},{28,24},{1,5},{5... | collective-permute-start | bytes 344072 | tf_op jit(solution)/shard_map/ppermute | solution.py:423
  31.0 5.4 %collective-permute-start.1 = (bf16[56,1024]{1,0:T(8,128)(2,1)}, bf16[56,1024]{1,0:T(8,128)(2,1)S(1)}, u32[]{:S(2)}, u32[]{:S(2)}) collective-permute-start(bf16[56,1024]{1,0:T(8,128)(2,1)} %get-tuple-element.45), channel_id=1, source_target_pairs={{0,8},{4,12},{8,0},{12,4},{16,24},{20,28},{24,16},{28,20},{1,9},{5... | collective-permute-start | bytes 344072 | tf_op jit(solution)/shard_map/ppermute | solution.py:423
  31.0 8.5 %collective-permute-start.2 = (bf16[56,1024]{1,0:T(8,128)(2,1)}, bf16[56,1024]{1,0:T(8,128)(2,1)S(1)}, u32[]{:S(2)}, u32[]{:S(2)}) collective-permute-start(bf16[56,1024]{1,0:T(8,128)(2,1)} %get-tuple-element.46), channel_id=1, source_target_pairs={{0,12},{4,8},{8,4},{12,0},{16,28},{20,24},{24,20},{28,16},{1,13},{... | collective-permute-start | bytes 344072 | tf_op jit(solution)/shard_map/ppermute | solution.py:423
  33.0 26.9 %collective-permute-start.9 = (bf16[8,64,512]{2,1,0:T(8,128)(2,1)}, bf16[8,64,512]{2,1,0:T(8,128)(2,1)S(1)}, u32[]{:S(2)}, u32[]{:S(2)}) collective-permute-start(bf16[8,64,512]{2,1,0:T(8,128)(2,1)} %all_to_all.10.refs_0_.own_ref.x_ref.refs_4_), channel_id=1, source_target_pairs={{0,1},{1,0},{2,3},{3,2},{4,5},{5,4},{6,7},{7,6},{8,9},{9,8},{10,11... | collective-permute-start | bytes 1572872 | tf_op jit(solution)/shard_map/ppermute | solution.py:423
  35.7 9.8 %collective-permute-start.3 = (bf16[56,1024]{1,0:T(8,128)(2,1)}, bf16[56,1024]{1,0:T(8,128)(2,1)S(1)}, u32[]{:S(2)}, u32[]{:S(2)}) collective-permute-start(bf16[56,1024]{1,0:T(8,128)(2,1)} %get-tuple-element.47), channel_id=1, source_target_pairs={{0,16},{4,20},{8,24},{12,28},{16,0},{20,4},{24,8},{28,12},{1,17},{... | collective-permute-start | bytes 344072 | tf_op jit(solution)/shard_map/ppermute | solution.py:423
  36.4 12.6 %collective-permute-start.4 = (bf16[56,1024]{1,0:T(8,128)(2,1)}, bf16[56,1024]{1,0:T(8,128)(2,1)S(1)}, u32[]{:S(2)}, u32[]{:S(2)}) collective-permute-start(bf16[56,1024]{1,0:T(8,128)(2,1)} %get-tuple-element.48), channel_id=1, source_target_pairs={{0,20},{4,16},{8,28},{12,24},{16,4},{20,0},{24,12},{28,8},{1,21},{... | collective-permute-start | bytes 344072 | tf_op jit(solution)/shard_map/ppermute | solution.py:423
  39.5 0.9 copy-start.14
  40.4 19.4 %copy-start.5 = (bf16[4,56,1024]{2,1,0:T(8,128)(2,1)}, bf16[4,56,1024]{2,1,0:T(8,128)(2,1)S(1)}, u32[]{:S(2)}) copy-start(bf16[4,56,1024]{2,1,0:T(8,128)(2,1)S(1)} %shard_map.144) | copy-start | bytes 1376260
  40.5 16.5 %collective-permute-start.7 = (bf16[224,1024]{1,0:T(8,128)(2,1)S(1)}, bf16[224,1024]{1,0:T(8,128)(2,1)S(1)}, u32[]{:S(2)}, u32[]{:S(2)}) collective-permute-start(bf16[224,1024]{1,0:T(8,128)(2,1)S(1)} %bitcast.39), channel_id=1, source_target_pairs={{0,1},{1,0},{2,3},{3,2},{4,5},{5,4},{6,7},{7,6},{8,9},{9,8},{10,11... | collective-permute-start | bytes 1376264 | tf_op jit(solution)/shard_map/ppermute | solution.py:423
  40.5 24.7 %collective-permute-start.11 = (bf16[8,64,512]{2,1,0:T(8,128)(2,1)}, bf16[8,64,512]{2,1,0:T(8,128)(2,1)S(1)}, u32[]{:S(2)}, u32[]{:S(2)}) collective-permute-start(bf16[8,64,512]{2,1,0:T(8,128)(2,1)} %collective-permute-done.10.refs_0_.refs_2_), channel_id=1, source_target_pairs={{0,1},{1,0},{2,3},{3,2},{4,5},{5,4},{6,7},{7,6},{8,9},{9,8},{10,11... | collective-permute-start | bytes 1572872 | tf_op jit(solution)/shard_map/ppermute | solution.py:423
  45.4 7.3 %collective-permute-start.5 = (bf16[56,1024]{1,0:T(8,128)(2,1)}, bf16[56,1024]{1,0:T(8,128)(2,1)S(1)}, u32[]{:S(2)}, u32[]{:S(2)}) collective-permute-start(bf16[56,1024]{1,0:T(8,128)(2,1)} %get-tuple-element.49), channel_id=1, source_target_pairs={{0,24},{4,28},{8,16},{12,20},{16,8},{20,12},{24,0},{28,4},{1,25},{... | collective-permute-start | bytes 344072 | tf_op jit(solution)/shard_map/ppermute | solution.py:423
  49.0 7.8 %collective-permute-start.6 = (bf16[56,1024]{1,0:T(8,128)(2,1)}, bf16[56,1024]{1,0:T(8,128)(2,1)S(1)}, u32[]{:S(2)}, u32[]{:S(2)}) collective-permute-start(bf16[56,1024]{1,0:T(8,128)(2,1)} %get-tuple-element.50), channel_id=1, source_target_pairs={{0,28},{4,24},{8,20},{12,16},{16,12},{20,8},{24,4},{28,0},{1,29},{... | collective-permute-start | bytes 344072 | tf_op jit(solution)/shard_map/ppermute | solution.py:423
  56.8 3.0 %copy-start.6 = (bf16[4,56,1024]{2,1,0:T(8,128)(2,1)}, bf16[4,56,1024]{2,1,0:T(8,128)(2,1)S(1)}, u32[]{:S(2)}) copy-start(bf16[4,56,1024]{2,1,0:T(8,128)(2,1)S(1)} %shard_map.145) | copy-start | bytes 1376260
  56.8 10.7 %collective-permute-start.8 = (bf16[224,1024]{1,0:T(8,128)(2,1)S(1)}, bf16[224,1024]{1,0:T(8,128)(2,1)S(1)}, u32[]{:S(2)}, u32[]{:S(2)}) collective-permute-start(bf16[224,1024]{1,0:T(8,128)(2,1)S(1)} %bitcast.42), channel_id=1, source_target_pairs={{0,1},{1,0},{2,3},{3,2},{4,5},{5,4},{6,7},{7,6},{8,9},{9,8},{10,11... | collective-permute-start | bytes 1376264 | tf_op jit(solution)/shard_map/ppermute | solution.py:423
  56.9 3.0 %copy-start.9 = (bf16[224,1024]{1,0:T(8,128)(2,1)}, bf16[224,1024]{1,0:T(8,128)(2,1)S(1)}, u32[]{:S(2)}) copy-start(bf16[224,1024]{1,0:T(8,128)(2,1)S(1)} %collective-permute-done.7.near_got.refs_2_) | copy-start | bytes 1376260
  56.9 1.8 %copy-start.2 = (bf16[1,512,2048]{2,1,0:T(8,128)(2,1)S(1)}, bf16[1,512,2048]{2,1,0:T(8,128)(2,1)}, u32[]{:S(2)}) copy-start(bf16[1,512,2048]{2,1,0:T(8,128)(2,1)} %param.12) | copy-start | bytes 6291460
  58.8 1.6 %copy-start = (bf16[1,2048,512]{2,1,0:T(8,128)(2,1)S(1)}, bf16[1,2048,512]{2,1,0:T(8,128)(2,1)}, u32[]{:S(2)}) copy-start(bf16[1,2048,512]{2,1,0:T(8,128)(2,1)} %param.10) | copy-start | bytes 6291460
  58.8 2.4 %copy-start.1 = (bf16[1,2048,512]{2,1,0:T(8,128)(2,1)S(1)}, bf16[1,2048,512]{2,1,0:T(8,128)(2,1)}, u32[]{:S(2)}) copy-start(bf16[1,2048,512]{2,1,0:T(8,128)(2,1)} %param.11) | copy-start | bytes 6291460
  59.9 3.6 %copy-start.8 = (bf16[8,64,512]{2,1,0:T(8,128)(2,1)}, bf16[8,64,512]{2,1,0:T(8,128)(2,1)S(1)}, u32[]{:S(2)}) copy-start(bf16[8,64,512]{2,1,0:T(8,128)(2,1)S(1)} %collective-permute-done.9.refs_1_) | copy-start | bytes 1572868
  65.2 2.3 %copy-start.7 = (bf16[8,64,512]{2,1,0:T(8,128)(2,1)}, bf16[8,64,512]{2,1,0:T(8,128)(2,1)S(1)}, u32[]{:S(2)}) copy-start(bf16[8,64,512]{2,1,0:T(8,128)(2,1)S(1)} %collective-permute-done.11.refs_0_.refs_3_) | copy-start | bytes 1572868
  65.2 2.3 %copy-start.3 = (bf16[1,512,2048]{2,1,0:T(8,128)(2,1)S(1)}, bf16[1,512,2048]{2,1,0:T(8,128)(2,1)}, u32[]{:S(2)}) copy-start(bf16[1,512,2048]{2,1,0:T(8,128)(2,1)} %param.12) | copy-start | bytes 6291460
  67.5 1.3 %copy-start.12 = (bf16[8,56,512]{2,1,0:T(8,128)(2,1)}, bf16[8,56,512]{2,1,0:T(8,128)(2,1)S(1)}, u32[]{:S(2)}) copy-start(bf16[8,56,512]{2,1,0:T(8,128)(2,1)S(1)} %get-tuple-element.56) | copy-start | bytes 1376260
  67.5 1.3 %copy-start.11 = (bf16[224,1024]{1,0:T(8,128)(2,1)}, bf16[224,1024]{1,0:T(8,128)(2,1)S(1)}, u32[]{:S(2)}) copy-start(bf16[224,1024]{1,0:T(8,128)(2,1)S(1)} %collective-permute-done.8.far_ref.refs_3_) | copy-start | bytes 1376260
  68.8 1.9 %copy-start.4 = (bf16[8,64,1024]{2,1,0:T(8,128)(2,1)}, bf16[8,64,1024]{2,1,0:T(8,128)(2,1)S(1)}, u32[]{:S(2)}) copy-start(bf16[8,64,1024]{2,1,0:T(8,128)(2,1)S(1)} %get-tuple-element.59.g_ref.refs_4_) | copy-start | bytes 3145732
  68.8 2.7 %collective-permute-start.15 = (bf16[1,448,512]{2,1,0:T(8,128)(2,1)S(1)}, bf16[1,448,512]{2,1,0:T(8,128)(2,1)S(1)}, u32[]{:S(2)}, u32[]{:S(2)}) collective-permute-start(bf16[1,448,512]{2,1,0:T(8,128)(2,1)S(1)} %get-tuple-element.64), channel_id=1, source_target_pairs={{0,1},{1,0},{2,3},{3,2},{4,5},{5,4},{6,7},{7,6},{8,9},{9,8},{10,11... | collective-permute-start | bytes 1376264 | tf_op jit(solution)/shard_map/ppermute | solution.py:423
  70.6 16.1 %collective-permute-start.12 = (bf16[448,512]{1,0:T(8,128)(2,1)S(1)}, bf16[448,512]{1,0:T(8,128)(2,1)S(1)}, u32[]{:S(2)}, u32[]{:S(2)}) collective-permute-start(bf16[448,512]{1,0:T(8,128)(2,1)S(1)} %bitcast.53), channel_id=1, source_target_pairs={{0,1},{1,0},{2,3},{3,2},{4,5},{5,4},{6,7},{7,6},{8,9},{9,8},{10,11... | collective-permute-start | bytes 1376264 | tf_op jit(solution)/shard_map/ppermute | solution.py:423
  71.5 15.2 %copy-start.13 = (bf16[2048,8]{0,1:T(8,128)(2,1)S(1)}, bf16[2048,8]{0,1:T(8,128)(2,1)}, u32[]{:S(2)}) copy-start(bf16[2048,8]{0,1:T(8,128)(2,1)} %param.9) | copy-start | bytes 98308
  71.6 15.4 %collective-permute-start.16 = (bf16[448,512]{1,0:T(8,128)(2,1)S(1)}, bf16[448,512]{1,0:T(8,128)(2,1)S(1)}, u32[]{:S(2)}, u32[]{:S(2)}) collective-permute-start(bf16[448,512]{1,0:T(8,128)(2,1)S(1)} %bitcast.48), channel_id=1, source_target_pairs={{0,2},{1,3},{2,0},{3,1},{4,6},{5,7},{6,4},{7,5},{8,10},{9,11},{10,... | collective-permute-start | bytes 1376264 | tf_op jit(solution)/shard_map/ppermute | solution.py:423
  72.2 1.2 collective-permute-start.13
  73.3 11.3 %collective-permute-start.14 = (f32[8,128]{1,0:T(8,128)S(1)}, f32[8,128]{1,0:T(8,128)S(1)}, u32[]{:S(2)}, u32[]{:S(2)}) collective-permute-start(f32[8,128]{1,0:T(8,128)S(1)} %shard_map.152.a_ref), channel_id=1, source_target_pairs={{0,2},{1,3},{2,0},{3,1},{4,6},{5,7},{6,4},{7,5},{8,10},{9,11},{10,... | collective-permute-start | bytes 12296 | tf_op jit(solution)/shard_map/ppermute | solution.py:423
  87.9 22.7 %all-to-all-start.1 = ((bf16[8,56,512]{2,1,0:T(8,128)(2,1)}), bf16[8,56,512]{2,1,0:T(8,128)(2,1)}, u32[]{:S(2)}, u32[]{:S(2)}) async-start(bf16[8,56,512]{2,1,0:T(8,128)(2,1)} %bitcast.13), calls=%async_computation.1 | async-start | bytes 917504 | tf_op jit(solution)/shard_map/all_to_all | solution.py:426
  92.2 6.9 %copy-start.15 = (f32[8,128]{1,0:T(8,128)S(1)}, f32[8,128]{1,0:T(8,128)}, u32[]{:S(2)}) copy-start(f32[8,128]{1,0:T(8,128)} %get-tuple-element.42.place_ref) | copy-start | bytes 12292
  98.6 4.1 %collective-permute-start.24 = (f32[2,2048]{1,0:T(2,128)}, f32[2,2048]{1,0:T(2,128)}, u32[]{:S(2)}, u32[]{:S(2)}) collective-permute-start(f32[2,2048]{1,0:T(2,128)} %bitcast.54), channel_id=1, source_target_pairs={{0,2},{1,3},{2,0},{3,1},{4,6},{5,7},{6,4},{7,5},{8,10},{9,11},{10,... | collective-permute-start | bytes 49160 | tf_op jit(solution)/shard_map/ppermute | solution.py:423
  99.1 0.6 copy-start.10
  99.8 13.4 %collective-permute-start.23 = (f32[2,2048]{1,0:T(2,128)}, f32[2,2048]{1,0:T(2,128)}, u32[]{:S(2)}, u32[]{:S(2)}) collective-permute-start(f32[2,2048]{1,0:T(2,128)} %bitcast.55), channel_id=1, source_target_pairs={{0,1},{1,0},{2,3},{3,2},{4,5},{5,4},{6,7},{7,6},{8,9},{9,8},{10,11... | collective-permute-start | bytes 49160 | tf_op jit(solution)/shard_map/ppermute | solution.py:423
  99.8 7.6 %collective-permute-start.20 = (f32[8,512]{1,0:T(8,128)}, f32[8,512]{1,0:T(8,128)}, u32[]{:S(2)}, u32[]{:S(2)}) collective-permute-start(f32[8,512]{1,0:T(8,128)} %get-tuple-element.67.a_ref), channel_id=1, source_target_pairs={{0,4},{4,0},{8,12},{12,8},{16,20},{20,16},{24,28},{28,24},{1,5},{5... | collective-permute-start | bytes 49160 | tf_op jit(solution)/shard_map/ppermute | solution.py:423
  102.6 10.6 %collective-permute-start.25 = (f32[2,2048]{1,0:T(2,128)}, f32[2,2048]{1,0:T(2,128)}, u32[]{:S(2)}, u32[]{:S(2)}) collective-permute-start(f32[2,2048]{1,0:T(2,128)} %collective-permute-done.24), channel_id=1, source_target_pairs={{0,1},{1,0},{2,3},{3,2},{4,5},{5,4},{6,7},{7,6},{8,9},{9,8},{10,11... | collective-permute-start | bytes 49160 | tf_op jit(solution)/shard_map/ppermute | solution.py:423
  108.7 5.3 %collective-permute-start.21 = (f32[8,512]{1,0:T(8,128)}, f32[8,512]{1,0:T(8,128)}, u32[]{:S(2)}, u32[]{:S(2)}) collective-permute-start(f32[8,512]{1,0:T(8,128)} %shard_map.160.a_ref), channel_id=1, source_target_pairs={{0,8},{4,12},{8,0},{12,4},{16,24},{20,28},{24,16},{28,20},{1,9},{5... | collective-permute-start | bytes 49160 | tf_op jit(solution)/shard_map/ppermute | solution.py:423
  112.6 5.9 %collective-permute-start.18 = (bf16[128,512]{1,0:T(8,128)(2,1)}, bf16[128,512]{1,0:T(8,128)(2,1)S(1)}, u32[]{:S(2)}, u32[]{:S(2)}) collective-permute-start(bf16[128,512]{1,0:T(8,128)(2,1)} %get-tuple-element.66), channel_id=1, source_target_pairs={{0,2},{1,3},{2,0},{3,1},{4,6},{5,7},{6,4},{7,5},{8,10},{9,11},{10,... | collective-permute-start | bytes 393224 | tf_op jit(solution)/shard_map/ppermute | solution.py:423
  114.7 4.6 %collective-permute-start.22 = (f32[8,512]{1,0:T(8,128)S(1)}, f32[8,512]{1,0:T(8,128)S(1)}, u32[]{:S(2)}, u32[]{:S(2)}) collective-permute-start(f32[8,512]{1,0:T(8,128)S(1)} %shard_map.161.a_ref), channel_id=1, source_target_pairs={{0,16},{4,20},{8,24},{12,28},{16,0},{20,4},{24,8},{28,12},{1,17},{... | collective-permute-start | bytes 49160 | tf_op jit(solution)/shard_map/ppermute | solution.py:423
  117.1 2.9 %collective-permute-start.17 = (bf16[128,512]{1,0:T(8,128)(2,1)}, bf16[128,512]{1,0:T(8,128)(2,1)S(1)}, u32[]{:S(2)}, u32[]{:S(2)}) collective-permute-start(bf16[128,512]{1,0:T(8,128)(2,1)} %get-tuple-element.66), channel_id=1, source_target_pairs={{0,1},{1,0},{2,3},{3,2},{4,5},{5,4},{6,7},{7,6},{8,9},{9,8},{10,11... | collective-permute-start | bytes 393224 | tf_op jit(solution)/shard_map/ppermute | solution.py:423
  118.5 1.5 %collective-permute-start.19 = (bf16[128,512]{1,0:T(8,128)(2,1)S(1)}, bf16[128,512]{1,0:T(8,128)(2,1)S(1)}, u32[]{:S(2)}, u32[]{:S(2)}) collective-permute-start(bf16[128,512]{1,0:T(8,128)(2,1)S(1)} %collective-permute-done.18.refs_2_), channel_id=1, source_target_pairs={{0,1},{1,0},{2,3},{3,2},{4,5},{5,4},{6,7},{7,6},{8,9},{9,8},{10,11... | collective-permute-start | bytes 393224 | tf_op jit(solution)/shard_map/ppermute | solution.py:423

commit v7 on v6

--- a/solution.py
+++ b/solution.py
@@ -55,9 +55,7 @@
     experts = router_ref.shape[0]
     cols = rows_ref.shape[2]
     start = pl.multiple_of(lax.axis_index("tp") * cols, 128)
-    for copy in copies:
-        copy.wait()
-    aff = jax.nn.sigmoid(dot(router_ref[...], tok_ref[...], 1, 1))
+    copies[1].wait()
     ids = lax.broadcasted_iota(jnp.int32, (experts, toks), 0)
     routed = routing_ref[...]
     named = jnp.zeros((experts, toks), F32)
@@ -68,6 +66,9 @@
     earlier = (before < after).astype(F32).astype(BF16)
     position = dot(named.astype(BF16), earlier)
     place = jnp.where(named > 0, position, -1.0)
+    copies[0].wait()
+    copies[2].wait()
+    aff = jax.nn.sigmoid(dot(router_ref[...], tok_ref[...], 1, 1))
     chosen = named * aff
     weights = chosen / jnp.sum(chosen, axis=0, keepdims=True)
     place_ref[...] = place
@@ -352,9 +353,16 @@
 def home_kernel(got_hbm, hot_hbm, token_out, whole_hbm, got_ref, hot_ref, own_ref, sems):
     cols = got_ref.shape[1]
     start = pl.multiple_of(lax.axis_index("tp") * cols, 128)
-    for copy in fetch(sems, (got_hbm, got_ref), (hot_hbm, hot_ref)):
-        copy.wait()
-    own_ref[...] = dot(hot_ref[...], got_ref[...], 0, 0).astype(BF16)
+    middle = got_ref.shape[0] // 2
+    first, second = slice(0, middle), slice(middle, 2 * middle)
+    copies = fetch(
+        sems, (hot_hbm, hot_ref), (got_hbm.at[first], got_ref.at[first]), (got_hbm.at[second], got_ref.at[second])
+    )
+    copies[0].wait()
+    copies[1].wait()
+    total = dot(hot_ref[first], got_ref[first], 0, 0)
+    copies[2].wait()
+    own_ref[...] = (total + dot(hot_ref[second], got_ref[second], 0, 0)).astype(BF16)
     copies = fetch(sems, (own_ref, token_out), (own_ref, whole_hbm.at[:, pl.ds(start, cols)]))
     for copy in copies:
         copy.wait()
@@ -571,7 +579,7 @@
     token_part, token_grad = call(
         home_kernel, (shape(toks, cols), shape(toks, width)),
         False, home_got, hot, hbm=(0, 1), limit=ALONE, out_hbm=True,
-        scratch=[buffer(count, cols), buffer(count, toks), buffer(toks, cols), DMAS((2,))],
+        scratch=[buffer(count, cols), buffer(count, toks), buffer(toks, cols), DMAS((3,))],
     )
     token_parts = spread(token_part)[1:]
     token_grad = pl.pallas_call(

time: 122 us -> 122 us (level)
  no operation moved by 1% of the time
where the time goes in v7:
time: 122 us; the launch traced here: 121 us
  Pallas kernels  36.1 us (30%)
  starting transfers between devices  30.6 us (25%)
  waiting for transfers between devices  25.3 us (21%)
  blocking collectives  21.9 us (18%)
  local copies, waits for them, and re-layouts  5.29 us (4%)
    ppermute x26, starting transfers between devices, swap(): return lax.ppermute(value, axis, [(i, i ^ bit) for i in range(size)])  26.3 us
    ppermute x26, waiting for transfers between devices, swap(): return lax.ppermute(value, axis, [(i, i ^ bit) for i in range(size)])  25.3 us
    pallas_call x21, Pallas kernels, call(): pl.pallas_call(kernel, out_shape=outs, in_specs=([SMEM] if scalar else []...  24.2 us
    all_to_all x1, blocking collectives, exchange(): return lax.all_to_all(value, 'ep', split_axis=0, concat_axis=0, tiled=True)  21.9 us
    pallas_call x1, Pallas kernels, layer(): pl.pallas_call(functools.partial(grads_kernel, shares), out_shape=(shape(...  6.38 us
    pallas_call x1, Pallas kernels, layer(): pl.pallas_call(functools.partial(down_kernel, slots), out_shape=(shape(hi...  4.71 us
    unnamed x32, local copies, waits for them, and re-layouts  4.68 us
    all_to_all x1, starting transfers between devices, exchange(): return lax.all_to_all(value, 'ep', split_axis=0, concat_axis=0, tiled=True)  4.29 us
  transfers between devices with their start and end apart: 27, of which 9 were waited for; matrix products, arithmetic and copies ran while one was open for 1% of the time, Pallas kernels for 25%

profile of v7, /device:TPU:0, one launch (start us, length us, event | category | flops | bytes accessed | tf_op | source)
XLA Modules:
  0.0 121.2 jit_solution(8937497096742239922)
XLA Ops:
  0.6 2.5 %shard_map.142 = (bf16[8,64,512]{2,1,0:T(8,128)(2,1)}, f32[8,128]{1,0:T(8,128)}) custom-call(bf16[128,2048]{1,0:T(8,128)(2,1)} %tok_hbm.1, s32[2,128]{1,0:T(2,128)} %bitcast.57, bf16[8,2048]{1,0:T(8,128)(2,1)} %bitcast.51), custom_call_target="tpu_custom_call" | custom-call | tf_op jit(solution)/shard_map/pallas_call | solution.py:386
  3.2 21.9 %all_to_all.10.refs_0_.own_ref.x_ref.refs_4_ = bf16[8,64,512]{2,1,0:T(8,128)(2,1)} all-to-all(bf16[8,64,512]{2,1,0:T(8,128)(2,1)} %get-tuple-element.51), channel_id=1, replica_groups=mesh['ep'=8,'tp'=4] {'ep'}, dimensions={0} | all-to-all | bytes 1048576 | tf_op jit(solution)/shard_map/all_to_all | solution.py:434
  25.1 1.5 %collective-permute-start.10 = (bf16[8,64,512]{2,1,0:T(8,128)(2,1)}, bf16[8,64,512]{2,1,0:T(8,128)(2,1)}, u32[]{:S(2)}, u32[]{:S(2)}) collective-permute-start(bf16[8,64,512]{2,1,0:T(8,128)(2,1)} %all_to_all.10.refs_0_.own_ref.x_ref.refs_4_), channel_id=1, source_target_pairs={{0,2},{1,3},{2,0},{3,1},{4,6},{5,7},{6,4},{7,5},{8,10},{9,11},{10,... | collective-permute-start | bytes 1572872 | tf_op jit(solution)/shard_map/ppermute | solution.py:431
  26.6 2.8 %shard_map.143 = (bf16[56,1024]{1,0:T(8,128)(2,1)}, bf16[56,1024]{1,0:T(8,128)(2,1)}, bf16[56,1024]{1,0:T(8,128)(2,1)}, bf16[56,1024]{1,0:T(8,128)(2,1)}, bf16[5...) custom-call(bf16[128,2048]{1,0:T(8,128)(2,1)} %cot_hbm.1, ...), custom_call_target="tpu_custom_call" | custom-call | flops 117440512 | tf_op jit(solution)/shard_map/pallas_call | solution.py:386
  29.5 1.5 %collective-permute-start = (bf16[56,1024]{1,0:T(8,128)(2,1)}, bf16[56,1024]{1,0:T(8,128)(2,1)S(1)}, u32[]{:S(2)}, u32[]{:S(2)}) collective-permute-start(bf16[56,1024]{1,0:T(8,128)(2,1)} %get-tuple-element.44), channel_id=1, source_target_pairs={{0,4},{4,0},{8,12},{12,8},{16,20},{20,16},{24,28},{28,24},{1,5},{5... | collective-permute-start | bytes 344072 | tf_op jit(solution)/shard_map/ppermute | solution.py:431
  31.0 2.1 %collective-permute-start.2 = (bf16[56,1024]{1,0:T(8,128)(2,1)}, bf16[56,1024]{1,0:T(8,128)(2,1)S(1)}, u32[]{:S(2)}, u32[]{:S(2)}) collective-permute-start(bf16[56,1024]{1,0:T(8,128)(2,1)} %get-tuple-element.46), channel_id=1, source_target_pairs={{0,12},{4,8},{8,4},{12,0},{16,28},{20,24},{24,20},{28,16},{1,13},{... | collective-permute-start | bytes 344072 | tf_op jit(solution)/shard_map/ppermute | solution.py:431
  33.0 2.6 %collective-permute-done.refs_1_ = bf16[56,1024]{1,0:T(8,128)(2,1)S(1)} collective-permute-done((bf16[56,1024]{1,0:T(8,128)(2,1)}, bf16[56,1024]{1,0:T(8,128)(2,1)S(1)}, u32[]{:S(2)}, u32[]{:S(2)}) %collective-permute-start) | collective-permute-done | bytes 114720 | tf_op jit(solution)/shard_map/ppermute | solution.py:431
  35.6 0.8 collective-permute-start.3
  36.4 3.1 %collective-permute-start.4 = (bf16[56,1024]{1,0:T(8,128)(2,1)}, bf16[56,1024]{1,0:T(8,128)(2,1)S(1)}, u32[]{:S(2)}, u32[]{:S(2)}) collective-permute-start(bf16[56,1024]{1,0:T(8,128)(2,1)} %get-tuple-element.48), channel_id=1, source_target_pairs={{0,20},{4,16},{8,28},{12,24},{16,4},{20,0},{24,12},{28,8},{1,21},{... | collective-permute-start | bytes 344072 | tf_op jit(solution)/shard_map/ppermute | solution.py:431
  39.5 0.9 copy-done.14
  40.4 0.1 collective-permute-start.7
  40.5 0.5 collective-permute-start.11
  41.0 4.4 %collective-permute-done.3.refs_0_ = bf16[56,1024]{1,0:T(8,128)(2,1)S(1)} collective-permute-done((bf16[56,1024]{1,0:T(8,128)(2,1)}, bf16[56,1024]{1,0:T(8,128)(2,1)S(1)}, u32[]{:S(2)}, u32[]{:S(2)}) %collective-permute-start.3) | collective-permute-done | bytes 114720 | tf_op jit(solution)/shard_map/ppermute | solution.py:431
  45.4 3.5 %collective-permute-start.5 = (bf16[56,1024]{1,0:T(8,128)(2,1)}, bf16[56,1024]{1,0:T(8,128)(2,1)S(1)}, u32[]{:S(2)}, u32[]{:S(2)}) collective-permute-start(bf16[56,1024]{1,0:T(8,128)(2,1)} %get-tuple-element.49), channel_id=1, source_target_pairs={{0,24},{4,28},{8,16},{12,20},{16,8},{20,12},{24,0},{28,4},{1,25},{... | collective-permute-start | bytes 344072 | tf_op jit(solution)/shard_map/ppermute | solution.py:431
  49.0 3.1 %collective-permute-start.6 = (bf16[56,1024]{1,0:T(8,128)(2,1)}, bf16[56,1024]{1,0:T(8,128)(2,1)S(1)}, u32[]{:S(2)}, u32[]{:S(2)}) collective-permute-start(bf16[56,1024]{1,0:T(8,128)(2,1)} %get-tuple-element.50), channel_id=1, source_target_pairs={{0,28},{4,24},{8,20},{12,16},{16,12},{20,8},{24,4},{28,0},{1,29},{... | collective-permute-start | bytes 344072 | tf_op jit(solution)/shard_map/ppermute | solution.py:431
  52.0 0.6 collective-permute-done.5.refs_2_
  52.7 4.1 %collective-permute-done.6.refs_3_ = bf16[56,1024]{1,0:T(8,128)(2,1)S(1)} collective-permute-done((bf16[56,1024]{1,0:T(8,128)(2,1)}, bf16[56,1024]{1,0:T(8,128)(2,1)S(1)}, u32[]{:S(2)}, u32[]{:S(2)}) %collective-permute-start.6) | collective-permute-done | bytes 114720 | tf_op jit(solution)/shard_map/ppermute | solution.py:431
  56.8 0.1 collective-permute-start.8
  56.9 0.0 copy-start.2
  56.9 1.8 %copy-done.2 = bf16[1,512,2048]{2,1,0:T(8,128)(2,1)S(1)} copy-done((bf16[1,512,2048]{2,1,0:T(8,128)(2,1)S(1)}, bf16[1,512,2048]{2,1,0:T(8,128)(2,1)}, u32[]{:S(2)}) %copy-start.2) | copy-done | bytes 2097176
  58.8 1.1 shard_map.146.back_ref
  59.9 0.0 copy-start.8
  59.9 0.4 copy-done
  60.3 0.8 copy-done.1
  61.2 2.3 %shard_map.147 = (f32[512,512]{1,0:T(8,128)S(1)}, f32[512,512]{1,0:T(8,128)S(1)}) custom-call(bf16[8,64,512]{2,1,0:T(8,128)(2,1)} %all_to_all.10.refs_0_.own_ref.x_ref.refs_4_, bf16[8,64,512]{2,1,0:T(8,128)(2,1)S(1)} %collective-permute-done.9.refs_1_, bf16[2048,512]{1,0:T(8,128)(2,1)S(1)} %bitcast.25, bf16[2048,512]{1,0:T(8,128)(2,1)S(1)} %bitcast.31), custom_call_target="tpu_custom_call" | custom-call | flops 469762048 | tf_op jit(solution)/shard_map/pallas_call | solution.py:386
  63.5 1.8 %shard_map.148 = (f32[512,512]{1,0:T(8,128)S(1)}, f32[512,512]{1,0:T(8,128)S(1)}) custom-call(f32[512,512]{1,0:T(8,128)S(1)} %get-tuple-element.52.got_g, f32[512,512]{1,0:T(8,128)S(1)} %get-tuple-element.53.got_u, bf16[8,64,512]{2,1,0:T(8,128)(2,1)} %collective-permute-done.10.refs_0_.refs_2_, bf16[2048,512]{1,0:T(8,128)(2,1)S(1)} %bitcast.26, ...), custom_call_target="tpu_custom_call" | custom-call | flops 469762048 | tf_op jit(solution)/shard_map/pallas_call | solution.py:386
  65.2 0.0 copy-start.3
  65.3 2.2 %shard_map.149 = (bf16[8,56,512]{2,1,0:T(8,128)(2,1)S(1)}, f32[8,56,512]{2,1,0:T(8,128)S(1)}, f32[8,56,512]{2,1,0:T(8,128)S(1)}) custom-call(f32[512,512]{1,0:T(8,128)S(1)} %get-tuple-element.54.got_g, f32[512,512]{1,0:T(8,128)S(1)} %get-tuple-element.55.got_u, bf16[8,64,512]{2,1,0:T(8,128)(2,1)} %all_to_all.10.refs_0_.own_ref.x_ref.refs_4_, ...), custom_call_target="tpu_custom_call" | custom-call | flops 939524096 | tf_op jit(solution)/shard_map/pallas_call | solution.py:386
  67.5 1.2 %shard_map.150 = (bf16[8,64,1024]{2,1,0:T(8,128)(2,1)S(1)}, bf16[1,448,512]{2,1,0:T(8,128)(2,1)S(1)}, f32[8,128]{1,0:T(8,128)S(1)}) custom-call(f32[2,224,512]{2,1,0:T(8,128)S(1)} %shard_map.146.back_ref, bf16[224,1024]{1,0:T(8,128)(2,1)S(1)} %collective-permute-done.8.far_ref.refs_3_, bf16[512,2048]{1,0:T(8,128)(2,1)S(1)} %bitcast.38, ...), custom_call_target="tpu_custom_call" | custom-call | flops 1409286144 | tf_op jit(solution)/shard_map/pallas_call | solution.py:386
  68.8 0.0 copy-start.4
  68.8 0.5 collective-permute-start.15
  69.3 1.3 %shard_map.151 = (bf16[8,56,512]{2,1,0:T(8,128)(2,1)S(1)}, f32[8,56,512]{2,1,0:T(8,128)S(1)}) custom-call(bf16[8,64,1024]{2,1,0:T(8,128)(2,1)S(1)} %get-tuple-element.59.g_ref.refs_4_, bf16[2048,512]{1,0:T(8,128)(2,1)S(1)} %bitcast.29, bf16[2048,512]{1,0:T(8,128)(2,1)S(1)} %bitcast.35), custom_call_target="tpu_custom_call" | custom-call | flops 939524096 | tf_op jit(solution)/shard_map/pallas_call | solution.py:386
  70.6 0.2 collective-permute-start.12
  70.7 0.7 shard_map.155.own_ref
  71.5 0.0 copy-start.13
  71.5 0.1 shard_map.156
  71.6 0.6 collective-permute-start.16
  72.2 0.1 collective-permute-start.13
  72.3 1.0 collective-permute-done.13.b_ref
  73.3 1.5 %collective-permute-start.14 = (f32[8,128]{1,0:T(8,128)S(1)}, f32[8,128]{1,0:T(8,128)S(1)}, u32[]{:S(2)}, u32[]{:S(2)}) collective-permute-start(f32[8,128]{1,0:T(8,128)S(1)} %shard_map.152.a_ref), channel_id=1, source_target_pairs={{0,2},{1,3},{2,0},{3,1},{4,6},{5,7},{6,4},{7,5},{8,10},{9,11},{10,... | collective-permute-start | bytes 12296 | tf_op jit(solution)/shard_map/ppermute | solution.py:431
  74.9 9.7 %collective-permute-done.14.b_ref = f32[8,128]{1,0:T(8,128)S(1)} collective-permute-done((f32[8,128]{1,0:T(8,128)S(1)}, f32[8,128]{1,0:T(8,128)S(1)}, u32[]{:S(2)}, u32[]{:S(2)}) %collective-permute-start.14) | collective-permute-done | bytes 4128 | tf_op jit(solution)/shard_map/ppermute | solution.py:431
  84.6 2.1 %shard_map.153 = (f32[448,128]{1,0:T(8,128)S(1)}, f32[8,512]{1,0:T(8,128)}) custom-call(f32[8,128]{1,0:T(8,128)S(1)} %shard_map.152.a_ref, f32[8,128]{1,0:T(8,128)S(1)} %collective-permute-done.14.b_ref, bf16[8,64,512]{2,1,0:T(8,128)(2,1)} %all_to_all.10.refs_0_.own_ref.x_ref.refs_4_), custom_call_target="tpu_custom_call" | custom-call | tf_op jit(solution)/shard_map/pallas_call | solution.py:386
  86.7 0.3 shard_map.154.base_ref
  87.0 0.9 shard_map.157
  87.9 4.3 %all-to-all-start.1 = ((bf16[8,56,512]{2,1,0:T(8,128)(2,1)}), bf16[8,56,512]{2,1,0:T(8,128)(2,1)}, u32[]{:S(2)}, u32[]{:S(2)}) async-start(bf16[8,56,512]{2,1,0:T(8,128)(2,1)} %bitcast.13), calls=%async_computation.1 | async-start | bytes 917504 | tf_op jit(solution)/shard_map/all_to_all | solution.py:434
  92.2 0.0 copy-start.15
  92.2 6.4 %grads.1 = (bf16[2048,512]{1,0:T(8,128)(2,1)}, bf16[2048,512]{1,0:T(8,128)(2,1)}, f32[4,2,512]{2,1,0:T(2,128)}) custom-call(s32[1]{0:T(128)} %bitcast.17.q_ref, bf16[8,64,512]{2,1,0:T(8,128)(2,1)} %all_to_all.10.refs_0_.own_ref.x_ref.refs_4_, bf16[8,64,512]{2,1,0:T(8,128)(2,1)} %copy-done.8, bf16[8,64,512]{2,1,0:T(8,128)(2,1)} %collective-permute-done.10.refs_0_.refs_2_, ...), custom_call_target="tpu_custom_call" | custom-call | flops 1879048192 | tf_op jit(solution)/shard_map/grads/pallas_call | solution.py:544
  98.6 0.5 collective-permute-start.24
  99.1 0.6 copy-done.10
  99.8 1.9 %collective-permute-start.20 = (f32[8,512]{1,0:T(8,128)}, f32[8,512]{1,0:T(8,128)}, u32[]{:S(2)}, u32[]{:S(2)}) collective-permute-start(f32[8,512]{1,0:T(8,128)} %get-tuple-element.67.a_ref), channel_id=1, source_target_pairs={{0,4},{4,0},{8,12},{12,8},{16,20},{20,16},{24,28},{28,24},{1,5},{5... | collective-permute-start | bytes 49160 | tf_op jit(solution)/shard_map/ppermute | solution.py:431
  101.7 0.9 collective-permute-done.24
  102.6 4.7 %down.1 = (bf16[512,2048]{1,0:T(8,128)(2,1)}, f32[1,512]{1,0:T(1,128)}) custom-call(s32[1]{0:T(128)} %bitcast.17.q_ref, bf16[224,1024]{1,0:T(8,128)(2,1)} %bitcast.41, bf16[224,1024]{1,0:T(8,128)(2,1)} %bitcast.44, bf16[224,1024]{1,0:T(8,128)(2,1)} %copy-done.9, bf16[224,1024]{1,0:T(8,128)(2,1)} %copy-done.11, ...), custom_call_target="tpu_custom_call" | custom-call | flops 939524096 | tf_op jit(solution)/shard_map/down/pallas_call | solution.py:557
  107.3 1.3 %shard_map.160.a_ref = f32[8,512]{1,0:T(8,128)} custom-call(f32[8,512]{1,0:T(8,128)} %get-tuple-element.67.a_ref, f32[8,512]{1,0:T(8,128)} %collective-permute-done.20.b_ref), custom_call_target="tpu_custom_call" | custom-call | tf_op jit(solution)/shard_map/pallas_call | solution.py:386
  108.7 1.9 %collective-permute-start.21 = (f32[8,512]{1,0:T(8,128)}, f32[8,512]{1,0:T(8,128)}, u32[]{:S(2)}, u32[]{:S(2)}) collective-permute-start(f32[8,512]{1,0:T(8,128)} %shard_map.160.a_ref), channel_id=1, source_target_pairs={{0,8},{4,12},{8,0},{12,4},{16,24},{20,28},{24,16},{28,20},{1,9},{5... | collective-permute-start | bytes 49160 | tf_op jit(solution)/shard_map/ppermute | solution.py:431
  110.6 2.1 %shard_map.159 = (bf16[128,512]{1,0:T(8,128)(2,1)}, bf16[128,2048]{1,0:T(8,128)(2,1)}) custom-call(bf16[448,512]{1,0:T(8,128)(2,1)} %bitcast.14.got_hbm, bf16[448,128]{1,0:T(8,128)(2,1)} %copy-done.10), custom_call_target="tpu_custom_call" | custom-call | tf_op jit(solution)/shard_map/pallas_call | solution.py:386
  112.7 0.6 collective-permute-start.18
  113.3 0.8 add_add_fusion
  114.1 0.7 shard_map.161.a_ref
  114.8 2.4 %collective-permute-start.22 = (f32[8,512]{1,0:T(8,128)S(1)}, f32[8,512]{1,0:T(8,128)S(1)}, u32[]{:S(2)}, u32[]{:S(2)}) collective-permute-start(f32[8,512]{1,0:T(8,128)S(1)} %shard_map.161.a_ref), channel_id=1, source_target_pairs={{0,16},{4,20},{8,24},{12,28},{16,0},{20,4},{24,8},{28,12},{1,17},{... | collective-permute-start | bytes 49160 | tf_op jit(solution)/shard_map/ppermute | solution.py:431
  117.2 1.4 %collective-permute-done.18.refs_2_ = bf16[128,512]{1,0:T(8,128)(2,1)S(1)} collective-permute-done((bf16[128,512]{1,0:T(8,128)(2,1)}, bf16[128,512]{1,0:T(8,128)(2,1)S(1)}, u32[]{:S(2)}, u32[]{:S(2)}) %collective-permute-start.18) | collective-permute-done | bytes 131104 | tf_op jit(solution)/shard_map/ppermute | solution.py:431
  118.6 0.6 fusion
  119.2 0.4 collective-permute-done.22.b_ref
  119.6 0.6 shard_map.162
  120.2 0.8 assemble.1
  (49 shorter events, 0.2 us)
Async XLA Ops:
  25.1 15.4 %collective-permute-start.10 = (bf16[8,64,512]{2,1,0:T(8,128)(2,1)}, bf16[8,64,512]{2,1,0:T(8,128)(2,1)}, u32[]{:S(2)}, u32[]{:S(2)}) collective-permute-start(bf16[8,64,512]{2,1,0:T(8,128)(2,1)} %all_to_all.10.refs_0_.own_ref.x_ref.refs_4_), channel_id=1, source_target_pairs={{0,2},{1,3},{2,0},{3,1},{4,6},{5,7},{6,4},{7,5},{8,10},{9,11},{10,... | collective-permute-start | bytes 1572872 | tf_op jit(solution)/shard_map/ppermute | solution.py:431
  29.5 6.2 %collective-permute-start = (bf16[56,1024]{1,0:T(8,128)(2,1)}, bf16[56,1024]{1,0:T(8,128)(2,1)S(1)}, u32[]{:S(2)}, u32[]{:S(2)}) collective-permute-start(bf16[56,1024]{1,0:T(8,128)(2,1)} %get-tuple-element.44), channel_id=1, source_target_pairs={{0,4},{4,0},{8,12},{12,8},{16,20},{20,16},{24,28},{28,24},{1,5},{5... | collective-permute-start | bytes 344072 | tf_op jit(solution)/shard_map/ppermute | solution.py:431
  31.0 5.4 %collective-permute-start.1 = (bf16[56,1024]{1,0:T(8,128)(2,1)}, bf16[56,1024]{1,0:T(8,128)(2,1)S(1)}, u32[]{:S(2)}, u32[]{:S(2)}) collective-permute-start(bf16[56,1024]{1,0:T(8,128)(2,1)} %get-tuple-element.45), channel_id=1, source_target_pairs={{0,8},{4,12},{8,0},{12,4},{16,24},{20,28},{24,16},{28,20},{1,9},{5... | collective-permute-start | bytes 344072 | tf_op jit(solution)/shard_map/ppermute | solution.py:431
  31.0 8.5 %collective-permute-start.2 = (bf16[56,1024]{1,0:T(8,128)(2,1)}, bf16[56,1024]{1,0:T(8,128)(2,1)S(1)}, u32[]{:S(2)}, u32[]{:S(2)}) collective-permute-start(bf16[56,1024]{1,0:T(8,128)(2,1)} %get-tuple-element.46), channel_id=1, source_target_pairs={{0,12},{4,8},{8,4},{12,0},{16,28},{20,24},{24,20},{28,16},{1,13},{... | collective-permute-start | bytes 344072 | tf_op jit(solution)/shard_map/ppermute | solution.py:431
  33.0 26.8 %collective-permute-start.9 = (bf16[8,64,512]{2,1,0:T(8,128)(2,1)}, bf16[8,64,512]{2,1,0:T(8,128)(2,1)S(1)}, u32[]{:S(2)}, u32[]{:S(2)}) collective-permute-start(bf16[8,64,512]{2,1,0:T(8,128)(2,1)} %all_to_all.10.refs_0_.own_ref.x_ref.refs_4_), channel_id=1, source_target_pairs={{0,1},{1,0},{2,3},{3,2},{4,5},{5,4},{6,7},{7,6},{8,9},{9,8},{10,11... | collective-permute-start | bytes 1572872 | tf_op jit(solution)/shard_map/ppermute | solution.py:431
  35.6 9.8 %collective-permute-start.3 = (bf16[56,1024]{1,0:T(8,128)(2,1)}, bf16[56,1024]{1,0:T(8,128)(2,1)S(1)}, u32[]{:S(2)}, u32[]{:S(2)}) collective-permute-start(bf16[56,1024]{1,0:T(8,128)(2,1)} %get-tuple-element.47), channel_id=1, source_target_pairs={{0,16},{4,20},{8,24},{12,28},{16,0},{20,4},{24,8},{28,12},{1,17},{... | collective-permute-start | bytes 344072 | tf_op jit(solution)/shard_map/ppermute | solution.py:431
  36.4 12.6 %collective-permute-start.4 = (bf16[56,1024]{1,0:T(8,128)(2,1)}, bf16[56,1024]{1,0:T(8,128)(2,1)S(1)}, u32[]{:S(2)}, u32[]{:S(2)}) collective-permute-start(bf16[56,1024]{1,0:T(8,128)(2,1)} %get-tuple-element.48), channel_id=1, source_target_pairs={{0,20},{4,16},{8,28},{12,24},{16,4},{20,0},{24,12},{28,8},{1,21},{... | collective-permute-start | bytes 344072 | tf_op jit(solution)/shard_map/ppermute | solution.py:431
  39.5 0.9 copy-start.14
  40.4 19.4 %copy-start.5 = (bf16[4,56,1024]{2,1,0:T(8,128)(2,1)}, bf16[4,56,1024]{2,1,0:T(8,128)(2,1)S(1)}, u32[]{:S(2)}) copy-start(bf16[4,56,1024]{2,1,0:T(8,128)(2,1)S(1)} %shard_map.144) | copy-start | bytes 1376260
  40.4 16.5 %collective-permute-start.7 = (bf16[224,1024]{1,0:T(8,128)(2,1)S(1)}, bf16[224,1024]{1,0:T(8,128)(2,1)S(1)}, u32[]{:S(2)}, u32[]{:S(2)}) collective-permute-start(bf16[224,1024]{1,0:T(8,128)(2,1)S(1)} %bitcast.39), channel_id=1, source_target_pairs={{0,1},{1,0},{2,3},{3,2},{4,5},{5,4},{6,7},{7,6},{8,9},{9,8},{10,11... | collective-permute-start | bytes 1376264 | tf_op jit(solution)/shard_map/ppermute | solution.py:431
  40.5 24.7 %collective-permute-start.11 = (bf16[8,64,512]{2,1,0:T(8,128)(2,1)}, bf16[8,64,512]{2,1,0:T(8,128)(2,1)S(1)}, u32[]{:S(2)}, u32[]{:S(2)}) collective-permute-start(bf16[8,64,512]{2,1,0:T(8,128)(2,1)} %collective-permute-done.10.refs_0_.refs_2_), channel_id=1, source_target_pairs={{0,1},{1,0},{2,3},{3,2},{4,5},{5,4},{6,7},{7,6},{8,9},{9,8},{10,11... | collective-permute-start | bytes 1572872 | tf_op jit(solution)/shard_map/ppermute | solution.py:431
  45.4 7.2 %collective-permute-start.5 = (bf16[56,1024]{1,0:T(8,128)(2,1)}, bf16[56,1024]{1,0:T(8,128)(2,1)S(1)}, u32[]{:S(2)}, u32[]{:S(2)}) collective-permute-start(bf16[56,1024]{1,0:T(8,128)(2,1)} %get-tuple-element.49), channel_id=1, source_target_pairs={{0,24},{4,28},{8,16},{12,20},{16,8},{20,12},{24,0},{28,4},{1,25},{... | collective-permute-start | bytes 344072 | tf_op jit(solution)/shard_map/ppermute | solution.py:431
  49.0 7.8 %collective-permute-start.6 = (bf16[56,1024]{1,0:T(8,128)(2,1)}, bf16[56,1024]{1,0:T(8,128)(2,1)S(1)}, u32[]{:S(2)}, u32[]{:S(2)}) collective-permute-start(bf16[56,1024]{1,0:T(8,128)(2,1)} %get-tuple-element.50), channel_id=1, source_target_pairs={{0,28},{4,24},{8,20},{12,16},{16,12},{20,8},{24,4},{28,0},{1,29},{... | collective-permute-start | bytes 344072 | tf_op jit(solution)/shard_map/ppermute | solution.py:431
  56.8 3.0 %copy-start.6 = (bf16[4,56,1024]{2,1,0:T(8,128)(2,1)}, bf16[4,56,1024]{2,1,0:T(8,128)(2,1)S(1)}, u32[]{:S(2)}) copy-start(bf16[4,56,1024]{2,1,0:T(8,128)(2,1)S(1)} %shard_map.145) | copy-start | bytes 1376260
  56.8 10.7 %collective-permute-start.8 = (bf16[224,1024]{1,0:T(8,128)(2,1)S(1)}, bf16[224,1024]{1,0:T(8,128)(2,1)S(1)}, u32[]{:S(2)}, u32[]{:S(2)}) collective-permute-start(bf16[224,1024]{1,0:T(8,128)(2,1)S(1)} %bitcast.42), channel_id=1, source_target_pairs={{0,1},{1,0},{2,3},{3,2},{4,5},{5,4},{6,7},{7,6},{8,9},{9,8},{10,11... | collective-permute-start | bytes 1376264 | tf_op jit(solution)/shard_map/ppermute | solution.py:431
  56.9 3.0 %copy-start.9 = (bf16[224,1024]{1,0:T(8,128)(2,1)}, bf16[224,1024]{1,0:T(8,128)(2,1)S(1)}, u32[]{:S(2)}) copy-start(bf16[224,1024]{1,0:T(8,128)(2,1)S(1)} %collective-permute-done.7.near_got.refs_2_) | copy-start | bytes 1376260
  56.9 1.8 %copy-start.2 = (bf16[1,512,2048]{2,1,0:T(8,128)(2,1)S(1)}, bf16[1,512,2048]{2,1,0:T(8,128)(2,1)}, u32[]{:S(2)}) copy-start(bf16[1,512,2048]{2,1,0:T(8,128)(2,1)} %param.12) | copy-start | bytes 6291460
  58.7 1.6 %copy-start = (bf16[1,2048,512]{2,1,0:T(8,128)(2,1)S(1)}, bf16[1,2048,512]{2,1,0:T(8,128)(2,1)}, u32[]{:S(2)}) copy-start(bf16[1,2048,512]{2,1,0:T(8,128)(2,1)} %param.10) | copy-start | bytes 6291460
  58.8 2.4 %copy-start.1 = (bf16[1,2048,512]{2,1,0:T(8,128)(2,1)S(1)}, bf16[1,2048,512]{2,1,0:T(8,128)(2,1)}, u32[]{:S(2)}) copy-start(bf16[1,2048,512]{2,1,0:T(8,128)(2,1)} %param.11) | copy-start | bytes 6291460
  59.9 3.6 %copy-start.8 = (bf16[8,64,512]{2,1,0:T(8,128)(2,1)}, bf16[8,64,512]{2,1,0:T(8,128)(2,1)S(1)}, u32[]{:S(2)}) copy-start(bf16[8,64,512]{2,1,0:T(8,128)(2,1)S(1)} %collective-permute-done.9.refs_1_) | copy-start | bytes 1572868
  65.2 2.3 %copy-start.7 = (bf16[8,64,512]{2,1,0:T(8,128)(2,1)}, bf16[8,64,512]{2,1,0:T(8,128)(2,1)S(1)}, u32[]{:S(2)}) copy-start(bf16[8,64,512]{2,1,0:T(8,128)(2,1)S(1)} %collective-permute-done.11.refs_0_.refs_3_) | copy-start | bytes 1572868
  65.2 2.3 %copy-start.3 = (bf16[1,512,2048]{2,1,0:T(8,128)(2,1)S(1)}, bf16[1,512,2048]{2,1,0:T(8,128)(2,1)}, u32[]{:S(2)}) copy-start(bf16[1,512,2048]{2,1,0:T(8,128)(2,1)} %param.12) | copy-start | bytes 6291460
  67.5 1.3 %copy-start.12 = (bf16[8,56,512]{2,1,0:T(8,128)(2,1)}, bf16[8,56,512]{2,1,0:T(8,128)(2,1)S(1)}, u32[]{:S(2)}) copy-start(bf16[8,56,512]{2,1,0:T(8,128)(2,1)S(1)} %get-tuple-element.56) | copy-start | bytes 1376260
  67.5 1.3 %copy-start.11 = (bf16[224,1024]{1,0:T(8,128)(2,1)}, bf16[224,1024]{1,0:T(8,128)(2,1)S(1)}, u32[]{:S(2)}) copy-start(bf16[224,1024]{1,0:T(8,128)(2,1)S(1)} %collective-permute-done.8.far_ref.refs_3_) | copy-start | bytes 1376260
  68.8 1.9 %copy-start.4 = (bf16[8,64,1024]{2,1,0:T(8,128)(2,1)}, bf16[8,64,1024]{2,1,0:T(8,128)(2,1)S(1)}, u32[]{:S(2)}) copy-start(bf16[8,64,1024]{2,1,0:T(8,128)(2,1)S(1)} %get-tuple-element.59.g_ref.refs_4_) | copy-start | bytes 3145732
  68.8 2.7 %collective-permute-start.15 = (bf16[1,448,512]{2,1,0:T(8,128)(2,1)S(1)}, bf16[1,448,512]{2,1,0:T(8,128)(2,1)S(1)}, u32[]{:S(2)}, u32[]{:S(2)}) collective-permute-start(bf16[1,448,512]{2,1,0:T(8,128)(2,1)S(1)} %get-tuple-element.64), channel_id=1, source_target_pairs={{0,1},{1,0},{2,3},{3,2},{4,5},{5,4},{6,7},{7,6},{8,9},{9,8},{10,11... | collective-permute-start | bytes 1376264 | tf_op jit(solution)/shard_map/ppermute | solution.py:431
  70.6 16.1 %collective-permute-start.12 = (bf16[448,512]{1,0:T(8,128)(2,1)S(1)}, bf16[448,512]{1,0:T(8,128)(2,1)S(1)}, u32[]{:S(2)}, u32[]{:S(2)}) collective-permute-start(bf16[448,512]{1,0:T(8,128)(2,1)S(1)} %bitcast.53), channel_id=1, source_target_pairs={{0,1},{1,0},{2,3},{3,2},{4,5},{5,4},{6,7},{7,6},{8,9},{9,8},{10,11... | collective-permute-start | bytes 1376264 | tf_op jit(solution)/shard_map/ppermute | solution.py:431
  71.5 15.2 %copy-start.13 = (bf16[2048,8]{0,1:T(8,128)(2,1)S(1)}, bf16[2048,8]{0,1:T(8,128)(2,1)}, u32[]{:S(2)}) copy-start(bf16[2048,8]{0,1:T(8,128)(2,1)} %param.9) | copy-start | bytes 98308
  71.6 15.4 %collective-permute-start.16 = (bf16[448,512]{1,0:T(8,128)(2,1)S(1)}, bf16[448,512]{1,0:T(8,128)(2,1)S(1)}, u32[]{:S(2)}, u32[]{:S(2)}) collective-permute-start(bf16[448,512]{1,0:T(8,128)(2,1)S(1)} %bitcast.48), channel_id=1, source_target_pairs={{0,2},{1,3},{2,0},{3,1},{4,6},{5,7},{6,4},{7,5},{8,10},{9,11},{10,... | collective-permute-start | bytes 1376264 | tf_op jit(solution)/shard_map/ppermute | solution.py:431
  72.2 1.2 collective-permute-start.13
  73.3 11.2 %collective-permute-start.14 = (f32[8,128]{1,0:T(8,128)S(1)}, f32[8,128]{1,0:T(8,128)S(1)}, u32[]{:S(2)}, u32[]{:S(2)}) collective-permute-start(f32[8,128]{1,0:T(8,128)S(1)} %shard_map.152.a_ref), channel_id=1, source_target_pairs={{0,2},{1,3},{2,0},{3,1},{4,6},{5,7},{6,4},{7,5},{8,10},{9,11},{10,... | collective-permute-start | bytes 12296 | tf_op jit(solution)/shard_map/ppermute | solution.py:431
  87.9 22.7 %all-to-all-start.1 = ((bf16[8,56,512]{2,1,0:T(8,128)(2,1)}), bf16[8,56,512]{2,1,0:T(8,128)(2,1)}, u32[]{:S(2)}, u32[]{:S(2)}) async-start(bf16[8,56,512]{2,1,0:T(8,128)(2,1)} %bitcast.13), calls=%async_computation.1 | async-start | bytes 917504 | tf_op jit(solution)/shard_map/all_to_all | solution.py:434
  92.2 6.9 %copy-start.15 = (f32[8,128]{1,0:T(8,128)S(1)}, f32[8,128]{1,0:T(8,128)}, u32[]{:S(2)}) copy-start(f32[8,128]{1,0:T(8,128)} %get-tuple-element.42.place_ref) | copy-start | bytes 12292
  98.6 4.1 %collective-permute-start.24 = (f32[2,2048]{1,0:T(2,128)}, f32[2,2048]{1,0:T(2,128)}, u32[]{:S(2)}, u32[]{:S(2)}) collective-permute-start(f32[2,2048]{1,0:T(2,128)} %bitcast.54), channel_id=1, source_target_pairs={{0,2},{1,3},{2,0},{3,1},{4,6},{5,7},{6,4},{7,5},{8,10},{9,11},{10,... | collective-permute-start | bytes 49160 | tf_op jit(solution)/shard_map/ppermute | solution.py:431
  99.1 0.6 copy-start.10
  99.8 13.5 %collective-permute-start.23 = (f32[2,2048]{1,0:T(2,128)}, f32[2,2048]{1,0:T(2,128)}, u32[]{:S(2)}, u32[]{:S(2)}) collective-permute-start(f32[2,2048]{1,0:T(2,128)} %bitcast.55), channel_id=1, source_target_pairs={{0,1},{1,0},{2,3},{3,2},{4,5},{5,4},{6,7},{7,6},{8,9},{9,8},{10,11... | collective-permute-start | bytes 49160 | tf_op jit(solution)/shard_map/ppermute | solution.py:431
  99.8 7.6 %collective-permute-start.20 = (f32[8,512]{1,0:T(8,128)}, f32[8,512]{1,0:T(8,128)}, u32[]{:S(2)}, u32[]{:S(2)}) collective-permute-start(f32[8,512]{1,0:T(8,128)} %get-tuple-element.67.a_ref), channel_id=1, source_target_pairs={{0,4},{4,0},{8,12},{12,8},{16,20},{20,16},{24,28},{28,24},{1,5},{5... | collective-permute-start | bytes 49160 | tf_op jit(solution)/shard_map/ppermute | solution.py:431
  102.6 10.6 %collective-permute-start.25 = (f32[2,2048]{1,0:T(2,128)}, f32[2,2048]{1,0:T(2,128)}, u32[]{:S(2)}, u32[]{:S(2)}) collective-permute-start(f32[2,2048]{1,0:T(2,128)} %collective-permute-done.24), channel_id=1, source_target_pairs={{0,1},{1,0},{2,3},{3,2},{4,5},{5,4},{6,7},{7,6},{8,9},{9,8},{10,11... | collective-permute-start | bytes 49160 | tf_op jit(solution)/shard_map/ppermute | solution.py:431
  108.7 5.4 %collective-permute-start.21 = (f32[8,512]{1,0:T(8,128)}, f32[8,512]{1,0:T(8,128)}, u32[]{:S(2)}, u32[]{:S(2)}) collective-permute-start(f32[8,512]{1,0:T(8,128)} %shard_map.160.a_ref), channel_id=1, source_target_pairs={{0,8},{4,12},{8,0},{12,4},{16,24},{20,28},{24,16},{28,20},{1,9},{5... | collective-permute-start | bytes 49160 | tf_op jit(solution)/shard_map/ppermute | solution.py:431
  112.7 5.9 %collective-permute-start.18 = (bf16[128,512]{1,0:T(8,128)(2,1)}, bf16[128,512]{1,0:T(8,128)(2,1)S(1)}, u32[]{:S(2)}, u32[]{:S(2)}) collective-permute-start(bf16[128,512]{1,0:T(8,128)(2,1)} %get-tuple-element.66), channel_id=1, source_target_pairs={{0,2},{1,3},{2,0},{3,1},{4,6},{5,7},{6,4},{7,5},{8,10},{9,11},{10,... | collective-permute-start | bytes 393224 | tf_op jit(solution)/shard_map/ppermute | solution.py:431
  114.8 4.8 %collective-permute-start.22 = (f32[8,512]{1,0:T(8,128)S(1)}, f32[8,512]{1,0:T(8,128)S(1)}, u32[]{:S(2)}, u32[]{:S(2)}) collective-permute-start(f32[8,512]{1,0:T(8,128)S(1)} %shard_map.161.a_ref), channel_id=1, source_target_pairs={{0,16},{4,20},{8,24},{12,28},{16,0},{20,4},{24,8},{28,12},{1,17},{... | collective-permute-start | bytes 49160 | tf_op jit(solution)/shard_map/ppermute | solution.py:431
  117.2 3.1 %collective-permute-start.17 = (bf16[128,512]{1,0:T(8,128)(2,1)}, bf16[128,512]{1,0:T(8,128)(2,1)S(1)}, u32[]{:S(2)}, u32[]{:S(2)}) collective-permute-start(bf16[128,512]{1,0:T(8,128)(2,1)} %get-tuple-element.66), channel_id=1, source_target_pairs={{0,1},{1,0},{2,3},{3,2},{4,5},{5,4},{6,7},{7,6},{8,9},{9,8},{10,11... | collective-permute-start | bytes 393224 | tf_op jit(solution)/shard_map/ppermute | solution.py:431
  118.6 1.6 %collective-permute-start.19 = (bf16[128,512]{1,0:T(8,128)(2,1)S(1)}, bf16[128,512]{1,0:T(8,128)(2,1)S(1)}, u32[]{:S(2)}, u32[]{:S(2)}) collective-permute-start(bf16[128,512]{1,0:T(8,128)(2,1)S(1)} %collective-permute-done.18.refs_2_), channel_id=1, source_target_pairs={{0,1},{1,0},{2,3},{3,2},{4,5},{5,4},{6,7},{7,6},{8,9},{9,8},{10,11... | collective-permute-start | bytes 393224 | tf_op jit(solution)/shard_map/ppermute | solution.py:431
